TPU v7x, 512 devices: a whole 4x8x8 slice. The times are simulated.
512 devices in a mesh: sp: 32 (over z, x), tp: 16 (over y, core).
Axes of the slice: x: 4, y: 8, z: 8, core: 2. Of those that a mesh axis runs over, the one named last changes fastest.
Arguments:
- queries: bfloat16 [512, 4096], P('tp', 'sp'), may hold values from -6 to 6
- input_key_matrix: bfloat16 [512, 4096], P('tp', 'sp'), may hold values from -6 to 6
- input_value_matrix: bfloat16 [1024, 4096], P('tp', 'sp'), may hold values from -6 to 6
- decay_preactivation: bfloat16 [512, 4096], P('tp', 'sp'), may hold values from -6 to 6
- extra_log_decay: float32 [512, 4096], P('tp', 'sp'), may hold values from -1 to 0, as said below
- channel_decay_speed: float32 [512], P('tp'), may hold values from 0 to 1, as said below
- output_weight_matrix: bfloat16 [2048, 1024], P(None, 'tp'), may hold values from -0.1875 to 0.1875
- stored_expert_rows: bfloat16 [4096, 2048], P('sp', 'tp'), may hold values from -6 to 6
- chosen_expert_index: int32 [4096, 2], P('sp'), may hold values from 0 to 31, all different within a row; in each aligned block of 128 rows (0 to 127, 128 to 255, ...) at most 12 rows name the same one
- expert_combine_weight: float32 [4096, 2], P('sp'), may hold values from 0.2 to 1
- cotangent: bfloat16 [4096, 2048], P('sp', 'tp'), may hold values from -6 to 6
- expert_gate_weight: bfloat16 [32, 2048, 2048], P('sp', None, 'tp'), may hold values from -0.125 to 0.125
- expert_up_weight: bfloat16 [32, 2048, 2048], P('sp', None, 'tp'), may hold values from -0.125 to 0.125
- expert_down_weight: bfloat16 [32, 2048, 2048], P('sp', 'tp'), may hold values from -0.125 to 0.125
Outputs:
- grad_queries: float32 [512, 4096], P('tp', 'sp')
- grad_keys: float32 [512, 4096], P('tp', 'sp')
- grad_values: float32 [1024, 4096], P('tp', 'sp')
- grad_logit: float32 [512, 4096], P('tp', 'sp')
- grad_out_proj: float32 [2048, 1024], P('sp', 'tp')
- grad_gate: bfloat16 [32, 2048, 2048], P('sp', None, 'tp')
- grad_up: bfloat16 [32, 2048, 2048], P('sp', None, 'tp')
- grad_down: bfloat16 [32, 2048, 2048], P('sp', 'tp')
Inputs may be any that keep to these rules, and one draw needn't show every extreme that they name: `chosen_expert_index`: each position names two different experts; in the rows of one device no expert is named more than 12 times. `channel_decay_speed`: positive. `extra_log_decay`: zero or negative.
All inputs are finite; a program needn't handle non-finite values.
Results may differ from a plain program's by a relative error of at most 0.023.
Values may be sent and summed in bfloat16 or wider, within the bound.
No kernel may reach another device: no remote copies, remote signals or barrier semaphores. Data moves between devices by JAX's collectives and lax.ppermute only.
A program may use at most 64 MiB of HBM per device.

v0:
```python
import jax
import jax.numpy as jnp
from jax import lax
from jax.sharding import PartitionSpec as P

KEY_DIM = 32
VAL_DIM = 64


def copy_for_each(shard, axis):
    copies = jnp.broadcast_to(shard, (lax.axis_size(axis), *shard.shape))
    return lax.all_to_all(copies, axis, split_axis=0, concat_axis=0, tiled=True)


def all_in_one(shard, axis):
    leaves = jax.tree.leaves(shard)
    turns = sorted(range(len(leaves)), key=lambda k: -leaves[k].size)
    width = (1, *leaves[turns[0]].shape)[-1]
    lines = [
        jnp.pad(leaves[k].reshape(-1), (0, -leaves[k].size % width)).reshape(-1, width)
        for k in turns
    ]
    both, at, found = (copy_for_each(jnp.concatenate(lines), axis), 0, {})
    for k, line in zip(turns, lines):
        slab = both[:, at : at + len(line)].reshape(len(both), -1)
        found[k] = slab[:, : leaves[k].size].reshape(-1, *leaves[k].shape)
        at += len(line)
    numbers = iter(range(len(leaves)))
    return jax.tree.map(lambda _: found[next(numbers)], shard)


def combined_pairwise(pieces, combine):
    while len(jax.tree.leaves(pieces)[0]) > 1:
        pieces = jax.vmap(combine)(
            *(jax.tree.map(lambda part: part[side::2], pieces) for side in (0, 1))
        )
    return jax.tree.map(lambda part: part[0], pieces)


def entering(shard, axis, combine, identity, reverse):
    peers, index = (lax.axis_size(axis), lax.axis_index(axis))
    passed = jnp.arange(peers) > index if reverse else jnp.arange(peers) < index

    def kept(part, zero, own):
        part = jnp.where(
            passed.reshape(-1, *(1 for _ in own.shape)), part, jnp.asarray(zero, own.dtype)
        )
        return part[::-1] if reverse else part

    pieces = all_in_one(shard, axis)
    return combined_pairwise(jax.tree.map(kept, pieces, identity, shard), combine)


def in_one_piece(arrays, axis, split_dim, concat_dim, along):
    both = jnp.concatenate(arrays, axis=along)
    whole, at, outs = (
        lax.all_to_all(both, axis, split_axis=split_dim, concat_axis=concat_dim, tiled=True),
        0,
        [],
    )
    for a in arrays:
        outs.append(lax.slice_in_dim(whole, at, at + a.shape[along], axis=along))
        at += a.shape[along]
    return tuple(outs)


def sent_together(arrays, axis, dim, along):
    widths = [a.shape[along] for a in arrays]
    both = jnp.concatenate(arrays, axis=along)
    whole = lax.all_gather(both, axis, axis=dim, tiled=True)
    return tuple(jnp.split(whole, [sum(widths[:k]) for k in range(1, len(widths))], axis=along))


def in_blocks(shard, dim, peers):
    before, after = (shard.shape[:dim], shard.shape[dim + 1 :])
    return jnp.moveaxis(shard.reshape(*before, peers, -1, *after), dim, 0)


def sum_at_owner(shard, axis, dim):
    peers = lax.axis_size(axis)
    blocks = lax.all_to_all(in_blocks(shard, dim, peers), axis, 0, 0, tiled=True)
    return jnp.sum(blocks.astype(jnp.float32), axis=0)


def joined_along(blocks, dim):
    blocks = jnp.moveaxis(blocks, 0, dim)
    dims = blocks.shape
    return blocks.reshape(*dims[:dim], dims[dim] * dims[dim + 1], *dims[dim + 2 :])


def gathered_copies(shard, axis, dim):
    blocks = copy_for_each(shard, axis)
    return joined_along(blocks, dim)


def collected_alike(shard, axis):
    leaves, found = (jax.tree.leaves(shard), {})
    for leading, a in enumerate(leaves):
        if leading not in found:
            alike = [k for k, b in enumerate(leaves) if b.dtype == a.dtype]
            got = (
                all_in_one([leaves[k] for k in alike], axis)
                if len(alike) > 1
                else [copy_for_each(a, axis)]
            )
            for k, b in zip(alike, got):
                found[k] = b
    numbers = iter(range(len(leaves)))
    return jax.tree.map(lambda _: found[next(numbers)], shard)


def entering_2(shard, axis, combine, identity, reverse):
    peers, index = (lax.axis_size(axis), lax.axis_index(axis))
    passed = jnp.arange(peers) > index if reverse else jnp.arange(peers) < index

    def kept(part, zero, own):
        part = jnp.where(
            passed.reshape(-1, *(1 for _ in own.shape)), part, jnp.asarray(zero, own.dtype)
        )
        return part[::-1] if reverse else part

    pieces = collected_alike(shard, axis)
    return combined_pairwise(jax.tree.map(kept, pieces, identity, shard), combine)


def combine(earlier, later):
    factor = earlier[0] * later[0]
    others = tuple(
        (
            later[0] * before_part + after_part
            for before_part, after_part in zip(earlier[1:], later[1:])
        )
    )
    return (factor,) + others


def summaries(key_feats, val_feats, decays):
    cumulative = jnp.cumsum(decays, axis=-1)
    total_log = cumulative[..., -1:]
    factor = jnp.exp(total_log)
    fwd_sum = jnp.einsum("hcs,hvs->hcv", key_feats * jnp.exp(total_log - cumulative), val_feats)
    bwd_sum = jnp.einsum("hcs,hvs->hcv", key_feats * jnp.exp(cumulative), val_feats)
    return (factor, fwd_sum, bwd_sum)


def mixing(scaled, key_feats, val_feats, decays, fwd_in, bwd_in):
    cumulative = jnp.cumsum(decays, axis=-1)
    total_log = cumulative[..., -1:]
    length = decays.shape[-1]
    lower_mask = lax.broadcasted_iota(jnp.int32, (length, length), 0) >= lax.broadcasted_iota(
        jnp.int32, (length, length), 1
    )
    log_gap = cumulative[..., :, None] - cumulative[..., None, :]
    weight = jnp.exp(jnp.where(lower_mask, log_gap, -log_gap))
    scores = jnp.einsum("hct,hcs,hcts->hts", scaled, key_feats, weight)
    inner_part = jnp.einsum("hts,hvs->hvt", scores, val_feats)
    carried = jnp.einsum("hct,hcv->hvt", scaled * jnp.exp(cumulative), fwd_in)
    carried = carried + jnp.einsum("hct,hcv->hvt", scaled * jnp.exp(total_log - cumulative), bwd_in)
    return inner_part + carried


def body(
    queries,
    input_key_matrix,
    input_value_matrix,
    decay_preactivation,
    extra_log_decay,
    channel_decay_speed,
    output_weight_matrix,
    stored_expert_rows,
    chosen_expert_index,
    expert_combine_weight,
    cotangent,
    expert_gate_weight,
    expert_up_weight,
    expert_down_weight,
):
    heads_here = input_value_matrix.shape[0] // VAL_DIM
    tok_rows = queries.shape[1]
    preactivation_single = decay_preactivation.astype(jnp.float32)
    decay_logarithm = (
        channel_decay_speed[:, None] * jax.nn.log_sigmoid(preactivation_single) + extra_log_decay
    )
    scaled = (queries.astype(jnp.float32) * KEY_DIM ** (-0.5)).reshape(
        heads_here, KEY_DIM, tok_rows
    )
    key_feats = input_key_matrix.astype(jnp.float32).reshape(heads_here, KEY_DIM, tok_rows)
    val_feats = input_value_matrix.astype(jnp.float32).reshape(heads_here, VAL_DIM, tok_rows)
    decays = decay_logarithm.reshape(heads_here, KEY_DIM, tok_rows)
    (factor, fwd_sum, bwd_sum), pull_sums = jax.vjp(summaries, key_feats, val_feats, decays)
    identity_pair = (jnp.ones_like(factor), jnp.zeros_like(fwd_sum))
    fwd_in = entering((factor, fwd_sum), "sp", combine, identity_pair, False)[1]
    bwd_in = entering((factor, bwd_sum), "sp", combine, identity_pair, True)[1]
    mixed, pull_mix = jax.vjp(mixing, scaled, key_feats, val_feats, decays, fwd_in, bwd_in)
    inv_rms = lax.rsqrt(jnp.mean(mixed * mixed, axis=1, keepdims=True) + 1e-06)
    normed = mixed * inv_rms
    mix_rows = normed.astype(jnp.bfloat16).reshape(-1, tok_rows)
    experts = lax.axis_size("sp")
    capacity = 3 * tok_rows // experts
    model_width = expert_gate_weight.shape[1]
    part_width = stored_expert_rows.shape[1]
    flat_ids = chosen_expert_index.reshape(-1)
    onehot = (flat_ids[:, None] == jnp.arange(experts, dtype=jnp.int32)[None, :]).astype(jnp.int32)
    slot_rank = jnp.sum((jnp.cumsum(onehot, axis=0) - onehot) * onehot, axis=1)
    slot_index = flat_ids * capacity + slot_rank
    slot_table = jnp.full((experts * capacity,), 2 * tok_rows, jnp.int32)
    slot_table = slot_table.at[slot_index].set(jnp.arange(2 * tok_rows, dtype=jnp.int32))
    weighted = (
        expert_combine_weight.reshape(-1, 1) * jnp.repeat(cotangent, 2, axis=0).astype(jnp.float32)
    ).astype(jnp.bfloat16)
    width_here = stored_expert_rows.shape[1]
    zero_row = jnp.zeros((1, width_here), jnp.bfloat16)
    from_inputs = jnp.concatenate([stored_expert_rows, zero_row], axis=0)[slot_table // 2]
    from_grads = jnp.concatenate([weighted, zero_row], axis=0)[slot_table]
    send_x = from_inputs.reshape(experts, capacity, width_here)
    send_dy = from_grads.reshape(experts, capacity, width_here)
    got_x, got_dy = in_one_piece((send_x, send_dy), "sp", 0, 0, 1)
    recv_x, recv_dy = sent_together((got_x, got_dy), "tp", 2, 0)
    rows_x = recv_x.reshape(-1, model_width)
    rows_dy = recv_dy.reshape(-1, model_width)
    gate_local = expert_gate_weight[0]
    up_local = expert_up_weight[0]
    down_local = expert_down_weight[0]
    contract_rows = (((0,), (0,)), ((), ()))
    contract_cols = (((1,), (1,)), ((), ()))
    gate_pre = jnp.dot(rows_x, gate_local, preferred_element_type=jnp.float32)
    up_pre = jnp.dot(rows_x, up_local, preferred_element_type=jnp.float32)
    gate_sig = jax.nn.sigmoid(gate_pre)
    gate_act = gate_pre * gate_sig
    hidden = (gate_act * up_pre).astype(jnp.bfloat16)
    grad_down = lax.dot_general(
        hidden, rows_dy, contract_rows, preferred_element_type=jnp.float32
    ).astype(jnp.bfloat16)
    grad_hidden = lax.dot_general(
        rows_dy, down_local, contract_cols, preferred_element_type=jnp.float32
    )
    grad_gate_pre = (grad_hidden * up_pre * gate_sig * (1.0 + gate_pre * (1.0 - gate_sig))).astype(
        jnp.bfloat16
    )
    grad_up_pre = (grad_hidden * gate_act).astype(jnp.bfloat16)
    grad_gate = lax.dot_general(
        rows_x, grad_gate_pre, contract_rows, preferred_element_type=jnp.float32
    ).astype(jnp.bfloat16)
    grad_up = lax.dot_general(
        rows_x, grad_up_pre, contract_rows, preferred_element_type=jnp.float32
    ).astype(jnp.bfloat16)
    partial_value = lax.dot_general(
        grad_gate_pre, gate_local, contract_cols, preferred_element_type=jnp.float32
    )
    partial_value = partial_value + lax.dot_general(
        grad_up_pre, up_local, contract_cols, preferred_element_type=jnp.float32
    )
    summed = sum_at_owner(
        partial_value.reshape(experts, capacity, model_width).astype(jnp.bfloat16), "tp", 2
    ).astype(jnp.bfloat16)
    returned_rows = lax.all_to_all(summed, "sp", split_axis=0, concat_axis=0, tiled=True).reshape(
        experts * capacity, part_width
    )
    picked = returned_rows[slot_index].astype(jnp.float32).reshape(tok_rows, 2, part_width)
    grad_rows = (cotangent.astype(jnp.float32) + picked[:, 0] + picked[:, 1]).astype(jnp.bfloat16)
    full_rows = gathered_copies(grad_rows, "tp", 1)
    grad_out_proj = sum_at_owner(
        lax.dot_general(
            full_rows, mix_rows, (((0,), (1,)), ((), ())), preferred_element_type=jnp.float32
        ).astype(jnp.bfloat16),
        "sp",
        0,
    )
    grad_normed = lax.dot_general(
        output_weight_matrix,
        full_rows,
        (((0,), (1,)), ((), ())),
        preferred_element_type=jnp.float32,
    )
    grad_normed = grad_normed.reshape(heads_here, VAL_DIM, tok_rows)
    grad_mixed = inv_rms * (
        grad_normed - normed * jnp.mean(grad_normed * normed, axis=1, keepdims=True)
    )
    cumulative = jnp.cumsum(decays, axis=-1)
    total_log = cumulative[..., -1:]
    fwd_source = jnp.einsum("hct,hvt->hcv", scaled * jnp.exp(cumulative), grad_mixed)
    bwd_source = jnp.einsum("hct,hvt->hcv", scaled * jnp.exp(total_log - cumulative), grad_mixed)
    grad_fwd_out = entering_2((factor, fwd_source), "sp", combine, identity_pair, True)[1]
    grad_bwd_out = entering_2((factor, bwd_source), "sp", combine, identity_pair, False)[1]
    grad_scaled, grad_keys_mix, grad_vals_mix, grad_decay_mix, unused_fwd, unused_bwd = pull_mix(
        grad_mixed
    )
    grad_factor = jnp.sum(grad_fwd_out * fwd_in + grad_bwd_out * bwd_in, axis=2, keepdims=True)
    grad_keys_sum, grad_vals_sum, grad_decay_sum = pull_sums(
        (grad_factor, grad_fwd_out, grad_bwd_out)
    )
    grad_queries = (grad_scaled * KEY_DIM ** (-0.5)).reshape(-1, tok_rows)
    grad_keys = (grad_keys_mix + grad_keys_sum).reshape(-1, tok_rows)
    grad_values = (grad_vals_mix + grad_vals_sum).reshape(-1, tok_rows)
    grad_decay = (grad_decay_mix + grad_decay_sum).reshape(-1, tok_rows)
    grad_logit = grad_decay * channel_decay_speed[:, None] * jax.nn.sigmoid(-preactivation_single)
    return (
        grad_queries,
        grad_keys,
        grad_values,
        grad_logit,
        grad_out_proj,
        grad_gate[None],
        grad_up[None],
        grad_down[None],
    )


def solution(mesh):
    in_specs = (
        P("tp", "sp"),
        P("tp", "sp"),
        P("tp", "sp"),
        P("tp", "sp"),
        P("tp", "sp"),
        P("tp"),
        P(None, "tp"),
        P("sp", "tp"),
        P("sp", None),
        P("sp", None),
        P("sp", "tp"),
        P("sp", None, "tp"),
        P("sp", None, "tp"),
        P("sp", "tp", None),
    )
    out_specs = (
        P("tp", "sp"),
        P("tp", "sp"),
        P("tp", "sp"),
        P("tp", "sp"),
        P("sp", "tp"),
        P("sp", None, "tp"),
        P("sp", None, "tp"),
        P("sp", "tp", None),
    )
    return jax.shard_map(body, mesh=mesh, in_specs=in_specs, out_specs=out_specs, check_vma=False)
```

profile of v0, /device:TPU:1, one launch (start us, length us, event | category | flops | bytes accessed | tf_op | source)
XLA Modules:
  0.0 270.2 jit_solution(10571165572555137523)
XLA Ops:
  7.2 0.8 copy.146
  8.4 0.7 broadcast_multiply_fusion
  10.2 1.4 scatter_custom_fusion
  11.7 0.8 copy.149
  12.6 0.8 broadcast_in_dim.132
  13.6 1.4 gather_fusion.1
  15.1 1.4 gather_fusion
  16.7 23.5 %all_to_all.45 = bf16[32,24,128]{2,1,0:T(8,128)(2,1)S(1)} all-to-all(bf16[32,24,128]{2,1,0:T(8,128)(2,1)S(1)} %pad_maximum_fusion.1), channel_id=1, replica_groups=mesh['sp'=32,'tp'=16] {'sp'}, dimensions={0} | all-to-all | bytes 393216 | tf_op jit(solution)/shard_map/all_to_all | solution.py:57
  40.2 0.7 pad_maximum_fusion
  42.0 1.1 reshape.612
  43.1 4.6 %all-to-all-start.1 = ((f32[32,1,2112]{2,1,0:T(1,128)}), f32[32,1,2112]{2,1,0:T(1,128)S(1)}, u32[]{:S(2)}, u32[]{:S(2)}) async-start(f32[32,1,2112]{2,1,0:T(1,128)} %reshape.612), calls=%async_computation.1 | async-start | bytes 557056 | tf_op jit(solution)/shard_map/all_to_all | solution.py:12
  47.8 1.1 reshape.610
  49.5 1.3 fusion.4
  50.8 7.4 %all-to-all-done.1 = f32[32,1,2112]{2,1,0:T(1,128)S(1)} async-done(((f32[32,1,2112]{2,1,0:T(1,128)}), f32[32,1,2112]{2,1,0:T(1,128)S(1)}, u32[]{:S(2)}, u32[]{:S(2)}) %all-to-all-start.1) | async-done | bytes 270368 | tf_op jit(solution)/shard_map/all_to_all | solution.py:12
  58.2 5.5 %all-to-all-start = ((f32[32,1,2112]{2,1,0:T(1,128)}), f32[32,1,2112]{2,1,0:T(1,128)S(1)}, u32[]{:S(2)}, u32[]{:S(2)}) async-start(f32[32,1,2112]{2,1,0:T(1,128)} %reshape.610), calls=%async_computation | async-start | bytes 557056 | tf_op jit(solution)/shard_map/all_to_all | solution.py:12
  63.8 0.8 convolution_bitcast_fusion.1
  65.1 1.3 reduce.21
  66.9 7.3 %all-to-all-done = f32[32,1,2112]{2,1,0:T(1,128)S(1)} async-done(((f32[32,1,2112]{2,1,0:T(1,128)}), f32[32,1,2112]{2,1,0:T(1,128)S(1)}, u32[]{:S(2)}, u32[]{:S(2)}) %all-to-all-start) | async-done | bytes 270368 | tf_op jit(solution)/shard_map/all_to_all | solution.py:12
  74.2 1.3 reduce.20
  77.0 14.4 %all-gather.2.cloned.1.call-done = bf16[64,12,2048]{2,1,0:T(8,128)(2,1)} async-done(((bf16[64,12,128]{2,1,0:T(8,128)(2,1)}), bf16[64,12,2048]{2,1,0:T(8,128)(2,1)}) %all-gather.2.cloned.1.call-update) | async-done | bytes 3145744 | tf_op jit(solution)/shard_map/all_gather | solution.py:70
  91.3 4.8 %fusion.130 = (bf16[32,12,2048]{2,1,0:T(8,128)(2,1)}, bf16[32,12,2048]{2,1,0:T(8,128)(2,1)}) fusion(bf16[64,12,2048]{2,1,0:T(8,128)(2,1)} %all-gather.2.cloned.1.call-done), kind=kLoop, calls=%fused_computation.235 | loop fusion | bytes 6291456 | tf_op jit(solution)/shard_map/split | solution.py:71
  96.2 2.5 reshape.550
  98.7 1.3 fusion.35
  100.0 1.3 fusion.38
  101.3 3.6 %reshape.549 = bf16[384,2048]{1,0:T(8,128)(2,1)} reshape(bf16[32,12,2048]{2,1,0:T(8,128)(2,1)} %get-tuple-element.55) | data formatting | bytes 3145728 | tf_op jit(solution)/shard_map/reshape | solution.py:220
  104.9 2.2 multiply_convert_fusion.1
  109.2 2.2 copy.186
  111.4 4.4 %all-to-all-start.3 = ((bf16[16,32,12,128]{3,1,2,0:T(8,128)(2,1)}), bf16[16,32,12,128]{3,1,2,0:T(8,128)(2,1)}, u32[]{:S(2)}, u32[]{:S(2)}) async-start(bf16[16,32,12,128]{3,1,2,0:T(8,128)(2,1)} %bitcast.355), calls=%async_computation.3 | async-start | bytes 3145728 | tf_op jit(solution)/shard_map/all_to_all | solution.py:81
  116.5 0.7 fusion.31
  117.6 0.7 slice_add_fusion.12
  119.2 35.3 %all-to-all-done.3 = bf16[16,32,12,128]{3,1,2,0:T(8,128)(2,1)} async-done(((bf16[16,32,12,128]{3,1,2,0:T(8,128)(2,1)}), bf16[16,32,12,128]{3,1,2,0:T(8,128)(2,1)}, u32[]{:S(2)}, u32[]{:S(2)}) %all-to-all-start.3) | async-done | bytes 1572896 | tf_op jit(solution)/shard_map/all_to_all | solution.py:81
  154.5 1.6 reduce_sum.106
  156.1 0.7 copy.151
  156.8 9.2 %all-to-all-start.4 = ((bf16[32,12,128]{2,1,0:T(8,128)(2,1)}), bf16[32,12,128]{2,1,0:T(8,128)(2,1)S(1)}, u32[]{:S(2)}, u32[]{:S(2)}) async-start(bf16[32,12,128]{2,1,0:T(8,128)(2,1)} %copy.151), calls=%async_computation.4 | async-start | bytes 262144 | tf_op jit(solution)/shard_map/all_to_all | solution.py:256
  166.1 10.3 %all-to-all-done.4 = bf16[32,12,128]{2,1,0:T(8,128)(2,1)S(1)} async-done(((bf16[32,12,128]{2,1,0:T(8,128)(2,1)}), bf16[32,12,128]{2,1,0:T(8,128)(2,1)S(1)}, u32[]{:S(2)}, u32[]{:S(2)}) %all-to-all-start.4) | async-done | bytes 98336 | tf_op jit(solution)/shard_map/all_to_all | solution.py:256
  176.4 1.0 gather_fusion.2
  177.6 0.9 broadcast_in_dim.134
  178.5 4.9 %all-to-all-start.5 = ((bf16[16,128,128]{1,2,0:T(8,128)(2,1)}), bf16[16,128,128]{1,2,0:T(8,128)(2,1)S(1)}, u32[]{:S(2)}, u32[]{:S(2)}) async-start(bf16[16,128,128]{1,2,0:T(8,128)(2,1)} %broadcast_in_dim.134), calls=%async_computation.5 | async-start | bytes 1048576 | tf_op jit(solution)/shard_map/all_to_all | solution.py:12
  183.8 1.4 fusion
  185.2 1.4 fusion.1
  186.6 1.3 fusion.2
  187.9 12.7 %all-to-all-done.5 = bf16[16,128,128]{1,2,0:T(8,128)(2,1)S(1)} async-done(((bf16[16,128,128]{1,2,0:T(8,128)(2,1)}), bf16[16,128,128]{1,2,0:T(8,128)(2,1)S(1)}, u32[]{:S(2)}, u32[]{:S(2)}) %all-to-all-start.5) | async-done | bytes 524320 | tf_op jit(solution)/shard_map/all_to_all | solution.py:12
  200.9 0.9 multiply_reduce_fusion
  204.3 1.1 reshape.618
  205.4 4.0 %all-to-all-start.8 = ((bf16[32,2,2048]{2,1,0:T(2,128)(2,1)}), bf16[32,2,2048]{2,1,0:T(2,128)(2,1)S(1)}, u32[]{:S(2)}, u32[]{:S(2)}) async-start(bf16[32,2,2048]{2,1,0:T(2,128)(2,1)} %reshape.618), calls=%async_computation.8 | async-start | bytes 524288 | tf_op jit(solution)/shard_map/all_to_all | solution.py:81
  209.5 1.1 reshape.614
  210.6 1.1 reshape.616
  211.8 0.9 fusion.9
  212.7 0.9 fusion.11
  213.6 8.3 %all-to-all-done.8 = bf16[32,2,2048]{2,1,0:T(2,128)(2,1)S(1)} async-done(((bf16[32,2,2048]{2,1,0:T(2,128)(2,1)}), bf16[32,2,2048]{2,1,0:T(2,128)(2,1)S(1)}, u32[]{:S(2)}, u32[]{:S(2)}) %all-to-all-start.8) | async-done | bytes 262176 | tf_op jit(solution)/shard_map/all_to_all | solution.py:81
  221.9 3.9 %all-to-all-start.7 = ((f32[32,1,2112]{2,1,0:T(1,128)}), f32[32,1,2112]{2,1,0:T(1,128)S(1)}, u32[]{:S(2)}, u32[]{:S(2)}) async-start(f32[32,1,2112]{2,1,0:T(1,128)} %reshape.614), calls=%async_computation.7 | async-start | bytes 557056 | tf_op jit(solution)/shard_map/all_to_all | solution.py:12
  225.9 2.1 fusion.17
  228.4 10.5 %all-to-all-done.7 = f32[32,1,2112]{2,1,0:T(1,128)S(1)} async-done(((f32[32,1,2112]{2,1,0:T(1,128)}), f32[32,1,2112]{2,1,0:T(1,128)S(1)}, u32[]{:S(2)}, u32[]{:S(2)}) %all-to-all-start.7) | async-done | bytes 270368 | tf_op jit(solution)/shard_map/all_to_all | solution.py:12
  238.9 4.1 %all-to-all-start.6 = ((f32[32,1,2112]{2,1,0:T(1,128)}), f32[32,1,2112]{2,1,0:T(1,128)S(1)}, u32[]{:S(2)}, u32[]{:S(2)}) async-start(f32[32,1,2112]{2,1,0:T(1,128)} %reshape.616), calls=%async_computation.6 | async-start | bytes 557056 | tf_op jit(solution)/shard_map/all_to_all | solution.py:12
  243.1 0.7 copy.162
  243.8 1.3 reduce.23
  245.7 8.6 %all-to-all-done.6 = f32[32,1,2112]{2,1,0:T(1,128)S(1)} async-done(((f32[32,1,2112]{2,1,0:T(1,128)}), f32[32,1,2112]{2,1,0:T(1,128)S(1)}, u32[]{:S(2)}, u32[]{:S(2)}) %all-to-all-start.6) | async-done | bytes 270368 | tf_op jit(solution)/shard_map/all_to_all | solution.py:12
  254.3 1.3 reduce.22
  257.6 0.8 fusion.91
  258.7 0.7 fusion.67
  259.4 1.2 reduce_window_sum.54
  260.6 1.2 reduce_window_sum.56
  261.9 0.7 fusion.56
  262.5 0.8 fusion.19
  (288 shorter events, 16.7 us)
Async XLA Ops:
  7.2 91.5 %copy-start = (bf16[1,2048,128]{2,1,0:T(8,128)(2,1)S(1)}, bf16[1,2048,128]{2,1,0:T(8,128)(2,1)}, u32[]{:S(2)}) copy-start(bf16[1,2048,128]{2,1,0:T(8,128)(2,1)} %param.25) | copy-start | bytes 1572868
  7.2 7.9 %copy-start.25 = (bf16[128,128]{1,0:T(8,128)(2,1)S(1)}, bf16[128,128]{1,0:T(8,128)(2,1)}, u32[]{:S(2)}) copy-start(bf16[128,128]{1,0:T(8,128)(2,1)} %param.21) | copy-start | bytes 98308
  7.2 84.2 %all-gather.2.cloned.1.call-start = ((), (), s32[]{:S(2)}) async-start(), calls=%async_computation.9 | async-start | bytes 4456448 | tf_op jit(solution)/shard_map/all_gather | solution.py:70
  13.5 27.4 %copy-start.26 = (bf16[32,128]{1,0:T(8,128)(2,1)S(1)}, bf16[32,128]{1,0:T(8,128)(2,1)}, u32[]{:S(2)}) copy-start(bf16[32,128]{1,0:T(8,128)(2,1)} %param.17) | copy-start | bytes 24580
  13.5 27.4 %copy-start.42 = (f32[32,128]{1,0:T(8,128)S(1)}, f32[32,128]{1,0:T(8,128)}, u32[]{:S(2)}) copy-start(f32[32,128]{1,0:T(8,128)} %param.18) | copy-start | bytes 49156
  13.5 27.4 %copy-start.61 = (f32[32]{0:T(128)S(1)}, f32[32]{0:T(128)}, u32[]{:S(2)}) copy-start(f32[32]{0:T(128)} %param.19) | copy-start | bytes 388
  13.6 28.0 %copy-start.6 = (bf16[64,128]{1,0:T(8,128)(2,1)S(1)}, bf16[64,128]{1,0:T(8,128)(2,1)}, u32[]{:S(2)}) copy-start(bf16[64,128]{1,0:T(8,128)(2,1)} %param.16) | copy-start | bytes 49156
  13.6 28.0 %copy-start.9 = (bf16[32,128]{1,0:T(8,128)(2,1)S(1)}, bf16[32,128]{1,0:T(8,128)(2,1)}, u32[]{:S(2)}) copy-start(bf16[32,128]{1,0:T(8,128)(2,1)} %param.15) | copy-start | bytes 24580
  41.0 8.5 %copy-start.11 = (bf16[32,128]{1,0:T(8,128)(2,1)S(1)}, bf16[32,128]{1,0:T(8,128)(2,1)}, u32[]{:S(2)}) copy-start(bf16[32,128]{1,0:T(8,128)(2,1)} %param.14) | copy-start | bytes 24580
  41.6 9.2 %copy-start.28 = (f32[32]{0:T(128)}, f32[32]{0:T(128)S(1)}, u32[]{:S(2)}) copy-start(f32[32]{0:T(128)S(1)} %get-tuple-element.50) | copy-start | bytes 388
  41.6 6.2 %copy-start.56 = (f32[1,64]{1,0:T(1,128)}, f32[1,64]{1,0:T(1,128)S(1)}, u32[]{:S(2)}) copy-start(f32[1,64]{1,0:T(1,128)S(1)} %pad_bitcast_fusion) | copy-start | bytes 772
  43.1 15.2 %all-to-all-start.1 = ((f32[32,1,2112]{2,1,0:T(1,128)}), f32[32,1,2112]{2,1,0:T(1,128)S(1)}, u32[]{:S(2)}, u32[]{:S(2)}) async-start(f32[32,1,2112]{2,1,0:T(1,128)} %reshape.612), calls=%async_computation.1 | async-start | bytes 557056 | tf_op jit(solution)/shard_map/all_to_all | solution.py:12
  47.7 18.8 %copy-start.36 = (f32[32,128]{1,0:T(8,128)}, f32[32,128]{1,0:T(8,128)S(1)}, u32[]{:S(2)}) copy-start(f32[32,128]{1,0:T(8,128)S(1)} %convert.5) | copy-start | bytes 49156
  48.9 25.3 %copy-start.40 = (pred[128,128]{1,0:T(8,128)(4,1)}, pred[128,128]{1,0:T(8,128)(4,1)S(1)}, u32[]{:S(2)}) copy-start(pred[128,128]{1,0:T(8,128)(4,1)S(1)} %iota_compare_fusion) | copy-start | bytes 49156
  49.5 16.9 %copy-start.38 = (f32[32,128]{1,0:T(8,128)}, f32[32,128]{1,0:T(8,128)S(1)}, u32[]{:S(2)}) copy-start(f32[32,128]{1,0:T(8,128)S(1)} %convert_multiply_fusion.2) | copy-start | bytes 49156
  50.8 23.3 %copy-start.15 = (bf16[128,128]{1,0:T(8,128)(2,1)}, bf16[128,128]{1,0:T(8,128)(2,1)S(1)}, u32[]{:S(2)}) copy-start(bf16[128,128]{1,0:T(8,128)(2,1)S(1)} %fusion.4) | copy-start | bytes 98308
  58.2 15.9 %all-to-all-start = ((f32[32,1,2112]{2,1,0:T(1,128)}), f32[32,1,2112]{2,1,0:T(1,128)S(1)}, u32[]{:S(2)}, u32[]{:S(2)}) async-start(f32[32,1,2112]{2,1,0:T(1,128)} %reshape.610), calls=%async_computation | async-start | bytes 557056 | tf_op jit(solution)/shard_map/all_to_all | solution.py:12
  63.8 10.3 %copy-start.50 = (pred[32]{0:T(512)(128)(4,1)}, pred[32]{0:T(512)(128)(4,1)S(1)}, u32[]{:S(2)}) copy-start(pred[32]{0:T(512)(128)(4,1)S(1)} %get-tuple-element.85) | copy-start | bytes 100
  63.8 11.8 %copy-start.47 = (pred[32]{0:T(512)(128)(4,1)}, pred[32]{0:T(512)(128)(4,1)S(1)}, u32[]{:S(2)}) copy-start(pred[32]{0:T(512)(128)(4,1)S(1)} %get-tuple-element.86) | copy-start | bytes 100
  66.7 7.5 %copy-start.17 = (f32[16,1,32,1]{2,0,3,1:T(8,128)}, f32[16,1,32,1]{2,0,3,1:T(8,128)S(1)}, u32[]{:S(2)}) copy-start(f32[16,1,32,1]{2,0,3,1:T(8,128)S(1)} %slice.351) | copy-start | bytes 6148
  66.7 7.4 %copy-start.21 = (f32[8,1,32,1]{2,0,3,1:T(8,128)}, f32[8,1,32,1]{2,0,3,1:T(8,128)S(1)}, u32[]{:S(2)}) copy-start(f32[8,1,32,1]{2,0,3,1:T(8,128)S(1)} %slice.353) | copy-start | bytes 3076
  66.8 7.4 %copy-start.32 = (f32[4,1,32,1]{2,0,3,1:T(4,128)}, f32[4,1,32,1]{2,0,3,1:T(4,128)S(1)}, u32[]{:S(2)}) copy-start(f32[4,1,32,1]{2,0,3,1:T(4,128)S(1)} %slice.355) | copy-start | bytes 1540
  66.9 29.3 %copy-start.43 = (f32[2,1,32,1]{2,0,3,1:T(2,128)}, f32[2,1,32,1]{2,0,3,1:T(2,128)S(1)}, u32[]{:S(2)}) copy-start(f32[2,1,32,1]{2,0,3,1:T(2,128)S(1)} %slice.357) | copy-start | bytes 772
  75.7 20.5 %copy-start.19 = (f32[16,1,32,1]{2,0,3,1:T(8,128)}, f32[16,1,32,1]{2,0,3,1:T(8,128)S(1)}, u32[]{:S(2)}) copy-start(f32[16,1,32,1]{2,0,3,1:T(8,128)S(1)} %slice.327) | copy-start | bytes 6148
  75.7 20.4 %copy-start.23 = (f32[8,1,32,1]{2,0,3,1:T(8,128)}, f32[8,1,32,1]{2,0,3,1:T(8,128)S(1)}, u32[]{:S(2)}) copy-start(f32[8,1,32,1]{2,0,3,1:T(8,128)S(1)} %slice.329) | copy-start | bytes 3076
  75.8 20.4 %copy-start.34 = (f32[4,1,32,1]{2,0,3,1:T(4,128)}, f32[4,1,32,1]{2,0,3,1:T(4,128)S(1)}, u32[]{:S(2)}) copy-start(f32[4,1,32,1]{2,0,3,1:T(4,128)S(1)} %slice.331) | copy-start | bytes 1540
  75.9 20.3 %copy-start.45 = (f32[2,1,32,1]{2,0,3,1:T(2,128)}, f32[2,1,32,1]{2,0,3,1:T(2,128)S(1)}, u32[]{:S(2)}) copy-start(f32[2,1,32,1]{2,0,3,1:T(2,128)S(1)} %slice.333) | copy-start | bytes 772
  107.1 1.7 copy-start.7
  111.4 43.1 %all-to-all-start.3 = ((bf16[16,32,12,128]{3,1,2,0:T(8,128)(2,1)}), bf16[16,32,12,128]{3,1,2,0:T(8,128)(2,1)}, u32[]{:S(2)}, u32[]{:S(2)}) async-start(bf16[16,32,12,128]{3,1,2,0:T(8,128)(2,1)} %bitcast.355), calls=%async_computation.3 | async-start | bytes 3145728 | tf_op jit(solution)/shard_map/all_to_all | solution.py:81
  115.8 1.6 copy-start.22
  115.8 1.7 copy-start.33
  115.8 1.8 copy-start.44
  115.8 2.5 copy-start.48
  116.5 2.4 copy-start.53
  116.5 2.0 copy-start.20
  118.5 47.6 %copy-start.63 = (f32[2,1,32,1]{2,0,3,1:T(2,128)S(1)}, f32[2,1,32,1]{2,0,3,1:T(2,128)}, u32[]{:S(2)}) copy-start(f32[2,1,32,1]{2,0,3,1:T(2,128)} %mul.479) | copy-start | bytes 772
  118.6 58.8 %copy-start.14 = (bf16[128,128]{1,0:T(8,128)(2,1)S(1)}, bf16[128,128]{1,0:T(8,128)(2,1)}, u32[]{:S(2)}) copy-start(bf16[128,128]{1,0:T(8,128)(2,1)} %param.24) | copy-start | bytes 98308
  156.1 27.3 %copy-start.12 = (f32[2,1,32,64]{3,2,0,1:T(8,128)S(1)}, f32[2,1,32,64]{3,2,0,1:T(8,128)}, u32[]{:S(2)}) copy-start(f32[2,1,32,64]{3,2,0,1:T(8,128)} %slice_add_fusion.12) | copy-start | bytes 49156
  156.1 27.3 %copy-start.13 = (f32[64,128]{1,0:T(8,128)S(1)}, f32[64,128]{1,0:T(8,128)}, u32[]{:S(2)}) copy-start(f32[64,128]{1,0:T(8,128)} %convolution_bitcast_fusion.1) | copy-start | bytes 98308
  156.1 27.3 %copy-start.29 = (f32[32]{0:T(128)S(1)}, f32[32]{0:T(128)}, u32[]{:S(2)}) copy-start(f32[32]{0:T(128)} %copy-done.28) | copy-start | bytes 388
  156.8 19.5 %all-to-all-start.4 = ((bf16[32,12,128]{2,1,0:T(8,128)(2,1)}), bf16[32,12,128]{2,1,0:T(8,128)(2,1)S(1)}, u32[]{:S(2)}, u32[]{:S(2)}) async-start(bf16[32,12,128]{2,1,0:T(8,128)(2,1)} %copy.151), calls=%async_computation.4 | async-start | bytes 262144 | tf_op jit(solution)/shard_map/all_to_all | solution.py:256
  166.1 17.6 %copy-start.58 = (f32[32]{0:T(128)}, f32[32]{0:T(128)S(1)}, u32[]{:S(2)}) copy-start(f32[32]{0:T(128)S(1)} %slice_bitcast_fusion.2) | copy-start | bytes 388
  177.5 7.7 %copy-start.8 = (bf16[384,128]{1,0:T(8,128)(2,1)S(1)}, bf16[384,128]{1,0:T(8,128)(2,1)}, u32[]{:S(2)}) copy-start(bf16[384,128]{1,0:T(8,128)(2,1)} %copy-done.7) | copy-start | bytes 294916
  178.5 22.1 %all-to-all-start.5 = ((bf16[16,128,128]{1,2,0:T(8,128)(2,1)}), bf16[16,128,128]{1,2,0:T(8,128)(2,1)S(1)}, u32[]{:S(2)}, u32[]{:S(2)}) async-start(bf16[16,128,128]{1,2,0:T(8,128)(2,1)} %broadcast_in_dim.134), calls=%async_computation.5 | async-start | bytes 1048576 | tf_op jit(solution)/shard_map/all_to_all | solution.py:12
  183.7 16.9 %copy-start.52 = (f32[128]{0:T(128)}, f32[128]{0:T(128)S(1)}, u32[]{:S(2)}) copy-start(f32[128]{0:T(128)S(1)} %add_rsqrt_fusion) | copy-start | bytes 1540
  183.7 2.9 %copy-start.1 = (bf16[384,2048]{1,0:T(8,128)(2,1)S(1)}, bf16[384,2048]{1,0:T(8,128)(2,1)}, u32[]{:S(2)}) copy-start(bf16[384,2048]{1,0:T(8,128)(2,1)} %reshape.549) | copy-start | bytes 4718596
  183.7 2.9 %copy-start.4 = (f32[384,128]{1,0:T(8,128)S(1)}, f32[384,128]{1,0:T(8,128)}, u32[]{:S(2)}) copy-start(f32[384,128]{1,0:T(8,128)} %fusion.35) | copy-start | bytes 589828
  183.7 2.8 %copy-start.5 = (f32[384,128]{1,0:T(8,128)S(1)}, f32[384,128]{1,0:T(8,128)}, u32[]{:S(2)}) copy-start(f32[384,128]{1,0:T(8,128)} %fusion.38) | copy-start | bytes 589828
  186.6 14.3 %copy-start.10 = (bf16[2048,64]{0,1:T(8,128)(2,1)S(1)}, bf16[2048,64]{0,1:T(8,128)(2,1)}, u32[]{:S(2)}) copy-start(bf16[2048,64]{0,1:T(8,128)(2,1)} %param.20) | copy-start | bytes 786436
  186.6 15.9 %copy-start.30 = (f32[32]{0:T(128)S(1)}, f32[32]{0:T(128)}, u32[]{:S(2)}) copy-start(f32[32]{0:T(128)} %copy-done.28) | copy-start | bytes 388
  186.6 16.4 %copy-start.59 = (f32[32]{0:T(128)S(1)}, f32[32]{0:T(128)}, u32[]{:S(2)}) copy-start(f32[32]{0:T(128)} %copy-done.58) | copy-start | bytes 388
  186.6 16.7 %copy-start.54 = (f32[32]{0:T(128)S(1)}, f32[32]{0:T(128)}, u32[]{:S(2)}) copy-start(f32[32]{0:T(128)} %copy-done.53) | copy-start | bytes 388
  200.9 8.5 %copy-start.57 = (f32[1,64]{1,0:T(1,128)S(1)}, f32[1,64]{1,0:T(1,128)}, u32[]{:S(2)}) copy-start(f32[1,64]{1,0:T(1,128)} %copy-done.56) | copy-start | bytes 772
  205.4 6.4 %copy-start.39 = (f32[32,128]{1,0:T(8,128)S(1)}, f32[32,128]{1,0:T(8,128)}, u32[]{:S(2)}) copy-start(f32[32,128]{1,0:T(8,128)} %copy-done.38) | copy-start | bytes 49156
  205.4 6.4 %copy-start.41 = (pred[128,128]{1,0:T(8,128)(4,1)S(1)}, pred[128,128]{1,0:T(8,128)(4,1)}, u32[]{:S(2)}) copy-start(pred[128,128]{1,0:T(8,128)(4,1)} %copy-done.40) | copy-start | bytes 49156
  205.4 16.5 %all-to-all-start.8 = ((bf16[32,2,2048]{2,1,0:T(2,128)(2,1)}), bf16[32,2,2048]{2,1,0:T(2,128)(2,1)S(1)}, u32[]{:S(2)}, u32[]{:S(2)}) async-start(bf16[32,2,2048]{2,1,0:T(2,128)(2,1)} %reshape.618), calls=%async_computation.8 | async-start | bytes 524288 | tf_op jit(solution)/shard_map/all_to_all | solution.py:81
  212.7 13.1 %copy-start.16 = (bf16[128,128]{1,0:T(8,128)(2,1)S(1)}, bf16[128,128]{1,0:T(8,128)(2,1)}, u32[]{:S(2)}) copy-start(bf16[128,128]{1,0:T(8,128)(2,1)} %copy-done.15) | copy-start | bytes 98308
  212.7 13.2 %copy-start.37 = (f32[32,128]{1,0:T(8,128)S(1)}, f32[32,128]{1,0:T(8,128)}, u32[]{:S(2)}) copy-start(f32[32,128]{1,0:T(8,128)} %copy-done.36) | copy-start | bytes 49156
  221.9 17.0 %all-to-all-start.7 = ((f32[32,1,2112]{2,1,0:T(1,128)}), f32[32,1,2112]{2,1,0:T(1,128)S(1)}, u32[]{:S(2)}, u32[]{:S(2)}) async-start(f32[32,1,2112]{2,1,0:T(1,128)} %reshape.614), calls=%async_computation.7 | async-start | bytes 557056 | tf_op jit(solution)/shard_map/all_to_all | solution.py:12
  225.9 19.4 %copy-start.51 = (pred[32]{0:T(512)(128)(4,1)S(1)}, pred[32]{0:T(512)(128)(4,1)}, u32[]{:S(2)}) copy-start(pred[32]{0:T(512)(128)(4,1)} %copy-done.50) | copy-start | bytes 100
  238.9 15.4 %all-to-all-start.6 = ((f32[32,1,2112]{2,1,0:T(1,128)}), f32[32,1,2112]{2,1,0:T(1,128)S(1)}, u32[]{:S(2)}, u32[]{:S(2)}) async-start(f32[32,1,2112]{2,1,0:T(1,128)} %reshape.616), calls=%async_computation.6 | async-start | bytes 557056 | tf_op jit(solution)/shard_map/all_to_all | solution.py:12
  243.8 11.9 %copy-start.49 = (pred[32]{0:T(512)(128)(4,1)S(1)}, pred[32]{0:T(512)(128)(4,1)}, u32[]{:S(2)}) copy-start(pred[32]{0:T(512)(128)(4,1)} %copy-done.47) | copy-start | bytes 100
  256.2 5.7 %copy-start.27 = (bf16[32,128]{1,0:T(8,128)(2,1)S(1)}, bf16[32,128]{1,0:T(8,128)(2,1)}, u32[]{:S(2)}) copy-start(bf16[32,128]{1,0:T(8,128)(2,1)} %param.17) | copy-start | bytes 24580
  256.2 5.6 %copy-start.62 = (f32[32]{0:T(128)S(1)}, f32[32]{0:T(128)}, u32[]{:S(2)}) copy-start(f32[32]{0:T(128)} %param.19) | copy-start | bytes 388
  (9 other events, 11.7 us)
Sparse Core Ops, SparseCore 0:
  41.1 50.2 all-gather.1
where the time goes:
time: 271 us; the launch traced here: 270 us
  waiting for transfers between devices  115 us (42%)
  starting transfers between devices  40.7 us (15%)
  local copies, waits for them, and re-layouts  35.2 us (13%)
  blocking collectives  23.5 us (9%)
  other arithmetic  23 us (8%)
  matrix products  17.7 us (7%)
  between operations  15.4 us (6%)
    all_to_all x5, waiting for transfers between devices, copy_for_each(): return lax.all_to_all(copies, axis, split_axis=0, concat_axis=0, tiled=True)  46.5 us
    all_to_all x2, waiting for transfers between devices, sum_at_owner(): lax.all_to_all(in_blocks(shard, dim, peers), axis, 0, 0, tiled=True)  43.6 us
    all_to_all x1, blocking collectives, in_one_piece(): lax.all_to_all(both, axis, split_axis=split_dim, concat_axis=concat_dim,...  23.5 us
    all_to_all x5, starting transfers between devices, copy_for_each(): return lax.all_to_all(copies, axis, split_axis=0, concat_axis=0, tiled=True)  23 us
    all_gather x1, waiting for transfers between devices, sent_together(): whole = lax.all_gather(both, axis, axis=dim, tiled=True)  14.4 us
    all_to_all x1, waiting for transfers between devices, body(): lax.all_to_all(summed, 'sp', split_axis=0, concat_axis=0, tiled=True)  10.3 us
    unnamed x142, local copies, waits for them, and re-layouts  9.82 us
    all_to_all x1, starting transfers between devices, body(): lax.all_to_all(summed, 'sp', split_axis=0, concat_axis=0, tiled=True)  9.18 us
  transfers between devices with their start and end apart: 9, of which 9 were waited for; matrix products, arithmetic and copies ran while one was open for 10% of the time, Pallas kernels for 0%

commit v1 on v0

v1 whole, which is shorter than its diff:
```python
import jax
import jax.numpy as jnp
from jax import lax
from jax.experimental import pallas as pl
from jax.experimental.pallas import tpu as pltpu
from jax.sharding import Mesh
from jax.sharding import PartitionSpec as P

KEY_DIM = 32
VAL_DIM = 64
TOK = 128
PEERS = 32
CAP = 12
PAD = 16
RING = 8
SLOTS = PEERS * PAD
ROWS = PEERS * CAP
WIDTH = 128
MODEL = 2048

F32 = jnp.float32
BF16 = jnp.bfloat16
EXACT = lax.Precision.HIGHEST


def dot(a, b, da, db, precision=None):
    return lax.dot_general(
        a, b, (((da,), (db,)), ((), ())), preferred_element_type=F32, precision=precision
    )


def iota(shape, dim):
    return lax.broadcasted_iota(jnp.int32, shape, dim)


def ones_where(mask, dtype=BF16):
    return jnp.where(mask, 1.0, 0.0).astype(dtype)


def split_two(value):
    high = value.astype(BF16).astype(F32)
    return high, (value - high).astype(BF16).astype(F32)


def split_three(value):
    high, rest = split_two(value)
    return high, rest, (value - high - rest).astype(BF16).astype(F32)


def compact_rows(shape, compact_dim):
    row = iota(shape, compact_dim)
    peer = (row * 5462) >> 16
    return peer * PAD + (row - peer * CAP) == iota(shape, 1 - compact_dim)


def row_of_peer(place):
    return iota((PEERS, SLOTS), 1) == iota((PEERS, SLOTS), 0) * PAD + place


def dispatch_kernel(
    ids_ref, share_ref, x_ref, cot_ref, key_ref, val_ref, pre_ref, extra_ref, speed_ref,
    send_ref, pick_ref, cum_ref,
):
    ids = ids_ref[...]
    expert = iota((TOK, PEERS), 1)
    named = [ones_where(ids[:, k : k + 1] == expert) for k in range(2)]
    row, col = iota((TOK, TOK), 0), iota((TOK, TOK), 1)
    earlier, same = ones_where(row < col), ones_where(row == col)
    rank = dot(named[0] + named[1], earlier, 0, 0)
    place = iota((PEERS, PAD, TOK), 1).astype(F32)
    cot = cot_ref[...].astype(F32)
    picks, grads = [], None
    for k in range(2):
        mine = dot(named[k], same, 0, 0)
        at = jnp.where(mine > 0.5, rank, -1.0)
        pick = jnp.where(at[:, None, :] == place, 1.0, 0.0).reshape(SLOTS, TOK).astype(BF16)
        weighted = (share_ref[:, k : k + 1] * cot).astype(BF16)
        part = dot(pick, weighted, 1, 0)
        grads = part if grads is None else grads + part
        picks.append(pick)
    pick = picks[0] + picks[1]
    pick_ref[...] = pick
    rows = jnp.concatenate([dot(pick, x_ref[...], 1, 0), grads], axis=1)

    pre = pre_ref[...].astype(F32)
    log_sig = jnp.minimum(pre, 0.0) - jnp.log1p(jnp.exp(-jnp.abs(pre)))
    diagonal = iota((KEY_DIM, KEY_DIM), 0) == iota((KEY_DIM, KEY_DIM), 1)
    speed = jnp.sum(jnp.where(diagonal, speed_ref[...], 0.0), axis=1, keepdims=True)
    decay = speed * log_sig + extra_ref[...]
    cum = dot(decay, ones_where(row <= col, F32), 1, 0, EXACT)
    cum_ref[...] = cum
    total = cum[:, TOK - 1 : TOK]
    keys, vals = key_ref[...].astype(F32), val_ref[...].astype(F32)
    sums = jnp.concatenate(
        [
            dot(keys * jnp.exp(total - cum), vals, 1, 1, EXACT),
            dot(keys * jnp.exp(cum), vals, 1, 1, EXACT),
        ],
        axis=1,
    )
    state = jnp.concatenate(split_two(sums), axis=1)
    lane = iota((KEY_DIM, 2 * WIDTH), 1)
    logs = jnp.zeros((KEY_DIM, 2 * WIDTH), F32)
    for k, part in enumerate(split_three(total)):
        logs = jnp.where(lane == k, part, logs)
    place = iota((PEERS, PAD, 2 * WIDTH), 1)
    block = rows.reshape(PEERS, PAD, 2 * WIDTH)
    block = jnp.where(place == CAP, state[:, None, :], block)
    block = jnp.where(place == CAP + 1, logs[:, None, :], block)
    send_ref[...] = block.astype(BF16)


def arrival_kernel(got_ref, copies_ref, back_ref):
    got = got_ref[...].reshape(SLOTS, 2 * WIDTH)
    rows = dot(ones_where(compact_rows((ROWS, SLOTS), 0)), got, 1, 0).astype(BF16)
    for k in range(RING):
        copies_ref[k] = rows
    both = dot(ones_where(row_of_peer(CAP)), got, 1, 0)
    state = both[:, :WIDTH] + both[:, WIDTH:]
    logs = dot(ones_where(row_of_peer(CAP + 1)), got, 1, 0)
    log = jnp.sum(logs, axis=1, keepdims=True)
    a, b = iota((PEERS, PEERS), 0), iota((PEERS, PEERS), 1)
    gap_fwd = dot(ones_where(b < a, F32), jnp.where(a > b, log, 0.0), 1, 0, EXACT)
    gap_bwd = dot(ones_where(b > a, F32), jnp.where(a < b, log, 0.0), 1, 0, EXACT)
    fwd = dot(jnp.where(b < a, jnp.exp(gap_fwd), 0.0), state, 1, 0, EXACT)
    bwd = dot(jnp.where(b > a, jnp.exp(gap_bwd), 0.0), state, 1, 0, EXACT)
    lane = iota((PEERS, WIDTH), 1)
    high, low = split_two(jnp.where(lane < VAL_DIM, fwd, bwd))
    peer = iota((PEERS, WIDTH), 0)
    spread = jnp.zeros((PEERS, WIDTH), F32)
    for k, part in enumerate(split_three(log)):
        spread = jnp.where(lane == peer + k * PEERS, part, spread)
    all_logs = jnp.sum(spread, axis=0, keepdims=True)
    place = iota((PEERS, PAD, WIDTH), 1)
    block = jnp.where(place == CAP, high[:, None, :], 0.0)
    block = jnp.where(place == CAP + 1, low[:, None, :], block)
    block = jnp.where(place == CAP + 2, all_logs[:, None, :], block)
    back_ref[...] = block.astype(BF16)


def expert_kernel(
    core_ref, own_ref, other_ref, gate_ref, up_ref, down_ref,
    x_ref, y_ref, grads_ref, hidden_ref,
):
    core = core_ref[0]
    for mine in range(2):

        @pl.when(core == mine)
        def _():
            for side, ref in ((mine, own_ref), (1 - mine, other_ref)):
                for k in range(RING):
                    at = slice((2 * k + side) * WIDTH, (2 * k + side + 1) * WIDTH)
                    x_ref[:, at] = ref[k, :, :WIDTH]
                    y_ref[:, at] = ref[k, :, WIDTH:]

    x, y = x_ref[...], y_ref[...]
    gate_pre = dot(x, gate_ref[...], 1, 0)
    up_pre = dot(x, up_ref[...], 1, 0)
    grad_hidden = dot(y, down_ref[...], 1, 1)
    gate_sig = jax.nn.sigmoid(gate_pre)
    gate_act = gate_pre * gate_sig
    hidden_ref[...] = (gate_act * up_pre).astype(BF16)
    grads_ref[:, :WIDTH] = (
        grad_hidden * up_pre * gate_sig * (1.0 + gate_pre * (1.0 - gate_sig))
    ).astype(BF16)
    grads_ref[:, WIDTH:] = (grad_hidden * gate_act).astype(BF16)


def partial_kernel(core_ref, grads_ref, gate_ref, up_ref, swapped_ref, out_ref):
    core = core_ref[0]
    both = jnp.concatenate([grads_ref[core], grads_ref[1 - core]], axis=1)
    for k in range(RING):
        at = 2 * k + core
        weights = jnp.concatenate(
            [gate_ref[at], up_ref[at], swapped_ref[0, k], swapped_ref[1, k]], axis=1
        )
        out_ref[k] = dot(both, weights, 1, 1).astype(BF16)


def return_kernel(parts_ref, back_ref, send_ref):
    total = parts_ref[0].astype(F32)
    for k in range(1, RING):
        total = total + parts_ref[k].astype(F32)
    rows = dot(ones_where(compact_rows((SLOTS, ROWS), 1)), total.astype(BF16), 1, 0)
    rows = rows.astype(BF16).reshape(PEERS, PAD, WIDTH)
    send_ref[...] = rows + back_ref[...]


def token_kernel(got_ref, pick_ref, cot_ref, copies_ref):
    got = got_ref[...].reshape(SLOTS, WIDTH)
    rows = (cot_ref[...].astype(F32) + dot(pick_ref[...], got, 0, 0)).astype(BF16)
    for k in range(RING):
        copies_ref[k] = rows


def state_kernel(place_ref, got_ref, state_ref, reach_ref):
    got = got_ref[...].reshape(SLOTS, WIDTH)
    state_ref[...] = dot(ones_where(row_of_peer(CAP) | row_of_peer(CAP + 1)), got, 1, 0)
    spread = dot(ones_where(row_of_peer(CAP + 2)), got, 1, 0).astype(BF16)
    lane, peer = iota((WIDTH, PEERS), 0), iota((WIDTH, PEERS), 1)
    fold = (lane == peer) | (lane == peer + PEERS) | (lane == peer + 2 * PEERS)
    logs = dot(spread, ones_where(fold), 1, 0)
    here = place_ref[0]
    a, b = iota((PEERS, PEERS), 0), iota((PEERS, PEERS), 1)
    later = dot(jnp.where(b > here, logs, 0.0), ones_where(a < b, F32), 1, 0, EXACT)
    before = dot(jnp.where(b < here, logs, 0.0), ones_where(a > b, F32), 1, 0, EXACT)
    later = jnp.where(b > here, jnp.exp(later), 0.0)
    before = jnp.where(b < here, jnp.exp(before), 0.0)
    lane = iota((KEY_DIM, WIDTH), 1)
    for k in range(PEERS):
        reach_ref[k] = jnp.where(lane < VAL_DIM, later[:, k : k + 1], before[:, k : k + 1])


def source_kernel(
    rows_ref, weight_ref, normed_ref, inv_ref, mix_ref, query_fwd_ref, query_bwd_ref,
    send_ref, grad_ref,
):
    rows = jnp.concatenate([rows_ref[c, k] for k in range(RING) for c in range(2)], axis=1)
    grad = dot(rows, weight_ref[...], 1, 0)
    normed = normed_ref[...]
    mean = jnp.mean(grad * normed, axis=1, keepdims=True)
    grad = inv_ref[...] * (grad - normed * mean)
    grad_ref[...] = grad
    state = jnp.concatenate(
        [
            dot(query_fwd_ref[...], grad, 1, 0, EXACT),
            dot(query_bwd_ref[...], grad, 1, 0, EXACT),
        ],
        axis=1,
    ).astype(BF16)
    lane = iota((KEY_DIM, WIDTH), 1)
    for k in range(2 * RING):
        part = dot(rows[:, k * WIDTH : (k + 1) * WIDTH], mix_ref[...], 0, 0)
        for half in range(2):
            at = half * VAL_DIM
            both = jnp.where(lane < VAL_DIM, part[at : at + 32], part[at + 32 : at + 64])
            send_ref[2 * k + half, :KEY_DIM] = both.astype(BF16)
            send_ref[2 * k + half, KEY_DIM:] = state


def final_kernel(
    got_ref, reach_ref, state_ref, cum_ref, key_ref, val_ref, pre_ref, speed_ref,
    keys_mix_ref, vals_mix_ref, decay_mix_ref,
    proj_ref, keys_ref, vals_ref, logit_ref,
):
    proj = got_ref[0, :KEY_DIM].astype(F32)
    flow = got_ref[0, KEY_DIM:].astype(F32) * reach_ref[0]
    for k in range(1, PEERS):
        proj = proj + got_ref[k, :KEY_DIM].astype(F32)
        flow = flow + got_ref[k, KEY_DIM:].astype(F32) * reach_ref[k]
    proj_ref[:KEY_DIM] = proj[:, :VAL_DIM]
    proj_ref[KEY_DIM:] = proj[:, VAL_DIM:]
    cum = cum_ref[...]
    total = cum[:, TOK - 1 : TOK]
    keys, vals = key_ref[...].astype(F32), val_ref[...].astype(F32)
    scale_fwd, scale_bwd = jnp.exp(total - cum), jnp.exp(cum)
    flow_fwd, flow_bwd = flow[:, :VAL_DIM], flow[:, VAL_DIM:]
    grad_fwd = dot(flow_fwd, vals, 1, 0, EXACT) * scale_fwd
    grad_bwd = dot(flow_bwd, vals, 1, 0, EXACT) * scale_bwd
    keys_ref[...] = keys_mix_ref[...] + grad_fwd + grad_bwd
    vals_ref[...] = (
        vals_mix_ref[...]
        + dot(flow_fwd, keys * scale_fwd, 0, 0, EXACT)
        + dot(flow_bwd, keys * scale_bwd, 0, 0, EXACT)
    )
    factor = jnp.exp(total) * jnp.sum(flow * state_ref[...], axis=1, keepdims=True)
    grad_fwd, grad_bwd = grad_fwd * keys, grad_bwd * keys
    at_end = factor + jnp.sum(grad_fwd, axis=1, keepdims=True)
    row, col = iota((TOK, TOK), 0), iota((TOK, TOK), 1)
    tail = dot(grad_bwd - grad_fwd, ones_where(row >= col, F32), 1, 0, EXACT)
    decay = decay_mix_ref[...] + tail + at_end
    diagonal = iota((KEY_DIM, KEY_DIM), 0) == iota((KEY_DIM, KEY_DIM), 1)
    speed = jnp.sum(jnp.where(diagonal, speed_ref[...], 0.0), axis=1, keepdims=True)
    pre = pre_ref[...].astype(F32)
    logit_ref[...] = decay * speed * jax.nn.sigmoid(-pre)


SCALAR = pl.BlockSpec(memory_space=pltpu.SMEM)
WHOLE = pl.BlockSpec(memory_space=pltpu.VMEM)


def call(kernel, outs, *args, scalars=0):
    shapes = [jax.ShapeDtypeStruct(shape, dtype) for shape, dtype in outs]
    return pl.pallas_call(
        kernel,
        out_shape=shapes,
        in_specs=[SCALAR] * scalars + [WHOLE] * (len(args) - scalars),
        out_specs=[WHOLE] * len(shapes),
    )(*args)


def inner(scaled, keys, vals, cum):
    row, col = iota((TOK, TOK), 0), iota((TOK, TOK), 1)
    gap = cum[:, :, None] - cum[:, None, :]
    weight = jnp.exp(jnp.where(row >= col, gap, -gap))
    scores = jnp.einsum("ct,cs,cts->ts", scaled, keys, weight)
    return jnp.einsum("ts,vs->vt", scores, vals)


def carried(scaled, cum, fwd_in, bwd_in):
    total = cum[:, -1:]
    return jnp.einsum("ct,cv->vt", scaled * jnp.exp(cum), fwd_in) + jnp.einsum(
        "ct,cv->vt", scaled * jnp.exp(total - cum), bwd_in
    )


def body(
    queries,
    input_key_matrix,
    input_value_matrix,
    decay_preactivation,
    extra_log_decay,
    channel_decay_speed,
    output_weight_matrix,
    stored_expert_rows,
    chosen_expert_index,
    expert_combine_weight,
    cotangent,
    expert_gate_weight,
    expert_up_weight,
    expert_down_weight,
):
    sp = ("z", "x")
    core = lax.axis_index("core")
    core_at = core.reshape(1).astype(jnp.int32)
    place_at = lax.axis_index(sp).reshape(1).astype(jnp.int32)
    speed = channel_decay_speed.reshape(1, KEY_DIM)
    swap = [(0, 1), (1, 0)]

    def exchanged(array, axis):
        return lax.all_to_all(array, axis, split_axis=0, concat_axis=0, tiled=True)

    gate, up, down = expert_gate_weight[0], expert_up_weight[0], expert_down_weight[0]
    gate_blocks = gate.reshape(2 * RING, WIDTH, WIDTH)
    up_blocks = up.reshape(2 * RING, WIDTH, WIDTH)
    send, pick, cum = call(
        dispatch_kernel,
        [((PEERS, PAD, 2 * WIDTH), BF16), ((SLOTS, TOK), BF16), ((KEY_DIM, TOK), F32)],
        chosen_expert_index,
        expert_combine_weight,
        stored_expert_rows,
        cotangent,
        input_key_matrix,
        input_value_matrix,
        decay_preactivation,
        extra_log_decay,
        speed,
    )
    got = exchanged(send, sp)
    copies, back = call(
        arrival_kernel,
        [((RING, ROWS, 2 * WIDTH), BF16), ((PEERS, PAD, WIDTH), BF16)],
        got,
    )
    own = exchanged(copies, "y")

    theirs = jnp.stack(
        [
            lax.dynamic_index_in_dim(
                w.reshape(RING, 2, WIDTH, WIDTH), 1 - core, axis=1, keepdims=False
            )
            for w in (gate, up)
        ]
    )
    swapped = lax.ppermute(theirs, "core", swap)

    other = lax.ppermute(own, "core", swap)
    rows_x, rows_dy, grads, hidden = call(
        expert_kernel,
        [
            ((ROWS, MODEL), BF16),
            ((ROWS, MODEL), BF16),
            ((ROWS, 2 * WIDTH), BF16),
            ((ROWS, WIDTH), BF16),
        ],
        core_at,
        own,
        other,
        gate,
        up,
        down,
        scalars=1,
    )
    grads_both = lax.all_gather(grads, "core", axis=0, tiled=False)
    (partials,) = call(
        partial_kernel,
        [((RING, ROWS, WIDTH), BF16)],
        core_at,
        grads_both,
        gate_blocks,
        up_blocks,
        swapped,
        scalars=1,
    )
    parts = exchanged(partials, "y")
    grad_both = dot(rows_x, grads, 0, 0).astype(BF16)
    grad_gate, grad_up = grad_both[:, :WIDTH], grad_both[:, WIDTH:]
    grad_down = dot(hidden, rows_dy, 0, 0).astype(BF16)
    (send,) = call(return_kernel, [((PEERS, PAD, WIDTH), BF16)], parts, back)
    returned = exchanged(send, sp)
    (copies,) = call(
        token_kernel, [((RING, TOK, WIDTH), BF16)], returned, pick, cotangent
    )
    full_rows = exchanged(copies, "y")
    full_rows = lax.all_gather(full_rows, "core", axis=0, tiled=False)

    state, reach = call(
        state_kernel,
        [((KEY_DIM, WIDTH), F32), ((PEERS, KEY_DIM, WIDTH), F32)],
        place_at,
        returned,
        scalars=1,
    )
    scaled = queries.astype(F32) * KEY_DIM ** (-0.5)
    keys = input_key_matrix.astype(F32)
    vals = input_value_matrix.astype(F32)
    fwd_in, bwd_in = state[:, :VAL_DIM], state[:, VAL_DIM:]
    inner_out, pull_inner = jax.vjp(inner, scaled, keys, vals, cum)
    carried_out, pull_carried = jax.vjp(
        lambda s, c: carried(s, c, fwd_in, bwd_in), scaled, cum
    )
    mixed = inner_out + carried_out
    inv_rms = lax.rsqrt(jnp.mean(mixed * mixed, axis=0, keepdims=True) + 1e-06)
    normed = mixed * inv_rms
    normed_t = normed.T
    mix_t = normed_t.astype(BF16)
    send, grad_mixed_t = call(
        source_kernel,
        [((PEERS, 2 * KEY_DIM, WIDTH), BF16), ((TOK, VAL_DIM), F32)],
        full_rows,
        output_weight_matrix,
        normed_t,
        inv_rms.reshape(TOK, 1),
        jnp.concatenate([mix_t, mix_t], axis=1),
        scaled * jnp.exp(cum),
        scaled * jnp.exp(cum[:, -1:] - cum),
    )
    got = exchanged(send, sp)
    grad_mixed = grad_mixed_t.T
    grad_scaled, grad_keys, grad_vals, grad_cum = pull_inner(grad_mixed)
    grad_scaled_in, grad_cum_in = pull_carried(grad_mixed)
    grad_queries = (grad_scaled + grad_scaled_in) * KEY_DIM ** (-0.5)
    tail_mask = ones_where(iota((TOK, TOK), 0) >= iota((TOK, TOK), 1), F32)
    grad_decay = dot(grad_cum + grad_cum_in, tail_mask, 1, 0, EXACT)
    grad_out_proj, grad_keys, grad_values, grad_logit = call(
        final_kernel,
        [
            ((2 * KEY_DIM, VAL_DIM), F32),
            ((KEY_DIM, TOK), F32),
            ((VAL_DIM, TOK), F32),
            ((KEY_DIM, TOK), F32),
        ],
        got,
        reach,
        state,
        cum,
        input_key_matrix,
        input_value_matrix,
        decay_preactivation,
        speed,
        grad_keys,
        grad_vals,
        grad_decay,
    )
    return (
        grad_queries,
        grad_keys,
        grad_values,
        grad_logit,
        grad_out_proj,
        grad_gate[None],
        grad_up[None],
        grad_down[None],
    )


def solution(mesh):
    fine = Mesh(mesh.devices.reshape(8, 4, 8, 2), ("z", "x", "y", "core"))
    sp, tp = ("z", "x"), ("y", "core")
    in_specs = (
        P(tp, sp),
        P(tp, sp),
        P(tp, sp),
        P(tp, sp),
        P(tp, sp),
        P(tp),
        P(None, tp),
        P(sp, tp),
        P(sp, None),
        P(sp, None),
        P(sp, tp),
        P(sp, None, tp),
        P(sp, None, tp),
        P(sp, tp, None),
    )
    out_specs = (
        P(tp, sp),
        P(tp, sp),
        P(tp, sp),
        P(tp, sp),
        P(sp, tp),
        P(sp, None, tp),
        P(sp, None, tp),
        P(sp, tp, None),
    )
    return jax.shard_map(body, mesh=fine, in_specs=in_specs, out_specs=out_specs, check_vma=False)
```

time: 271 us -> 195 us (0.72)
  waiting for transfers between devices: 115 us -> 37.8 us
  blocking collectives: 23.5 us -> 78.3 us
  Pallas kernels: 0 us -> 25.7 us
  local copies, waits for them, and re-layouts: 35.2 us -> 9.73 us
  other arithmetic: 23 us -> 4.9 us
  starting transfers between devices: 40.7 us -> 23.7 us
  between operations: 15.4 us -> 0.95 us
  matrix products: 17.7 us -> 12.5 us
    all_to_all x8 -> x4, waiting for transfers between devices: 100 us -> 36.8 us  [exchanged(): return lax.all_to_all(array, axis, split_axis=0, concat_axis=0, tiled=True)]
    all_to_all x1 -> x2, blocking collectives: 23.5 us -> 68.9 us  [exchanged(): return lax.all_to_all(array, axis, split_axis=0, concat_axis=0, tiled=True)]
    pallas_call x0 -> x9, Pallas kernels: none -> 25.7 us  [call(): pl.pallas_call(kernel, out_shape=shapes, in_specs=[SCALAR] * scalars + [W...]
    all_to_all x8 -> x4, starting transfers between devices: 40.6 us -> 15.9 us  [exchanged(): return lax.all_to_all(array, axis, split_axis=0, concat_axis=0, tiled=True)]
    all_gather x1 -> x0, waiting for transfers between devices: 14.4 us -> none  [sent_together(): whole = lax.all_gather(both, axis, axis=dim, tiled=True)]
    all_gather x0 -> x2, blocking collectives: none -> 9.38 us  [the longest x1 5.49 us: body(): full_rows = lax.all_gather(full_rows, 'core', axis=0, tiled=False)]
    ppermute x0 -> x2, starting transfers between devices: none -> 7.86 us  [the longest x1 5.94 us: body(): other = lax.ppermute(own, 'core', swap)]
    reshape x10 -> x1, local copies, waits for them, and re-layouts: 7.11 us -> 0.09 us  [carried(): total - cum]
  transfers between devices with their start and end apart: 9 -> 6, of which waited for: 9 -> 5; matrix products, arithmetic and copies ran while one was open for 10% -> 10% of each run, Pallas kernels for 0% -> 4%
where the time goes in v1:
time: 195 us; the launch traced here: 194 us
  blocking collectives  78.3 us (40%)
  waiting for transfers between devices  37.8 us (19%)
  Pallas kernels  25.7 us (13%)
  starting transfers between devices  23.7 us (12%)
  matrix products  12.5 us (6%)
  local copies, waits for them, and re-layouts  9.73 us (5%)
  other arithmetic  4.9 us (3%)
    all_to_all x2, blocking collectives, exchanged(): return lax.all_to_all(array, axis, split_axis=0, concat_axis=0, tiled=True)  68.9 us
    all_to_all x4, waiting for transfers between devices, exchanged(): return lax.all_to_all(array, axis, split_axis=0, concat_axis=0, tiled=True)  36.8 us
    pallas_call x9, Pallas kernels, call(): pl.pallas_call(kernel, out_shape=shapes, in_specs=[SCALAR] * scalars + [W...  25.7 us
    all_to_all x4, starting transfers between devices, exchanged(): return lax.all_to_all(array, axis, split_axis=0, concat_axis=0, tiled=True)  15.9 us
    unnamed x61, local copies, waits for them, and re-layouts  7.64 us
    ppermute x1, starting transfers between devices, body(): other = lax.ppermute(own, 'core', swap)  5.94 us
    all_gather x1, blocking collectives, body(): full_rows = lax.all_gather(full_rows, 'core', axis=0, tiled=False)  5.49 us
    dot_general x3, matrix products, dot(): lax.dot_general(a, b, (((da,), (db,)), ((), ())), preferred_element_type=...  4.28 us
  transfers between devices with their start and end apart: 6, of which 5 were waited for; matrix products, arithmetic and copies ran while one was open for 10% of the time, Pallas kernels for 4%

profile of v1, /device:TPU:1, one launch (start us, length us, event | category | flops | bytes accessed | tf_op | source)
XLA Modules:
  0.0 193.6 jit_solution(3035413347797894980)
XLA Ops:
  0.6 1.4 copy.55.ids_ref
  2.0 1.4 copy.56.share_ref
  3.5 2.6 %shard_map.197 = (bf16[32,16,256]{2,1,0:T(8,128)(2,1)}, bf16[512,128]{1,0:T(8,128)(2,1)}, f32[32,128]{1,0:T(8,128)}) custom-call(s32[128,2]{1,0:T(8,128)} %copy.55.ids_ref, f32[128,2]{1,0:T(8,128)} %copy.56.share_ref, bf16[128,128]{1,0:T(8,128)(2,1)} %x_ref.1, bf16[128,128]{1,0:T(8,128)(2,1)} %cot_ref.3, bf16[32,128]{1,0:T(8,128)(2,1)} %key_ref.3, ...), custom_call_target="tpu_custom_call" | custom-call | tf_op jit(solution)/shard_map/pallas_call | solution.py:284
  6.0 25.1 %all_to_all.30.got_ref = bf16[32,16,256]{2,1,0:T(8,128)(2,1)} all-to-all(bf16[32,16,256]{2,1,0:T(8,128)(2,1)} %get-tuple-element.25), channel_id=1, replica_groups=mesh['z'=8,'x'=4,'y'=8,'core'=2] {'z','x'}, dimensions={0} | all-to-all | bytes 524288 | tf_op jit(solution)/shard_map/all_to_all | solution.py:331
  31.1 2.5 %shard_map.198 = (bf16[8,384,256]{2,1,0:T(8,128)(2,1)}, bf16[32,16,128]{2,1,0:T(8,128)(2,1)}) custom-call(bf16[32,16,256]{2,1,0:T(8,128)(2,1)} %all_to_all.30.got_ref), custom_call_target="tpu_custom_call" | custom-call | tf_op jit(solution)/shard_map/pallas_call | solution.py:284
  33.6 43.8 %all_to_all.31.own_ref = bf16[8,384,256]{2,1,0:T(8,128)(2,1)S(1)} all-to-all(bf16[8,384,256]{2,1,0:T(8,128)(2,1)} %get-tuple-element.26), channel_id=1, replica_groups=mesh['z'=8,'x'=4,'y'=8,'core'=2] {'y'}, dimensions={0} | all-to-all | bytes 3145728 | tf_op jit(solution)/shard_map/all_to_all | solution.py:331
  77.5 5.9 %collective-permute-start = (bf16[8,384,256]{2,1,0:T(8,128)(2,1)S(1)}, bf16[8,384,256]{2,1,0:T(8,128)(2,1)}, u32[]{:S(2)}, u32[]{:S(2)}) collective-permute-start(bf16[8,384,256]{2,1,0:T(8,128)(2,1)S(1)} %all_to_all.31.own_ref), channel_id=1, source_target_pairs={{0,1},{1,0},{2,3},{3,2},{4,5},{5,4},{6,7},{7,6},{8,9},{9,8},{10,11... | collective-permute-start | bytes 4718600 | tf_op jit(solution)/shard_map/ppermute | solution.py:367
  83.4 0.0 copy-done.1
  83.4 0.0 copy-done.2
  83.5 0.1 pad_maximum_fusion
  83.6 1.9 collective-permute-start.1
  85.5 1.1 collective-permute-done.other_ref
  86.6 5.3 %shard_map.199 = (bf16[384,2048]{1,0:T(8,128)(2,1)}, bf16[384,2048]{1,0:T(8,128)(2,1)}, bf16[384,256]{1,0:T(8,128)(2,1)}, bf16[384,128]{1,0:T(8,128)(2,1)}) custom-call(s32[1]{0:T(128)} %bitcast.2.core_ref, bf16[8,384,256]{2,1,0:T(8,128)(2,1)} %copy-done, bf16[8,384,256]{2,1,0:T(8,128)(2,1)} %collective-permute-done.other_ref, bf16[2048,128]{1,0:T(8,128)(2,1)} %bitcast.73, ...), custom_call_target="tpu_custom_call" | custom-call | tf_op jit(solution)/shard_map/pallas_call | solution.py:284
  91.9 3.9 %all-gather = bf16[768,256]{1,0:T(8,128)(2,1)} all-gather(bf16[384,256]{1,0:T(8,128)(2,1)} %get-tuple-element.27), channel_id=2, replica_groups=mesh['z'=8,'x'=4,'y'=8,'core'=2] {'core'}, dimensions={0}, use_global_device_ids=true | all-gather | bytes 589824 | tf_op jit(solution)/shard_map/all_gather | solution.py:384
  95.8 0.0 collective-permute-done.1.swapped_ref
  95.8 0.8 copy-done.8
  96.6 3.4 %shard_map.200 = bf16[8,384,128]{2,1,0:T(8,128)(2,1)} custom-call(s32[1]{0:T(128)} %bitcast.2.core_ref, bf16[2,384,256]{2,1,0:T(8,128)(2,1)} %bitcast.80, bf16[16,128,128]{2,1,0:T(8,128)(2,1)} %bitcast.74, bf16[16,128,128]{2,1,0:T(8,128)(2,1)} %bitcast.77, bf16[2,8,128,128]{3,2,1,0:T(8,128)(2,1)} %copy-done.8), custom_call_target="tpu_custom_call" | custom-call | tf_op jit(solution)/shard_map/pallas_call | solution.py:284
  100.0 3.7 %all-to-all-start.2 = ((bf16[8,384,128]{2,1,0:T(8,128)(2,1)}), bf16[8,384,128]{2,1,0:T(8,128)(2,1)S(1)}, u32[]{:S(2)}, u32[]{:S(2)}) async-start(bf16[8,384,128]{2,1,0:T(8,128)(2,1)} %shard_map.200), calls=%async_computation.2 | async-start | bytes 1572864 | tf_op jit(solution)/shard_map/all_to_all | solution.py:331
  103.7 1.0 copy.63.weight_ref
  104.7 0.0 copy-start.23
  104.7 0.2 slice_reduce_fusion
  104.9 0.1 fusion.45
  105.0 0.0 copy-start.15
  105.0 0.0 copy-start.14
  105.1 0.3 copy-done.23
  105.3 0.1 copy-done.27
  105.5 0.2 copy-done.25
  105.6 1.3 fusion.2
  106.9 0.0 copy-start.16
  106.9 0.1 fusion.55
  107.0 2.2 %convolution_convert_fusion = bf16[2048,256]{1,0:T(8,128)(2,1)S(1)} fusion(bf16[384,2048]{1,0:T(8,128)(2,1)} %get-tuple-element.39, bf16[384,256]{1,0:T(8,128)(2,1)S(1)} %copy-done.13), kind=kOutput, calls=%fused_computation.3 | convolution fusion | flops 403177472 | bytes 2818048 | tf_op jit(solution)/shard_map/dot_general | solution.py:27
  109.2 18.0 %all-to-all-done.2.parts_ref = bf16[8,384,128]{2,1,0:T(8,128)(2,1)S(1)} async-done(((bf16[8,384,128]{2,1,0:T(8,128)(2,1)}), bf16[8,384,128]{2,1,0:T(8,128)(2,1)S(1)}, u32[]{:S(2)}, u32[]{:S(2)}) %all-to-all-start.2) | async-done | bytes 786464 | tf_op jit(solution)/shard_map/all_to_all | solution.py:331
  127.2 0.9 copy-done.3
  128.1 2.2 %shard_map.201 = bf16[32,16,128]{2,1,0:T(8,128)(2,1)} custom-call(bf16[8,384,128]{2,1,0:T(8,128)(2,1)} %copy-done.3, bf16[32,16,128]{2,1,0:T(8,128)(2,1)} %get-tuple-element.28.back_ref), custom_call_target="tpu_custom_call" | custom-call | tf_op jit(solution)/shard_map/pallas_call | solution.py:284
  130.4 4.8 %all-to-all-start.3 = ((bf16[32,16,128]{2,1,0:T(8,128)(2,1)}), bf16[32,16,128]{2,1,0:T(8,128)(2,1)S(1)}, u32[]{:S(2)}, u32[]{:S(2)}) async-start(bf16[32,16,128]{2,1,0:T(8,128)(2,1)} %shard_map.201), calls=%async_computation.3 | async-start | bytes 262144 | tf_op jit(solution)/shard_map/all_to_all | solution.py:331
  135.2 1.0 slice_bitcast_fusion
  136.3 1.3 fusion
  137.5 7.0 %all-to-all-done.3.got_ref = bf16[32,16,128]{2,1,0:T(8,128)(2,1)S(1)} async-done(((bf16[32,16,128]{2,1,0:T(8,128)(2,1)}), bf16[32,16,128]{2,1,0:T(8,128)(2,1)S(1)}, u32[]{:S(2)}, u32[]{:S(2)}) %all-to-all-start.3) | async-done | bytes 131104 | tf_op jit(solution)/shard_map/all_to_all | solution.py:331
  144.6 0.7 copy-done.6
  145.2 1.9 shard_map.202
  147.1 3.4 %all-to-all-start.4 = ((bf16[8,128,128]{2,1,0:T(8,128)(2,1)}), bf16[8,128,128]{2,1,0:T(8,128)(2,1)S(1)}, u32[]{:S(2)}, u32[]{:S(2)}) async-start(bf16[8,128,128]{2,1,0:T(8,128)(2,1)} %shard_map.202), calls=%async_computation.4 | async-start | bytes 524288 | tf_op jit(solution)/shard_map/all_to_all | solution.py:331
  150.5 2.6 %shard_map.203 = (f32[32,128]{1,0:T(8,128)}, f32[32,32,128]{2,1,0:T(8,128)}) custom-call(s32[1]{0:T(128)} %bitcast.17.place_ref, bf16[32,16,128]{2,1,0:T(8,128)(2,1)} %copy-done.6), custom_call_target="tpu_custom_call" | custom-call | tf_op jit(solution)/shard_map/pallas_call | solution.py:284
  153.1 1.0 fusion.42
  154.1 1.0 fusion.21
  155.2 0.7 copy.64.inv_ref
  155.9 0.7 fusion.53
  156.6 0.7 pad_maximum_fusion.1.mix_ref
  157.3 2.4 %all-to-all-done.4 = bf16[8,128,128]{2,1,0:T(8,128)(2,1)S(1)} async-done(((bf16[8,128,128]{2,1,0:T(8,128)(2,1)}), bf16[8,128,128]{2,1,0:T(8,128)(2,1)S(1)}, u32[]{:S(2)}, u32[]{:S(2)}) %all-to-all-start.4) | async-done | bytes 262176 | tf_op jit(solution)/shard_map/all_to_all | solution.py:331
  159.7 5.5 %all-gather.1 = bf16[16,128,128]{2,1,0:T(8,128)(2,1)} all-gather(bf16[8,128,128]{2,1,0:T(8,128)(2,1)S(1)} %all-to-all-done.4), channel_id=3, replica_groups=mesh['z'=8,'x'=4,'y'=8,'core'=2] {'core'}, dimensions={0}, use_global_device_ids=true | all-gather | bytes 786432 | tf_op jit(solution)/shard_map/all_gather | solution.py:405
  165.2 2.8 %shard_map.204 = (bf16[32,64,128]{2,1,0:T(8,128)(2,1)}, f32[128,64]{1,0:T(8,128)}) custom-call(bf16[2,8,128,128]{3,2,1,0:T(8,128)(2,1)} %bitcast.79, bf16[2048,64]{1,0:T(8,128)(2,1)} %copy.63.weight_ref, f32[128,64]{1,0:T(8,128)} %get-tuple-element.45.normed_ref, f32[128,1]{1,0:T(8,128)} %copy.64.inv_ref, bf16[128,128]{1,0:T(8,128)(2,1)} %pad_maximum_fusion.1.mix_ref, ...), custom_call_target="tpu_custom_call" | custom-call | tf_op jit(solution)/shard_map/pallas_call | solution.py:284
  168.0 1.0 fusion.56
  169.0 1.0 fusion.40
  170.0 3.9 %all-to-all-start.5 = ((bf16[32,64,128]{2,1,0:T(8,128)(2,1)}), bf16[32,64,128]{2,1,0:T(8,128)(2,1)S(1)}, u32[]{:S(2)}, u32[]{:S(2)}) async-start(bf16[32,64,128]{2,1,0:T(8,128)(2,1)} %get-tuple-element.33), calls=%async_computation.5 | async-start | bytes 1048576 | tf_op jit(solution)/shard_map/all_to_all | solution.py:331
  173.9 0.0 copy-start.17
  174.0 0.9 fusion.8
  174.9 0.9 fusion.46
  175.8 0.1 copy.65
  175.9 2.1 %fusion.11 = (f32[32,128]{1,0:T(8,128)S(1)}, f32[32,128]{1,0:T(8,128)S(1)}) fusion(f32[128,128]{1,0:T(8,128)S(1)} %fusion.56, f32[32,128]{1,0:T(8,128)S(1)} %copy-done.22, f32[32,128]{1,0:T(8,128)S(1)} %copy-done.26, f32[32,128]{1,0:T(8,128)S(1)} %copy-done.10, pred[128,128]{1,0:T(8,128)(4,1)S(1)} %copy-done.24), kind=kLoop, calls=%fused_computation.15 | loop fusion | flops 6283264 | bytes 163840 | tf_op jit(solution)/shard_map/transpose(jvp())/reduce_sum | solution.py:294
  178.0 0.8 fusion.23.decay_mix_ref
  178.9 0.8 fusion.57.vals_mix_ref
  179.6 1.5 fusion.6
  181.2 9.3 %all-to-all-done.5.got_ref = bf16[32,64,128]{2,1,0:T(8,128)(2,1)S(1)} async-done(((bf16[32,64,128]{2,1,0:T(8,128)(2,1)}), bf16[32,64,128]{2,1,0:T(8,128)(2,1)S(1)}, u32[]{:S(2)}, u32[]{:S(2)}) %all-to-all-start.5) | async-done | bytes 524320 | tf_op jit(solution)/shard_map/all_to_all | solution.py:331
  190.4 0.8 copy-done.4
  191.3 2.4 %shard_map.205 = (f32[64,64]{1,0:T(8,128)}, f32[32,128]{1,0:T(8,128)}, f32[64,128]{1,0:T(8,128)}, f32[32,128]{1,0:T(8,128)}) custom-call(bf16[32,64,128]{2,1,0:T(8,128)(2,1)} %copy-done.4, f32[32,32,128]{2,1,0:T(8,128)} %get-tuple-element.34.reach_ref, f32[32,128]{1,0:T(8,128)} %get-tuple-element.31.state_ref, f32[32,128]{1,0:T(8,128)} %get-tuple-element.30.cum_ref, ...), custom_call_target="tpu_custom_call" | custom-call | tf_op jit(solution)/shard_map/pallas_call | solution.py:284
  (48 shorter events, 0.2 us)
Async XLA Ops:
  33.6 49.8 %copy-start.1 = (bf16[1,2048,128]{2,1,0:T(8,128)(2,1)S(1)}, bf16[1,2048,128]{2,1,0:T(8,128)(2,1)}, u32[]{:S(2)}) copy-start(bf16[1,2048,128]{2,1,0:T(8,128)(2,1)} %param.25) | copy-start | bytes 1572868
  33.6 49.8 %copy-start.2 = (bf16[1,2048,128]{2,1,0:T(8,128)(2,1)S(1)}, bf16[1,2048,128]{2,1,0:T(8,128)(2,1)}, u32[]{:S(2)}) copy-start(bf16[1,2048,128]{2,1,0:T(8,128)(2,1)} %param.26) | copy-start | bytes 1572868
  77.5 9.1 %copy-start = (bf16[8,384,256]{2,1,0:T(8,128)(2,1)}, bf16[8,384,256]{2,1,0:T(8,128)(2,1)S(1)}, u32[]{:S(2)}) copy-start(bf16[8,384,256]{2,1,0:T(8,128)(2,1)S(1)} %all_to_all.31.own_ref) | copy-start | bytes 4718596
  77.5 9.1 %collective-permute-start = (bf16[8,384,256]{2,1,0:T(8,128)(2,1)S(1)}, bf16[8,384,256]{2,1,0:T(8,128)(2,1)}, u32[]{:S(2)}, u32[]{:S(2)}) collective-permute-start(bf16[8,384,256]{2,1,0:T(8,128)(2,1)S(1)} %all_to_all.31.own_ref), channel_id=1, source_target_pairs={{0,1},{1,0},{2,3},{3,2},{4,5},{5,4},{6,7},{7,6},{8,9},{9,8},{10,11... | collective-permute-start | bytes 4718600 | tf_op jit(solution)/shard_map/ppermute | solution.py:367
  83.6 12.2 %collective-permute-start.1 = (bf16[2,8,128,128]{3,2,1,0:T(8,128)(2,1)S(1)}, bf16[2,8,128,128]{3,2,1,0:T(8,128)(2,1)S(1)}, u32[]{:S(2)}, u32[]{:S(2)}) collective-permute-start(bf16[2,8,128,128]{3,2,1,0:T(8,128)(2,1)S(1)} %pad_maximum_fusion), channel_id=1, source_target_pairs={{0,1},{1,0},{2,3},{3,2},{4,5},{5,4},{6,7},{7,6},{8,9},{9,8},{10,11... | collective-permute-start | bytes 1572872 | tf_op jit(solution)/shard_map/ppermute | solution.py:365
  95.8 0.8 copy-start.8
  96.6 7.1 %copy-start.19 = (bf16[32,128]{1,0:T(8,128)(2,1)S(1)}, bf16[32,128]{1,0:T(8,128)(2,1)}, u32[]{:S(2)}) copy-start(bf16[32,128]{1,0:T(8,128)(2,1)} %key_ref.3) | copy-start | bytes 24580
  96.6 7.1 %copy-start.12 = (bf16[2048,64]{0,1:T(8,128)(2,1)S(1)}, bf16[2048,64]{0,1:T(8,128)(2,1)}, u32[]{:S(2)}) copy-start(bf16[2048,64]{0,1:T(8,128)(2,1)} %param.20) | copy-start | bytes 786436
  100.0 4.8 %copy-start.10 = (f32[32,128]{1,0:T(8,128)S(1)}, f32[32,128]{1,0:T(8,128)}, u32[]{:S(2)}) copy-start(f32[32,128]{1,0:T(8,128)} %get-tuple-element.30.cum_ref) | copy-start | bytes 49156
  100.0 5.0 %copy-start.20 = (bf16[32,128]{1,0:T(8,128)(2,1)S(1)}, bf16[32,128]{1,0:T(8,128)(2,1)}, u32[]{:S(2)}) copy-start(bf16[32,128]{1,0:T(8,128)(2,1)} %param.14) | copy-start | bytes 24580
  100.0 6.9 %copy-start.11 = (bf16[64,128]{1,0:T(8,128)(2,1)S(1)}, bf16[64,128]{1,0:T(8,128)(2,1)}, u32[]{:S(2)}) copy-start(bf16[64,128]{1,0:T(8,128)(2,1)} %val_ref.3) | copy-start | bytes 49156
  100.0 7.1 %copy-start.13 = (bf16[384,256]{1,0:T(8,128)(2,1)S(1)}, bf16[384,256]{1,0:T(8,128)(2,1)}, u32[]{:S(2)}) copy-start(bf16[384,256]{1,0:T(8,128)(2,1)} %get-tuple-element.27) | copy-start | bytes 589828
  100.0 27.3 %all-to-all-start.2 = ((bf16[8,384,128]{2,1,0:T(8,128)(2,1)}), bf16[8,384,128]{2,1,0:T(8,128)(2,1)S(1)}, u32[]{:S(2)}, u32[]{:S(2)}) async-start(bf16[8,384,128]{2,1,0:T(8,128)(2,1)} %shard_map.200), calls=%async_computation.2 | async-start | bytes 1572864 | tf_op jit(solution)/shard_map/all_to_all | solution.py:331
  103.7 1.4 copy-start.21
  104.7 0.6 copy-start.23
  104.9 0.5 copy-start.27
  105.0 0.6 copy-start.25
  105.0 48.1 %copy-start.15 = (f32[32,128]{1,0:T(8,128)}, f32[32,128]{1,0:T(8,128)S(1)}, u32[]{:S(2)}) copy-start(f32[32,128]{1,0:T(8,128)S(1)} %get-tuple-element.51.query_fwd_ref) | copy-start | bytes 49156
  105.0 49.1 %copy-start.14 = (f32[32,128]{1,0:T(8,128)}, f32[32,128]{1,0:T(8,128)S(1)}, u32[]{:S(2)}) copy-start(f32[32,128]{1,0:T(8,128)S(1)} %get-tuple-element.50.query_bwd_ref) | copy-start | bytes 49156
  106.9 2.3 %copy-start.16 = (bf16[128,128]{1,0:T(8,128)(2,1)}, bf16[128,128]{1,0:T(8,128)(2,1)S(1)}, u32[]{:S(2)}) copy-start(bf16[128,128]{1,0:T(8,128)(2,1)S(1)} %fusion.2) | copy-start | bytes 98308
  127.2 0.9 copy-start.3
  128.1 8.1 %copy-start.5 = (bf16[384,2048]{1,0:T(8,128)(2,1)S(1)}, bf16[384,2048]{1,0:T(8,128)(2,1)}, u32[]{:S(2)}) copy-start(bf16[384,2048]{1,0:T(8,128)(2,1)} %get-tuple-element.41) | copy-start | bytes 4718596
  130.4 5.9 %copy-start.18 = (bf16[384,128]{1,0:T(8,128)(2,1)S(1)}, bf16[384,128]{1,0:T(8,128)(2,1)}, u32[]{:S(2)}) copy-start(bf16[384,128]{1,0:T(8,128)(2,1)} %get-tuple-element.40) | copy-start | bytes 294916
  130.4 14.2 %all-to-all-start.3 = ((bf16[32,16,128]{2,1,0:T(8,128)(2,1)}), bf16[32,16,128]{2,1,0:T(8,128)(2,1)S(1)}, u32[]{:S(2)}, u32[]{:S(2)}) async-start(bf16[32,16,128]{2,1,0:T(8,128)(2,1)} %shard_map.201), calls=%async_computation.3 | async-start | bytes 262144 | tf_op jit(solution)/shard_map/all_to_all | solution.py:331
  144.6 0.7 copy-start.6
  147.1 12.6 %all-to-all-start.4 = ((bf16[8,128,128]{2,1,0:T(8,128)(2,1)}), bf16[8,128,128]{2,1,0:T(8,128)(2,1)S(1)}, u32[]{:S(2)}, u32[]{:S(2)}) async-start(bf16[8,128,128]{2,1,0:T(8,128)(2,1)} %shard_map.202), calls=%async_computation.4 | async-start | bytes 524288 | tf_op jit(solution)/shard_map/all_to_all | solution.py:331
  153.1 15.9 %copy-start.9 = (f32[32,128]{1,0:T(8,128)S(1)}, f32[32,128]{1,0:T(8,128)}, u32[]{:S(2)}) copy-start(f32[32,128]{1,0:T(8,128)} %get-tuple-element.31.state_ref) | copy-start | bytes 49156
  157.3 16.6 %copy-start.24 = (pred[128,128]{1,0:T(8,128)(4,1)S(1)}, pred[128,128]{1,0:T(8,128)(4,1)}, u32[]{:S(2)}) copy-start(pred[128,128]{1,0:T(8,128)(4,1)} %copy-done.23) | copy-start | bytes 49156
  170.0 20.5 %all-to-all-start.5 = ((bf16[32,64,128]{2,1,0:T(8,128)(2,1)}), bf16[32,64,128]{2,1,0:T(8,128)(2,1)S(1)}, u32[]{:S(2)}, u32[]{:S(2)}) async-start(bf16[32,64,128]{2,1,0:T(8,128)(2,1)} %get-tuple-element.33), calls=%async_computation.5 | async-start | bytes 1048576 | tf_op jit(solution)/shard_map/all_to_all | solution.py:331
  173.9 1.0 copy-start.7
  173.9 1.0 copy-start.28
  173.9 2.0 %copy-start.22 = (f32[32,128]{1,0:T(8,128)S(1)}, f32[32,128]{1,0:T(8,128)}, u32[]{:S(2)}) copy-start(f32[32,128]{1,0:T(8,128)} %copy-done.21) | copy-start | bytes 49156
  173.9 2.0 %copy-start.26 = (f32[32,128]{1,0:T(8,128)S(1)}, f32[32,128]{1,0:T(8,128)}, u32[]{:S(2)}) copy-start(f32[32,128]{1,0:T(8,128)} %copy-done.25) | copy-start | bytes 49156
  173.9 4.9 %copy-start.17 = (bf16[128,128]{1,0:T(8,128)(2,1)S(1)}, bf16[128,128]{1,0:T(8,128)(2,1)}, u32[]{:S(2)}) copy-start(bf16[128,128]{1,0:T(8,128)(2,1)} %copy-done.16) | copy-start | bytes 98308
  190.4 0.8 copy-start.4

commit v2 on v1

--- a/solution.py
+++ b/solution.py
@@ -279,13 +279,21 @@
 WHOLE = pl.BlockSpec(memory_space=pltpu.VMEM)
 
 
-def call(kernel, outs, *args, scalars=0):
-    shapes = [jax.ShapeDtypeStruct(shape, dtype) for shape, dtype in outs]
+def on_chip(array):
+    return pltpu.with_memory_space_constraint(array, pltpu.VMEM)
+
+
+def call(kernel, outs, *args, scalars=0, stored=()):
+    shapes = [
+        (jax.ShapeDtypeStruct if k in stored else pltpu.VMEM)(shape, dtype)
+        for k, (shape, dtype) in enumerate(outs)
+    ]
     return pl.pallas_call(
         kernel,
         out_shape=shapes,
         in_specs=[SCALAR] * scalars + [WHOLE] * (len(args) - scalars),
         out_specs=[WHOLE] * len(shapes),
+        compiler_params=pltpu.CompilerParams(vmem_limit_bytes=24 << 20),
     )(*args)
 
 
@@ -346,7 +354,7 @@
         extra_log_decay,
         speed,
     )
-    got = exchanged(send, sp)
+    got = on_chip(exchanged(send, sp))
     copies, back = call(
         arrival_kernel,
         [((RING, ROWS, 2 * WIDTH), BF16), ((PEERS, PAD, WIDTH), BF16)],
@@ -374,30 +382,31 @@
             ((ROWS, WIDTH), BF16),
         ],
         core_at,
-        own,
-        other,
+        on_chip(own),
+        on_chip(other),
         gate,
         up,
         down,
         scalars=1,
+        stored=(0, 1),
     )
     grads_both = lax.all_gather(grads, "core", axis=0, tiled=False)
     (partials,) = call(
         partial_kernel,
         [((RING, ROWS, WIDTH), BF16)],
         core_at,
-        grads_both,
+        on_chip(grads_both),
         gate_blocks,
         up_blocks,
-        swapped,
+        on_chip(swapped),
         scalars=1,
     )
     parts = exchanged(partials, "y")
     grad_both = dot(rows_x, grads, 0, 0).astype(BF16)
     grad_gate, grad_up = grad_both[:, :WIDTH], grad_both[:, WIDTH:]
     grad_down = dot(hidden, rows_dy, 0, 0).astype(BF16)
-    (send,) = call(return_kernel, [((PEERS, PAD, WIDTH), BF16)], parts, back)
-    returned = exchanged(send, sp)
+    (send,) = call(return_kernel, [((PEERS, PAD, WIDTH), BF16)], on_chip(parts), on_chip(back))
+    returned = on_chip(exchanged(send, sp))
     (copies,) = call(
         token_kernel, [((RING, TOK, WIDTH), BF16)], returned, pick, cotangent
     )
@@ -427,7 +436,7 @@
     send, grad_mixed_t = call(
         source_kernel,
         [((PEERS, 2 * KEY_DIM, WIDTH), BF16), ((TOK, VAL_DIM), F32)],
-        full_rows,
+        on_chip(full_rows),
         output_weight_matrix,
         normed_t,
         inv_rms.reshape(TOK, 1),
@@ -450,7 +459,7 @@
             ((VAL_DIM, TOK), F32),
             ((KEY_DIM, TOK), F32),
         ],
-        got,
+        on_chip(got),
         reach,
         state,
         cum,
@@ -461,6 +470,7 @@
         grad_keys,
         grad_vals,
         grad_decay,
+        stored=range(4),
     )
     return (
         grad_queries,

time: 195 us -> 182 us (0.933)
  Pallas kernels: 25.7 us -> 12.8 us
  waiting for transfers between devices: 37.8 us -> 43.3 us
  matrix products: 12.5 us -> 7.11 us
  local copies, waits for them, and re-layouts: 9.73 us -> 13.9 us
  blocking collectives: 78.3 us -> 75.9 us
    pallas_call x9, Pallas kernels: 25.7 us -> 12.8 us  [call(): pl.pallas_call(kernel, out_shape=shapes, in_specs=[SCALAR] * scalars + [W...]
    all_to_all x4, waiting for transfers between devices: 36.8 us -> 42.2 us  [exchanged(): return lax.all_to_all(array, axis, split_axis=0, concat_axis=0, tiled=True)]
    unnamed x61 -> x59, local copies, waits for them, and re-layouts: 7.64 us -> 11.2 us
  transfers between devices with their start and end apart: 6 -> 6, of which waited for: 5 -> 5; matrix products, arithmetic and copies ran while one was open for 10% -> 8% of each run, Pallas kernels for 4% -> 3%
where the time goes in v2:
time: 182 us; the launch traced here: 181 us
  blocking collectives  75.9 us (42%)
  waiting for transfers between devices  43.3 us (24%)
  starting transfers between devices  23.7 us (13%)
  local copies, waits for them, and re-layouts  13.9 us (8%)
  Pallas kernels  12.8 us (7%)
  matrix products  7.11 us (4%)
  other arithmetic  3.68 us (2%)
    all_to_all x2, blocking collectives, exchanged(): return lax.all_to_all(array, axis, split_axis=0, concat_axis=0, tiled=True)  68.5 us
    all_to_all x4, waiting for transfers between devices, exchanged(): return lax.all_to_all(array, axis, split_axis=0, concat_axis=0, tiled=True)  42.2 us
    all_to_all x4, starting transfers between devices, exchanged(): return lax.all_to_all(array, axis, split_axis=0, concat_axis=0, tiled=True)  15.7 us
    pallas_call x9, Pallas kernels, call(): pl.pallas_call(kernel, out_shape=shapes, in_specs=[SCALAR] * scalars + [W...  12.8 us
    unnamed x59, local copies, waits for them, and re-layouts  11.2 us
    ppermute x1, starting transfers between devices, body(): other = lax.ppermute(own, 'core', swap)  6.06 us
    all_gather x1, blocking collectives, body(): full_rows = lax.all_gather(full_rows, 'core', axis=0, tiled=False)  5.36 us
  transfers between devices with their start and end apart: 6, of which 5 were waited for; matrix products, arithmetic and copies ran while one was open for 8% of the time, Pallas kernels for 3%

profile of v2, /device:TPU:1, one launch (start us, length us, event | category | flops | bytes accessed | tf_op | source)
XLA Modules:
  0.0 181.3 jit_solution(6735094314482597832)
XLA Ops:
  0.6 0.8 copy.55.ids_ref
  1.4 0.8 copy.56.share_ref
  2.2 0.7 copy-done.5
  2.9 0.8 copy-done.7
  3.7 0.7 copy-done.13
  4.4 0.7 copy-done.15
  5.1 0.8 copy-done.17
  5.8 0.7 copy-done.18
  6.6 0.7 copy-done.19
  7.2 0.9 shard_map.197
  8.1 24.8 %all_to_all.30.got_ref = bf16[32,16,256]{2,1,0:T(8,128)(2,1)S(1)} all-to-all(bf16[32,16,256]{2,1,0:T(8,128)(2,1)S(1)} %get-tuple-element.25), channel_id=1, replica_groups=mesh['z'=8,'x'=4,'y'=8,'core'=2] {'z','x'}, dimensions={0} | all-to-all | bytes 524288 | tf_op jit(solution)/shard_map/all_to_all | solution.py:339
  33.0 0.8 shard_map.198
  33.8 0.0 copy-start.1
  33.8 43.6 %all_to_all.31.own_ref = bf16[8,384,256]{2,1,0:T(8,128)(2,1)S(1)} all-to-all(bf16[8,384,256]{2,1,0:T(8,128)(2,1)S(1)} %get-tuple-element.26), channel_id=1, replica_groups=mesh['z'=8,'x'=4,'y'=8,'core'=2] {'y'}, dimensions={0} | all-to-all | bytes 3145728 | tf_op jit(solution)/shard_map/all_to_all | solution.py:339
  77.5 6.1 %collective-permute-start = (bf16[8,384,256]{2,1,0:T(8,128)(2,1)S(1)}, bf16[8,384,256]{2,1,0:T(8,128)(2,1)}, u32[]{:S(2)}, u32[]{:S(2)}) collective-permute-start(bf16[8,384,256]{2,1,0:T(8,128)(2,1)S(1)} %all_to_all.31.own_ref), channel_id=1, source_target_pairs={{0,1},{1,0},{2,3},{3,2},{4,5},{5,4},{6,7},{7,6},{8,9},{9,8},{10,11... | collective-permute-start | bytes 4718600 | tf_op jit(solution)/shard_map/ppermute | solution.py:375
  83.6 0.1 pad_maximum_fusion
  83.7 1.9 %collective-permute-start.1 = (bf16[2,8,128,128]{3,2,1,0:T(8,128)(2,1)S(1)}, bf16[2,8,128,128]{3,2,1,0:T(8,128)(2,1)S(1)}, u32[]{:S(2)}, u32[]{:S(2)}) collective-permute-start(bf16[2,8,128,128]{3,2,1,0:T(8,128)(2,1)S(1)} %pad_maximum_fusion), channel_id=1, source_target_pairs={{0,1},{1,0},{2,3},{3,2},{4,5},{5,4},{6,7},{7,6},{8,9},{9,8},{10,11... | collective-permute-start | bytes 1572872 | tf_op jit(solution)/shard_map/ppermute | solution.py:373
  85.6 1.1 collective-permute-done.other_ref
  86.7 3.7 %shard_map.199 = (bf16[384,2048]{1,0:T(8,128)(2,1)S(1)}, bf16[384,2048]{1,0:T(8,128)(2,1)S(1)}, bf16[384,256]{1,0:T(8,128)(2,1)S(1)}, bf16[384,128]{1,0:T(8,128)(2,1)S(1)}) custom-call(s32[1]{0:T(128)} %bitcast.2.core_ref, bf16[8,384,256]{2,1,0:T(8,128)(2,1)S(1)} %all_to_all.31.own_ref, bf16[8,384,256]{2,1,0:T(8,128)(2,1)} %collective-permute-done.other_ref, ...), custom_call_target="tpu_custom_call" | custom-call | tf_op jit(solution)/shard_map/pallas_call | solution.py:291
  90.4 1.2 copy-done.2
  91.6 1.2 copy-done.21
  92.8 2.1 %all-gather = bf16[768,256]{1,0:T(8,128)(2,1)S(1)} all-gather(bf16[384,256]{1,0:T(8,128)(2,1)S(1)} %get-tuple-element.27), channel_id=2, replica_groups=mesh['z'=8,'x'=4,'y'=8,'core'=2] {'core'}, dimensions={0}, use_global_device_ids=true | all-gather | bytes 589824 | tf_op jit(solution)/shard_map/all_gather | solution.py:393
  94.9 1.9 %shard_map.200 = bf16[8,384,128]{2,1,0:T(8,128)(2,1)} custom-call(s32[1]{0:T(128)} %bitcast.2.core_ref, bf16[2,384,256]{2,1,0:T(8,128)(2,1)S(1)} %bitcast.80, bf16[16,128,128]{2,1,0:T(8,128)(2,1)S(1)} %bitcast.75, bf16[16,128,128]{2,1,0:T(8,128)(2,1)S(1)} %bitcast.78, bf16[2,8,128,128]{3,2,1,0:T(8,128)(2,1)S(1)} %collective-permute-done.1.swapped_ref), custom_call_target="tpu_custom_call" | custom-call | tf_op jit(solution)/shard_map/pallas_call | solution.py:291
  96.7 3.7 %all-to-all-start.2 = ((bf16[8,384,128]{2,1,0:T(8,128)(2,1)}), bf16[8,384,128]{2,1,0:T(8,128)(2,1)S(1)}, u32[]{:S(2)}, u32[]{:S(2)}) async-start(bf16[8,384,128]{2,1,0:T(8,128)(2,1)} %shard_map.200), calls=%async_computation.2 | async-start | bytes 1572864 | tf_op jit(solution)/shard_map/all_to_all | solution.py:339
  100.4 1.2 copy.63.weight_ref
  101.7 0.2 slice_reduce_fusion
  101.9 0.0 copy-start.26
  101.9 0.1 fusion.45
  102.0 0.4 copy-done.26
  102.4 0.6 copy-done.24
  103.0 1.3 fusion.2
  104.3 0.1 fusion.55
  104.4 0.0 copy-start.10
  104.4 1.8 convolution_convert_fusion
  106.2 17.8 %all-to-all-done.2.parts_ref = bf16[8,384,128]{2,1,0:T(8,128)(2,1)S(1)} async-done(((bf16[8,384,128]{2,1,0:T(8,128)(2,1)}), bf16[8,384,128]{2,1,0:T(8,128)(2,1)S(1)}, u32[]{:S(2)}, u32[]{:S(2)}) %all-to-all-start.2) | async-done | bytes 786464 | tf_op jit(solution)/shard_map/all_to_all | solution.py:339
  124.0 1.0 shard_map.201
  125.0 4.7 %all-to-all-start.3 = ((bf16[32,16,128]{2,1,0:T(8,128)(2,1)}), bf16[32,16,128]{2,1,0:T(8,128)(2,1)S(1)}, u32[]{:S(2)}, u32[]{:S(2)}) async-start(bf16[32,16,128]{2,1,0:T(8,128)(2,1)} %shard_map.201), calls=%async_computation.3 | async-start | bytes 262144 | tf_op jit(solution)/shard_map/all_to_all | solution.py:339
  129.7 2.2 %slice_bitcast_fusion = (bf16[1,2048,128]{2,1,0:T(8,128)(2,1)}, bf16[1,2048,128]{2,1,0:T(8,128)(2,1)}) fusion(bf16[2048,256]{1,0:T(8,128)(2,1)} %convolution_convert_fusion), kind=kLoop, calls=%fused_computation.25 | loop fusion | bytes 2097152 | tf_op jit(solution)/shard_map/broadcast_in_dim | solution.py:482
  131.9 1.3 fusion
  133.2 5.8 %all-to-all-done.3.got_ref = bf16[32,16,128]{2,1,0:T(8,128)(2,1)S(1)} async-done(((bf16[32,16,128]{2,1,0:T(8,128)(2,1)}), bf16[32,16,128]{2,1,0:T(8,128)(2,1)S(1)}, u32[]{:S(2)}, u32[]{:S(2)}) %all-to-all-start.3) | async-done | bytes 131104 | tf_op jit(solution)/shard_map/all_to_all | solution.py:339
  139.0 0.9 shard_map.202
  139.9 3.4 %all-to-all-start.4 = ((bf16[8,128,128]{2,1,0:T(8,128)(2,1)}), bf16[8,128,128]{2,1,0:T(8,128)(2,1)S(1)}, u32[]{:S(2)}, u32[]{:S(2)}) async-start(bf16[8,128,128]{2,1,0:T(8,128)(2,1)} %shard_map.202), calls=%async_computation.4 | async-start | bytes 524288 | tf_op jit(solution)/shard_map/all_to_all | solution.py:339
  143.4 0.9 shard_map.203
  144.2 0.2 fusion.42
  144.5 0.3 fusion.21
  144.8 0.1 copy.64.inv_ref
  144.9 0.1 fusion.53
  145.0 0.1 pad_maximum_fusion.1.mix_ref
  145.1 7.5 %all-to-all-done.4 = bf16[8,128,128]{2,1,0:T(8,128)(2,1)S(1)} async-done(((bf16[8,128,128]{2,1,0:T(8,128)(2,1)}), bf16[8,128,128]{2,1,0:T(8,128)(2,1)S(1)}, u32[]{:S(2)}, u32[]{:S(2)}) %all-to-all-start.4) | async-done | bytes 262176 | tf_op jit(solution)/shard_map/all_to_all | solution.py:339
  152.5 5.4 %all-gather.1 = bf16[16,128,128]{2,1,0:T(8,128)(2,1)S(1)} all-gather(bf16[8,128,128]{2,1,0:T(8,128)(2,1)S(1)} %all-to-all-done.4), channel_id=3, replica_groups=mesh['z'=8,'x'=4,'y'=8,'core'=2] {'core'}, dimensions={0}, use_global_device_ids=true | all-gather | bytes 786432 | tf_op jit(solution)/shard_map/all_gather | solution.py:414
  157.9 1.6 shard_map.204
  159.5 0.1 fusion.56
  159.6 0.1 fusion.40
  159.7 3.9 %all-to-all-start.5 = ((bf16[32,64,128]{2,1,0:T(8,128)(2,1)}), bf16[32,64,128]{2,1,0:T(8,128)(2,1)S(1)}, u32[]{:S(2)}, u32[]{:S(2)}) async-start(bf16[32,64,128]{2,1,0:T(8,128)(2,1)} %get-tuple-element.33), calls=%async_computation.5 | async-start | bytes 1048576 | tf_op jit(solution)/shard_map/all_to_all | solution.py:339
  163.6 0.0 copy-start.27
  163.7 0.9 fusion.8
  164.6 0.9 fusion.46
  165.5 0.1 copy.65
  165.6 2.1 %fusion.11 = (f32[32,128]{1,0:T(8,128)S(1)}, f32[32,128]{1,0:T(8,128)S(1)}) fusion(f32[128,128]{1,0:T(8,128)S(1)} %fusion.56, f32[32,128]{1,0:T(8,128)S(1)} %convert.3, f32[32,128]{1,0:T(8,128)S(1)} %copy-done.25, f32[32,128]{1,0:T(8,128)S(1)} %get-tuple-element.30.cum_ref, pred[128,128]{1,0:T(8,128)(4,1)S(1)} %iota_compare_fusion), kind=kLoop, calls=%fused_computation.15 | loop fusion | flops 6283264 | bytes 163840 | tf_op jit(solution)/shard_map/transpose(jvp())/reduce_sum | solution.py:302
  167.7 0.2 fusion.23.decay_mix_ref
  167.9 0.2 fusion.57.vals_mix_ref
  168.1 0.9 fusion.6
  169.1 11.1 %all-to-all-done.5.got_ref = bf16[32,64,128]{2,1,0:T(8,128)(2,1)S(1)} async-done(((bf16[32,64,128]{2,1,0:T(8,128)(2,1)}), bf16[32,64,128]{2,1,0:T(8,128)(2,1)S(1)}, u32[]{:S(2)}, u32[]{:S(2)}) %all-to-all-start.5) | async-done | bytes 524320 | tf_op jit(solution)/shard_map/all_to_all | solution.py:339
  180.2 1.1 shard_map.205
  (46 shorter events, 0.2 us)
Async XLA Ops:
  2.2 0.7 copy-start.5
  2.9 0.8 copy-start.7
  3.7 0.7 copy-start.13
  4.4 0.7 copy-start.15
  5.1 0.8 copy-start.17
  5.8 0.7 copy-start.18
  6.6 0.7 copy-start.19
  33.8 43.7 %copy-start.9 = (bf16[32,16,128]{2,1,0:T(8,128)(2,1)}, bf16[32,16,128]{2,1,0:T(8,128)(2,1)S(1)}, u32[]{:S(2)}) copy-start(bf16[32,16,128]{2,1,0:T(8,128)(2,1)S(1)} %get-tuple-element.28.back_ref) | copy-start | bytes 393220
  33.8 49.7 %copy-start = (bf16[1,2048,128]{2,1,0:T(8,128)(2,1)S(1)}, bf16[1,2048,128]{2,1,0:T(8,128)(2,1)}, u32[]{:S(2)}) copy-start(bf16[1,2048,128]{2,1,0:T(8,128)(2,1)} %param.25) | copy-start | bytes 1572868
  33.8 49.7 %copy-start.1 = (bf16[1,2048,128]{2,1,0:T(8,128)(2,1)S(1)}, bf16[1,2048,128]{2,1,0:T(8,128)(2,1)}, u32[]{:S(2)}) copy-start(bf16[1,2048,128]{2,1,0:T(8,128)(2,1)} %param.26) | copy-start | bytes 1572868
  77.5 9.2 %copy-start.4 = (bf16[1,128,2048]{2,1,0:T(8,128)(2,1)S(1)}, bf16[1,128,2048]{2,1,0:T(8,128)(2,1)}, u32[]{:S(2)}) copy-start(bf16[1,128,2048]{2,1,0:T(8,128)(2,1)} %param.27) | copy-start | bytes 1572868
  77.5 9.2 %collective-permute-start = (bf16[8,384,256]{2,1,0:T(8,128)(2,1)S(1)}, bf16[8,384,256]{2,1,0:T(8,128)(2,1)}, u32[]{:S(2)}, u32[]{:S(2)}) collective-permute-start(bf16[8,384,256]{2,1,0:T(8,128)(2,1)S(1)} %all_to_all.31.own_ref), channel_id=1, source_target_pairs={{0,1},{1,0},{2,3},{3,2},{4,5},{5,4},{6,7},{7,6},{8,9},{9,8},{10,11... | collective-permute-start | bytes 4718600 | tf_op jit(solution)/shard_map/ppermute | solution.py:375
  83.7 11.2 %collective-permute-start.1 = (bf16[2,8,128,128]{3,2,1,0:T(8,128)(2,1)S(1)}, bf16[2,8,128,128]{3,2,1,0:T(8,128)(2,1)S(1)}, u32[]{:S(2)}, u32[]{:S(2)}) collective-permute-start(bf16[2,8,128,128]{3,2,1,0:T(8,128)(2,1)S(1)} %pad_maximum_fusion), channel_id=1, source_target_pairs={{0,1},{1,0},{2,3},{3,2},{4,5},{5,4},{6,7},{7,6},{8,9},{9,8},{10,11... | collective-permute-start | bytes 1572872 | tf_op jit(solution)/shard_map/ppermute | solution.py:373
  90.4 1.2 copy-start.2
  91.6 1.2 copy-start.21
  92.8 2.1 %copy-start.11 = (bf16[384,128]{1,0:T(8,128)(2,1)}, bf16[384,128]{1,0:T(8,128)(2,1)S(1)}, u32[]{:S(2)}) copy-start(bf16[384,128]{1,0:T(8,128)(2,1)S(1)} %get-tuple-element.40) | copy-start | bytes 294916
  94.9 5.6 %copy-start.14 = (bf16[32,128]{1,0:T(8,128)(2,1)S(1)}, bf16[32,128]{1,0:T(8,128)(2,1)}, u32[]{:S(2)}) copy-start(bf16[32,128]{1,0:T(8,128)(2,1)} %key_ref.3) | copy-start | bytes 24580
  96.7 5.2 %copy-start.23 = (bf16[32,128]{1,0:T(8,128)(2,1)S(1)}, bf16[32,128]{1,0:T(8,128)(2,1)}, u32[]{:S(2)}) copy-start(bf16[32,128]{1,0:T(8,128)(2,1)} %param.14) | copy-start | bytes 24580
  96.7 7.5 %copy-start.6 = (bf16[64,128]{1,0:T(8,128)(2,1)S(1)}, bf16[64,128]{1,0:T(8,128)(2,1)}, u32[]{:S(2)}) copy-start(bf16[64,128]{1,0:T(8,128)(2,1)} %val_ref.3) | copy-start | bytes 49156
  96.7 7.7 %copy-start.22 = (bf16[384,2048]{1,0:T(8,128)(2,1)S(1)}, bf16[384,2048]{1,0:T(8,128)(2,1)}, u32[]{:S(2)}) copy-start(bf16[384,2048]{1,0:T(8,128)(2,1)} %copy-done.21) | copy-start | bytes 4718596
  96.7 27.2 %all-to-all-start.2 = ((bf16[8,384,128]{2,1,0:T(8,128)(2,1)}), bf16[8,384,128]{2,1,0:T(8,128)(2,1)S(1)}, u32[]{:S(2)}, u32[]{:S(2)}) async-start(bf16[8,384,128]{2,1,0:T(8,128)(2,1)} %shard_map.200), calls=%async_computation.2 | async-start | bytes 1572864 | tf_op jit(solution)/shard_map/all_to_all | solution.py:339
  101.9 0.5 copy-start.26
  102.4 0.6 copy-start.24
  104.4 19.6 %copy-start.10 = (bf16[32,16,128]{2,1,0:T(8,128)(2,1)S(1)}, bf16[32,16,128]{2,1,0:T(8,128)(2,1)}, u32[]{:S(2)}) copy-start(bf16[32,16,128]{2,1,0:T(8,128)(2,1)} %copy-done.9) | copy-start | bytes 393220
  124.0 7.9 %copy-start.3 = (bf16[384,2048]{1,0:T(8,128)(2,1)S(1)}, bf16[384,2048]{1,0:T(8,128)(2,1)}, u32[]{:S(2)}) copy-start(bf16[384,2048]{1,0:T(8,128)(2,1)} %copy-done.2) | copy-start | bytes 4718596
  124.0 7.9 %copy-start.12 = (bf16[384,128]{1,0:T(8,128)(2,1)S(1)}, bf16[384,128]{1,0:T(8,128)(2,1)}, u32[]{:S(2)}) copy-start(bf16[384,128]{1,0:T(8,128)(2,1)} %copy-done.11) | copy-start | bytes 294916
  125.0 14.1 %all-to-all-start.3 = ((bf16[32,16,128]{2,1,0:T(8,128)(2,1)}), bf16[32,16,128]{2,1,0:T(8,128)(2,1)S(1)}, u32[]{:S(2)}, u32[]{:S(2)}) async-start(bf16[32,16,128]{2,1,0:T(8,128)(2,1)} %shard_map.201), calls=%async_computation.3 | async-start | bytes 262144 | tf_op jit(solution)/shard_map/all_to_all | solution.py:339
  131.9 7.1 %copy-start.8 = (bf16[128,128]{1,0:T(8,128)(2,1)S(1)}, bf16[128,128]{1,0:T(8,128)(2,1)}, u32[]{:S(2)}) copy-start(bf16[128,128]{1,0:T(8,128)(2,1)} %cot_ref.3) | copy-start | bytes 98308
  139.9 12.6 %all-to-all-start.4 = ((bf16[8,128,128]{2,1,0:T(8,128)(2,1)}), bf16[8,128,128]{2,1,0:T(8,128)(2,1)S(1)}, u32[]{:S(2)}, u32[]{:S(2)}) async-start(bf16[8,128,128]{2,1,0:T(8,128)(2,1)} %shard_map.202), calls=%async_computation.4 | async-start | bytes 524288 | tf_op jit(solution)/shard_map/all_to_all | solution.py:339
  159.7 20.5 %all-to-all-start.5 = ((bf16[32,64,128]{2,1,0:T(8,128)(2,1)}), bf16[32,64,128]{2,1,0:T(8,128)(2,1)S(1)}, u32[]{:S(2)}, u32[]{:S(2)}) async-start(bf16[32,64,128]{2,1,0:T(8,128)(2,1)} %get-tuple-element.33), calls=%async_computation.5 | async-start | bytes 1048576 | tf_op jit(solution)/shard_map/all_to_all | solution.py:339
  163.6 1.0 copy-start.27
  163.6 2.0 %copy-start.25 = (f32[32,128]{1,0:T(8,128)S(1)}, f32[32,128]{1,0:T(8,128)}, u32[]{:S(2)}) copy-start(f32[32,128]{1,0:T(8,128)} %copy-done.24) | copy-start | bytes 49156
  168.1 12.1 %copy-start.16 = (bf16[32,128]{1,0:T(8,128)(2,1)S(1)}, bf16[32,128]{1,0:T(8,128)(2,1)}, u32[]{:S(2)}) copy-start(bf16[32,128]{1,0:T(8,128)(2,1)} %pre_ref.3) | copy-start | bytes 24580
  168.1 12.1 %copy-start.20 = (f32[32]{0:T(128)S(1)}, f32[32]{0:T(128)}, u32[]{:S(2)}) copy-start(f32[32]{0:T(128)} %param.19) | copy-start | bytes 388

commit v3 on v2

--- a/solution.py
+++ b/solution.py
@@ -61,21 +61,18 @@
     ids_ref, share_ref, x_ref, cot_ref, key_ref, val_ref, pre_ref, extra_ref, speed_ref,
     send_ref, pick_ref, cum_ref,
 ):
-    ids = ids_ref[...]
-    expert = iota((TOK, PEERS), 1)
-    named = [ones_where(ids[:, k : k + 1] == expert) for k in range(2)]
+    expert = iota((PEERS, TOK), 0)
+    named = [ids_ref[k : k + 1, :] == expert for k in range(2)]
     row, col = iota((TOK, TOK), 0), iota((TOK, TOK), 1)
-    earlier, same = ones_where(row < col), ones_where(row == col)
-    rank = dot(named[0] + named[1], earlier, 0, 0)
+    rank = dot(ones_where(named[0] | named[1]), ones_where(row < col), 1, 0)
     place = iota((PEERS, PAD, TOK), 1).astype(F32)
     cot = cot_ref[...].astype(F32)
     picks, grads = [], None
     for k in range(2):
-        mine = dot(named[k], same, 0, 0)
-        at = jnp.where(mine > 0.5, rank, -1.0)
+        at = jnp.where(named[k], rank, -1.0)
         pick = jnp.where(at[:, None, :] == place, 1.0, 0.0).reshape(SLOTS, TOK).astype(BF16)
-        weighted = (share_ref[:, k : k + 1] * cot).astype(BF16)
-        part = dot(pick, weighted, 1, 0)
+        share = jnp.sum(jnp.where(row == col, share_ref[k : k + 1, :], 0.0), axis=1, keepdims=True)
+        part = dot(pick, (share * cot).astype(BF16), 1, 0)
         grads = part if grads is None else grads + part
         picks.append(pick)
     pick = picks[0] + picks[1]
@@ -110,11 +107,12 @@
     send_ref[...] = block.astype(BF16)
 
 
-def arrival_kernel(got_ref, copies_ref, back_ref):
+def arrival_kernel(got_ref, x_ref, copies_ref, back_ref):
     got = got_ref[...].reshape(SLOTS, 2 * WIDTH)
     rows = dot(ones_where(compact_rows((ROWS, SLOTS), 0)), got, 1, 0).astype(BF16)
+    x_ref[...] = rows[:, :WIDTH]
     for k in range(RING):
-        copies_ref[k] = rows
+        copies_ref[k] = rows[:, WIDTH:]
     both = dot(ones_where(row_of_peer(CAP)), got, 1, 0)
     state = both[:, :WIDTH] + both[:, WIDTH:]
     logs = dot(ones_where(row_of_peer(CAP + 1)), got, 1, 0)
@@ -138,25 +136,25 @@
     back_ref[...] = block.astype(BF16)
 
 
-def expert_kernel(
-    core_ref, own_ref, other_ref, gate_ref, up_ref, down_ref,
-    x_ref, y_ref, grads_ref, hidden_ref,
-):
+def forward_kernel(core_ref, own_ref, other_ref, gate_ref, up_ref, pre_ref):
     core = core_ref[0]
-    for mine in range(2):
-
-        @pl.when(core == mine)
-        def _():
-            for side, ref in ((mine, own_ref), (1 - mine, other_ref)):
-                for k in range(RING):
-                    at = slice((2 * k + side) * WIDTH, (2 * k + side + 1) * WIDTH)
-                    x_ref[:, at] = ref[k, :, :WIDTH]
-                    y_ref[:, at] = ref[k, :, WIDTH:]
-
-    x, y = x_ref[...], y_ref[...]
-    gate_pre = dot(x, gate_ref[...], 1, 0)
-    up_pre = dot(x, up_ref[...], 1, 0)
-    grad_hidden = dot(y, down_ref[...], 1, 1)
+    total = jnp.zeros((ROWS, 2 * WIDTH), F32)
+    for k in range(RING):
+        for side, ref in ((core, own_ref), (1 - core, other_ref)):
+            at = 2 * k + side
+            weights = jnp.concatenate([gate_ref[at], up_ref[at]], axis=1)
+            total = total + dot(ref[k], weights, 1, 0)
+    pre_ref[...] = total
+
+
+def hidden_kernel(core_ref, own_ref, other_ref, down_ref, pre_ref, grads_ref, hidden_ref):
+    core = core_ref[0]
+    grad_hidden = jnp.zeros((ROWS, WIDTH), F32)
+    for k in range(RING):
+        for side, ref in ((core, own_ref), (1 - core, other_ref)):
+            at = pl.multiple_of((2 * k + side) * WIDTH, WIDTH)
+            grad_hidden = grad_hidden + dot(ref[k], down_ref[:, pl.ds(at, WIDTH)], 1, 1)
+    gate_pre, up_pre = pre_ref[:, :WIDTH], pre_ref[:, WIDTH:]
     gate_sig = jax.nn.sigmoid(gate_pre)
     gate_act = gate_pre * gate_sig
     hidden_ref[...] = (gate_act * up_pre).astype(BF16)
@@ -164,6 +162,22 @@
         grad_hidden * up_pre * gate_sig * (1.0 + gate_pre * (1.0 - gate_sig))
     ).astype(BF16)
     grads_ref[:, WIDTH:] = (grad_hidden * gate_act).astype(BF16)
+
+
+def weight_kernel(
+    core_ref, x_ref, other_x_ref, y_ref, other_y_ref, grads_ref, hidden_ref,
+    gate_ref, up_ref, down_ref,
+):
+    core = core_ref[0]
+    grads, hidden = grads_ref[...], hidden_ref[...]
+    for k in range(RING):
+        for side, x, y in ((core, x_ref, y_ref), (1 - core, other_x_ref, other_y_ref)):
+            at = 2 * k + side
+            both = dot(x[k], grads, 0, 0).astype(BF16)
+            gate_ref[at] = both[:, :WIDTH]
+            up_ref[at] = both[:, WIDTH:]
+            lanes = pl.ds(pl.multiple_of(at * WIDTH, WIDTH), WIDTH)
+            down_ref[:, lanes] = dot(hidden, y[k], 0, 0).astype(BF16)
 
 
 def partial_kernel(core_ref, grads_ref, gate_ref, up_ref, swapped_ref, out_ref):
@@ -216,7 +230,7 @@
     send_ref, grad_ref,
 ):
     rows = jnp.concatenate([rows_ref[c, k] for k in range(RING) for c in range(2)], axis=1)
-    grad = dot(rows, weight_ref[...], 1, 0)
+    grad = dot(rows, weight_ref[...], 1, 1)
     normed = normed_ref[...]
     mean = jnp.mean(grad * normed, axis=1, keepdims=True)
     grad = inv_ref[...] * (grad - normed * mean)
@@ -283,6 +297,10 @@
     return pltpu.with_memory_space_constraint(array, pltpu.VMEM)
 
 
+def off_chip(array):
+    return pltpu.with_memory_space_constraint(array, pltpu.HBM)
+
+
 def call(kernel, outs, *args, scalars=0, stored=()):
     shapes = [
         (jax.ShapeDtypeStruct if k in stored else pltpu.VMEM)(shape, dtype)
@@ -344,23 +362,24 @@
     send, pick, cum = call(
         dispatch_kernel,
         [((PEERS, PAD, 2 * WIDTH), BF16), ((SLOTS, TOK), BF16), ((KEY_DIM, TOK), F32)],
-        chosen_expert_index,
-        expert_combine_weight,
-        stored_expert_rows,
-        cotangent,
-        input_key_matrix,
-        input_value_matrix,
-        decay_preactivation,
-        extra_log_decay,
-        speed,
+        off_chip(chosen_expert_index.T),
+        off_chip(expert_combine_weight.T),
+        off_chip(stored_expert_rows),
+        off_chip(cotangent),
+        off_chip(input_key_matrix),
+        off_chip(input_value_matrix),
+        off_chip(decay_preactivation),
+        off_chip(extra_log_decay),
+        off_chip(speed),
     )
     got = on_chip(exchanged(send, sp))
-    copies, back = call(
+    rows_x, copies, back = call(
         arrival_kernel,
-        [((RING, ROWS, 2 * WIDTH), BF16), ((PEERS, PAD, WIDTH), BF16)],
+        [((ROWS, WIDTH), BF16), ((RING, ROWS, WIDTH), BF16), ((PEERS, PAD, WIDTH), BF16)],
         got,
     )
-    own = exchanged(copies, "y")
+    own_y = exchanged(copies, "y")
+    own_x = lax.all_gather(rows_x, "y", axis=0, tiled=False)
 
     theirs = jnp.stack(
         [
@@ -372,23 +391,27 @@
     )
     swapped = lax.ppermute(theirs, "core", swap)
 
-    other = lax.ppermute(own, "core", swap)
-    rows_x, rows_dy, grads, hidden = call(
-        expert_kernel,
-        [
-            ((ROWS, MODEL), BF16),
-            ((ROWS, MODEL), BF16),
-            ((ROWS, 2 * WIDTH), BF16),
-            ((ROWS, WIDTH), BF16),
-        ],
+    other_x = lax.ppermute(own_x, "core", swap)
+    other_y = lax.ppermute(own_y, "core", swap)
+    (pre,) = call(
+        forward_kernel,
+        [((ROWS, 2 * WIDTH), F32)],
         core_at,
-        on_chip(own),
-        on_chip(other),
-        gate,
-        up,
+        own_x,
+        other_x,
+        gate_blocks,
+        up_blocks,
+        scalars=1,
+    )
+    grads, hidden = call(
+        hidden_kernel,
+        [((ROWS, 2 * WIDTH), BF16), ((ROWS, WIDTH), BF16)],
+        core_at,
+        own_y,
+        other_y,
         down,
+        pre,
         scalars=1,
-        stored=(0, 1),
     )
     grads_both = lax.all_gather(grads, "core", axis=0, tiled=False)
     (partials,) = call(
@@ -398,18 +421,16 @@
         on_chip(grads_both),
         gate_blocks,
         up_blocks,
-        on_chip(swapped),
+        swapped,
         scalars=1,
     )
     parts = exchanged(partials, "y")
-    grad_both = dot(rows_x, grads, 0, 0).astype(BF16)
-    grad_gate, grad_up = grad_both[:, :WIDTH], grad_both[:, WIDTH:]
-    grad_down = dot(hidden, rows_dy, 0, 0).astype(BF16)
     (send,) = call(return_kernel, [((PEERS, PAD, WIDTH), BF16)], on_chip(parts), on_chip(back))
     returned = on_chip(exchanged(send, sp))
     (copies,) = call(
         token_kernel, [((RING, TOK, WIDTH), BF16)], returned, pick, cotangent
     )
+    cum, copies = lax.optimization_barrier((cum, copies))
     full_rows = exchanged(copies, "y")
     full_rows = lax.all_gather(full_rows, "core", axis=0, tiled=False)
 
@@ -437,14 +458,32 @@
         source_kernel,
         [((PEERS, 2 * KEY_DIM, WIDTH), BF16), ((TOK, VAL_DIM), F32)],
         on_chip(full_rows),
-        output_weight_matrix,
+        output_weight_matrix.T,
         normed_t,
         inv_rms.reshape(TOK, 1),
         jnp.concatenate([mix_t, mix_t], axis=1),
         scaled * jnp.exp(cum),
         scaled * jnp.exp(cum[:, -1:] - cum),
     )
+    send, grads, hidden = lax.optimization_barrier((send, grads, hidden))
     got = exchanged(send, sp)
+    grad_gate, grad_up, grad_down = call(
+        weight_kernel,
+        [
+            ((2 * RING, WIDTH, WIDTH), BF16),
+            ((2 * RING, WIDTH, WIDTH), BF16),
+            ((WIDTH, MODEL), BF16),
+        ],
+        core_at,
+        own_x,
+        other_x,
+        own_y,
+        other_y,
+        grads,
+        hidden,
+        scalars=1,
+        stored=range(3),
+    )
     grad_mixed = grad_mixed_t.T
     grad_scaled, grad_keys, grad_vals, grad_cum = pull_inner(grad_mixed)
     grad_scaled_in, grad_cum_in = pull_carried(grad_mixed)
@@ -478,8 +517,8 @@
         grad_values,
         grad_logit,
         grad_out_proj,
-        grad_gate[None],
-        grad_up[None],
+        grad_gate.reshape(1, MODEL, WIDTH),
+        grad_up.reshape(1, MODEL, WIDTH),
         grad_down[None],
     )
 

time: 182 us -> 180 us (0.989)
  waiting for transfers between devices: 43.3 us -> 23 us
  blocking collectives: 75.9 us -> 96 us
  local copies, waits for them, and re-layouts: 13.9 us -> 2.18 us
  starting transfers between devices: 23.7 us -> 32.8 us
  Pallas kernels: 12.8 us -> 15.9 us
  matrix products: 7.11 us -> 4.08 us
    all_gather x0 -> x1, blocking collectives: none -> 35.2 us  [body(): own_x = lax.all_gather(rows_x, 'y', axis=0, tiled=False)]
    all_to_all x4, waiting for transfers between devices: 42.2 us -> 22.9 us  [exchanged(): return lax.all_to_all(array, axis, split_axis=0, concat_axis=0, tiled=True)]
    all_to_all x2, blocking collectives: 68.5 us -> 53.1 us  [exchanged(): return lax.all_to_all(array, axis, split_axis=0, concat_axis=0, tiled=True)]
    unnamed x59 -> x44, local copies, waits for them, and re-layouts: 11.2 us -> 1.75 us
    ppermute x1 -> x2, starting transfers between devices: 6.06 us -> 10.9 us  [the longest x1 8.95 us: body(): other_x = lax.ppermute(own_x, 'core', swap)]
    all_to_all x4, starting transfers between devices: 15.7 us -> 19.5 us  [exchanged(): return lax.all_to_all(array, axis, split_axis=0, concat_axis=0, tiled=True)]
    dot_general x3 -> x1, matrix products: 3.25 us -> 0.23 us  [dot(): lax.dot_general(a, b, (((da,), (db,)), ((), ())), preferred_element_type=...]
    pallas_call x9 -> x11, Pallas kernels: 12.8 us -> 15.9 us  [call(): pl.pallas_call(kernel, out_shape=shapes, in_specs=[SCALAR] * scalars + [W...]
  transfers between devices with their start and end apart: 6 -> 7, of which waited for: 5 -> 3; matrix products, arithmetic and copies ran while one was open for 8% -> 4% of each run, Pallas kernels for 3% -> 4%
where the time goes in v3:
time: 180 us; the launch traced here: 179 us
  blocking collectives  96 us (53%)
  starting transfers between devices  32.8 us (18%)
  waiting for transfers between devices  23 us (13%)
  Pallas kernels  15.9 us (9%)
  matrix products  4.08 us (2%)
  other arithmetic  3.68 us (2%)
  local copies, waits for them, and re-layouts  2.18 us (1%)
    all_to_all x2, blocking collectives, exchanged(): return lax.all_to_all(array, axis, split_axis=0, concat_axis=0, tiled=True)  53.1 us
    all_gather x1, blocking collectives, body(): own_x = lax.all_gather(rows_x, 'y', axis=0, tiled=False)  35.2 us
    all_to_all x4, waiting for transfers between devices, exchanged(): return lax.all_to_all(array, axis, split_axis=0, concat_axis=0, tiled=True)  22.9 us
    all_to_all x4, starting transfers between devices, exchanged(): return lax.all_to_all(array, axis, split_axis=0, concat_axis=0, tiled=True)  19.5 us
    pallas_call x11, Pallas kernels, call(): pl.pallas_call(kernel, out_shape=shapes, in_specs=[SCALAR] * scalars + [W...  15.9 us
    ppermute x1, starting transfers between devices, body(): other_x = lax.ppermute(own_x, 'core', swap)  8.95 us
    all_gather x1, blocking collectives, body(): full_rows = lax.all_gather(full_rows, 'core', axis=0, tiled=False)  5.57 us
  transfers between devices with their start and end apart: 7, of which 3 were waited for; matrix products, arithmetic and copies ran while one was open for 4% of the time, Pallas kernels for 4%

profile of v3, /device:TPU:1, one launch (start us, length us, event | category | flops | bytes accessed | tf_op | source)
XLA Modules:
  0.0 178.6 jit_solution(13499665522885159491)
XLA Ops:
  0.6 1.6 shard_map.197
  2.3 24.8 %all_to_all.30.got_ref = bf16[32,16,256]{2,1,0:T(8,128)(2,1)S(1)} all-to-all(bf16[32,16,256]{2,1,0:T(8,128)(2,1)S(1)} %get-tuple-element.33), channel_id=1, replica_groups=mesh['z'=8,'x'=4,'y'=8,'core'=2] {'z','x'}, dimensions={0} | all-to-all | bytes 524288 | tf_op jit(solution)/shard_map/all_to_all | solution.py:357
  27.1 1.3 shard_map.198
  28.4 0.7 copy-done.10
  29.0 6.8 %all-to-all-start.1 = ((bf16[8,384,128]{2,1,0:T(8,128)(2,1)}), bf16[8,384,128]{2,1,0:T(8,128)(2,1)S(1)}, u32[]{:S(2)}, u32[]{:S(2)}) async-start(bf16[8,384,128]{2,1,0:T(8,128)(2,1)} %get-tuple-element.34), calls=%async_computation.1 | async-start | bytes 1572864 | tf_op jit(solution)/shard_map/all_to_all | solution.py:357
  35.8 35.2 %all-gather = bf16[3072,128]{1,0:T(8,128)(2,1)S(1)} all-gather(bf16[384,128]{1,0:T(8,128)(2,1)S(1)} %get-tuple-element.35), channel_id=2, replica_groups=mesh['z'=8,'x'=4,'y'=8,'core'=2] {'y'}, dimensions={0}, use_global_device_ids=true | all-gather | bytes 884736 | tf_op jit(solution)/shard_map/all_gather | solution.py:382
  71.0 9.0 %collective-permute-start.1 = (bf16[8,384,128]{2,1,0:T(8,128)(2,1)S(1)}, bf16[8,384,128]{2,1,0:T(8,128)(2,1)S(1)}, u32[]{:S(2)}, u32[]{:S(2)}) collective-permute-start(bf16[8,384,128]{2,1,0:T(8,128)(2,1)S(1)} %bitcast.68), channel_id=1, source_target_pairs={{0,1},{1,0},{2,3},{3,2},{4,5},{5,4},{6,7},{7,6},{8,9},{9,8},{10,11... | collective-permute-start | bytes 2359304 | tf_op jit(solution)/shard_map/ppermute | solution.py:394
  80.0 0.0 all-to-all-done.1.own_ref.y_ref
  80.0 1.9 %collective-permute-start = (bf16[8,384,128]{2,1,0:T(8,128)(2,1)S(1)}, bf16[8,384,128]{2,1,0:T(8,128)(2,1)}, u32[]{:S(2)}, u32[]{:S(2)}) collective-permute-start(bf16[8,384,128]{2,1,0:T(8,128)(2,1)S(1)} %all-to-all-done.1.own_ref.y_ref), channel_id=1, source_target_pairs={{0,1},{1,0},{2,3},{3,2},{4,5},{5,4},{6,7},{7,6},{8,9},{9,8},{10,11... | collective-permute-start | bytes 2359304 | tf_op jit(solution)/shard_map/ppermute | solution.py:395
  81.9 0.0 copy-done.1
  82.0 0.0 copy-done
  82.0 0.1 pad_maximum_fusion
  82.1 2.4 %collective-permute-start.2 = (bf16[2,8,128,128]{3,2,1,0:T(8,128)(2,1)S(1)}, bf16[2,8,128,128]{3,2,1,0:T(8,128)(2,1)S(1)}, u32[]{:S(2)}, u32[]{:S(2)}) collective-permute-start(bf16[2,8,128,128]{3,2,1,0:T(8,128)(2,1)S(1)} %pad_maximum_fusion), channel_id=1, source_target_pairs={{0,1},{1,0},{2,3},{3,2},{4,5},{5,4},{6,7},{7,6},{8,9},{9,8},{10,11... | collective-permute-start | bytes 1572872 | tf_op jit(solution)/shard_map/ppermute | solution.py:392
  84.5 0.0 collective-permute-done.1.other_ref.other_x_ref
  84.5 0.0 copy-start.6
  84.5 1.0 shard_map.199.pre_ref
  85.5 0.0 collective-permute-done.other_ref.other_y_ref
  85.5 0.1 copy-done.6
  85.5 1.7 shard_map.200
  87.3 0.0 copy-start.2
  87.3 0.0 copy-start.12
  87.3 2.1 %all-gather.1 = bf16[768,256]{1,0:T(8,128)(2,1)S(1)} all-gather(bf16[384,256]{1,0:T(8,128)(2,1)S(1)} %get-tuple-element.51.grads_ref), channel_id=3, replica_groups=mesh['z'=8,'x'=4,'y'=8,'core'=2] {'core'}, dimensions={0}, use_global_device_ids=true | all-gather | bytes 589824 | tf_op jit(solution)/shard_map/all_gather | solution.py:416
  89.4 0.0 collective-permute-done.2.swapped_ref
  89.4 1.0 shard_map.201
  90.4 0.0 copy-start.11
  90.4 28.3 %all_to_all.31.parts_ref = bf16[8,384,128]{2,1,0:T(8,128)(2,1)S(1)} all-to-all(bf16[8,384,128]{2,1,0:T(8,128)(2,1)S(1)} %shard_map.201), channel_id=1, replica_groups=mesh['z'=8,'x'=4,'y'=8,'core'=2] {'y'}, dimensions={0} | all-to-all | bytes 1572864 | tf_op jit(solution)/shard_map/all_to_all | solution.py:357
  118.7 1.0 shard_map.202
  119.7 4.6 %all-to-all-start.3 = ((bf16[32,16,128]{2,1,0:T(8,128)(2,1)}), bf16[32,16,128]{2,1,0:T(8,128)(2,1)S(1)}, u32[]{:S(2)}, u32[]{:S(2)}) async-start(bf16[32,16,128]{2,1,0:T(8,128)(2,1)} %shard_map.202), calls=%async_computation.3 | async-start | bytes 262144 | tf_op jit(solution)/shard_map/all_to_all | solution.py:357
  124.3 0.0 copy-done.14
  124.3 0.0 copy-start.18
  124.4 0.0 copy-start.20
  124.4 9.3 %all-to-all-done.3.got_ref = bf16[32,16,128]{2,1,0:T(8,128)(2,1)S(1)} async-done(((bf16[32,16,128]{2,1,0:T(8,128)(2,1)}), bf16[32,16,128]{2,1,0:T(8,128)(2,1)S(1)}, u32[]{:S(2)}, u32[]{:S(2)}) %all-to-all-start.3) | async-done | bytes 131104 | tf_op jit(solution)/shard_map/all_to_all | solution.py:357
  133.7 0.9 shard_map.203
  134.6 0.2 slice_reduce_fusion
  134.8 4.2 %all-to-all-start.4 = ((bf16[8,128,128]{2,1,0:T(8,128)(2,1)}), bf16[8,128,128]{2,1,0:T(8,128)(2,1)}, u32[]{:S(2)}, u32[]{:S(2)}) async-start(bf16[8,128,128]{2,1,0:T(8,128)(2,1)} %shard_map.203), calls=%async_computation.4 | async-start | bytes 524288 | tf_op jit(solution)/shard_map/all_to_all | solution.py:357
  139.0 0.1 fusion.44
  139.1 1.3 fusion.1
  140.4 0.1 fusion.54
  140.5 0.9 shard_map.204
  141.4 0.2 fusion.41
  141.6 0.3 fusion.20
  141.9 0.1 copy.52.inv_ref
  142.1 0.1 fusion.52
  142.2 0.1 pad_maximum_fusion.1.mix_ref
  142.3 6.0 %all-to-all-done.4 = bf16[8,128,128]{2,1,0:T(8,128)(2,1)} async-done(((bf16[8,128,128]{2,1,0:T(8,128)(2,1)}), bf16[8,128,128]{2,1,0:T(8,128)(2,1)}, u32[]{:S(2)}, u32[]{:S(2)}) %all-to-all-start.4) | async-done | bytes 262176 | tf_op jit(solution)/shard_map/all_to_all | solution.py:357
  148.2 5.6 %all-gather.2 = bf16[16,128,128]{2,1,0:T(8,128)(2,1)S(1)} all-gather(bf16[8,128,128]{2,1,0:T(8,128)(2,1)} %all-to-all-done.4), channel_id=4, replica_groups=mesh['z'=8,'x'=4,'y'=8,'core'=2] {'core'}, dimensions={0}, use_global_device_ids=true | all-gather | bytes 786432 | tf_op jit(solution)/shard_map/all_gather | solution.py:435
  153.8 0.9 copy-done.8
  154.8 1.8 %shard_map.205 = (bf16[32,64,128]{2,1,0:T(8,128)(2,1)}, f32[128,64]{1,0:T(8,128)S(1)}) custom-call(bf16[2,8,128,128]{3,2,1,0:T(8,128)(2,1)S(1)} %bitcast.77, bf16[64,2048]{1,0:T(8,128)(2,1)S(1)} %bitcast.80, f32[128,64]{1,0:T(8,128)S(1)} %get-tuple-element.59.normed_ref, f32[128,1]{1,0:T(8,128)S(1)} %copy.52.inv_ref, ...), custom_call_target="tpu_custom_call" | custom-call | tf_op jit(solution)/shard_map/pallas_call | solution.py:309
  156.6 0.1 fusion.55
  156.7 0.1 fusion.39
  156.8 3.9 %all-to-all-start.5 = ((bf16[32,64,128]{2,1,0:T(8,128)(2,1)}), bf16[32,64,128]{2,1,0:T(8,128)(2,1)S(1)}, u32[]{:S(2)}, u32[]{:S(2)}) async-start(bf16[32,64,128]{2,1,0:T(8,128)(2,1)} %get-tuple-element.45), calls=%async_computation.5 | async-start | bytes 1048576 | tf_op jit(solution)/shard_map/all_to_all | solution.py:357
  160.8 0.0 copy-start.3
  160.8 0.0 copy-start.13
  160.8 0.9 fusion.7
  161.7 0.9 fusion.45
  162.6 0.1 copy.53
  162.7 0.0 copy-start.19
  162.7 3.5 %shard_map.207 = (bf16[16,128,128]{2,1,0:T(8,128)(2,1)}, bf16[16,128,128]{2,1,0:T(8,128)(2,1)}, bf16[128,2048]{1,0:T(8,128)(2,1)}) custom-call(s32[1]{0:T(128)} %bitcast.5.core_ref, bf16[8,384,128]{2,1,0:T(8,128)(2,1)S(1)} %bitcast.70, bf16[8,384,128]{2,1,0:T(8,128)(2,1)S(1)} %collective-permute-done.1.other_ref.other_x_ref, ...), custom_call_target="tpu_custom_call" | custom-call | tf_op jit(solution)/shard_map/pallas_call | solution.py:309
  166.3 2.1 %fusion.10 = (f32[32,128]{1,0:T(8,128)S(1)}, f32[32,128]{1,0:T(8,128)S(1)}) fusion(f32[128,128]{1,0:T(8,128)S(1)} %fusion.55, f32[32,128]{1,0:T(8,128)S(1)} %copy-done.19, f32[32,128]{1,0:T(8,128)S(1)} %get-tuple-element.64, f32[32,128]{1,0:T(8,128)S(1)} %get-tuple-element.40.cum_ref, pred[128,128]{1,0:T(8,128)(4,1)S(1)} %copy-done.21), kind=kLoop, calls=%fused_computation.12 | loop fusion | flops 6283264 | bytes 163840 | tf_op jit(solution)/shard_map/transpose(jvp())/reduce_sum | solution.py:320
  168.4 0.2 fusion.22.decay_mix_ref
  168.6 0.2 fusion.56.vals_mix_ref
  168.8 0.9 fusion.5
  169.7 7.7 %all-to-all-done.5.got_ref = bf16[32,64,128]{2,1,0:T(8,128)(2,1)S(1)} async-done(((bf16[32,64,128]{2,1,0:T(8,128)(2,1)}), bf16[32,64,128]{2,1,0:T(8,128)(2,1)S(1)}, u32[]{:S(2)}, u32[]{:S(2)}) %all-to-all-start.5) | async-done | bytes 524320 | tf_op jit(solution)/shard_map/all_to_all | solution.py:357
  177.4 1.1 shard_map.206
  (33 shorter events, 0.1 us)
Async XLA Ops:
  28.4 0.7 copy-start.10
  28.4 53.6 %copy-start.1 = (bf16[1,2048,128]{2,1,0:T(8,128)(2,1)S(1)}, bf16[1,2048,128]{2,1,0:T(8,128)(2,1)}, u32[]{:S(2)}) copy-start(bf16[1,2048,128]{2,1,0:T(8,128)(2,1)} %param.26) | copy-start | bytes 1572868
  29.0 51.0 %all-to-all-start.1 = ((bf16[8,384,128]{2,1,0:T(8,128)(2,1)}), bf16[8,384,128]{2,1,0:T(8,128)(2,1)S(1)}, u32[]{:S(2)}, u32[]{:S(2)}) async-start(bf16[8,384,128]{2,1,0:T(8,128)(2,1)} %get-tuple-element.34), calls=%async_computation.1 | async-start | bytes 1572864 | tf_op jit(solution)/shard_map/all_to_all | solution.py:357
  35.8 46.1 %copy-start = (bf16[1,2048,128]{2,1,0:T(8,128)(2,1)S(1)}, bf16[1,2048,128]{2,1,0:T(8,128)(2,1)}, u32[]{:S(2)}) copy-start(bf16[1,2048,128]{2,1,0:T(8,128)(2,1)} %param.25) | copy-start | bytes 1572868
  71.0 13.5 %collective-permute-start.1 = (bf16[8,384,128]{2,1,0:T(8,128)(2,1)S(1)}, bf16[8,384,128]{2,1,0:T(8,128)(2,1)S(1)}, u32[]{:S(2)}, u32[]{:S(2)}) collective-permute-start(bf16[8,384,128]{2,1,0:T(8,128)(2,1)S(1)} %bitcast.68), channel_id=1, source_target_pairs={{0,1},{1,0},{2,3},{3,2},{4,5},{5,4},{6,7},{7,6},{8,9},{9,8},{10,11... | collective-permute-start | bytes 2359304 | tf_op jit(solution)/shard_map/ppermute | solution.py:394
  80.0 5.5 %collective-permute-start = (bf16[8,384,128]{2,1,0:T(8,128)(2,1)S(1)}, bf16[8,384,128]{2,1,0:T(8,128)(2,1)}, u32[]{:S(2)}, u32[]{:S(2)}) collective-permute-start(bf16[8,384,128]{2,1,0:T(8,128)(2,1)S(1)} %all-to-all-done.1.own_ref.y_ref), channel_id=1, source_target_pairs={{0,1},{1,0},{2,3},{3,2},{4,5},{5,4},{6,7},{7,6},{8,9},{9,8},{10,11... | collective-permute-start | bytes 2359304 | tf_op jit(solution)/shard_map/ppermute | solution.py:395
  82.1 7.3 %collective-permute-start.2 = (bf16[2,8,128,128]{3,2,1,0:T(8,128)(2,1)S(1)}, bf16[2,8,128,128]{3,2,1,0:T(8,128)(2,1)S(1)}, u32[]{:S(2)}, u32[]{:S(2)}) collective-permute-start(bf16[2,8,128,128]{3,2,1,0:T(8,128)(2,1)S(1)} %pad_maximum_fusion), channel_id=1, source_target_pairs={{0,1},{1,0},{2,3},{3,2},{4,5},{5,4},{6,7},{7,6},{8,9},{9,8},{10,11... | collective-permute-start | bytes 1572872 | tf_op jit(solution)/shard_map/ppermute | solution.py:392
  84.5 1.0 copy-start.6
  87.3 2.1 %copy-start.2 = (bf16[384,256]{1,0:T(8,128)(2,1)}, bf16[384,256]{1,0:T(8,128)(2,1)S(1)}, u32[]{:S(2)}) copy-start(bf16[384,256]{1,0:T(8,128)(2,1)S(1)} %get-tuple-element.51.grads_ref) | copy-start | bytes 589828
  87.3 3.1 %copy-start.12 = (bf16[384,128]{1,0:T(8,128)(2,1)}, bf16[384,128]{1,0:T(8,128)(2,1)S(1)}, u32[]{:S(2)}) copy-start(bf16[384,128]{1,0:T(8,128)(2,1)S(1)} %get-tuple-element.52.hidden_ref) | copy-start | bytes 294916
  90.4 28.3 %copy-start.11 = (bf16[32,16,128]{2,1,0:T(8,128)(2,1)S(1)}, bf16[32,16,128]{2,1,0:T(8,128)(2,1)}, u32[]{:S(2)}) copy-start(bf16[32,16,128]{2,1,0:T(8,128)(2,1)} %copy-done.10) | copy-start | bytes 393220
  118.7 5.6 %copy-start.14 = (bf16[32,128]{1,0:T(8,128)(2,1)S(1)}, bf16[32,128]{1,0:T(8,128)(2,1)}, u32[]{:S(2)}) copy-start(bf16[32,128]{1,0:T(8,128)(2,1)} %key_ref.3) | copy-start | bytes 24580
  118.7 15.0 %copy-start.9 = (bf16[128,128]{1,0:T(8,128)(2,1)S(1)}, bf16[128,128]{1,0:T(8,128)(2,1)}, u32[]{:S(2)}) copy-start(bf16[128,128]{1,0:T(8,128)(2,1)} %cot_ref.3) | copy-start | bytes 98308
  119.7 19.3 %copy-start.17 = (bf16[32,128]{1,0:T(8,128)(2,1)S(1)}, bf16[32,128]{1,0:T(8,128)(2,1)}, u32[]{:S(2)}) copy-start(bf16[32,128]{1,0:T(8,128)(2,1)} %param.14) | copy-start | bytes 24580
  119.7 14.0 %all-to-all-start.3 = ((bf16[32,16,128]{2,1,0:T(8,128)(2,1)}), bf16[32,16,128]{2,1,0:T(8,128)(2,1)S(1)}, u32[]{:S(2)}, u32[]{:S(2)}) async-start(bf16[32,16,128]{2,1,0:T(8,128)(2,1)} %shard_map.202), calls=%async_computation.3 | async-start | bytes 262144 | tf_op jit(solution)/shard_map/all_to_all | solution.py:357
  124.3 16.0 %copy-start.18 = (f32[32,128]{1,0:T(8,128)}, f32[32,128]{1,0:T(8,128)S(1)}, u32[]{:S(2)}) copy-start(f32[32,128]{1,0:T(8,128)S(1)} %convert.3) | copy-start | bytes 49156
  124.4 16.0 %copy-start.20 = (pred[128,128]{1,0:T(8,128)(4,1)}, pred[128,128]{1,0:T(8,128)(4,1)S(1)}, u32[]{:S(2)}) copy-start(pred[128,128]{1,0:T(8,128)(4,1)S(1)} %iota_compare_fusion) | copy-start | bytes 49156
  134.8 5.6 %copy-start.7 = (bf16[64,128]{1,0:T(8,128)(2,1)S(1)}, bf16[64,128]{1,0:T(8,128)(2,1)}, u32[]{:S(2)}) copy-start(bf16[64,128]{1,0:T(8,128)(2,1)} %val_ref.3) | copy-start | bytes 49156
  134.8 13.5 %all-to-all-start.4 = ((bf16[8,128,128]{2,1,0:T(8,128)(2,1)}), bf16[8,128,128]{2,1,0:T(8,128)(2,1)}, u32[]{:S(2)}, u32[]{:S(2)}) async-start(bf16[8,128,128]{2,1,0:T(8,128)(2,1)} %shard_map.203), calls=%async_computation.4 | async-start | bytes 524288 | tf_op jit(solution)/shard_map/all_to_all | solution.py:357
  141.4 12.4 %copy-start.4 = (f32[32,32,128]{2,1,0:T(8,128)}, f32[32,32,128]{2,1,0:T(8,128)S(1)}, u32[]{:S(2)}) copy-start(f32[32,32,128]{2,1,0:T(8,128)S(1)} %get-tuple-element.46.reach_ref) | copy-start | bytes 1572868
  153.8 1.0 copy-start.8
  156.6 4.2 %copy-start.21 = (pred[128,128]{1,0:T(8,128)(4,1)S(1)}, pred[128,128]{1,0:T(8,128)(4,1)}, u32[]{:S(2)}) copy-start(pred[128,128]{1,0:T(8,128)(4,1)} %copy-done.20) | copy-start | bytes 49156
  156.8 20.6 %all-to-all-start.5 = ((bf16[32,64,128]{2,1,0:T(8,128)(2,1)}), bf16[32,64,128]{2,1,0:T(8,128)(2,1)S(1)}, u32[]{:S(2)}, u32[]{:S(2)}) async-start(bf16[32,64,128]{2,1,0:T(8,128)(2,1)} %get-tuple-element.45), calls=%async_computation.5 | async-start | bytes 1048576 | tf_op jit(solution)/shard_map/all_to_all | solution.py:357
  160.8 2.0 %copy-start.3 = (bf16[384,256]{1,0:T(8,128)(2,1)S(1)}, bf16[384,256]{1,0:T(8,128)(2,1)}, u32[]{:S(2)}) copy-start(bf16[384,256]{1,0:T(8,128)(2,1)} %copy-done.2) | copy-start | bytes 589828
  160.8 2.0 %copy-start.13 = (bf16[384,128]{1,0:T(8,128)(2,1)S(1)}, bf16[384,128]{1,0:T(8,128)(2,1)}, u32[]{:S(2)}) copy-start(bf16[384,128]{1,0:T(8,128)(2,1)} %copy-done.12) | copy-start | bytes 294916
  162.7 3.6 %copy-start.19 = (f32[32,128]{1,0:T(8,128)S(1)}, f32[32,128]{1,0:T(8,128)}, u32[]{:S(2)}) copy-start(f32[32,128]{1,0:T(8,128)} %copy-done.18) | copy-start | bytes 49156
  168.8 8.6 %copy-start.5 = (f32[32,32,128]{2,1,0:T(8,128)S(1)}, f32[32,32,128]{2,1,0:T(8,128)}, u32[]{:S(2)}) copy-start(f32[32,32,128]{2,1,0:T(8,128)} %copy-done.4) | copy-start | bytes 1572868
  168.8 8.6 %copy-start.15 = (bf16[32,128]{1,0:T(8,128)(2,1)S(1)}, bf16[32,128]{1,0:T(8,128)(2,1)}, u32[]{:S(2)}) copy-start(bf16[32,128]{1,0:T(8,128)(2,1)} %pre_ref.3) | copy-start | bytes 24580
  168.8 8.6 %copy-start.16 = (f32[32]{0:T(128)S(1)}, f32[32]{0:T(128)}, u32[]{:S(2)}) copy-start(f32[32]{0:T(128)} %param.19) | copy-start | bytes 388

commit v4 on v3

--- a/solution.py
+++ b/solution.py
@@ -15,6 +15,7 @@
 RING = 8
 SLOTS = PEERS * PAD
 ROWS = PEERS * CAP
+HALF = ROWS // 2
 WIDTH = 128
 MODEL = 2048
 
@@ -107,12 +108,12 @@
     send_ref[...] = block.astype(BF16)
 
 
-def arrival_kernel(got_ref, x_ref, copies_ref, back_ref):
+def arrival_kernel(got_ref, first_ref, second_ref, back_ref):
     got = got_ref[...].reshape(SLOTS, 2 * WIDTH)
     rows = dot(ones_where(compact_rows((ROWS, SLOTS), 0)), got, 1, 0).astype(BF16)
-    x_ref[...] = rows[:, :WIDTH]
     for k in range(RING):
-        copies_ref[k] = rows[:, WIDTH:]
+        first_ref[k] = rows[:HALF]
+        second_ref[k] = rows[HALF:]
     both = dot(ones_where(row_of_peer(CAP)), got, 1, 0)
     state = both[:, :WIDTH] + both[:, WIDTH:]
     logs = dot(ones_where(row_of_peer(CAP + 1)), got, 1, 0)
@@ -136,25 +137,20 @@
     back_ref[...] = block.astype(BF16)
 
 
-def forward_kernel(core_ref, own_ref, other_ref, gate_ref, up_ref, pre_ref):
+def expert_kernel(
+    core_ref, own_ref, other_ref, gate_ref, up_ref, down_ref, grads_ref, hidden_ref
+):
     core = core_ref[0]
-    total = jnp.zeros((ROWS, 2 * WIDTH), F32)
+    pre = jnp.zeros((HALF, 2 * WIDTH), F32)
+    grad_hidden = jnp.zeros((HALF, WIDTH), F32)
     for k in range(RING):
         for side, ref in ((core, own_ref), (1 - core, other_ref)):
             at = 2 * k + side
             weights = jnp.concatenate([gate_ref[at], up_ref[at]], axis=1)
-            total = total + dot(ref[k], weights, 1, 0)
-    pre_ref[...] = total
-
-
-def hidden_kernel(core_ref, own_ref, other_ref, down_ref, pre_ref, grads_ref, hidden_ref):
-    core = core_ref[0]
-    grad_hidden = jnp.zeros((ROWS, WIDTH), F32)
-    for k in range(RING):
-        for side, ref in ((core, own_ref), (1 - core, other_ref)):
-            at = pl.multiple_of((2 * k + side) * WIDTH, WIDTH)
-            grad_hidden = grad_hidden + dot(ref[k], down_ref[:, pl.ds(at, WIDTH)], 1, 1)
-    gate_pre, up_pre = pre_ref[:, :WIDTH], pre_ref[:, WIDTH:]
+            pre = pre + dot(ref[k, :, :WIDTH], weights, 1, 0)
+            lanes = pl.ds(pl.multiple_of(at * WIDTH, WIDTH), WIDTH)
+            grad_hidden = grad_hidden + dot(ref[k, :, WIDTH:], down_ref[:, lanes], 1, 1)
+    gate_pre, up_pre = pre[:, :WIDTH], pre[:, WIDTH:]
     gate_sig = jax.nn.sigmoid(gate_pre)
     gate_act = gate_pre * gate_sig
     hidden_ref[...] = (gate_act * up_pre).astype(BF16)
@@ -165,19 +161,27 @@
 
 
 def weight_kernel(
-    core_ref, x_ref, other_x_ref, y_ref, other_y_ref, grads_ref, hidden_ref,
+    core_ref, own_a_ref, other_a_ref, own_b_ref, other_b_ref,
+    grads_a_ref, grads_b_ref, hidden_a_ref, hidden_b_ref,
     gate_ref, up_ref, down_ref,
 ):
     core = core_ref[0]
-    grads, hidden = grads_ref[...], hidden_ref[...]
+    grads = (grads_a_ref[...], grads_b_ref[...])
+    hidden = (hidden_a_ref[...], hidden_b_ref[...])
     for k in range(RING):
-        for side, x, y in ((core, x_ref, y_ref), (1 - core, other_x_ref, other_y_ref)):
+        for side, rows in (
+            (core, (own_a_ref, own_b_ref)),
+            (1 - core, (other_a_ref, other_b_ref)),
+        ):
             at = 2 * k + side
-            both = dot(x[k], grads, 0, 0).astype(BF16)
-            gate_ref[at] = both[:, :WIDTH]
-            up_ref[at] = both[:, WIDTH:]
+            both, down = (
+                sum(dot(r[k, :, :WIDTH], g, 0, 0) for r, g in zip(rows, grads)),
+                sum(dot(h, r[k, :, WIDTH:], 0, 0) for r, h in zip(rows, hidden)),
+            )
+            gate_ref[at] = both[:, :WIDTH].astype(BF16)
+            up_ref[at] = both[:, WIDTH:].astype(BF16)
             lanes = pl.ds(pl.multiple_of(at * WIDTH, WIDTH), WIDTH)
-            down_ref[:, lanes] = dot(hidden, y[k], 0, 0).astype(BF16)
+            down_ref[:, lanes] = down.astype(BF16)
 
 
 def partial_kernel(core_ref, grads_ref, gate_ref, up_ref, swapped_ref, out_ref):
@@ -191,11 +195,15 @@
         out_ref[k] = dot(both, weights, 1, 1).astype(BF16)
 
 
-def return_kernel(parts_ref, back_ref, send_ref):
-    total = parts_ref[0].astype(F32)
-    for k in range(1, RING):
-        total = total + parts_ref[k].astype(F32)
-    rows = dot(ones_where(compact_rows((SLOTS, ROWS), 1)), total.astype(BF16), 1, 0)
+def return_kernel(first_ref, second_ref, back_ref, send_ref):
+    halves = []
+    for ref in (first_ref, second_ref):
+        total = ref[0].astype(F32)
+        for k in range(1, RING):
+            total = total + ref[k].astype(F32)
+        halves.append(total.astype(BF16))
+    total = jnp.concatenate(halves, axis=0)
+    rows = dot(ones_where(compact_rows((SLOTS, ROWS), 1)), total, 1, 0)
     rows = rows.astype(BF16).reshape(PEERS, PAD, WIDTH)
     send_ref[...] = rows + back_ref[...]
 
@@ -303,7 +311,7 @@
 
 def call(kernel, outs, *args, scalars=0, stored=()):
     shapes = [
-        (jax.ShapeDtypeStruct if k in stored else pltpu.VMEM)(shape, dtype)
+        (pltpu.HBM if k in stored else pltpu.VMEM)(shape, dtype)
         for k, (shape, dtype) in enumerate(outs)
     ]
     return pl.pallas_call(
@@ -371,16 +379,21 @@
         off_chip(decay_preactivation),
         off_chip(extra_log_decay),
         off_chip(speed),
+        stored=(1,),
     )
     got = on_chip(exchanged(send, sp))
-    rows_x, copies, back = call(
+    first, second, back = call(
         arrival_kernel,
-        [((ROWS, WIDTH), BF16), ((RING, ROWS, WIDTH), BF16), ((PEERS, PAD, WIDTH), BF16)],
+        [
+            ((RING, HALF, 2 * WIDTH), BF16),
+            ((RING, HALF, 2 * WIDTH), BF16),
+            ((PEERS, PAD, WIDTH), BF16),
+        ],
         got,
-    )
-    own_y = exchanged(copies, "y")
-    own_x = lax.all_gather(rows_x, "y", axis=0, tiled=False)
-
+        stored=range(3),
+    )
+    own_a = exchanged(first, "y")
+    own_b = exchanged(second, "y")
     theirs = jnp.stack(
         [
             lax.dynamic_index_in_dim(
@@ -391,44 +404,49 @@
     )
     swapped = lax.ppermute(theirs, "core", swap)
 
-    other_x = lax.ppermute(own_x, "core", swap)
-    other_y = lax.ppermute(own_y, "core", swap)
-    (pre,) = call(
-        forward_kernel,
-        [((ROWS, 2 * WIDTH), F32)],
-        core_at,
-        own_x,
-        other_x,
-        gate_blocks,
-        up_blocks,
-        scalars=1,
-    )
-    grads, hidden = call(
-        hidden_kernel,
-        [((ROWS, 2 * WIDTH), BF16), ((ROWS, WIDTH), BF16)],
-        core_at,
-        own_y,
-        other_y,
-        down,
-        pre,
-        scalars=1,
-    )
-    grads_both = lax.all_gather(grads, "core", axis=0, tiled=False)
-    (partials,) = call(
-        partial_kernel,
-        [((RING, ROWS, WIDTH), BF16)],
-        core_at,
-        on_chip(grads_both),
-        gate_blocks,
-        up_blocks,
-        swapped,
-        scalars=1,
-    )
-    parts = exchanged(partials, "y")
-    (send,) = call(return_kernel, [((PEERS, PAD, WIDTH), BF16)], on_chip(parts), on_chip(back))
+    def expert(own):
+        other = lax.ppermute(own, "core", swap)
+        grads, hidden = call(
+            expert_kernel,
+            [((HALF, 2 * WIDTH), BF16), ((HALF, WIDTH), BF16)],
+            core_at,
+            off_chip(own),
+            off_chip(other),
+            gate_blocks,
+            up_blocks,
+            down,
+            scalars=1,
+            stored=range(2),
+        )
+        grads_both = lax.all_gather(grads, "core", axis=0, tiled=False)
+        (partials,) = call(
+            partial_kernel,
+            [((RING, HALF, WIDTH), BF16)],
+            core_at,
+            on_chip(grads_both),
+            gate_blocks,
+            up_blocks,
+            swapped,
+            scalars=1,
+            stored=(0,),
+        )
+        return other, grads, hidden, partials
+
+    other_a, grads_a, hidden_a, partials_a = expert(own_a)
+    own_b, partials_a = lax.optimization_barrier((own_b, partials_a))
+    parts_a = exchanged(partials_a, "y")
+    other_b, grads_b, hidden_b, partials_b = expert(own_b)
+    parts_b = exchanged(partials_b, "y")
+    (send,) = call(
+        return_kernel,
+        [((PEERS, PAD, WIDTH), BF16)],
+        on_chip(parts_a),
+        on_chip(parts_b),
+        off_chip(back),
+    )
     returned = on_chip(exchanged(send, sp))
     (copies,) = call(
-        token_kernel, [((RING, TOK, WIDTH), BF16)], returned, pick, cotangent
+        token_kernel, [((RING, TOK, WIDTH), BF16)], returned, off_chip(pick), off_chip(cotangent)
     )
     cum, copies = lax.optimization_barrier((cum, copies))
     full_rows = exchanged(copies, "y")
@@ -458,14 +476,14 @@
         source_kernel,
         [((PEERS, 2 * KEY_DIM, WIDTH), BF16), ((TOK, VAL_DIM), F32)],
         on_chip(full_rows),
-        output_weight_matrix.T,
+        off_chip(output_weight_matrix.T),
         normed_t,
         inv_rms.reshape(TOK, 1),
         jnp.concatenate([mix_t, mix_t], axis=1),
         scaled * jnp.exp(cum),
         scaled * jnp.exp(cum[:, -1:] - cum),
     )
-    send, grads, hidden = lax.optimization_barrier((send, grads, hidden))
+    send, grads_a, grads_b = lax.optimization_barrier((send, grads_a, grads_b))
     got = exchanged(send, sp)
     grad_gate, grad_up, grad_down = call(
         weight_kernel,
@@ -475,12 +493,14 @@
             ((WIDTH, MODEL), BF16),
         ],
         core_at,
-        own_x,
-        other_x,
-        own_y,
-        other_y,
-        grads,
-        hidden,
+        off_chip(own_a),
+        off_chip(other_a),
+        off_chip(own_b),
+        off_chip(other_b),
+        off_chip(grads_a),
+        off_chip(grads_b),
+        off_chip(hidden_a),
+        off_chip(hidden_b),
         scalars=1,
         stored=range(3),
     )

time: 180 us -> 186 us (1.033)
  blocking collectives: 96 us -> 79.4 us
  waiting for transfers between devices: 23 us -> 35.7 us
  Pallas kernels: 15.9 us -> 24.6 us
  starting transfers between devices: 32.8 us -> 35.3 us
    all_gather x2, blocking collectives: 37.3 us -> 4.43 us  [expert(): grads_both = lax.all_gather(grads, 'core', axis=0, tiled=False)]
    all_to_all x2 -> x3, blocking collectives: 53.1 us -> 69.4 us  [exchanged(): return lax.all_to_all(array, axis, split_axis=0, concat_axis=0, tiled=True)]
    all_to_all x4 -> x5, waiting for transfers between devices: 22.9 us -> 35.7 us  [exchanged(): return lax.all_to_all(array, axis, split_axis=0, concat_axis=0, tiled=True)]
    pallas_call x11 -> x12, Pallas kernels: 15.9 us -> 24.6 us  [call(): pl.pallas_call(kernel, out_shape=shapes, in_specs=[SCALAR] * scalars + [W...]
    all_to_all x4 -> x5, starting transfers between devices: 19.5 us -> 21.6 us  [exchanged(): return lax.all_to_all(array, axis, split_axis=0, concat_axis=0, tiled=True)]
  transfers between devices with their start and end apart: 7 -> 8, of which waited for: 3 -> 5; matrix products, arithmetic and copies ran while one was open for 4% -> 4% of each run, Pallas kernels for 4% -> 7%
where the time goes in v4:
time: 186 us; the launch traced here: 185 us
  blocking collectives  79.4 us (43%)
  waiting for transfers between devices  35.7 us (19%)
  starting transfers between devices  35.3 us (19%)
  Pallas kernels  24.6 us (13%)
  matrix products  4.08 us (2%)
  other arithmetic  3.68 us (2%)
    all_to_all x3, blocking collectives, exchanged(): return lax.all_to_all(array, axis, split_axis=0, concat_axis=0, tiled=True)  69.4 us
    all_to_all x5, waiting for transfers between devices, exchanged(): return lax.all_to_all(array, axis, split_axis=0, concat_axis=0, tiled=True)  35.7 us
    pallas_call x12, Pallas kernels, call(): pl.pallas_call(kernel, out_shape=shapes, in_specs=[SCALAR] * scalars + [W...  24.6 us
    all_to_all x5, starting transfers between devices, exchanged(): return lax.all_to_all(array, axis, split_axis=0, concat_axis=0, tiled=True)  21.6 us
    ppermute x2, starting transfers between devices, expert(): other = lax.ppermute(own, 'core', swap)  11.7 us
    all_gather x1, blocking collectives, body(): full_rows = lax.all_gather(full_rows, 'core', axis=0, tiled=False)  5.6 us
    all_gather x2, blocking collectives, expert(): grads_both = lax.all_gather(grads, 'core', axis=0, tiled=False)  4.43 us
  transfers between devices with their start and end apart: 8, of which 5 were waited for; matrix products, arithmetic and copies ran while one was open for 4% of the time, Pallas kernels for 7%

profile of v4, /device:TPU:1, one launch (start us, length us, event | category | flops | bytes accessed | tf_op | source)
XLA Modules:
  0.0 185.1 jit_solution(6988062773533977518)
XLA Ops:
  0.6 1.8 shard_map.197
  2.4 24.8 %all_to_all.40.got_ref = bf16[32,16,256]{2,1,0:T(8,128)(2,1)S(1)} all-to-all(bf16[32,16,256]{2,1,0:T(8,128)(2,1)S(1)} %get-tuple-element.37), channel_id=1, replica_groups=mesh['z'=8,'x'=4,'y'=8,'core'=2] {'z','x'}, dimensions={0} | all-to-all | bytes 524288 | tf_op jit(solution)/shard_map/all_to_all | solution.py:365
  27.2 1.5 shard_map.198
  28.7 26.9 %all_to_all.41.own_ref.own_a_ref = bf16[8,192,256]{2,1,0:T(8,128)(2,1)S(1)} all-to-all(bf16[8,192,256]{2,1,0:T(8,128)(2,1)} %get-tuple-element.39), channel_id=1, replica_groups=mesh['z'=8,'x'=4,'y'=8,'core'=2] {'y'}, dimensions={0} | all-to-all | bytes 1572864 | tf_op jit(solution)/shard_map/all_to_all | solution.py:365
  55.6 4.4 %all-to-all-start.1 = ((bf16[8,192,256]{2,1,0:T(8,128)(2,1)}), bf16[8,192,256]{2,1,0:T(8,128)(2,1)}, u32[]{:S(2)}, u32[]{:S(2)}) async-start(bf16[8,192,256]{2,1,0:T(8,128)(2,1)} %get-tuple-element.38), calls=%async_computation.1 | async-start | bytes 1572864 | tf_op jit(solution)/shard_map/all_to_all | solution.py:365
  60.0 0.0 copy-done.7
  60.0 5.9 %collective-permute-start = (bf16[8,192,256]{2,1,0:T(8,128)(2,1)S(1)}, bf16[8,192,256]{2,1,0:T(8,128)(2,1)}, u32[]{:S(2)}, u32[]{:S(2)}) collective-permute-start(bf16[8,192,256]{2,1,0:T(8,128)(2,1)S(1)} %all_to_all.41.own_ref.own_a_ref), channel_id=1, source_target_pairs={{0,1},{1,0},{2,3},{3,2},{4,5},{5,4},{6,7},{7,6},{8,9},{9,8},{10,11... | collective-permute-start | bytes 2359304 | tf_op jit(solution)/shard_map/ppermute | solution.py:408
  65.9 0.0 copy-done
  65.9 0.0 copy-done.1
  66.0 0.0 copy-start.2
  66.0 0.1 pad_maximum_fusion
  66.1 2.1 %collective-permute-start.1 = (bf16[2,8,128,128]{3,2,1,0:T(8,128)(2,1)S(1)}, bf16[2,8,128,128]{3,2,1,0:T(8,128)(2,1)S(1)}, u32[]{:S(2)}, u32[]{:S(2)}) collective-permute-start(bf16[2,8,128,128]{3,2,1,0:T(8,128)(2,1)S(1)} %pad_maximum_fusion), channel_id=1, source_target_pairs={{0,1},{1,0},{2,3},{3,2},{4,5},{5,4},{6,7},{7,6},{8,9},{9,8},{10,11... | collective-permute-start | bytes 1572872 | tf_op jit(solution)/shard_map/ppermute | solution.py:405
  68.1 0.0 collective-permute-done.other_ref.other_a_ref
  68.1 0.0 copy-done.2
  68.1 2.9 %shard_map.199 = (bf16[192,256]{1,0:T(8,128)(2,1)}, bf16[192,128]{1,0:T(8,128)(2,1)}) custom-call(s32[1]{0:T(128)} %bitcast.5.core_ref, bf16[8,192,256]{2,1,0:T(8,128)(2,1)} %copy-done.7, bf16[8,192,256]{2,1,0:T(8,128)(2,1)} %collective-permute-done.other_ref.other_a_ref, bf16[16,128,128]{2,1,0:T(8,128)(2,1)S(1)} %bitcast.69, ...), custom_call_target="tpu_custom_call" | custom-call | tf_op jit(solution)/shard_map/pallas_call | solution.py:317
  71.0 2.3 %all-gather = bf16[384,256]{1,0:T(8,128)(2,1)S(1)} all-gather(bf16[192,256]{1,0:T(8,128)(2,1)} %get-tuple-element.57.grads_a_ref), channel_id=2, replica_groups=mesh['z'=8,'x'=4,'y'=8,'core'=2] {'core'}, dimensions={0}, use_global_device_ids=true | all-gather | bytes 294912 | tf_op jit(solution)/shard_map/all_gather | solution.py:421
  73.3 0.0 collective-permute-done.1.swapped_ref
  73.3 1.3 shard_map.200
  74.7 5.6 %all-to-all-done.1.own_ref.own_b_ref = bf16[8,192,256]{2,1,0:T(8,128)(2,1)} async-done(((bf16[8,192,256]{2,1,0:T(8,128)(2,1)}), bf16[8,192,256]{2,1,0:T(8,128)(2,1)}, u32[]{:S(2)}, u32[]{:S(2)}) %all-to-all-start.1) | async-done | bytes 786464 | tf_op jit(solution)/shard_map/all_to_all | solution.py:365
  80.2 5.7 %collective-permute-start.2 = (bf16[8,192,256]{2,1,0:T(8,128)(2,1)}, bf16[8,192,256]{2,1,0:T(8,128)(2,1)S(1)}, u32[]{:S(2)}, u32[]{:S(2)}) collective-permute-start(bf16[8,192,256]{2,1,0:T(8,128)(2,1)} %all-to-all-done.1.own_ref.own_b_ref), channel_id=1, source_target_pairs={{0,1},{1,0},{2,3},{3,2},{4,5},{5,4},{6,7},{7,6},{8,9},{9,8},{10,11... | collective-permute-start | bytes 2359304 | tf_op jit(solution)/shard_map/ppermute | solution.py:408
  86.0 3.5 %all-to-all-start.3 = ((bf16[8,192,128]{2,1,0:T(8,128)(2,1)}), bf16[8,192,128]{2,1,0:T(8,128)(2,1)S(1)}, u32[]{:S(2)}, u32[]{:S(2)}) async-start(bf16[8,192,128]{2,1,0:T(8,128)(2,1)} %shard_map.200), calls=%async_computation.3 | async-start | bytes 786432 | tf_op jit(solution)/shard_map/all_to_all | solution.py:365
  89.4 0.0 collective-permute-done.2.other_ref.other_b_ref
  89.4 0.0 copy-start.8
  89.5 0.9 copy-done.8
  90.3 2.9 %shard_map.201 = (bf16[192,256]{1,0:T(8,128)(2,1)}, bf16[192,128]{1,0:T(8,128)(2,1)}) custom-call(s32[1]{0:T(128)} %bitcast.5.core_ref, bf16[8,192,256]{2,1,0:T(8,128)(2,1)} %all-to-all-done.1.own_ref.own_b_ref, bf16[8,192,256]{2,1,0:T(8,128)(2,1)} %copy-done.8, bf16[16,128,128]{2,1,0:T(8,128)(2,1)S(1)} %bitcast.71, bf16[16,128,128]{2,1,0:T(8,128)(2,1)S(1)} %bitcast.76, ...), custom_call_target="tpu_custom_call" | custom-call | tf_op jit(solution)/shard_map/pallas_call | solution.py:317
  93.2 2.1 %all-gather.1 = bf16[384,256]{1,0:T(8,128)(2,1)S(1)} all-gather(bf16[192,256]{1,0:T(8,128)(2,1)} %get-tuple-element.58.grads_b_ref), channel_id=3, replica_groups=mesh['z'=8,'x'=4,'y'=8,'core'=2] {'core'}, dimensions={0}, use_global_device_ids=true | all-gather | bytes 294912 | tf_op jit(solution)/shard_map/all_gather | solution.py:421
  95.4 1.3 shard_map.202
  96.7 7.9 %all-to-all-done.3.first_ref = bf16[8,192,128]{2,1,0:T(8,128)(2,1)S(1)} async-done(((bf16[8,192,128]{2,1,0:T(8,128)(2,1)}), bf16[8,192,128]{2,1,0:T(8,128)(2,1)S(1)}, u32[]{:S(2)}, u32[]{:S(2)}) %all-to-all-start.3) | async-done | bytes 393248 | tf_op jit(solution)/shard_map/all_to_all | solution.py:365
  104.6 17.8 %all_to_all.42.second_ref = bf16[8,192,128]{2,1,0:T(8,128)(2,1)S(1)} all-to-all(bf16[8,192,128]{2,1,0:T(8,128)(2,1)} %shard_map.202), channel_id=1, replica_groups=mesh['z'=8,'x'=4,'y'=8,'core'=2] {'y'}, dimensions={0} | all-to-all | bytes 786432 | tf_op jit(solution)/shard_map/all_to_all | solution.py:365
  122.3 1.9 %shard_map.203 = bf16[32,16,128]{2,1,0:T(8,128)(2,1)} custom-call(bf16[8,192,128]{2,1,0:T(8,128)(2,1)S(1)} %all-to-all-done.3.first_ref, bf16[8,192,128]{2,1,0:T(8,128)(2,1)S(1)} %all_to_all.42.second_ref, bf16[32,16,128]{2,1,0:T(8,128)(2,1)} %get-tuple-element.44.back_ref), custom_call_target="tpu_custom_call" | custom-call | tf_op jit(solution)/shard_map/pallas_call | solution.py:317
  124.2 6.3 %all-to-all-start.5 = ((bf16[32,16,128]{2,1,0:T(8,128)(2,1)}), bf16[32,16,128]{2,1,0:T(8,128)(2,1)S(1)}, u32[]{:S(2)}, u32[]{:S(2)}) async-start(bf16[32,16,128]{2,1,0:T(8,128)(2,1)} %shard_map.203), calls=%async_computation.5 | async-start | bytes 262144 | tf_op jit(solution)/shard_map/all_to_all | solution.py:365
  130.5 0.0 copy-done.4
  130.6 9.3 %all-to-all-done.5.got_ref = bf16[32,16,128]{2,1,0:T(8,128)(2,1)S(1)} async-done(((bf16[32,16,128]{2,1,0:T(8,128)(2,1)}), bf16[32,16,128]{2,1,0:T(8,128)(2,1)S(1)}, u32[]{:S(2)}, u32[]{:S(2)}) %all-to-all-start.5) | async-done | bytes 131104 | tf_op jit(solution)/shard_map/all_to_all | solution.py:365
  139.9 1.8 shard_map.204
  141.7 0.2 slice_reduce_fusion
  141.9 3.6 %all-to-all-start.6 = ((bf16[8,128,128]{2,1,0:T(8,128)(2,1)}), bf16[8,128,128]{2,1,0:T(8,128)(2,1)S(1)}, u32[]{:S(2)}, u32[]{:S(2)}) async-start(bf16[8,128,128]{2,1,0:T(8,128)(2,1)} %shard_map.204), calls=%async_computation.6 | async-start | bytes 524288 | tf_op jit(solution)/shard_map/all_to_all | solution.py:365
  145.5 0.0 copy-done.9
  145.5 0.1 fusion.44
  145.6 1.3 fusion.1
  146.8 0.0 copy-done.3
  146.9 0.1 fusion.54
  147.0 0.9 shard_map.205
  147.9 0.2 fusion.41
  148.1 0.3 fusion.20
  148.4 0.1 copy.52.inv_ref
  148.5 0.1 fusion.52
  148.6 0.1 pad_maximum_fusion.1.mix_ref
  148.7 6.1 %all-to-all-done.6 = bf16[8,128,128]{2,1,0:T(8,128)(2,1)S(1)} async-done(((bf16[8,128,128]{2,1,0:T(8,128)(2,1)}), bf16[8,128,128]{2,1,0:T(8,128)(2,1)S(1)}, u32[]{:S(2)}, u32[]{:S(2)}) %all-to-all-start.6) | async-done | bytes 262176 | tf_op jit(solution)/shard_map/all_to_all | solution.py:365
  154.8 5.6 %all-gather.2 = bf16[16,128,128]{2,1,0:T(8,128)(2,1)S(1)} all-gather(bf16[8,128,128]{2,1,0:T(8,128)(2,1)S(1)} %all-to-all-done.6), channel_id=4, replica_groups=mesh['z'=8,'x'=4,'y'=8,'core'=2] {'core'}, dimensions={0}, use_global_device_ids=true | all-gather | bytes 786432 | tf_op jit(solution)/shard_map/all_gather | solution.py:453
  160.4 2.8 %shard_map.206 = (bf16[32,64,128]{2,1,0:T(8,128)(2,1)}, f32[128,64]{1,0:T(8,128)S(1)}) custom-call(bf16[2,8,128,128]{3,2,1,0:T(8,128)(2,1)S(1)} %bitcast.78, bf16[64,2048]{1,0:T(8,128)(2,1)} %bitcast.87, f32[128,64]{1,0:T(8,128)S(1)} %get-tuple-element.67.normed_ref, f32[128,1]{1,0:T(8,128)S(1)} %copy.52.inv_ref, ...), custom_call_target="tpu_custom_call" | custom-call | tf_op jit(solution)/shard_map/pallas_call | solution.py:317
  163.1 0.1 fusion.55
  163.3 0.1 fusion.39
  163.4 3.9 %all-to-all-start.7 = ((bf16[32,64,128]{2,1,0:T(8,128)(2,1)}), bf16[32,64,128]{2,1,0:T(8,128)(2,1)S(1)}, u32[]{:S(2)}, u32[]{:S(2)}) async-start(bf16[32,64,128]{2,1,0:T(8,128)(2,1)} %get-tuple-element.51), calls=%async_computation.7 | async-start | bytes 1048576 | tf_op jit(solution)/shard_map/all_to_all | solution.py:365
  167.3 0.9 fusion.7
  168.3 0.9 fusion.45
  169.2 0.1 copy.53
  169.3 4.3 %shard_map.208 = (bf16[16,128,128]{2,1,0:T(8,128)(2,1)}, bf16[16,128,128]{2,1,0:T(8,128)(2,1)}, bf16[128,2048]{1,0:T(8,128)(2,1)}) custom-call(s32[1]{0:T(128)} %bitcast.5.core_ref, bf16[8,192,256]{2,1,0:T(8,128)(2,1)} %copy-done.7, bf16[8,192,256]{2,1,0:T(8,128)(2,1)} %collective-permute-done.other_ref.other_a_ref, ...), custom_call_target="tpu_custom_call" | custom-call | tf_op jit(solution)/shard_map/pallas_call | solution.py:317
  173.6 2.1 %fusion.10 = (f32[32,128]{1,0:T(8,128)S(1)}, f32[32,128]{1,0:T(8,128)S(1)}) fusion(f32[128,128]{1,0:T(8,128)S(1)} %fusion.55, f32[32,128]{1,0:T(8,128)S(1)} %convert.3, f32[32,128]{1,0:T(8,128)S(1)} %get-tuple-element.72, f32[32,128]{1,0:T(8,128)S(1)} %get-tuple-element.47.cum_ref, pred[128,128]{1,0:T(8,128)(4,1)S(1)} %iota_compare_fusion), kind=kLoop, calls=%fused_computation.12 | loop fusion | flops 6283264 | bytes 163840 | tf_op jit(solution)/shard_map/transpose(jvp())/reduce_sum | solution.py:328
  175.7 0.2 fusion.22.decay_mix_ref
  175.9 0.2 fusion.56.vals_mix_ref
  176.1 0.9 fusion.5
  177.0 6.9 %all-to-all-done.7.got_ref = bf16[32,64,128]{2,1,0:T(8,128)(2,1)S(1)} async-done(((bf16[32,64,128]{2,1,0:T(8,128)(2,1)}), bf16[32,64,128]{2,1,0:T(8,128)(2,1)S(1)}, u32[]{:S(2)}, u32[]{:S(2)}) %all-to-all-start.7) | async-done | bytes 524320 | tf_op jit(solution)/shard_map/all_to_all | solution.py:365
  184.0 0.0 copy-done.6
  184.0 1.1 shard_map.207
  (13 shorter events, 0.1 us)
Async XLA Ops:
  55.6 4.4 %copy-start.7 = (bf16[8,192,256]{2,1,0:T(8,128)(2,1)}, bf16[8,192,256]{2,1,0:T(8,128)(2,1)S(1)}, u32[]{:S(2)}) copy-start(bf16[8,192,256]{2,1,0:T(8,128)(2,1)S(1)} %all_to_all.41.own_ref.own_a_ref) | copy-start | bytes 2359300
  55.6 10.3 %copy-start = (bf16[1,2048,128]{2,1,0:T(8,128)(2,1)S(1)}, bf16[1,2048,128]{2,1,0:T(8,128)(2,1)}, u32[]{:S(2)}) copy-start(bf16[1,2048,128]{2,1,0:T(8,128)(2,1)} %param.25) | copy-start | bytes 1572868
  55.6 10.3 %copy-start.1 = (bf16[1,2048,128]{2,1,0:T(8,128)(2,1)S(1)}, bf16[1,2048,128]{2,1,0:T(8,128)(2,1)}, u32[]{:S(2)}) copy-start(bf16[1,2048,128]{2,1,0:T(8,128)(2,1)} %param.26) | copy-start | bytes 1572868
  55.6 24.6 %all-to-all-start.1 = ((bf16[8,192,256]{2,1,0:T(8,128)(2,1)}), bf16[8,192,256]{2,1,0:T(8,128)(2,1)}, u32[]{:S(2)}, u32[]{:S(2)}) async-start(bf16[8,192,256]{2,1,0:T(8,128)(2,1)} %get-tuple-element.38), calls=%async_computation.1 | async-start | bytes 1572864 | tf_op jit(solution)/shard_map/all_to_all | solution.py:365
  60.0 8.2 %collective-permute-start = (bf16[8,192,256]{2,1,0:T(8,128)(2,1)S(1)}, bf16[8,192,256]{2,1,0:T(8,128)(2,1)}, u32[]{:S(2)}, u32[]{:S(2)}) collective-permute-start(bf16[8,192,256]{2,1,0:T(8,128)(2,1)S(1)} %all_to_all.41.own_ref.own_a_ref), channel_id=1, source_target_pairs={{0,1},{1,0},{2,3},{3,2},{4,5},{5,4},{6,7},{7,6},{8,9},{9,8},{10,11... | collective-permute-start | bytes 2359304 | tf_op jit(solution)/shard_map/ppermute | solution.py:408
  66.0 2.1 %copy-start.2 = (bf16[1,128,2048]{2,1,0:T(8,128)(2,1)S(1)}, bf16[1,128,2048]{2,1,0:T(8,128)(2,1)}, u32[]{:S(2)}) copy-start(bf16[1,128,2048]{2,1,0:T(8,128)(2,1)} %param.27) | copy-start | bytes 1572868
  66.1 7.3 %collective-permute-start.1 = (bf16[2,8,128,128]{3,2,1,0:T(8,128)(2,1)S(1)}, bf16[2,8,128,128]{3,2,1,0:T(8,128)(2,1)S(1)}, u32[]{:S(2)}, u32[]{:S(2)}) collective-permute-start(bf16[2,8,128,128]{3,2,1,0:T(8,128)(2,1)S(1)} %pad_maximum_fusion), channel_id=1, source_target_pairs={{0,1},{1,0},{2,3},{3,2},{4,5},{5,4},{6,7},{7,6},{8,9},{9,8},{10,11... | collective-permute-start | bytes 1572872 | tf_op jit(solution)/shard_map/ppermute | solution.py:405
  80.2 9.2 %collective-permute-start.2 = (bf16[8,192,256]{2,1,0:T(8,128)(2,1)}, bf16[8,192,256]{2,1,0:T(8,128)(2,1)S(1)}, u32[]{:S(2)}, u32[]{:S(2)}) collective-permute-start(bf16[8,192,256]{2,1,0:T(8,128)(2,1)} %all-to-all-done.1.own_ref.own_b_ref), channel_id=1, source_target_pairs={{0,1},{1,0},{2,3},{3,2},{4,5},{5,4},{6,7},{7,6},{8,9},{9,8},{10,11... | collective-permute-start | bytes 2359304 | tf_op jit(solution)/shard_map/ppermute | solution.py:408
  86.0 18.6 %all-to-all-start.3 = ((bf16[8,192,128]{2,1,0:T(8,128)(2,1)}), bf16[8,192,128]{2,1,0:T(8,128)(2,1)S(1)}, u32[]{:S(2)}, u32[]{:S(2)}) async-start(bf16[8,192,128]{2,1,0:T(8,128)(2,1)} %shard_map.200), calls=%async_computation.3 | async-start | bytes 786432 | tf_op jit(solution)/shard_map/all_to_all | solution.py:365
  89.4 0.9 copy-start.8
  122.3 8.2 %copy-start.4 = (bf16[32,128]{1,0:T(8,128)(2,1)S(1)}, bf16[32,128]{1,0:T(8,128)(2,1)}, u32[]{:S(2)}) copy-start(bf16[32,128]{1,0:T(8,128)(2,1)} %key_ref.3) | copy-start | bytes 24580
  124.2 21.3 %copy-start.9 = (bf16[32,128]{1,0:T(8,128)(2,1)S(1)}, bf16[32,128]{1,0:T(8,128)(2,1)}, u32[]{:S(2)}) copy-start(bf16[32,128]{1,0:T(8,128)(2,1)} %param.14) | copy-start | bytes 24580
  124.2 15.7 %all-to-all-start.5 = ((bf16[32,16,128]{2,1,0:T(8,128)(2,1)}), bf16[32,16,128]{2,1,0:T(8,128)(2,1)S(1)}, u32[]{:S(2)}, u32[]{:S(2)}) async-start(bf16[32,16,128]{2,1,0:T(8,128)(2,1)} %shard_map.203), calls=%async_computation.5 | async-start | bytes 262144 | tf_op jit(solution)/shard_map/all_to_all | solution.py:365
  141.9 5.0 %copy-start.3 = (bf16[64,128]{1,0:T(8,128)(2,1)S(1)}, bf16[64,128]{1,0:T(8,128)(2,1)}, u32[]{:S(2)}) copy-start(bf16[64,128]{1,0:T(8,128)(2,1)} %val_ref.3) | copy-start | bytes 49156
  141.9 12.9 %all-to-all-start.6 = ((bf16[8,128,128]{2,1,0:T(8,128)(2,1)}), bf16[8,128,128]{2,1,0:T(8,128)(2,1)S(1)}, u32[]{:S(2)}, u32[]{:S(2)}) async-start(bf16[8,128,128]{2,1,0:T(8,128)(2,1)} %shard_map.204), calls=%async_computation.6 | async-start | bytes 524288 | tf_op jit(solution)/shard_map/all_to_all | solution.py:365
  163.4 20.6 %all-to-all-start.7 = ((bf16[32,64,128]{2,1,0:T(8,128)(2,1)}), bf16[32,64,128]{2,1,0:T(8,128)(2,1)S(1)}, u32[]{:S(2)}, u32[]{:S(2)}) async-start(bf16[32,64,128]{2,1,0:T(8,128)(2,1)} %get-tuple-element.51), calls=%async_computation.7 | async-start | bytes 1048576 | tf_op jit(solution)/shard_map/all_to_all | solution.py:365
  176.1 7.9 %copy-start.5 = (bf16[32,128]{1,0:T(8,128)(2,1)S(1)}, bf16[32,128]{1,0:T(8,128)(2,1)}, u32[]{:S(2)}) copy-start(bf16[32,128]{1,0:T(8,128)(2,1)} %pre_ref.3) | copy-start | bytes 24580
  176.1 7.9 %copy-start.6 = (f32[32]{0:T(128)S(1)}, f32[32]{0:T(128)}, u32[]{:S(2)}) copy-start(f32[32]{0:T(128)} %param.19) | copy-start | bytes 388

commit v5 on v3

--- a/solution.py
+++ b/solution.py
@@ -5,6 +5,7 @@
 from jax.experimental.pallas import tpu as pltpu
 from jax.sharding import Mesh
 from jax.sharding import PartitionSpec as P
+
 
 KEY_DIM = 32
 VAL_DIM = 64
@@ -107,12 +108,11 @@
     send_ref[...] = block.astype(BF16)
 
 
-def arrival_kernel(got_ref, x_ref, copies_ref, back_ref):
+def arrival_kernel(got_ref, copies_ref, back_ref):
     got = got_ref[...].reshape(SLOTS, 2 * WIDTH)
     rows = dot(ones_where(compact_rows((ROWS, SLOTS), 0)), got, 1, 0).astype(BF16)
-    x_ref[...] = rows[:, :WIDTH]
     for k in range(RING):
-        copies_ref[k] = rows[:, WIDTH:]
+        copies_ref[k] = rows
     both = dot(ones_where(row_of_peer(CAP)), got, 1, 0)
     state = both[:, :WIDTH] + both[:, WIDTH:]
     logs = dot(ones_where(row_of_peer(CAP + 1)), got, 1, 0)
@@ -136,59 +136,84 @@
     back_ref[...] = block.astype(BF16)
 
 
-def forward_kernel(core_ref, own_ref, other_ref, gate_ref, up_ref, pre_ref):
+def slice_kernel(core_ref, gate_ref, up_ref, down_ref, out_ref):
+    other = 1 - core_ref[0]
+    for k in range(RING):
+        at = 2 * k + other
+        out_ref[0, k] = gate_ref[at]
+        out_ref[1, k] = up_ref[at]
+        out_ref[2, k] = down_ref[:, pl.ds(pl.multiple_of(at * WIDTH, WIDTH), WIDTH)]
+
+
+def forward_kernel(core_ref, rows_ref, gate_ref, up_ref, down_ref, swapped_ref, out_ref, send_ref):
     core = core_ref[0]
-    total = jnp.zeros((ROWS, 2 * WIDTH), F32)
-    for k in range(RING):
-        for side, ref in ((core, own_ref), (1 - core, other_ref)):
-            at = 2 * k + side
-            weights = jnp.concatenate([gate_ref[at], up_ref[at]], axis=1)
-            total = total + dot(ref[k], weights, 1, 0)
-    pre_ref[...] = total
-
-
-def hidden_kernel(core_ref, own_ref, other_ref, down_ref, pre_ref, grads_ref, hidden_ref):
-    core = core_ref[0]
-    grad_hidden = jnp.zeros((ROWS, WIDTH), F32)
-    for k in range(RING):
-        for side, ref in ((core, own_ref), (1 - core, other_ref)):
-            at = pl.multiple_of((2 * k + side) * WIDTH, WIDTH)
-            grad_hidden = grad_hidden + dot(ref[k], down_ref[:, pl.ds(at, WIDTH)], 1, 1)
-    gate_pre, up_pre = pre_ref[:, :WIDTH], pre_ref[:, WIDTH:]
-    gate_sig = jax.nn.sigmoid(gate_pre)
-    gate_act = gate_pre * gate_sig
-    hidden_ref[...] = (gate_act * up_pre).astype(BF16)
-    grads_ref[:, :WIDTH] = (
-        grad_hidden * up_pre * gate_sig * (1.0 + gate_pre * (1.0 - gate_sig))
-    ).astype(BF16)
-    grads_ref[:, WIDTH:] = (grad_hidden * gate_act).astype(BF16)
-
-
-def weight_kernel(
-    core_ref, x_ref, other_x_ref, y_ref, other_y_ref, grads_ref, hidden_ref,
-    gate_ref, up_ref, down_ref,
+    pre = jnp.zeros((ROWS, 4 * WIDTH), F32)
+    grad = jnp.zeros((ROWS, 2 * WIDTH), F32)
+    for k in range(0, RING, 2):
+        weights, downs = [], []
+        for j in (k, k + 1):
+            at = 2 * j + core
+            parts = [gate_ref[at], up_ref[at], swapped_ref[0, j], swapped_ref[1, j]]
+            weights.append(jnp.concatenate(parts, axis=1))
+            lanes = pl.ds(pl.multiple_of(at * WIDTH, WIDTH), WIDTH)
+            downs.append(jnp.concatenate([down_ref[:, lanes], swapped_ref[2, j]], axis=0))
+        x = jnp.concatenate([rows_ref[k, :, :WIDTH], rows_ref[k + 1, :, :WIDTH]], axis=1)
+        y = jnp.concatenate([rows_ref[k, :, WIDTH:], rows_ref[k + 1, :, WIDTH:]], axis=1)
+        pre = pre + dot(x, jnp.concatenate(weights, axis=0), 1, 0)
+        grad = grad + dot(y, jnp.concatenate(downs, axis=1), 1, 1)
+    mine = jnp.concatenate([pre[:, : 2 * WIDTH], grad[:, :WIDTH]], axis=1)
+    theirs = jnp.concatenate([pre[:, 2 * WIDTH :], grad[:, WIDTH:]], axis=1)
+    out_ref[0] = mine
+    out_ref[1] = theirs
+    send_ref[0] = theirs.astype(BF16)
+    send_ref[1] = mine.astype(BF16)
+
+
+def partial_kernel(
+    core_ref, own_ref, got_ref, gate_ref, up_ref, swapped_ref, out_ref, grads_ref, hidden_ref
 ):
     core = core_ref[0]
-    grads, hidden = grads_ref[...], hidden_ref[...]
-    for k in range(RING):
-        for side, x, y in ((core, x_ref, y_ref), (1 - core, other_x_ref, other_y_ref)):
-            at = 2 * k + side
-            both = dot(x[k], grads, 0, 0).astype(BF16)
-            gate_ref[at] = both[:, :WIDTH]
-            up_ref[at] = both[:, WIDTH:]
-            lanes = pl.ds(pl.multiple_of(at * WIDTH, WIDTH), WIDTH)
-            down_ref[:, lanes] = dot(hidden, y[k], 0, 0).astype(BF16)
-
-
-def partial_kernel(core_ref, grads_ref, gate_ref, up_ref, swapped_ref, out_ref):
-    core = core_ref[0]
-    both = jnp.concatenate([grads_ref[core], grads_ref[1 - core]], axis=1)
+    grads = []
+    for half in range(2):
+        total = own_ref[half] + got_ref[half].astype(F32)
+        gate_pre, up_pre = total[:, :WIDTH], total[:, WIDTH : 2 * WIDTH]
+        grad_hidden = total[:, 2 * WIDTH :]
+        gate_sig = jax.nn.sigmoid(gate_pre)
+        gate_act = gate_pre * gate_sig
+        hidden_ref[:, half * WIDTH : (half + 1) * WIDTH] = (gate_act * up_pre).astype(BF16)
+        slope = gate_sig * (1.0 + gate_pre * (1.0 - gate_sig))
+        grads.append((grad_hidden * up_pre * slope).astype(BF16))
+        grads.append((grad_hidden * gate_act).astype(BF16))
+    grads = jnp.concatenate(grads, axis=1)
+    grads_ref[...] = grads
     for k in range(RING):
         at = 2 * k + core
         weights = jnp.concatenate(
             [gate_ref[at], up_ref[at], swapped_ref[0, k], swapped_ref[1, k]], axis=1
         )
-        out_ref[k] = dot(both, weights, 1, 1).astype(BF16)
+        out_ref[k] = dot(grads, weights, 1, 1).astype(BF16)
+
+
+def weight_kernel(rows_ref, grads_ref, hidden_ref, own_ref, send_ref):
+    grads, hidden = grads_ref[...], hidden_ref[...]
+    for k in range(RING):
+        both = dot(rows_ref[k, :, :WIDTH], grads, 0, 0).astype(BF16)
+        down = dot(hidden, rows_ref[k, :, WIDTH:], 0, 0).astype(BF16)
+        for half, ref in enumerate((own_ref, send_ref)):
+            at = 2 * half * WIDTH
+            ref[0, k] = both[:, at : at + WIDTH]
+            ref[1, k] = both[:, at + WIDTH : at + 2 * WIDTH]
+            ref[2, k] = down[half * WIDTH : (half + 1) * WIDTH]
+
+
+def joined_kernel(core_ref, own_ref, got_ref, gate_ref, up_ref, down_ref):
+    core = core_ref[0]
+    for k in range(RING):
+        for side, ref in ((core, own_ref), (1 - core, got_ref)):
+            at = 2 * k + side
+            gate_ref[at] = ref[0, k]
+            up_ref[at] = ref[1, k]
+            down_ref[:, pl.ds(pl.multiple_of(at * WIDTH, WIDTH), WIDTH)] = ref[2, k]
 
 
 def return_kernel(parts_ref, back_ref, send_ref):
@@ -220,36 +245,40 @@
     before = dot(jnp.where(b < here, logs, 0.0), ones_where(a > b, F32), 1, 0, EXACT)
     later = jnp.where(b > here, jnp.exp(later), 0.0)
     before = jnp.where(b < here, jnp.exp(before), 0.0)
-    lane = iota((KEY_DIM, WIDTH), 1)
+    half = KEY_DIM // 2
+    first = iota((half, WIDTH), 1) < VAL_DIM
     for k in range(PEERS):
-        reach_ref[k] = jnp.where(lane < VAL_DIM, later[:, k : k + 1], before[:, k : k + 1])
+        for side, value in enumerate((later, before)):
+            column = value[:, k : k + 1]
+            reach_ref[side, k] = jnp.where(first, column[:half], column[half:])
 
 
 def source_kernel(
-    rows_ref, weight_ref, normed_ref, inv_ref, mix_ref, query_fwd_ref, query_bwd_ref,
+    place_ref, rows_ref, weight_ref, normed_ref, inv_ref, mix_ref, query_fwd_ref, query_bwd_ref,
     send_ref, grad_ref,
 ):
+    here = place_ref[0]
     rows = jnp.concatenate([rows_ref[c, k] for k in range(RING) for c in range(2)], axis=1)
     grad = dot(rows, weight_ref[...], 1, 1)
     normed = normed_ref[...]
     mean = jnp.mean(grad * normed, axis=1, keepdims=True)
     grad = inv_ref[...] * (grad - normed * mean)
     grad_ref[...] = grad
-    state = jnp.concatenate(
-        [
-            dot(query_fwd_ref[...], grad, 1, 0, EXACT),
-            dot(query_bwd_ref[...], grad, 1, 0, EXACT),
-        ],
-        axis=1,
-    ).astype(BF16)
+    twice = jnp.concatenate([grad, grad], axis=1)
+    half = KEY_DIM // 2
+    first = iota((half, WIDTH), 1) < VAL_DIM
+    states = []
+    for ref in (query_fwd_ref, query_bwd_ref):
+        state = dot(ref[...], twice, 1, 0, EXACT)
+        states.append(jnp.where(first, state[:half], state[half:]))
     lane = iota((KEY_DIM, WIDTH), 1)
     for k in range(2 * RING):
         part = dot(rows[:, k * WIDTH : (k + 1) * WIDTH], mix_ref[...], 0, 0)
-        for half in range(2):
-            at = half * VAL_DIM
+        for side in range(2):
+            at, peer = side * VAL_DIM, 2 * k + side
             both = jnp.where(lane < VAL_DIM, part[at : at + 32], part[at + 32 : at + 64])
-            send_ref[2 * k + half, :KEY_DIM] = both.astype(BF16)
-            send_ref[2 * k + half, KEY_DIM:] = state
+            send_ref[peer, :KEY_DIM] = both.astype(BF16)
+            send_ref[peer, KEY_DIM:] = jnp.where(peer < here, states[0], states[1]).astype(BF16)
 
 
 def final_kernel(
@@ -258,17 +287,21 @@
     proj_ref, keys_ref, vals_ref, logit_ref,
 ):
     proj = got_ref[0, :KEY_DIM].astype(F32)
-    flow = got_ref[0, KEY_DIM:].astype(F32) * reach_ref[0]
+    flow = got_ref[0, KEY_DIM:].astype(F32)
+    packed = [flow * reach_ref[0, 0], flow * reach_ref[1, 0]]
     for k in range(1, PEERS):
         proj = proj + got_ref[k, :KEY_DIM].astype(F32)
-        flow = flow + got_ref[k, KEY_DIM:].astype(F32) * reach_ref[k]
+        flow = got_ref[k, KEY_DIM:].astype(F32)
+        packed = [total + flow * reach_ref[side, k] for side, total in enumerate(packed)]
+    flow_fwd, flow_bwd = (
+        jnp.concatenate([total[:, :VAL_DIM], total[:, VAL_DIM:]], axis=0) for total in packed
+    )
     proj_ref[:KEY_DIM] = proj[:, :VAL_DIM]
     proj_ref[KEY_DIM:] = proj[:, VAL_DIM:]
     cum = cum_ref[...]
     total = cum[:, TOK - 1 : TOK]
     keys, vals = key_ref[...].astype(F32), val_ref[...].astype(F32)
     scale_fwd, scale_bwd = jnp.exp(total - cum), jnp.exp(cum)
-    flow_fwd, flow_bwd = flow[:, :VAL_DIM], flow[:, VAL_DIM:]
     grad_fwd = dot(flow_fwd, vals, 1, 0, EXACT) * scale_fwd
     grad_bwd = dot(flow_bwd, vals, 1, 0, EXACT) * scale_bwd
     keys_ref[...] = keys_mix_ref[...] + grad_fwd + grad_bwd
@@ -277,7 +310,9 @@
         + dot(flow_fwd, keys * scale_fwd, 0, 0, EXACT)
         + dot(flow_bwd, keys * scale_bwd, 0, 0, EXACT)
     )
-    factor = jnp.exp(total) * jnp.sum(flow * state_ref[...], axis=1, keepdims=True)
+    state = state_ref[...]
+    flow = flow_fwd * state[:, :VAL_DIM] + flow_bwd * state[:, VAL_DIM:]
+    factor = jnp.exp(total) * jnp.sum(flow, axis=1, keepdims=True)
     grad_fwd, grad_bwd = grad_fwd * keys, grad_bwd * keys
     at_end = factor + jnp.sum(grad_fwd, axis=1, keepdims=True)
     row, col = iota((TOK, TOK), 0), iota((TOK, TOK), 1)
@@ -303,7 +338,7 @@
 
 def call(kernel, outs, *args, scalars=0, stored=()):
     shapes = [
-        (jax.ShapeDtypeStruct if k in stored else pltpu.VMEM)(shape, dtype)
+        (pltpu.HBM if k in stored else pltpu.VMEM)(shape, dtype)
         for k, (shape, dtype) in enumerate(outs)
     ]
     return pl.pallas_call(
@@ -315,10 +350,9 @@
     )(*args)
 
 
-def inner(scaled, keys, vals, cum):
-    row, col = iota((TOK, TOK), 0), iota((TOK, TOK), 1)
+def inner(scaled, keys, vals, cum, lower):
     gap = cum[:, :, None] - cum[:, None, :]
-    weight = jnp.exp(jnp.where(row >= col, gap, -gap))
+    weight = jnp.exp(jnp.where(lower, gap, -gap))
     scores = jnp.einsum("ct,cs,cts->ts", scaled, keys, weight)
     return jnp.einsum("ts,vs->vt", scores, vals)
 
@@ -371,81 +405,85 @@
         off_chip(decay_preactivation),
         off_chip(extra_log_decay),
         off_chip(speed),
-    )
-    got = on_chip(exchanged(send, sp))
-    rows_x, copies, back = call(
+        stored=(1,),
+    )
+    got = exchanged(send, sp)
+    (theirs,) = call(
+        slice_kernel,
+        [((3, RING, WIDTH, WIDTH), BF16)],
+        core_at,
+        off_chip(gate_blocks),
+        off_chip(up_blocks),
+        off_chip(down),
+        scalars=1,
+        stored=(0,),
+    )
+    swapped = lax.ppermute(theirs, "core", swap)
+    copies, back = call(
         arrival_kernel,
-        [((ROWS, WIDTH), BF16), ((RING, ROWS, WIDTH), BF16), ((PEERS, PAD, WIDTH), BF16)],
-        got,
-    )
-    own_y = exchanged(copies, "y")
-    own_x = lax.all_gather(rows_x, "y", axis=0, tiled=False)
-
-    theirs = jnp.stack(
-        [
-            lax.dynamic_index_in_dim(
-                w.reshape(RING, 2, WIDTH, WIDTH), 1 - core, axis=1, keepdims=False
-            )
-            for w in (gate, up)
-        ]
-    )
-    swapped = lax.ppermute(theirs, "core", swap)
-
-    other_x = lax.ppermute(own_x, "core", swap)
-    other_y = lax.ppermute(own_y, "core", swap)
-    (pre,) = call(
+        [((RING, ROWS, 2 * WIDTH), BF16), ((PEERS, PAD, WIDTH), BF16)],
+        on_chip(got),
+        stored=(0, 1),
+    )
+    rows = exchanged(copies, "y")
+    own, send = call(
         forward_kernel,
-        [((ROWS, 2 * WIDTH), F32)],
+        [((2, ROWS, 3 * WIDTH), F32), ((2, ROWS, 3 * WIDTH), BF16)],
         core_at,
-        own_x,
-        other_x,
+        rows,
         gate_blocks,
         up_blocks,
+        down,
+        swapped,
         scalars=1,
     )
-    grads, hidden = call(
-        hidden_kernel,
-        [((ROWS, 2 * WIDTH), BF16), ((ROWS, WIDTH), BF16)],
+    crossed = lax.ppermute(send, "core", swap)
+    partials, grads, hidden = call(
+        partial_kernel,
+        [
+            ((RING, ROWS, WIDTH), BF16),
+            ((ROWS, 4 * WIDTH), BF16),
+            ((ROWS, 2 * WIDTH), BF16),
+        ],
         core_at,
-        own_y,
-        other_y,
-        down,
-        pre,
-        scalars=1,
-    )
-    grads_both = lax.all_gather(grads, "core", axis=0, tiled=False)
-    (partials,) = call(
-        partial_kernel,
-        [((RING, ROWS, WIDTH), BF16)],
-        core_at,
-        on_chip(grads_both),
+        on_chip(own),
+        on_chip(crossed),
         gate_blocks,
         up_blocks,
         swapped,
         scalars=1,
+        stored=(1, 2),
     )
     parts = exchanged(partials, "y")
-    (send,) = call(return_kernel, [((PEERS, PAD, WIDTH), BF16)], on_chip(parts), on_chip(back))
+    (send,) = call(
+        return_kernel, [((PEERS, PAD, WIDTH), BF16)], on_chip(parts), off_chip(back)
+    )
     returned = on_chip(exchanged(send, sp))
     (copies,) = call(
-        token_kernel, [((RING, TOK, WIDTH), BF16)], returned, pick, cotangent
-    )
-    cum, copies = lax.optimization_barrier((cum, copies))
+        token_kernel, [((RING, TOK, WIDTH), BF16)], returned, off_chip(pick), off_chip(cotangent)
+    )
+    row = iota((TOK, TOK), 0)
+    cum, queries, key_in, val_in, row, copies = lax.optimization_barrier(
+        (cum, queries, input_key_matrix, input_value_matrix, row, copies)
+    )
     full_rows = exchanged(copies, "y")
     full_rows = lax.all_gather(full_rows, "core", axis=0, tiled=False)
 
     state, reach = call(
         state_kernel,
-        [((KEY_DIM, WIDTH), F32), ((PEERS, KEY_DIM, WIDTH), F32)],
+        [((KEY_DIM, WIDTH), F32), ((2, PEERS, KEY_DIM // 2, WIDTH), F32)],
         place_at,
         returned,
         scalars=1,
     )
     scaled = queries.astype(F32) * KEY_DIM ** (-0.5)
-    keys = input_key_matrix.astype(F32)
-    vals = input_value_matrix.astype(F32)
+    keys = key_in.astype(F32)
+    vals = val_in.astype(F32)
+    lower = row >= iota((TOK, TOK), 1)
     fwd_in, bwd_in = state[:, :VAL_DIM], state[:, VAL_DIM:]
-    inner_out, pull_inner = jax.vjp(inner, scaled, keys, vals, cum)
+    inner_out, pull_inner = jax.vjp(
+        lambda *args: inner(*args, lower), scaled, keys, vals, cum
+    )
     carried_out, pull_carried = jax.vjp(
         lambda s, c: carried(s, c, fwd_in, bwd_in), scaled, cum
     )
@@ -454,33 +492,43 @@
     normed = mixed * inv_rms
     normed_t = normed.T
     mix_t = normed_t.astype(BF16)
+    mix_twice = jnp.concatenate([mix_t, mix_t], axis=1)
+    query_fwd = scaled * jnp.exp(cum)
+    query_bwd = scaled * jnp.exp(cum[:, -1:] - cum)
     send, grad_mixed_t = call(
         source_kernel,
-        [((PEERS, 2 * KEY_DIM, WIDTH), BF16), ((TOK, VAL_DIM), F32)],
+        [((PEERS, 3 * KEY_DIM // 2, WIDTH), BF16), ((TOK, VAL_DIM), F32)],
+        place_at,
         on_chip(full_rows),
-        output_weight_matrix.T,
+        off_chip(output_weight_matrix.T),
         normed_t,
         inv_rms.reshape(TOK, 1),
-        jnp.concatenate([mix_t, mix_t], axis=1),
-        scaled * jnp.exp(cum),
-        scaled * jnp.exp(cum[:, -1:] - cum),
+        mix_twice,
+        query_fwd,
+        query_bwd,
+        scalars=1,
     )
     send, grads, hidden = lax.optimization_barrier((send, grads, hidden))
     got = exchanged(send, sp)
+    own, send = call(
+        weight_kernel,
+        [((3, RING, WIDTH, WIDTH), BF16)] * 2,
+        off_chip(rows),
+        off_chip(grads),
+        off_chip(hidden),
+        stored=range(2),
+    )
+    crossed = lax.ppermute(send, "core", swap)
     grad_gate, grad_up, grad_down = call(
-        weight_kernel,
+        joined_kernel,
         [
             ((2 * RING, WIDTH, WIDTH), BF16),
             ((2 * RING, WIDTH, WIDTH), BF16),
             ((WIDTH, MODEL), BF16),
         ],
         core_at,
-        own_x,
-        other_x,
-        own_y,
-        other_y,
-        grads,
-        hidden,
+        off_chip(own),
+        off_chip(crossed),
         scalars=1,
         stored=range(3),
     )
@@ -552,4 +600,5 @@
         P(sp, None, tp),
         P(sp, tp, None),
     )
+
     return jax.shard_map(body, mesh=fine, in_specs=in_specs, out_specs=out_specs, check_vma=False)

time: 180 us -> 184 us (1.022)
  waiting for transfers between devices: 23 us -> 63.7 us
  blocking collectives: 96 us -> 56.3 us
  Pallas kernels: 15.9 us -> 23.1 us
  starting transfers between devices: 32.8 us -> 28.3 us
    all_gather x2 -> x0, blocking collectives: 37.3 us -> none  [the longest x1 35.2 us: body(): own_x = lax.all_gather(rows_x, 'y', axis=0, tiled=False)]
    all_to_all x4, waiting for transfers between devices: 22.9 us -> 60 us  [exchanged(): return lax.all_to_all(array, axis, split_axis=0, concat_axis=0, tiled=True)]
    pallas_call x11 -> x12, Pallas kernels: 15.9 us -> 23.1 us  [call(): pl.pallas_call(kernel, out_shape=shapes, in_specs=[SCALAR] * scalars + [W...]
    ppermute x2, starting transfers between devices: 10.9 us -> 4.66 us  [body(): crossed = lax.ppermute(send, 'core', swap)]
    ppermute x1, starting transfers between devices: 2.41 us -> 4.63 us  [body(): swapped = lax.ppermute(theirs, 'core', swap)]
    all_to_all x2, blocking collectives: 53.1 us -> 50.9 us  [exchanged(): return lax.all_to_all(array, axis, split_axis=0, concat_axis=0, tiled=True)]
    ppermute x1, waiting for transfers between devices: 0.01 us -> 2.1 us  [body(): swapped = lax.ppermute(theirs, 'core', swap)]
  transfers between devices with their start and end apart: 7 -> 7, of which waited for: 3 -> 6; matrix products, arithmetic and copies ran while one was open for 4% -> 4% of each run, Pallas kernels for 4% -> 2%
where the time goes in v5:
time: 184 us; the launch traced here: 183 us
  waiting for transfers between devices  63.7 us (35%)
  blocking collectives  56.3 us (31%)
  starting transfers between devices  28.3 us (15%)
  Pallas kernels  23.1 us (13%)
  matrix products  4.11 us (2%)
  other arithmetic  3.64 us (2%)
  local copies, waits for them, and re-layouts  2.82 us (2%)
    all_to_all x4, waiting for transfers between devices, exchanged(): return lax.all_to_all(array, axis, split_axis=0, concat_axis=0, tiled=True)  60 us
    all_to_all x2, blocking collectives, exchanged(): return lax.all_to_all(array, axis, split_axis=0, concat_axis=0, tiled=True)  50.9 us
    pallas_call x12, Pallas kernels, call(): pl.pallas_call(kernel, out_shape=shapes, in_specs=[SCALAR] * scalars + [W...  23.1 us
    all_to_all x4, starting transfers between devices, exchanged(): return lax.all_to_all(array, axis, split_axis=0, concat_axis=0, tiled=True)  19 us
    all_gather x1, blocking collectives, body(): full_rows = lax.all_gather(full_rows, 'core', axis=0, tiled=False)  5.37 us
    ppermute x2, starting transfers between devices, body(): crossed = lax.ppermute(send, 'core', swap)  4.66 us
    ppermute x1, starting transfers between devices, body(): swapped = lax.ppermute(theirs, 'core', swap)  4.63 us
  transfers between devices with their start and end apart: 7, of which 6 were waited for; matrix products, arithmetic and copies ran while one was open for 4% of the time, Pallas kernels for 2%

profile of v5, /device:TPU:1, one launch (start us, length us, event | category | flops | bytes accessed | tf_op | source)
XLA Modules:
  0.0 182.9 jit_solution(6453025690434981605)
XLA Ops:
  0.6 1.8 shard_map.197
  2.4 24.8 %all_to_all.30.got_ref = bf16[32,16,256]{2,1,0:T(8,128)(2,1)S(1)} all-to-all(bf16[32,16,256]{2,1,0:T(8,128)(2,1)S(1)} %get-tuple-element.41), channel_id=1, replica_groups=mesh['z'=8,'x'=4,'y'=8,'core'=2] {'z','x'}, dimensions={0} | all-to-all | bytes 524288 | tf_op jit(solution)/shard_map/all_to_all | solution.py:391
  27.2 1.5 shard_map.198
  28.7 6.8 %all-to-all-start.1 = ((bf16[8,384,256]{2,1,0:T(8,128)(2,1)}), bf16[8,384,256]{2,1,0:T(8,128)(2,1)S(1)}, u32[]{:S(2)}, u32[]{:S(2)}) async-start(bf16[8,384,256]{2,1,0:T(8,128)(2,1)} %get-tuple-element.42), calls=%async_computation.1 | async-start | bytes 3145728 | tf_op jit(solution)/shard_map/all_to_all | solution.py:391
  35.6 0.0 copy-start.2
  35.6 2.4 %shard_map.199 = bf16[3,8,128,128]{3,2,1,0:T(8,128)(2,1)} custom-call(s32[1]{0:T(128)} %bitcast.6.core_ref, bf16[16,128,128]{2,1,0:T(8,128)(2,1)} %bitcast.60, bf16[16,128,128]{2,1,0:T(8,128)(2,1)} %bitcast.63, bf16[128,2048]{1,0:T(8,128)(2,1)} %bitcast.66), custom_call_target="tpu_custom_call" | custom-call | tf_op jit(solution)/shard_map/pallas_call | solution.py:344
  38.0 4.6 %collective-permute-start = (bf16[3,8,128,128]{3,2,1,0:T(8,128)(2,1)}, bf16[3,8,128,128]{3,2,1,0:T(8,128)(2,1)S(1)}, u32[]{:S(2)}, u32[]{:S(2)}) collective-permute-start(bf16[3,8,128,128]{3,2,1,0:T(8,128)(2,1)} %shard_map.199), channel_id=1, source_target_pairs={{0,1},{1,0},{2,3},{3,2},{4,5},{5,4},{6,7},{7,6},{8,9},{9,8},{10,11... | collective-permute-start | bytes 2359304 | tf_op jit(solution)/shard_map/ppermute | solution.py:421
  42.6 2.1 %collective-permute-done.swapped_ref = bf16[3,8,128,128]{3,2,1,0:T(8,128)(2,1)S(1)} collective-permute-done((bf16[3,8,128,128]{3,2,1,0:T(8,128)(2,1)}, bf16[3,8,128,128]{3,2,1,0:T(8,128)(2,1)S(1)}, u32[]{:S(2)}, u32[]{:S(2)}) %collective-permute-start) | collective-permute-done | bytes 786464 | tf_op jit(solution)/shard_map/ppermute | solution.py:421
  44.7 31.2 %all-to-all-done.1.rows_ref = bf16[8,384,256]{2,1,0:T(8,128)(2,1)S(1)} async-done(((bf16[8,384,256]{2,1,0:T(8,128)(2,1)}), bf16[8,384,256]{2,1,0:T(8,128)(2,1)S(1)}, u32[]{:S(2)}, u32[]{:S(2)}) %all-to-all-start.1) | async-done | bytes 1572896 | tf_op jit(solution)/shard_map/all_to_all | solution.py:391
  76.0 0.0 copy-done.1
  76.0 0.0 copy-done.2
  76.0 0.0 copy-start.3
  76.0 1.0 copy-done.3
  77.0 0.0 copy-start
  77.0 0.8 shard_map.200
  77.8 0.4 copy-done
  78.2 2.4 %collective-permute-start.1 = (bf16[2,384,384]{2,1,0:T(8,128)(2,1)S(1)}, bf16[2,384,384]{2,1,0:T(8,128)(2,1)S(1)}, u32[]{:S(2)}, u32[]{:S(2)}) collective-permute-start(bf16[2,384,384]{2,1,0:T(8,128)(2,1)S(1)} %get-tuple-element.44), channel_id=1, source_target_pairs={{0,1},{1,0},{2,3},{3,2},{4,5},{5,4},{6,7},{7,6},{8,9},{9,8},{10,11... | collective-permute-start | bytes 1769480 | tf_op jit(solution)/shard_map/ppermute | solution.py:440
  80.6 1.6 collective-permute-done.1.got_ref
  82.2 1.6 shard_map.201
  83.8 0.0 copy-start.5
  83.8 0.0 copy-start.9
  83.8 26.1 %all_to_all.31.parts_ref = bf16[8,384,128]{2,1,0:T(8,128)(2,1)S(1)} all-to-all(bf16[8,384,128]{2,1,0:T(8,128)(2,1)S(1)} %get-tuple-element.45), channel_id=1, replica_groups=mesh['z'=8,'x'=4,'y'=8,'core'=2] {'y'}, dimensions={0} | all-to-all | bytes 1572864 | tf_op jit(solution)/shard_map/all_to_all | solution.py:391
  109.9 1.9 %shard_map.202 = bf16[32,16,128]{2,1,0:T(8,128)(2,1)} custom-call(bf16[8,384,128]{2,1,0:T(8,128)(2,1)S(1)} %all_to_all.31.parts_ref, bf16[32,16,128]{2,1,0:T(8,128)(2,1)} %get-tuple-element.46.back_ref), custom_call_target="tpu_custom_call" | custom-call | tf_op jit(solution)/shard_map/pallas_call | solution.py:344
  111.8 0.0 copy-start.4
  111.8 4.8 %all-to-all-start.3 = ((bf16[32,16,128]{2,1,0:T(8,128)(2,1)}), bf16[32,16,128]{2,1,0:T(8,128)(2,1)S(1)}, u32[]{:S(2)}, u32[]{:S(2)}) async-start(bf16[32,16,128]{2,1,0:T(8,128)(2,1)} %shard_map.202), calls=%async_computation.3 | async-start | bytes 262144 | tf_op jit(solution)/shard_map/all_to_all | solution.py:391
  116.6 9.3 %all-to-all-done.3.got_ref = bf16[32,16,128]{2,1,0:T(8,128)(2,1)S(1)} async-done(((bf16[32,16,128]{2,1,0:T(8,128)(2,1)}), bf16[32,16,128]{2,1,0:T(8,128)(2,1)S(1)}, u32[]{:S(2)}, u32[]{:S(2)}) %all-to-all-start.3) | async-done | bytes 131104 | tf_op jit(solution)/shard_map/all_to_all | solution.py:391
  126.0 1.8 %shard_map.203 = bf16[8,128,128]{2,1,0:T(8,128)(2,1)} custom-call(bf16[32,16,128]{2,1,0:T(8,128)(2,1)S(1)} %all-to-all-done.3.got_ref, bf16[512,128]{1,0:T(8,128)(2,1)} %get-tuple-element.47.pick_ref, bf16[128,128]{1,0:T(8,128)(2,1)} %cot_ref.3), custom_call_target="tpu_custom_call" | custom-call | tf_op jit(solution)/shard_map/pallas_call | solution.py:344
  127.8 0.2 slice_reduce_fusion
  128.0 0.0 copy-done.5
  128.1 0.0 copy-done.9
  128.1 0.1 fusion.38
  128.1 0.9 shard_map.204
  129.0 0.2 fusion.35
  129.2 0.2 convolution_add_fusion.1
  129.5 0.1 copy.43
  129.6 3.4 %all-to-all-start.4 = ((bf16[8,128,128]{2,1,0:T(8,128)(2,1)}), bf16[8,128,128]{2,1,0:T(8,128)(2,1)S(1)}, u32[]{:S(2)}, u32[]{:S(2)}) async-start(bf16[8,128,128]{2,1,0:T(8,128)(2,1)} %shard_map.203), calls=%async_computation.4 | async-start | bytes 524288 | tf_op jit(solution)/shard_map/all_to_all | solution.py:391
  133.0 1.3 multiply_reduce_fusion
  134.3 0.0 copy-done.4
  134.3 0.2 multiply_reduce_fusion.1
  134.6 0.1 copy.44.inv_ref
  134.7 0.1 fusion.46
  134.8 0.1 pad_maximum_fusion.mix_ref
  134.9 7.3 %all-to-all-done.4 = bf16[8,128,128]{2,1,0:T(8,128)(2,1)S(1)} async-done(((bf16[8,128,128]{2,1,0:T(8,128)(2,1)}), bf16[8,128,128]{2,1,0:T(8,128)(2,1)S(1)}, u32[]{:S(2)}, u32[]{:S(2)}) %all-to-all-start.4) | async-done | bytes 262176 | tf_op jit(solution)/shard_map/all_to_all | solution.py:391
  142.2 5.4 %all-gather = bf16[16,128,128]{2,1,0:T(8,128)(2,1)S(1)} all-gather(bf16[8,128,128]{2,1,0:T(8,128)(2,1)S(1)} %all-to-all-done.4), channel_id=2, replica_groups=mesh['z'=8,'x'=4,'y'=8,'core'=2] {'core'}, dimensions={0}, use_global_device_ids=true | all-gather | bytes 786432 | tf_op jit(solution)/shard_map/all_gather | solution.py:470
  147.5 2.8 %shard_map.205 = (bf16[32,48,128]{2,1,0:T(8,128)(2,1)}, f32[128,64]{1,0:T(8,128)S(1)}) custom-call(s32[1]{0:T(128)} %bitcast.2.place_ref, bf16[2,8,128,128]{3,2,1,0:T(8,128)(2,1)S(1)} %bitcast.68, bf16[64,2048]{1,0:T(8,128)(2,1)} %bitcast.73, f32[128,64]{1,0:T(8,128)S(1)} %get-tuple-element.75.normed_ref, f32[128,1]{1,0:T(8,128)S(1)} %copy.44.inv_ref, ...), custom_call_target="tpu_custom_call" | custom-call | tf_op jit(solution)/shard_map/pallas_call | solution.py:344
  150.3 0.1 fusion.47
  150.4 0.1 fusion.33
  150.6 3.8 %shard_map.207 = (bf16[3,8,128,128]{3,2,1,0:T(8,128)(2,1)}, bf16[3,8,128,128]{3,2,1,0:T(8,128)(2,1)}) custom-call(bf16[8,384,256]{2,1,0:T(8,128)(2,1)} %copy-done, bf16[384,512]{1,0:T(8,128)(2,1)} %get-tuple-element.65.grads_ref, bf16[384,256]{1,0:T(8,128)(2,1)} %get-tuple-element.66.hidden_ref), custom_call_target="tpu_custom_call" | custom-call | tf_op jit(solution)/shard_map/pallas_call | solution.py:344
  154.4 2.3 %collective-permute-start.2 = (bf16[3,8,128,128]{3,2,1,0:T(8,128)(2,1)}, bf16[3,8,128,128]{3,2,1,0:T(8,128)(2,1)S(1)}, u32[]{:S(2)}, u32[]{:S(2)}) collective-permute-start(bf16[3,8,128,128]{3,2,1,0:T(8,128)(2,1)} %get-tuple-element.68), channel_id=1, source_target_pairs={{0,1},{1,0},{2,3},{3,2},{4,5},{5,4},{6,7},{7,6},{8,9},{9,8},{10,11... | collective-permute-start | bytes 2359304 | tf_op jit(solution)/shard_map/ppermute | solution.py:521
  156.7 2.1 %fusion.7 = (f32[32,128]{1,0:T(8,128)S(1)}, f32[32,128]{1,0:T(8,128)S(1)}) fusion(f32[128,128]{1,0:T(8,128)S(1)} %fusion.47, f32[32,128]{1,0:T(8,128)S(1)} %get-tuple-element.80, f32[32,128]{1,0:T(8,128)S(1)} %convert.3, f32[32,128]{1,0:T(8,128)S(1)} %get-tuple-element.51.cum_ref, pred[128,128]{1,0:T(8,128)(4,1)S(1)} %iota_compare_fusion.1), kind=kLoop, calls=%fused_computation.10 | loop fusion | flops 6283264 | bytes 163840 | tf_op jit(solution)/shard_map/transpose(jvp())/reduce_sum | solution.py:354
  158.8 0.9 fusion.4
  159.7 3.9 %all-to-all-start.5 = ((bf16[32,48,128]{2,1,0:T(8,128)(2,1)}), bf16[32,48,128]{2,1,0:T(8,128)(2,1)S(1)}, u32[]{:S(2)}, u32[]{:S(2)}) async-start(bf16[32,48,128]{2,1,0:T(8,128)(2,1)} %get-tuple-element.59), calls=%async_computation.5 | async-start | bytes 786432 | tf_op jit(solution)/shard_map/all_to_all | solution.py:391
  163.6 0.9 fusion.39
  164.5 0.1 copy.45
  164.6 0.2 fusion.16.decay_mix_ref
  164.9 0.2 fusion.48.vals_mix_ref
  165.1 0.9 fusion.2
  166.0 12.1 %all-to-all-done.5.got_ref = bf16[32,48,128]{2,1,0:T(8,128)(2,1)S(1)} async-done(((bf16[32,48,128]{2,1,0:T(8,128)(2,1)}), bf16[32,48,128]{2,1,0:T(8,128)(2,1)S(1)}, u32[]{:S(2)}, u32[]{:S(2)}) %all-to-all-start.5) | async-done | bytes 393248 | tf_op jit(solution)/shard_map/all_to_all | solution.py:391
  178.1 0.0 copy-done.6
  178.1 0.0 copy-done.7
  178.1 1.1 shard_map.206
  179.3 0.0 collective-permute-done.2.got_ref
  179.3 0.9 copy-done.8
  180.2 2.7 %shard_map.208 = (bf16[16,128,128]{2,1,0:T(8,128)(2,1)}, bf16[16,128,128]{2,1,0:T(8,128)(2,1)}, bf16[128,2048]{1,0:T(8,128)(2,1)}) custom-call(s32[1]{0:T(128)} %bitcast.6.core_ref, bf16[3,8,128,128]{3,2,1,0:T(8,128)(2,1)} %get-tuple-element.67.own_ref, bf16[3,8,128,128]{3,2,1,0:T(8,128)(2,1)} %copy-done.8), custom_call_target="tpu_custom_call" | custom-call | tf_op jit(solution)/shard_map/pallas_call | solution.py:344
  (8 shorter events, 0.0 us)
Async XLA Ops:
  28.7 47.2 %all-to-all-start.1 = ((bf16[8,384,256]{2,1,0:T(8,128)(2,1)}), bf16[8,384,256]{2,1,0:T(8,128)(2,1)S(1)}, u32[]{:S(2)}, u32[]{:S(2)}) async-start(bf16[8,384,256]{2,1,0:T(8,128)(2,1)} %get-tuple-element.42), calls=%async_computation.1 | async-start | bytes 3145728 | tf_op jit(solution)/shard_map/all_to_all | solution.py:391
  35.6 40.4 %copy-start.1 = (bf16[1,2048,128]{2,1,0:T(8,128)(2,1)S(1)}, bf16[1,2048,128]{2,1,0:T(8,128)(2,1)}, u32[]{:S(2)}) copy-start(bf16[1,2048,128]{2,1,0:T(8,128)(2,1)} %param.25) | copy-start | bytes 1572868
  35.6 40.4 %copy-start.2 = (bf16[1,2048,128]{2,1,0:T(8,128)(2,1)S(1)}, bf16[1,2048,128]{2,1,0:T(8,128)(2,1)}, u32[]{:S(2)}) copy-start(bf16[1,2048,128]{2,1,0:T(8,128)(2,1)} %param.26) | copy-start | bytes 1572868
  38.0 6.7 %collective-permute-start = (bf16[3,8,128,128]{3,2,1,0:T(8,128)(2,1)}, bf16[3,8,128,128]{3,2,1,0:T(8,128)(2,1)S(1)}, u32[]{:S(2)}, u32[]{:S(2)}) collective-permute-start(bf16[3,8,128,128]{3,2,1,0:T(8,128)(2,1)} %shard_map.199), channel_id=1, source_target_pairs={{0,1},{1,0},{2,3},{3,2},{4,5},{5,4},{6,7},{7,6},{8,9},{9,8},{10,11... | collective-permute-start | bytes 2359304 | tf_op jit(solution)/shard_map/ppermute | solution.py:421
  76.0 1.0 copy-start.3
  77.0 1.2 copy-start
  78.2 4.0 %collective-permute-start.1 = (bf16[2,384,384]{2,1,0:T(8,128)(2,1)S(1)}, bf16[2,384,384]{2,1,0:T(8,128)(2,1)S(1)}, u32[]{:S(2)}, u32[]{:S(2)}) collective-permute-start(bf16[2,384,384]{2,1,0:T(8,128)(2,1)S(1)} %get-tuple-element.44), channel_id=1, source_target_pairs={{0,1},{1,0},{2,3},{3,2},{4,5},{5,4},{6,7},{7,6},{8,9},{9,8},{10,11... | collective-permute-start | bytes 1769480 | tf_op jit(solution)/shard_map/ppermute | solution.py:440
  83.8 44.3 %copy-start.5 = (bf16[32,128]{1,0:T(8,128)(2,1)S(1)}, bf16[32,128]{1,0:T(8,128)(2,1)}, u32[]{:S(2)}) copy-start(bf16[32,128]{1,0:T(8,128)(2,1)} %key_ref.3) | copy-start | bytes 24580
  83.8 44.3 %copy-start.9 = (bf16[32,128]{1,0:T(8,128)(2,1)S(1)}, bf16[32,128]{1,0:T(8,128)(2,1)}, u32[]{:S(2)}) copy-start(bf16[32,128]{1,0:T(8,128)(2,1)} %param.14) | copy-start | bytes 24580
  111.8 22.5 %copy-start.4 = (bf16[64,128]{1,0:T(8,128)(2,1)S(1)}, bf16[64,128]{1,0:T(8,128)(2,1)}, u32[]{:S(2)}) copy-start(bf16[64,128]{1,0:T(8,128)(2,1)} %val_ref.3) | copy-start | bytes 49156
  111.8 14.2 %all-to-all-start.3 = ((bf16[32,16,128]{2,1,0:T(8,128)(2,1)}), bf16[32,16,128]{2,1,0:T(8,128)(2,1)S(1)}, u32[]{:S(2)}, u32[]{:S(2)}) async-start(bf16[32,16,128]{2,1,0:T(8,128)(2,1)} %shard_map.202), calls=%async_computation.3 | async-start | bytes 262144 | tf_op jit(solution)/shard_map/all_to_all | solution.py:391
  129.6 12.6 %all-to-all-start.4 = ((bf16[8,128,128]{2,1,0:T(8,128)(2,1)}), bf16[8,128,128]{2,1,0:T(8,128)(2,1)S(1)}, u32[]{:S(2)}, u32[]{:S(2)}) async-start(bf16[8,128,128]{2,1,0:T(8,128)(2,1)} %shard_map.203), calls=%async_computation.4 | async-start | bytes 524288 | tf_op jit(solution)/shard_map/all_to_all | solution.py:391
  154.4 24.8 %collective-permute-start.2 = (bf16[3,8,128,128]{3,2,1,0:T(8,128)(2,1)}, bf16[3,8,128,128]{3,2,1,0:T(8,128)(2,1)S(1)}, u32[]{:S(2)}, u32[]{:S(2)}) collective-permute-start(bf16[3,8,128,128]{3,2,1,0:T(8,128)(2,1)} %get-tuple-element.68), channel_id=1, source_target_pairs={{0,1},{1,0},{2,3},{3,2},{4,5},{5,4},{6,7},{7,6},{8,9},{9,8},{10,11... | collective-permute-start | bytes 2359304 | tf_op jit(solution)/shard_map/ppermute | solution.py:521
  159.7 18.4 %all-to-all-start.5 = ((bf16[32,48,128]{2,1,0:T(8,128)(2,1)}), bf16[32,48,128]{2,1,0:T(8,128)(2,1)S(1)}, u32[]{:S(2)}, u32[]{:S(2)}) async-start(bf16[32,48,128]{2,1,0:T(8,128)(2,1)} %get-tuple-element.59), calls=%async_computation.5 | async-start | bytes 786432 | tf_op jit(solution)/shard_map/all_to_all | solution.py:391
  165.1 13.1 %copy-start.6 = (bf16[32,128]{1,0:T(8,128)(2,1)S(1)}, bf16[32,128]{1,0:T(8,128)(2,1)}, u32[]{:S(2)}) copy-start(bf16[32,128]{1,0:T(8,128)(2,1)} %pre_ref.3) | copy-start | bytes 24580
  165.1 13.1 %copy-start.7 = (f32[32]{0:T(128)S(1)}, f32[32]{0:T(128)}, u32[]{:S(2)}) copy-start(f32[32]{0:T(128)} %param.19) | copy-start | bytes 388
  179.3 0.9 copy-start.8

commit v6 on v5

--- a/solution.py
+++ b/solution.py
@@ -136,27 +136,25 @@
     back_ref[...] = block.astype(BF16)
 
 
-def slice_kernel(core_ref, gate_ref, up_ref, down_ref, out_ref):
-    other = 1 - core_ref[0]
-    for k in range(RING):
-        at = 2 * k + other
-        out_ref[0, k] = gate_ref[at]
-        out_ref[1, k] = up_ref[at]
-        out_ref[2, k] = down_ref[:, pl.ds(pl.multiple_of(at * WIDTH, WIDTH), WIDTH)]
-
-
-def forward_kernel(core_ref, rows_ref, gate_ref, up_ref, down_ref, swapped_ref, out_ref, send_ref):
+def slice_kernel(core_ref, place_ref, gate_ref, up_ref, down_ref, own_ref, out_ref):
     core = core_ref[0]
+    for side, ref in ((core, own_ref), (1 - core, out_ref)):
+        for k in range(RING):
+            at = 2 * k + side
+            ref[0, k] = gate_ref[at]
+            ref[1, k] = up_ref[at]
+            ref[2, k] = down_ref[:, pl.ds(pl.multiple_of(at * WIDTH, WIDTH), WIDTH)]
+
+
+def forward_kernel(rows_ref, own_ref, swapped_ref, out_ref, send_ref):
     pre = jnp.zeros((ROWS, 4 * WIDTH), F32)
     grad = jnp.zeros((ROWS, 2 * WIDTH), F32)
     for k in range(0, RING, 2):
         weights, downs = [], []
         for j in (k, k + 1):
-            at = 2 * j + core
-            parts = [gate_ref[at], up_ref[at], swapped_ref[0, j], swapped_ref[1, j]]
+            parts = [own_ref[0, j], own_ref[1, j], swapped_ref[0, j], swapped_ref[1, j]]
             weights.append(jnp.concatenate(parts, axis=1))
-            lanes = pl.ds(pl.multiple_of(at * WIDTH, WIDTH), WIDTH)
-            downs.append(jnp.concatenate([down_ref[:, lanes], swapped_ref[2, j]], axis=0))
+            downs.append(jnp.concatenate([own_ref[2, j], swapped_ref[2, j]], axis=0))
         x = jnp.concatenate([rows_ref[k, :, :WIDTH], rows_ref[k + 1, :, :WIDTH]], axis=1)
         y = jnp.concatenate([rows_ref[k, :, WIDTH:], rows_ref[k + 1, :, WIDTH:]], axis=1)
         pre = pre + dot(x, jnp.concatenate(weights, axis=0), 1, 0)
@@ -170,9 +168,8 @@
 
 
 def partial_kernel(
-    core_ref, own_ref, got_ref, gate_ref, up_ref, swapped_ref, out_ref, grads_ref, hidden_ref
+    own_ref, got_ref, kept_ref, swapped_ref, out_ref, grads_ref, hidden_ref
 ):
-    core = core_ref[0]
     grads = []
     for half in range(2):
         total = own_ref[half] + got_ref[half].astype(F32)
@@ -187,9 +184,8 @@
     grads = jnp.concatenate(grads, axis=1)
     grads_ref[...] = grads
     for k in range(RING):
-        at = 2 * k + core
         weights = jnp.concatenate(
-            [gate_ref[at], up_ref[at], swapped_ref[0, k], swapped_ref[1, k]], axis=1
+            [kept_ref[0, k], kept_ref[1, k], swapped_ref[0, k], swapped_ref[1, k]], axis=1
         )
         out_ref[k] = dot(grads, weights, 1, 1).astype(BF16)
 
@@ -408,17 +404,6 @@
         stored=(1,),
     )
     got = exchanged(send, sp)
-    (theirs,) = call(
-        slice_kernel,
-        [((3, RING, WIDTH, WIDTH), BF16)],
-        core_at,
-        off_chip(gate_blocks),
-        off_chip(up_blocks),
-        off_chip(down),
-        scalars=1,
-        stored=(0,),
-    )
-    swapped = lax.ppermute(theirs, "core", swap)
     copies, back = call(
         arrival_kernel,
         [((RING, ROWS, 2 * WIDTH), BF16), ((PEERS, PAD, WIDTH), BF16)],
@@ -426,16 +411,24 @@
         stored=(0, 1),
     )
     rows = exchanged(copies, "y")
+    kept, theirs = call(
+        slice_kernel,
+        [((3, RING, WIDTH, WIDTH), BF16)] * 2,
+        core_at,
+        place_at,
+        off_chip(gate_blocks),
+        off_chip(up_blocks),
+        off_chip(down),
+        scalars=2,
+        stored=(1,),
+    )
+    swapped = lax.ppermute(theirs, "core", swap)
     own, send = call(
         forward_kernel,
         [((2, ROWS, 3 * WIDTH), F32), ((2, ROWS, 3 * WIDTH), BF16)],
-        core_at,
         rows,
-        gate_blocks,
-        up_blocks,
-        down,
+        on_chip(kept),
         swapped,
-        scalars=1,
     )
     crossed = lax.ppermute(send, "core", swap)
     partials, grads, hidden = call(
@@ -445,13 +438,10 @@
             ((ROWS, 4 * WIDTH), BF16),
             ((ROWS, 2 * WIDTH), BF16),
         ],
-        core_at,
         on_chip(own),
         on_chip(crossed),
-        gate_blocks,
-        up_blocks,
+        on_chip(kept),
         swapped,
-        scalars=1,
         stored=(1, 2),
     )
     parts = exchanged(partials, "y")
@@ -508,7 +498,6 @@
         query_bwd,
         scalars=1,
     )
-    send, grads, hidden = lax.optimization_barrier((send, grads, hidden))
     got = exchanged(send, sp)
     own, send = call(
         weight_kernel,
@@ -528,7 +517,7 @@
         ],
         core_at,
         off_chip(own),
-        off_chip(crossed),
+        crossed,
         scalars=1,
         stored=range(3),
     )

time: 184 us -> 174 us (0.946)
  blocking collectives: 56.3 us -> 30.2 us
  waiting for transfers between devices: 63.7 us -> 78.1 us
  starting transfers between devices: 28.3 us -> 31.8 us
  local copies, waits for them, and re-layouts: 2.82 us -> 0.88 us
    all_to_all x2 -> x1, blocking collectives: 50.9 us -> 24.8 us  [exchanged(): return lax.all_to_all(array, axis, split_axis=0, concat_axis=0, tiled=True)]
    all_to_all x4 -> x5, waiting for transfers between devices: 60 us -> 74.4 us  [exchanged(): return lax.all_to_all(array, axis, split_axis=0, concat_axis=0, tiled=True)]
    all_to_all x4 -> x5, starting transfers between devices: 19 us -> 22.4 us  [exchanged(): return lax.all_to_all(array, axis, split_axis=0, concat_axis=0, tiled=True)]
    unnamed x20 -> x12, local copies, waits for them, and re-layouts: 2.34 us -> 0.4 us
  transfers between devices with their start and end apart: 7 -> 8, of which waited for: 6 -> 7; matrix products, arithmetic and copies ran while one was open for 4% -> 2% of each run, Pallas kernels for 2% -> 6%
where the time goes in v6:
time: 174 us; the launch traced here: 173 us
  waiting for transfers between devices  78.1 us (45%)
  starting transfers between devices  31.8 us (18%)
  blocking collectives  30.2 us (17%)
  Pallas kernels  23.3 us (13%)
  matrix products  4.11 us (2%)
  other arithmetic  3.66 us (2%)
    all_to_all x5, waiting for transfers between devices, exchanged(): return lax.all_to_all(array, axis, split_axis=0, concat_axis=0, tiled=True)  74.4 us
    all_to_all x1, blocking collectives, exchanged(): return lax.all_to_all(array, axis, split_axis=0, concat_axis=0, tiled=True)  24.8 us
    pallas_call x12, Pallas kernels, call(): pl.pallas_call(kernel, out_shape=shapes, in_specs=[SCALAR] * scalars + [W...  23.3 us
    all_to_all x5, starting transfers between devices, exchanged(): return lax.all_to_all(array, axis, split_axis=0, concat_axis=0, tiled=True)  22.4 us
    all_gather x1, blocking collectives, body(): full_rows = lax.all_gather(full_rows, 'core', axis=0, tiled=False)  5.36 us
    ppermute x2, starting transfers between devices, body(): crossed = lax.ppermute(send, 'core', swap)  4.72 us
    ppermute x1, starting transfers between devices, body(): swapped = lax.ppermute(theirs, 'core', swap)  4.63 us
  transfers between devices with their start and end apart: 8, of which 7 were waited for; matrix products, arithmetic and copies ran while one was open for 2% of the time, Pallas kernels for 6%

profile of v6, /device:TPU:1, one launch (start us, length us, event | category | flops | bytes accessed | tf_op | source)
XLA Modules:
  0.0 172.8 jit_solution(948791273080225303)
XLA Ops:
  0.6 1.8 %shard_map.197 = (bf16[32,16,256]{2,1,0:T(8,128)(2,1)S(1)}, bf16[512,128]{1,0:T(8,128)(2,1)}, f32[32,128]{1,0:T(8,128)S(1)}) custom-call(s32[2,128]{1,0:T(2,128)} %bitcast.72, f32[2,128]{1,0:T(2,128)} %bitcast.73, bf16[128,128]{1,0:T(8,128)(2,1)} %x_ref.1, bf16[128,128]{1,0:T(8,128)(2,1)} %cot_ref.3, bf16[32,128]{1,0:T(8,128)(2,1)} %key_ref.3, ...), custom_call_target="tpu_custom_call" | custom-call | tf_op jit(solution)/shard_map/pallas_call | solution.py:340
  2.4 24.8 %all_to_all.30.got_ref = bf16[32,16,256]{2,1,0:T(8,128)(2,1)S(1)} all-to-all(bf16[32,16,256]{2,1,0:T(8,128)(2,1)S(1)} %get-tuple-element.40), channel_id=1, replica_groups=mesh['z'=8,'x'=4,'y'=8,'core'=2] {'z','x'}, dimensions={0} | all-to-all | bytes 524288 | tf_op jit(solution)/shard_map/all_to_all | solution.py:387
  27.2 1.5 shard_map.198
  28.7 6.8 %all-to-all-start.1 = ((bf16[8,384,256]{2,1,0:T(8,128)(2,1)}), bf16[8,384,256]{2,1,0:T(8,128)(2,1)S(1)}, u32[]{:S(2)}, u32[]{:S(2)}) async-start(bf16[8,384,256]{2,1,0:T(8,128)(2,1)} %get-tuple-element.41), calls=%async_computation.1 | async-start | bytes 3145728 | tf_op jit(solution)/shard_map/all_to_all | solution.py:387
  35.5 2.4 %shard_map.199 = (bf16[3,8,128,128]{3,2,1,0:T(8,128)(2,1)S(1)}, bf16[3,8,128,128]{3,2,1,0:T(8,128)(2,1)}) custom-call(s32[1]{0:T(128)} %bitcast.6.core_ref, s32[1]{0:T(128)} %bitcast.2.place_ref, bf16[16,128,128]{2,1,0:T(8,128)(2,1)} %bitcast.65, bf16[16,128,128]{2,1,0:T(8,128)(2,1)} %bitcast.66, bf16[128,2048]{1,0:T(8,128)(2,1)} %bitcast.67), custom_call_target="tpu_custom_call" | custom-call | tf_op jit(solution)/shard_map/pallas_call | solution.py:340
  38.0 4.6 %collective-permute-start = (bf16[3,8,128,128]{3,2,1,0:T(8,128)(2,1)}, bf16[3,8,128,128]{3,2,1,0:T(8,128)(2,1)S(1)}, u32[]{:S(2)}, u32[]{:S(2)}) collective-permute-start(bf16[3,8,128,128]{3,2,1,0:T(8,128)(2,1)} %get-tuple-element.43), channel_id=1, source_target_pairs={{0,1},{1,0},{2,3},{3,2},{4,5},{5,4},{6,7},{7,6},{8,9},{9,8},{10,11... | collective-permute-start | bytes 2359304 | tf_op jit(solution)/shard_map/ppermute | solution.py:425
  42.6 2.1 %collective-permute-done.swapped_ref = bf16[3,8,128,128]{3,2,1,0:T(8,128)(2,1)S(1)} collective-permute-done((bf16[3,8,128,128]{3,2,1,0:T(8,128)(2,1)}, bf16[3,8,128,128]{3,2,1,0:T(8,128)(2,1)S(1)}, u32[]{:S(2)}, u32[]{:S(2)}) %collective-permute-start) | collective-permute-done | bytes 786464 | tf_op jit(solution)/shard_map/ppermute | solution.py:425
  44.7 31.3 %all-to-all-done.1.rows_ref = bf16[8,384,256]{2,1,0:T(8,128)(2,1)S(1)} async-done(((bf16[8,384,256]{2,1,0:T(8,128)(2,1)}), bf16[8,384,256]{2,1,0:T(8,128)(2,1)S(1)}, u32[]{:S(2)}, u32[]{:S(2)}) %all-to-all-start.1) | async-done | bytes 1572896 | tf_op jit(solution)/shard_map/all_to_all | solution.py:387
  76.0 0.0 copy-start
  76.0 0.8 shard_map.200
  76.8 0.4 copy-done
  77.1 2.4 %collective-permute-start.1 = (bf16[2,384,384]{2,1,0:T(8,128)(2,1)S(1)}, bf16[2,384,384]{2,1,0:T(8,128)(2,1)S(1)}, u32[]{:S(2)}, u32[]{:S(2)}) collective-permute-start(bf16[2,384,384]{2,1,0:T(8,128)(2,1)S(1)} %get-tuple-element.45), channel_id=1, source_target_pairs={{0,1},{1,0},{2,3},{3,2},{4,5},{5,4},{6,7},{7,6},{8,9},{9,8},{10,11... | collective-permute-start | bytes 1769480 | tf_op jit(solution)/shard_map/ppermute | solution.py:433
  79.5 1.6 collective-permute-done.1.got_ref
  81.2 2.0 %shard_map.201 = (bf16[8,384,128]{2,1,0:T(8,128)(2,1)}, bf16[384,512]{1,0:T(8,128)(2,1)}, bf16[384,256]{1,0:T(8,128)(2,1)}) custom-call(f32[2,384,384]{2,1,0:T(8,128)S(1)} %get-tuple-element.44.own_ref, bf16[2,384,384]{2,1,0:T(8,128)(2,1)S(1)} %collective-permute-done.1.got_ref, bf16[3,8,128,128]{3,2,1,0:T(8,128)(2,1)S(1)} %get-tuple-element.42.own_ref.kept_ref, ...), custom_call_target="tpu_custom_call" | custom-call | tf_op jit(solution)/shard_map/pallas_call | solution.py:340
  83.1 3.5 %all-to-all-start.2 = ((bf16[8,384,128]{2,1,0:T(8,128)(2,1)}), bf16[8,384,128]{2,1,0:T(8,128)(2,1)S(1)}, u32[]{:S(2)}, u32[]{:S(2)}) async-start(bf16[8,384,128]{2,1,0:T(8,128)(2,1)} %get-tuple-element.46), calls=%async_computation.2 | async-start | bytes 1572864 | tf_op jit(solution)/shard_map/all_to_all | solution.py:387
  86.7 3.8 %shard_map.207 = (bf16[3,8,128,128]{3,2,1,0:T(8,128)(2,1)}, bf16[3,8,128,128]{3,2,1,0:T(8,128)(2,1)}) custom-call(bf16[8,384,256]{2,1,0:T(8,128)(2,1)} %copy-done, bf16[384,512]{1,0:T(8,128)(2,1)} %get-tuple-element.63.grads_ref, bf16[384,256]{1,0:T(8,128)(2,1)} %get-tuple-element.64.hidden_ref), custom_call_target="tpu_custom_call" | custom-call | tf_op jit(solution)/shard_map/pallas_call | solution.py:340
  90.5 2.3 %collective-permute-start.2 = (bf16[3,8,128,128]{3,2,1,0:T(8,128)(2,1)}, bf16[3,8,128,128]{3,2,1,0:T(8,128)(2,1)S(1)}, u32[]{:S(2)}, u32[]{:S(2)}) collective-permute-start(bf16[3,8,128,128]{3,2,1,0:T(8,128)(2,1)} %get-tuple-element.66), channel_id=1, source_target_pairs={{0,1},{1,0},{2,3},{3,2},{4,5},{5,4},{6,7},{7,6},{8,9},{9,8},{10,11... | collective-permute-start | bytes 2359304 | tf_op jit(solution)/shard_map/ppermute | solution.py:510
  92.8 17.4 %all-to-all-done.2.parts_ref = bf16[8,384,128]{2,1,0:T(8,128)(2,1)S(1)} async-done(((bf16[8,384,128]{2,1,0:T(8,128)(2,1)}), bf16[8,384,128]{2,1,0:T(8,128)(2,1)S(1)}, u32[]{:S(2)}, u32[]{:S(2)}) %all-to-all-start.2) | async-done | bytes 786464 | tf_op jit(solution)/shard_map/all_to_all | solution.py:387
  110.2 0.0 copy-start.2
  110.2 0.0 copy-start.5
  110.2 1.9 %shard_map.202 = bf16[32,16,128]{2,1,0:T(8,128)(2,1)} custom-call(bf16[8,384,128]{2,1,0:T(8,128)(2,1)S(1)} %all-to-all-done.2.parts_ref, bf16[32,16,128]{2,1,0:T(8,128)(2,1)} %get-tuple-element.47.back_ref), custom_call_target="tpu_custom_call" | custom-call | tf_op jit(solution)/shard_map/pallas_call | solution.py:340
  112.1 4.7 %all-to-all-start.3 = ((bf16[32,16,128]{2,1,0:T(8,128)(2,1)}), bf16[32,16,128]{2,1,0:T(8,128)(2,1)S(1)}, u32[]{:S(2)}, u32[]{:S(2)}) async-start(bf16[32,16,128]{2,1,0:T(8,128)(2,1)} %shard_map.202), calls=%async_computation.3 | async-start | bytes 262144 | tf_op jit(solution)/shard_map/all_to_all | solution.py:387
  116.9 0.0 collective-permute-done.2.got_ref
  116.9 2.5 %shard_map.208 = (bf16[16,128,128]{2,1,0:T(8,128)(2,1)}, bf16[16,128,128]{2,1,0:T(8,128)(2,1)}, bf16[128,2048]{1,0:T(8,128)(2,1)}) custom-call(s32[1]{0:T(128)} %bitcast.6.core_ref, bf16[3,8,128,128]{3,2,1,0:T(8,128)(2,1)} %get-tuple-element.65.own_ref, bf16[3,8,128,128]{3,2,1,0:T(8,128)(2,1)S(1)} %collective-permute-done.2.got_ref), custom_call_target="tpu_custom_call" | custom-call | tf_op jit(solution)/shard_map/pallas_call | solution.py:340
  119.4 0.0 copy-start.1
  119.4 6.8 %all-to-all-done.3.got_ref = bf16[32,16,128]{2,1,0:T(8,128)(2,1)S(1)} async-done(((bf16[32,16,128]{2,1,0:T(8,128)(2,1)}), bf16[32,16,128]{2,1,0:T(8,128)(2,1)S(1)}, u32[]{:S(2)}, u32[]{:S(2)}) %all-to-all-start.3) | async-done | bytes 131104 | tf_op jit(solution)/shard_map/all_to_all | solution.py:387
  126.2 1.8 %shard_map.203 = bf16[8,128,128]{2,1,0:T(8,128)(2,1)} custom-call(bf16[32,16,128]{2,1,0:T(8,128)(2,1)S(1)} %all-to-all-done.3.got_ref, bf16[512,128]{1,0:T(8,128)(2,1)} %get-tuple-element.48.pick_ref, bf16[128,128]{1,0:T(8,128)(2,1)} %cot_ref.3), custom_call_target="tpu_custom_call" | custom-call | tf_op jit(solution)/shard_map/pallas_call | solution.py:340
  128.1 0.2 slice_reduce_fusion
  128.3 0.0 copy-done.2
  128.3 0.0 copy-done.5
  128.3 0.1 fusion.38
  128.4 0.9 shard_map.204
  129.3 0.2 fusion.35
  129.5 0.2 convolution_add_fusion.1
  129.7 0.1 copy.43
  129.8 3.4 %all-to-all-start.4 = ((bf16[8,128,128]{2,1,0:T(8,128)(2,1)}), bf16[8,128,128]{2,1,0:T(8,128)(2,1)S(1)}, u32[]{:S(2)}, u32[]{:S(2)}) async-start(bf16[8,128,128]{2,1,0:T(8,128)(2,1)} %shard_map.203), calls=%async_computation.4 | async-start | bytes 524288 | tf_op jit(solution)/shard_map/all_to_all | solution.py:387
  133.2 1.3 multiply_reduce_fusion
  134.5 0.0 copy-done.1
  134.5 0.2 multiply_reduce_fusion.1
  134.8 0.1 copy.44.inv_ref
  134.9 0.1 fusion.46
  135.0 0.1 pad_maximum_fusion.mix_ref
  135.1 7.3 %all-to-all-done.4 = bf16[8,128,128]{2,1,0:T(8,128)(2,1)S(1)} async-done(((bf16[8,128,128]{2,1,0:T(8,128)(2,1)}), bf16[8,128,128]{2,1,0:T(8,128)(2,1)S(1)}, u32[]{:S(2)}, u32[]{:S(2)}) %all-to-all-start.4) | async-done | bytes 262176 | tf_op jit(solution)/shard_map/all_to_all | solution.py:387
  142.4 5.4 %all-gather = bf16[16,128,128]{2,1,0:T(8,128)(2,1)S(1)} all-gather(bf16[8,128,128]{2,1,0:T(8,128)(2,1)S(1)} %all-to-all-done.4), channel_id=2, replica_groups=mesh['z'=8,'x'=4,'y'=8,'core'=2] {'core'}, dimensions={0}, use_global_device_ids=true | all-gather | bytes 786432 | tf_op jit(solution)/shard_map/all_gather | solution.py:460
  147.8 2.8 %shard_map.205 = (bf16[32,48,128]{2,1,0:T(8,128)(2,1)}, f32[128,64]{1,0:T(8,128)S(1)}) custom-call(s32[1]{0:T(128)} %bitcast.2.place_ref, bf16[2,8,128,128]{3,2,1,0:T(8,128)(2,1)S(1)} %bitcast.60, bf16[64,2048]{1,0:T(8,128)(2,1)} %bitcast.68, f32[128,64]{1,0:T(8,128)S(1)} %get-tuple-element.73.normed_ref, f32[128,1]{1,0:T(8,128)S(1)} %copy.44.inv_ref, ...), custom_call_target="tpu_custom_call" | custom-call | tf_op jit(solution)/shard_map/pallas_call | solution.py:340
  150.6 0.1 fusion.47
  150.7 0.1 fusion.33
  150.8 2.1 %fusion.7 = (f32[32,128]{1,0:T(8,128)S(1)}, f32[32,128]{1,0:T(8,128)S(1)}) fusion(f32[128,128]{1,0:T(8,128)S(1)} %fusion.47, f32[32,128]{1,0:T(8,128)S(1)} %get-tuple-element.78, f32[32,128]{1,0:T(8,128)S(1)} %convert.3, f32[32,128]{1,0:T(8,128)S(1)} %get-tuple-element.52.cum_ref, pred[128,128]{1,0:T(8,128)(4,1)S(1)} %iota_compare_fusion.1), kind=kLoop, calls=%fused_computation.10 | loop fusion | flops 6283264 | bytes 163840 | tf_op jit(solution)/shard_map/transpose(jvp())/reduce_sum | solution.py:350
  152.9 0.9 fusion.4
  153.9 3.9 %all-to-all-start.5 = ((bf16[32,48,128]{2,1,0:T(8,128)(2,1)}), bf16[32,48,128]{2,1,0:T(8,128)(2,1)S(1)}, u32[]{:S(2)}, u32[]{:S(2)}) async-start(bf16[32,48,128]{2,1,0:T(8,128)(2,1)} %get-tuple-element.57), calls=%async_computation.5 | async-start | bytes 786432 | tf_op jit(solution)/shard_map/all_to_all | solution.py:387
  157.8 0.9 fusion.39
  158.7 0.1 copy.45
  158.8 0.2 fusion.16.decay_mix_ref
  159.0 0.2 fusion.48.vals_mix_ref
  159.2 0.0 copy-start.3
  159.2 0.0 copy-start.4
  159.2 0.9 fusion.2
  160.1 11.6 %all-to-all-done.5.got_ref = bf16[32,48,128]{2,1,0:T(8,128)(2,1)S(1)} async-done(((bf16[32,48,128]{2,1,0:T(8,128)(2,1)}), bf16[32,48,128]{2,1,0:T(8,128)(2,1)S(1)}, u32[]{:S(2)}, u32[]{:S(2)}) %all-to-all-start.5) | async-done | bytes 393248 | tf_op jit(solution)/shard_map/all_to_all | solution.py:387
  171.7 0.0 copy-done.3
  171.7 0.0 copy-done.4
  171.7 1.1 shard_map.206
  (4 shorter events, 0.0 us)
Async XLA Ops:
  28.7 47.3 %all-to-all-start.1 = ((bf16[8,384,256]{2,1,0:T(8,128)(2,1)}), bf16[8,384,256]{2,1,0:T(8,128)(2,1)S(1)}, u32[]{:S(2)}, u32[]{:S(2)}) async-start(bf16[8,384,256]{2,1,0:T(8,128)(2,1)} %get-tuple-element.41), calls=%async_computation.1 | async-start | bytes 3145728 | tf_op jit(solution)/shard_map/all_to_all | solution.py:387
  38.0 6.7 %collective-permute-start = (bf16[3,8,128,128]{3,2,1,0:T(8,128)(2,1)}, bf16[3,8,128,128]{3,2,1,0:T(8,128)(2,1)S(1)}, u32[]{:S(2)}, u32[]{:S(2)}) collective-permute-start(bf16[3,8,128,128]{3,2,1,0:T(8,128)(2,1)} %get-tuple-element.43), channel_id=1, source_target_pairs={{0,1},{1,0},{2,3},{3,2},{4,5},{5,4},{6,7},{7,6},{8,9},{9,8},{10,11... | collective-permute-start | bytes 2359304 | tf_op jit(solution)/shard_map/ppermute | solution.py:425
  76.0 1.2 copy-start
  77.1 4.0 %collective-permute-start.1 = (bf16[2,384,384]{2,1,0:T(8,128)(2,1)S(1)}, bf16[2,384,384]{2,1,0:T(8,128)(2,1)S(1)}, u32[]{:S(2)}, u32[]{:S(2)}) collective-permute-start(bf16[2,384,384]{2,1,0:T(8,128)(2,1)S(1)} %get-tuple-element.45), channel_id=1, source_target_pairs={{0,1},{1,0},{2,3},{3,2},{4,5},{5,4},{6,7},{7,6},{8,9},{9,8},{10,11... | collective-permute-start | bytes 1769480 | tf_op jit(solution)/shard_map/ppermute | solution.py:433
  83.1 27.1 %all-to-all-start.2 = ((bf16[8,384,128]{2,1,0:T(8,128)(2,1)}), bf16[8,384,128]{2,1,0:T(8,128)(2,1)S(1)}, u32[]{:S(2)}, u32[]{:S(2)}) async-start(bf16[8,384,128]{2,1,0:T(8,128)(2,1)} %get-tuple-element.46), calls=%async_computation.2 | async-start | bytes 1572864 | tf_op jit(solution)/shard_map/all_to_all | solution.py:387
  90.5 26.4 %collective-permute-start.2 = (bf16[3,8,128,128]{3,2,1,0:T(8,128)(2,1)}, bf16[3,8,128,128]{3,2,1,0:T(8,128)(2,1)S(1)}, u32[]{:S(2)}, u32[]{:S(2)}) collective-permute-start(bf16[3,8,128,128]{3,2,1,0:T(8,128)(2,1)} %get-tuple-element.66), channel_id=1, source_target_pairs={{0,1},{1,0},{2,3},{3,2},{4,5},{5,4},{6,7},{7,6},{8,9},{9,8},{10,11... | collective-permute-start | bytes 2359304 | tf_op jit(solution)/shard_map/ppermute | solution.py:510
  110.2 18.1 %copy-start.2 = (bf16[32,128]{1,0:T(8,128)(2,1)S(1)}, bf16[32,128]{1,0:T(8,128)(2,1)}, u32[]{:S(2)}) copy-start(bf16[32,128]{1,0:T(8,128)(2,1)} %key_ref.3) | copy-start | bytes 24580
  110.2 18.1 %copy-start.5 = (bf16[32,128]{1,0:T(8,128)(2,1)S(1)}, bf16[32,128]{1,0:T(8,128)(2,1)}, u32[]{:S(2)}) copy-start(bf16[32,128]{1,0:T(8,128)(2,1)} %param.14) | copy-start | bytes 24580
  112.1 14.1 %all-to-all-start.3 = ((bf16[32,16,128]{2,1,0:T(8,128)(2,1)}), bf16[32,16,128]{2,1,0:T(8,128)(2,1)S(1)}, u32[]{:S(2)}, u32[]{:S(2)}) async-start(bf16[32,16,128]{2,1,0:T(8,128)(2,1)} %shard_map.202), calls=%async_computation.3 | async-start | bytes 262144 | tf_op jit(solution)/shard_map/all_to_all | solution.py:387
  119.4 15.2 %copy-start.1 = (bf16[64,128]{1,0:T(8,128)(2,1)S(1)}, bf16[64,128]{1,0:T(8,128)(2,1)}, u32[]{:S(2)}) copy-start(bf16[64,128]{1,0:T(8,128)(2,1)} %val_ref.3) | copy-start | bytes 49156
  129.8 12.6 %all-to-all-start.4 = ((bf16[8,128,128]{2,1,0:T(8,128)(2,1)}), bf16[8,128,128]{2,1,0:T(8,128)(2,1)S(1)}, u32[]{:S(2)}, u32[]{:S(2)}) async-start(bf16[8,128,128]{2,1,0:T(8,128)(2,1)} %shard_map.203), calls=%async_computation.4 | async-start | bytes 524288 | tf_op jit(solution)/shard_map/all_to_all | solution.py:387
  153.9 17.8 %all-to-all-start.5 = ((bf16[32,48,128]{2,1,0:T(8,128)(2,1)}), bf16[32,48,128]{2,1,0:T(8,128)(2,1)S(1)}, u32[]{:S(2)}, u32[]{:S(2)}) async-start(bf16[32,48,128]{2,1,0:T(8,128)(2,1)} %get-tuple-element.57), calls=%async_computation.5 | async-start | bytes 786432 | tf_op jit(solution)/shard_map/all_to_all | solution.py:387
  159.2 12.5 %copy-start.3 = (bf16[32,128]{1,0:T(8,128)(2,1)S(1)}, bf16[32,128]{1,0:T(8,128)(2,1)}, u32[]{:S(2)}) copy-start(bf16[32,128]{1,0:T(8,128)(2,1)} %pre_ref.3) | copy-start | bytes 24580
  159.2 12.5 %copy-start.4 = (f32[32]{0:T(128)S(1)}, f32[32]{0:T(128)}, u32[]{:S(2)}) copy-start(f32[32]{0:T(128)} %param.19) | copy-start | bytes 388

commit v7 on v6

--- a/solution.py
+++ b/solution.py
@@ -16,7 +16,9 @@
 RING = 8
 SLOTS = PEERS * PAD
 ROWS = PEERS * CAP
+LEAD = PEERS * 8
 WIDTH = 128
+HALF = WIDTH // 2
 MODEL = 2048
 
 F32 = jnp.float32
@@ -48,37 +50,53 @@
     return high, rest, (value - high - rest).astype(BF16).astype(F32)
 
 
-def compact_rows(shape, compact_dim):
+def slot_rows(shape, compact_dim):
     row = iota(shape, compact_dim)
-    peer = (row * 5462) >> 16
-    return peer * PAD + (row - peer * CAP) == iota(shape, 1 - compact_dim)
+    tail = row - LEAD
+    lead_at = (row >> 3) * PAD + (row & 7)
+    tail_at = (tail >> 2) * PAD + 8 + (tail & 3)
+    return jnp.where(row < LEAD, lead_at, tail_at) == iota(shape, 1 - compact_dim)
 
 
 def row_of_peer(place):
     return iota((PEERS, SLOTS), 1) == iota((PEERS, SLOTS), 0) * PAD + place
 
 
+def column_of(row_ref, k):
+    diagonal = iota((TOK, TOK), 0) == iota((TOK, TOK), 1)
+    return jnp.sum(jnp.where(diagonal, row_ref[k : k + 1, :], 0.0), axis=1, keepdims=True)
+
+
+def swap_halves(value):
+    return jnp.concatenate([value[:, HALF:], value[:, :HALF]], axis=1)
+
+
 def dispatch_kernel(
     ids_ref, share_ref, x_ref, cot_ref, key_ref, val_ref, pre_ref, extra_ref, speed_ref,
-    send_ref, pick_ref, cum_ref,
+    send_ref, token_ref, pick_ref, lead_ref, tail_ref, cum_ref,
 ):
     expert = iota((PEERS, TOK), 0)
     named = [ids_ref[k : k + 1, :] == expert for k in range(2)]
     row, col = iota((TOK, TOK), 0), iota((TOK, TOK), 1)
     rank = dot(ones_where(named[0] | named[1]), ones_where(row < col), 1, 0)
     place = iota((PEERS, PAD, TOK), 1).astype(F32)
-    cot = cot_ref[...].astype(F32)
-    picks, grads = [], None
+    lead = iota((PEERS, 8, TOK), 1)
+    tail = (8 + (lead & 3)).astype(F32)
+    lead = lead.astype(F32)
+    x, cot = x_ref[...].astype(F32), cot_ref[...].astype(F32)
+    token_ref[...] = jnp.concatenate([cot[:, HALF:], x[:, HALF:]], axis=1).astype(BF16)
+    picks, rows = [], None
     for k in range(2):
-        at = jnp.where(named[k], rank, -1.0)
-        pick = jnp.where(at[:, None, :] == place, 1.0, 0.0).reshape(SLOTS, TOK).astype(BF16)
-        share = jnp.sum(jnp.where(row == col, share_ref[k : k + 1, :], 0.0), axis=1, keepdims=True)
-        part = dot(pick, (share * cot).astype(BF16), 1, 0)
-        grads = part if grads is None else grads + part
+        at = jnp.where(named[k], rank, -1.0)[:, None, :]
+        pick = jnp.where(at == place, 1.0, 0.0).reshape(SLOTS, TOK).astype(BF16)
+        lead_ref[k] = jnp.where(at == lead, 1.0, 0.0).reshape(LEAD, TOK).astype(BF16)
+        tail_ref[k] = jnp.where(at == tail, 1.0, 0.0).reshape(LEAD, TOK).astype(BF16)
+        weighted = column_of(share_ref, k) * cot[:, :HALF]
+        both = jnp.concatenate([x[:, :HALF], weighted], axis=1).astype(BF16)
+        part = dot(pick, both, 1, 0)
+        rows = part if rows is None else rows + part
         picks.append(pick)
-    pick = picks[0] + picks[1]
-    pick_ref[...] = pick
-    rows = jnp.concatenate([dot(pick, x_ref[...], 1, 0), grads], axis=1)
+    pick_ref[...] = picks[0] + picks[1]
 
     pre = pre_ref[...].astype(F32)
     log_sig = jnp.minimum(pre, 0.0) - jnp.log1p(jnp.exp(-jnp.abs(pre)))
@@ -96,26 +114,40 @@
         ],
         axis=1,
     )
-    state = jnp.concatenate(split_two(sums), axis=1)
-    lane = iota((KEY_DIM, 2 * WIDTH), 1)
-    logs = jnp.zeros((KEY_DIM, 2 * WIDTH), F32)
+    high, low = split_two(sums)
+    lane = iota((KEY_DIM, WIDTH), 1)
+    logs = jnp.zeros((KEY_DIM, WIDTH), F32)
     for k, part in enumerate(split_three(total)):
         logs = jnp.where(lane == k, part, logs)
-    place = iota((PEERS, PAD, 2 * WIDTH), 1)
-    block = rows.reshape(PEERS, PAD, 2 * WIDTH)
-    block = jnp.where(place == CAP, state[:, None, :], block)
-    block = jnp.where(place == CAP + 1, logs[:, None, :], block)
+    place = iota((PEERS, PAD, WIDTH), 1)
+    block = rows.reshape(PEERS, PAD, WIDTH)
+    for k, part in enumerate((high, low, logs)):
+        block = jnp.where(place == CAP + k, part[:, None, :], block)
     send_ref[...] = block.astype(BF16)
 
 
-def arrival_kernel(got_ref, copies_ref, back_ref):
-    got = got_ref[...].reshape(SLOTS, 2 * WIDTH)
-    rows = dot(ones_where(compact_rows((ROWS, SLOTS), 0)), got, 1, 0).astype(BF16)
-    for k in range(RING):
-        copies_ref[k] = rows
-    both = dot(ones_where(row_of_peer(CAP)), got, 1, 0)
-    state = both[:, :WIDTH] + both[:, WIDTH:]
-    logs = dot(ones_where(row_of_peer(CAP + 1)), got, 1, 0)
+def spread_kernel(tokens_ref, share_ref, lead_ref, tail_ref, send_ref):
+    lane = iota((TOK, WIDTH), 1)
+    lead, first, second = 0.0, 0.0, 0.0
+    for k in range(2):
+        share = jnp.where(lane < HALF, column_of(share_ref, k), 1.0)
+        rows = [(share * tokens_ref[y].astype(F32)).astype(BF16) for y in range(RING)]
+        low = jnp.concatenate(rows[: RING // 2], axis=1)
+        high = jnp.concatenate(rows[RING // 2 :], axis=1)
+        lead = lead + dot(lead_ref[k], jnp.concatenate([low, high], axis=1), 1, 0)
+        first = first + dot(tail_ref[k], low, 1, 0)
+        second = second + dot(tail_ref[k], high, 1, 0)
+    width = RING * WIDTH
+    send_ref[:, :width] = lead.astype(BF16)
+    upper = (iota((LEAD, width // 2), 0) & 7) < 4
+    send_ref[:, width:] = jnp.where(upper, first, second).astype(BF16)
+
+
+def arrival_kernel(got_ref, rows_ref, back_ref):
+    got = got_ref[...].reshape(SLOTS, WIDTH)
+    rows_ref[...] = dot(ones_where(slot_rows((ROWS, SLOTS), 0)), got, 1, 0).astype(BF16)
+    state = dot(ones_where(row_of_peer(CAP) | row_of_peer(CAP + 1)), got, 1, 0)
+    logs = dot(ones_where(row_of_peer(CAP + 2)), got, 1, 0)
     log = jnp.sum(logs, axis=1, keepdims=True)
     a, b = iota((PEERS, PEERS), 0), iota((PEERS, PEERS), 1)
     gap_fwd = dot(ones_where(b < a, F32), jnp.where(a > b, log, 0.0), 1, 0, EXACT)
@@ -143,10 +175,26 @@
             at = 2 * k + side
             ref[0, k] = gate_ref[at]
             ref[1, k] = up_ref[at]
-            ref[2, k] = down_ref[:, pl.ds(pl.multiple_of(at * WIDTH, WIDTH), WIDTH)]
-
-
-def forward_kernel(rows_ref, own_ref, swapped_ref, out_ref, send_ref):
+            lanes = pl.ds(pl.multiple_of(at * WIDTH, WIDTH), WIDTH)
+            ref[2, k] = swap_halves(down_ref[:, lanes].astype(F32)).astype(BF16)
+
+
+def forward_kernel(near_ref, far_ref, own_ref, swapped_ref, out_ref, send_ref, rows_ref):
+    width = RING * WIDTH
+    tail = far_ref[:, width:]
+    row, source = iota((LEAD // 2, LEAD), 0), iota((LEAD // 2, LEAD), 1)
+    upper = source == (row >> 2) * 8 + (row & 3)
+    lower = source == (row >> 2) * 8 + 4 + (row & 3)
+    tail = [dot(ones_where(take), tail, 1, 0).astype(BF16) for take in (upper, lower)]
+    first = iota((ROWS, WIDTH), 1) < HALF
+    for k in range(RING):
+        at = slice(k * WIDTH, (k + 1) * WIDTH)
+        within = (k % (RING // 2)) * WIDTH
+        last = tail[k // (RING // 2)][:, within : within + WIDTH]
+        far = jnp.concatenate([far_ref[:, at], last], axis=0).astype(F32)
+        near = near_ref[k].astype(F32)
+        rows_ref[k, :, :WIDTH] = jnp.where(first, near, far).astype(BF16)
+        rows_ref[k, :, WIDTH:] = jnp.where(first, far, near).astype(BF16)
     pre = jnp.zeros((ROWS, 4 * WIDTH), F32)
     grad = jnp.zeros((ROWS, 2 * WIDTH), F32)
     for k in range(0, RING, 2):
@@ -194,7 +242,7 @@
     grads, hidden = grads_ref[...], hidden_ref[...]
     for k in range(RING):
         both = dot(rows_ref[k, :, :WIDTH], grads, 0, 0).astype(BF16)
-        down = dot(hidden, rows_ref[k, :, WIDTH:], 0, 0).astype(BF16)
+        down = swap_halves(dot(hidden, rows_ref[k, :, WIDTH:], 0, 0)).astype(BF16)
         for half, ref in enumerate((own_ref, send_ref)):
             at = 2 * half * WIDTH
             ref[0, k] = both[:, at : at + WIDTH]
@@ -216,7 +264,7 @@
     total = parts_ref[0].astype(F32)
     for k in range(1, RING):
         total = total + parts_ref[k].astype(F32)
-    rows = dot(ones_where(compact_rows((SLOTS, ROWS), 1)), total.astype(BF16), 1, 0)
+    rows = dot(ones_where(slot_rows((SLOTS, ROWS), 1)), total.astype(BF16), 1, 0)
     rows = rows.astype(BF16).reshape(PEERS, PAD, WIDTH)
     send_ref[...] = rows + back_ref[...]
 
@@ -389,11 +437,19 @@
     gate, up, down = expert_gate_weight[0], expert_up_weight[0], expert_down_weight[0]
     gate_blocks = gate.reshape(2 * RING, WIDTH, WIDTH)
     up_blocks = up.reshape(2 * RING, WIDTH, WIDTH)
-    send, pick, cum = call(
+    ids, share = off_chip(chosen_expert_index.T), off_chip(expert_combine_weight.T)
+    send, token, pick, lead, tail, cum = call(
         dispatch_kernel,
-        [((PEERS, PAD, 2 * WIDTH), BF16), ((SLOTS, TOK), BF16), ((KEY_DIM, TOK), F32)],
-        off_chip(chosen_expert_index.T),
-        off_chip(expert_combine_weight.T),
+        [
+            ((PEERS, PAD, WIDTH), BF16),
+            ((TOK, WIDTH), BF16),
+            ((SLOTS, TOK), BF16),
+            ((2, LEAD, TOK), BF16),
+            ((2, LEAD, TOK), BF16),
+            ((KEY_DIM, TOK), F32),
+        ],
+        ids,
+        share,
         off_chip(stored_expert_rows),
         off_chip(cotangent),
         off_chip(input_key_matrix),
@@ -401,16 +457,27 @@
         off_chip(decay_preactivation),
         off_chip(extra_log_decay),
         off_chip(speed),
+        stored=(0, 2),
+    )
+    got = exchanged(send, sp)
+    tokens = lax.all_gather(token, "y", axis=0, tiled=False)
+    (send,) = call(
+        spread_kernel,
+        [((LEAD, 12 * WIDTH), BF16)],
+        on_chip(tokens),
+        share,
+        on_chip(lead),
+        on_chip(tail),
+        stored=(0,),
+    )
+    far = exchanged(send.reshape(PEERS, 8, 12 * WIDTH), sp).reshape(LEAD, 12 * WIDTH)
+    rows, back = call(
+        arrival_kernel,
+        [((ROWS, WIDTH), BF16), ((PEERS, PAD, WIDTH), BF16)],
+        on_chip(got),
         stored=(1,),
     )
-    got = exchanged(send, sp)
-    copies, back = call(
-        arrival_kernel,
-        [((RING, ROWS, 2 * WIDTH), BF16), ((PEERS, PAD, WIDTH), BF16)],
-        on_chip(got),
-        stored=(0, 1),
-    )
-    rows = exchanged(copies, "y")
+    near = lax.all_gather(rows, "y", axis=0, tiled=False)
     kept, theirs = call(
         slice_kernel,
         [((3, RING, WIDTH, WIDTH), BF16)] * 2,
@@ -423,10 +490,15 @@
         stored=(1,),
     )
     swapped = lax.ppermute(theirs, "core", swap)
-    own, send = call(
+    own, send, rows = call(
         forward_kernel,
-        [((2, ROWS, 3 * WIDTH), F32), ((2, ROWS, 3 * WIDTH), BF16)],
-        rows,
+        [
+            ((2, ROWS, 3 * WIDTH), F32),
+            ((2, ROWS, 3 * WIDTH), BF16),
+            ((RING, ROWS, 2 * WIDTH), BF16),
+        ],
+        near,
+        far,
         on_chip(kept),
         swapped,
     )

time: 174 us -> 192 us (1.10)
  waiting for transfers between devices: 78.1 us -> 44.5 us
  starting transfers between devices: 31.8 us -> 63.7 us
  blocking collectives: 30.2 us -> 47.2 us
  Pallas kernels: 23.3 us -> 26.3 us
    all_gather x0 -> x2, blocking collectives: none -> 41.8 us  [the longest x1 21.2 us: body(): near = lax.all_gather(rows, 'y', axis=0, tiled=False)]
    all_to_all x5 -> x6, waiting for transfers between devices: 74.4 us -> 42.9 us  [exchanged(): return lax.all_to_all(array, axis, split_axis=0, concat_axis=0, tiled=True)]
    all_to_all x1 -> x0, blocking collectives: 24.8 us -> none  [exchanged(): return lax.all_to_all(array, axis, split_axis=0, concat_axis=0, tiled=True)]
    all_to_all x5 -> x6, starting transfers between devices: 22.4 us -> 45.1 us  [exchanged(): return lax.all_to_all(array, axis, split_axis=0, concat_axis=0, tiled=True)]
    ppermute x2, starting transfers between devices: 4.72 us -> 9.36 us  [body(): crossed = lax.ppermute(send, 'core', swap)]
    ppermute x1, starting transfers between devices: 4.63 us -> 9.19 us  [body(): swapped = lax.ppermute(theirs, 'core', swap)]
    pallas_call x12 -> x13, Pallas kernels: 23.3 us -> 26.3 us  [call(): pl.pallas_call(kernel, out_shape=shapes, in_specs=[SCALAR] * scalars + [W...]
    ppermute x1, waiting for transfers between devices: 2.1 us -> 0.01 us  [body(): swapped = lax.ppermute(theirs, 'core', swap)]
  transfers between devices with their start and end apart: 8 -> 9, of which waited for: 7 -> 5; matrix products, arithmetic and copies ran while one was open for 2% -> 2% of each run, Pallas kernels for 6% -> 8%
where the time goes in v7:
time: 192 us; the launch traced here: 191 us
  starting transfers between devices  63.7 us (33%)
  blocking collectives  47.2 us (25%)
  waiting for transfers between devices  44.5 us (23%)
  Pallas kernels  26.3 us (14%)
  matrix products  4.11 us (2%)
  other arithmetic  3.66 us (2%)
    all_to_all x6, starting transfers between devices, exchanged(): return lax.all_to_all(array, axis, split_axis=0, concat_axis=0, tiled=True)  45.1 us
    all_to_all x6, waiting for transfers between devices, exchanged(): return lax.all_to_all(array, axis, split_axis=0, concat_axis=0, tiled=True)  42.9 us
    pallas_call x13, Pallas kernels, call(): pl.pallas_call(kernel, out_shape=shapes, in_specs=[SCALAR] * scalars + [W...  26.3 us
    all_gather x1, blocking collectives, body(): near = lax.all_gather(rows, 'y', axis=0, tiled=False)  21.2 us
    all_gather x1, blocking collectives, body(): tokens = lax.all_gather(token, 'y', axis=0, tiled=False)  20.7 us
    ppermute x2, starting transfers between devices, body(): crossed = lax.ppermute(send, 'core', swap)  9.36 us
    ppermute x1, starting transfers between devices, body(): swapped = lax.ppermute(theirs, 'core', swap)  9.19 us
    all_gather x1, blocking collectives, body(): full_rows = lax.all_gather(full_rows, 'core', axis=0, tiled=False)  5.36 us
  transfers between devices with their start and end apart: 9, of which 5 were waited for; matrix products, arithmetic and copies ran while one was open for 2% of the time, Pallas kernels for 8%

profile of v7, /device:TPU:1, one launch (start us, length us, event | category | flops | bytes accessed | tf_op | source)
XLA Modules:
  0.0 190.8 jit_solution(11668554050300918022)
XLA Ops:
  0.6 2.2 %shard_map.197 = (bf16[32,16,128]{2,1,0:T(8,128)(2,1)}, bf16[128,128]{1,0:T(8,128)(2,1)S(1)}, bf16[512,128]{1,0:T(8,128)(2,1)}, bf16[2,256,128]{2,1,0:T(8,128)(2...) custom-call(s32[2,128]{1,0:T(2,128)} %bitcast.82, f32[2,128]{1,0:T(2,128)} %bitcast.79, ...), custom_call_target="tpu_custom_call" | custom-call | tf_op jit(solution)/shard_map/pallas_call | solution.py:388
  2.8 13.7 %all-to-all-start = ((bf16[32,16,128]{2,1,0:T(8,128)(2,1)}), bf16[32,16,128]{2,1,0:T(8,128)(2,1)S(1)}, u32[]{:S(2)}, u32[]{:S(2)}) async-start(bf16[32,16,128]{2,1,0:T(8,128)(2,1)} %get-tuple-element.44), calls=%async_computation | async-start | bytes 262144 | tf_op jit(solution)/shard_map/all_to_all | solution.py:435
  16.6 20.7 %all-gather.1 = bf16[1024,128]{1,0:T(8,128)(2,1)S(1)} all-gather(bf16[128,128]{1,0:T(8,128)(2,1)S(1)} %get-tuple-element.46), channel_id=3, replica_groups=mesh['z'=8,'x'=4,'y'=8,'core'=2] {'y'}, dimensions={0}, use_global_device_ids=true | all-gather | bytes 294912 | tf_op jit(solution)/shard_map/all_gather | solution.py:463
  37.2 2.4 %shard_map.199 = bf16[256,1536]{1,0:T(8,128)(2,1)} custom-call(bf16[8,128,128]{2,1,0:T(8,128)(2,1)S(1)} %bitcast.67, f32[2,128]{1,0:T(2,128)} %bitcast.80, bf16[2,256,128]{2,1,0:T(8,128)(2,1)S(1)} %get-tuple-element.47.lead_ref, bf16[2,256,128]{2,1,0:T(8,128)(2,1)S(1)} %get-tuple-element.48.tail_ref), custom_call_target="tpu_custom_call" | custom-call | tf_op jit(solution)/shard_map/pallas_call | solution.py:388
  39.6 0.0 all-to-all-done.got_ref
  39.6 9.1 %all-to-all-start.1 = ((bf16[32,8,1536]{2,1,0:T(8,128)(2,1)}), bf16[32,8,1536]{2,1,0:T(8,128)(2,1)S(1)}, u32[]{:S(2)}, u32[]{:S(2)}) async-start(bf16[32,8,1536]{2,1,0:T(8,128)(2,1)} %bitcast.72), calls=%async_computation.1 | async-start | bytes 1572864 | tf_op jit(solution)/shard_map/all_to_all | solution.py:435
  48.7 2.5 %shard_map.200 = (bf16[3,8,128,128]{3,2,1,0:T(8,128)(2,1)S(1)}, bf16[3,8,128,128]{3,2,1,0:T(8,128)(2,1)}) custom-call(s32[1]{0:T(128)} %bitcast.10.core_ref, s32[1]{0:T(128)} %bitcast.2.place_ref, bf16[16,128,128]{2,1,0:T(8,128)(2,1)} %bitcast.73, bf16[16,128,128]{2,1,0:T(8,128)(2,1)} %bitcast.74, bf16[128,2048]{1,0:T(8,128)(2,1)} %bitcast.75), custom_call_target="tpu_custom_call" | custom-call | tf_op jit(solution)/shard_map/pallas_call | solution.py:388
  51.3 9.2 %collective-permute-start = (bf16[3,8,128,128]{3,2,1,0:T(8,128)(2,1)}, bf16[3,8,128,128]{3,2,1,0:T(8,128)(2,1)S(1)}, u32[]{:S(2)}, u32[]{:S(2)}) collective-permute-start(bf16[3,8,128,128]{3,2,1,0:T(8,128)(2,1)} %get-tuple-element.50), channel_id=1, source_target_pairs={{0,1},{1,0},{2,3},{3,2},{4,5},{5,4},{6,7},{7,6},{8,9},{9,8},{10,11... | collective-permute-start | bytes 2359304 | tf_op jit(solution)/shard_map/ppermute | solution.py:492
  60.5 1.4 shard_map.198
  61.9 21.2 %all-gather = bf16[3072,128]{1,0:T(8,128)(2,1)S(1)} all-gather(bf16[384,128]{1,0:T(8,128)(2,1)S(1)} %get-tuple-element.45), channel_id=2, replica_groups=mesh['z'=8,'x'=4,'y'=8,'core'=2] {'y'}, dimensions={0}, use_global_device_ids=true | all-gather | bytes 884736 | tf_op jit(solution)/shard_map/all_gather | solution.py:480
  83.0 0.0 collective-permute-done.swapped_ref
  83.0 0.0 all-to-all-done.1
  83.0 1.0 shard_map.201
  84.0 0.0 copy-start
  84.0 6.9 %collective-permute-start.1 = (bf16[2,384,384]{2,1,0:T(8,128)(2,1)S(1)}, bf16[2,384,384]{2,1,0:T(8,128)(2,1)S(1)}, u32[]{:S(2)}, u32[]{:S(2)}) collective-permute-start(bf16[2,384,384]{2,1,0:T(8,128)(2,1)S(1)} %get-tuple-element.52), channel_id=1, source_target_pairs={{0,1},{1,0},{2,3},{3,2},{4,5},{5,4},{6,7},{7,6},{8,9},{9,8},{10,11... | collective-permute-start | bytes 1769480 | tf_op jit(solution)/shard_map/ppermute | solution.py:505
  90.9 1.6 collective-permute-done.1.got_ref
  92.5 2.0 %shard_map.202 = (bf16[8,384,128]{2,1,0:T(8,128)(2,1)}, bf16[384,512]{1,0:T(8,128)(2,1)}, bf16[384,256]{1,0:T(8,128)(2,1)}) custom-call(f32[2,384,384]{2,1,0:T(8,128)S(1)} %get-tuple-element.51.own_ref, bf16[2,384,384]{2,1,0:T(8,128)(2,1)S(1)} %collective-permute-done.1.got_ref, bf16[3,8,128,128]{3,2,1,0:T(8,128)(2,1)S(1)} %get-tuple-element.49.own_ref.kept_ref, ...), custom_call_target="tpu_custom_call" | custom-call | tf_op jit(solution)/shard_map/pallas_call | solution.py:388
  94.5 0.0 copy-done
  94.5 5.6 %all-to-all-start.2 = ((bf16[8,384,128]{2,1,0:T(8,128)(2,1)}), bf16[8,384,128]{2,1,0:T(8,128)(2,1)S(1)}, u32[]{:S(2)}, u32[]{:S(2)}) async-start(bf16[8,384,128]{2,1,0:T(8,128)(2,1)} %get-tuple-element.53), calls=%async_computation.2 | async-start | bytes 1572864 | tf_op jit(solution)/shard_map/all_to_all | solution.py:435
  100.1 3.9 %shard_map.208 = (bf16[3,8,128,128]{3,2,1,0:T(8,128)(2,1)}, bf16[3,8,128,128]{3,2,1,0:T(8,128)(2,1)}) custom-call(bf16[8,384,256]{2,1,0:T(8,128)(2,1)} %copy-done, bf16[384,512]{1,0:T(8,128)(2,1)} %get-tuple-element.71.grads_ref, bf16[384,256]{1,0:T(8,128)(2,1)} %get-tuple-element.72.hidden_ref), custom_call_target="tpu_custom_call" | custom-call | tf_op jit(solution)/shard_map/pallas_call | solution.py:388
  103.9 2.5 %collective-permute-start.2 = (bf16[3,8,128,128]{3,2,1,0:T(8,128)(2,1)}, bf16[3,8,128,128]{3,2,1,0:T(8,128)(2,1)S(1)}, u32[]{:S(2)}, u32[]{:S(2)}) collective-permute-start(bf16[3,8,128,128]{3,2,1,0:T(8,128)(2,1)} %get-tuple-element.74), channel_id=1, source_target_pairs={{0,1},{1,0},{2,3},{3,2},{4,5},{5,4},{6,7},{7,6},{8,9},{9,8},{10,11... | collective-permute-start | bytes 2359304 | tf_op jit(solution)/shard_map/ppermute | solution.py:582
  106.5 17.2 %all-to-all-done.2.parts_ref = bf16[8,384,128]{2,1,0:T(8,128)(2,1)S(1)} async-done(((bf16[8,384,128]{2,1,0:T(8,128)(2,1)}), bf16[8,384,128]{2,1,0:T(8,128)(2,1)S(1)}, u32[]{:S(2)}, u32[]{:S(2)}) %all-to-all-start.2) | async-done | bytes 786464 | tf_op jit(solution)/shard_map/all_to_all | solution.py:435
  123.6 0.0 copy-start.2
  123.6 0.0 copy-start.5
  123.6 1.9 %shard_map.203 = bf16[32,16,128]{2,1,0:T(8,128)(2,1)} custom-call(bf16[8,384,128]{2,1,0:T(8,128)(2,1)S(1)} %all-to-all-done.2.parts_ref, bf16[32,16,128]{2,1,0:T(8,128)(2,1)} %get-tuple-element.54.back_ref), custom_call_target="tpu_custom_call" | custom-call | tf_op jit(solution)/shard_map/pallas_call | solution.py:388
  125.5 9.4 %all-to-all-start.3 = ((bf16[32,16,128]{2,1,0:T(8,128)(2,1)}), bf16[32,16,128]{2,1,0:T(8,128)(2,1)S(1)}, u32[]{:S(2)}, u32[]{:S(2)}) async-start(bf16[32,16,128]{2,1,0:T(8,128)(2,1)} %shard_map.203), calls=%async_computation.3 | async-start | bytes 262144 | tf_op jit(solution)/shard_map/all_to_all | solution.py:435
  134.9 0.0 collective-permute-done.2.got_ref
  135.0 2.5 %shard_map.209 = (bf16[16,128,128]{2,1,0:T(8,128)(2,1)}, bf16[16,128,128]{2,1,0:T(8,128)(2,1)}, bf16[128,2048]{1,0:T(8,128)(2,1)}) custom-call(s32[1]{0:T(128)} %bitcast.10.core_ref, bf16[3,8,128,128]{3,2,1,0:T(8,128)(2,1)} %get-tuple-element.73.own_ref, bf16[3,8,128,128]{3,2,1,0:T(8,128)(2,1)S(1)} %collective-permute-done.2.got_ref), custom_call_target="tpu_custom_call" | custom-call | tf_op jit(solution)/shard_map/pallas_call | solution.py:388
  137.4 0.0 copy-start.1
  137.4 6.8 %all-to-all-done.3.got_ref = bf16[32,16,128]{2,1,0:T(8,128)(2,1)S(1)} async-done(((bf16[32,16,128]{2,1,0:T(8,128)(2,1)}), bf16[32,16,128]{2,1,0:T(8,128)(2,1)S(1)}, u32[]{:S(2)}, u32[]{:S(2)}) %all-to-all-start.3) | async-done | bytes 131104 | tf_op jit(solution)/shard_map/all_to_all | solution.py:435
  144.3 1.8 shard_map.204
  146.1 0.2 slice_reduce_fusion
  146.3 0.0 copy-done.2
  146.4 0.0 copy-done.5
  146.4 0.1 fusion.38
  146.5 0.9 shard_map.205
  147.3 0.2 fusion.35
  147.5 0.2 convolution_add_fusion.1
  147.8 0.1 copy.43
  147.9 3.4 %all-to-all-start.4 = ((bf16[8,128,128]{2,1,0:T(8,128)(2,1)}), bf16[8,128,128]{2,1,0:T(8,128)(2,1)S(1)}, u32[]{:S(2)}, u32[]{:S(2)}) async-start(bf16[8,128,128]{2,1,0:T(8,128)(2,1)} %shard_map.204), calls=%async_computation.4 | async-start | bytes 524288 | tf_op jit(solution)/shard_map/all_to_all | solution.py:435
  151.3 1.3 multiply_reduce_fusion
  152.6 0.0 copy-done.1
  152.6 0.2 multiply_reduce_fusion.1
  152.9 0.1 copy.44.inv_ref
  153.0 0.1 fusion.46
  153.1 0.1 pad_maximum_fusion.mix_ref
  153.2 7.3 %all-to-all-done.4 = bf16[8,128,128]{2,1,0:T(8,128)(2,1)S(1)} async-done(((bf16[8,128,128]{2,1,0:T(8,128)(2,1)}), bf16[8,128,128]{2,1,0:T(8,128)(2,1)S(1)}, u32[]{:S(2)}, u32[]{:S(2)}) %all-to-all-start.4) | async-done | bytes 262176 | tf_op jit(solution)/shard_map/all_to_all | solution.py:435
  160.5 5.4 %all-gather.2 = bf16[16,128,128]{2,1,0:T(8,128)(2,1)S(1)} all-gather(bf16[8,128,128]{2,1,0:T(8,128)(2,1)S(1)} %all-to-all-done.4), channel_id=4, replica_groups=mesh['z'=8,'x'=4,'y'=8,'core'=2] {'core'}, dimensions={0}, use_global_device_ids=true | all-gather | bytes 786432 | tf_op jit(solution)/shard_map/all_gather | solution.py:532
  165.8 2.8 %shard_map.206 = (bf16[32,48,128]{2,1,0:T(8,128)(2,1)}, f32[128,64]{1,0:T(8,128)S(1)}) custom-call(s32[1]{0:T(128)} %bitcast.2.place_ref, bf16[2,8,128,128]{3,2,1,0:T(8,128)(2,1)S(1)} %bitcast.66, bf16[64,2048]{1,0:T(8,128)(2,1)} %bitcast.76, f32[128,64]{1,0:T(8,128)S(1)} %get-tuple-element.81.normed_ref, f32[128,1]{1,0:T(8,128)S(1)} %copy.44.inv_ref, ...), custom_call_target="tpu_custom_call" | custom-call | tf_op jit(solution)/shard_map/pallas_call | solution.py:388
  168.6 0.1 fusion.47
  168.7 0.1 fusion.33
  168.9 2.1 %fusion.7 = (f32[32,128]{1,0:T(8,128)S(1)}, f32[32,128]{1,0:T(8,128)S(1)}) fusion(f32[128,128]{1,0:T(8,128)S(1)} %fusion.47, f32[32,128]{1,0:T(8,128)S(1)} %get-tuple-element.86, f32[32,128]{1,0:T(8,128)S(1)} %convert.3, f32[32,128]{1,0:T(8,128)S(1)} %get-tuple-element.59.cum_ref, pred[128,128]{1,0:T(8,128)(4,1)S(1)} %iota_compare_fusion.1), kind=kLoop, calls=%fused_computation.10 | loop fusion | flops 6283264 | bytes 163840 | tf_op jit(solution)/shard_map/transpose(jvp())/reduce_sum | solution.py:398
  171.0 0.9 fusion.4
  171.9 3.9 %all-to-all-start.5 = ((bf16[32,48,128]{2,1,0:T(8,128)(2,1)}), bf16[32,48,128]{2,1,0:T(8,128)(2,1)S(1)}, u32[]{:S(2)}, u32[]{:S(2)}) async-start(bf16[32,48,128]{2,1,0:T(8,128)(2,1)} %get-tuple-element.64), calls=%async_computation.5 | async-start | bytes 786432 | tf_op jit(solution)/shard_map/all_to_all | solution.py:435
  175.8 0.9 fusion.39
  176.7 0.1 copy.45
  176.8 0.2 fusion.16.decay_mix_ref
  177.1 0.2 fusion.48.vals_mix_ref
  177.2 0.0 copy-start.3
  177.2 0.9 fusion.2
  178.2 11.5 %all-to-all-done.5.got_ref = bf16[32,48,128]{2,1,0:T(8,128)(2,1)S(1)} async-done(((bf16[32,48,128]{2,1,0:T(8,128)(2,1)}), bf16[32,48,128]{2,1,0:T(8,128)(2,1)S(1)}, u32[]{:S(2)}, u32[]{:S(2)}) %all-to-all-start.5) | async-done | bytes 393248 | tf_op jit(solution)/shard_map/all_to_all | solution.py:435
  189.7 0.0 copy-done.3
  189.7 0.0 copy-done.4
  189.7 1.1 shard_map.207
  (5 shorter events, 0.0 us)
Async XLA Ops:
  2.8 36.8 %all-to-all-start = ((bf16[32,16,128]{2,1,0:T(8,128)(2,1)}), bf16[32,16,128]{2,1,0:T(8,128)(2,1)S(1)}, u32[]{:S(2)}, u32[]{:S(2)}) async-start(bf16[32,16,128]{2,1,0:T(8,128)(2,1)} %get-tuple-element.44), calls=%async_computation | async-start | bytes 262144 | tf_op jit(solution)/shard_map/all_to_all | solution.py:435
  39.6 43.5 %all-to-all-start.1 = ((bf16[32,8,1536]{2,1,0:T(8,128)(2,1)}), bf16[32,8,1536]{2,1,0:T(8,128)(2,1)S(1)}, u32[]{:S(2)}, u32[]{:S(2)}) async-start(bf16[32,8,1536]{2,1,0:T(8,128)(2,1)} %bitcast.72), calls=%async_computation.1 | async-start | bytes 1572864 | tf_op jit(solution)/shard_map/all_to_all | solution.py:435
  51.3 31.8 %collective-permute-start = (bf16[3,8,128,128]{3,2,1,0:T(8,128)(2,1)}, bf16[3,8,128,128]{3,2,1,0:T(8,128)(2,1)S(1)}, u32[]{:S(2)}, u32[]{:S(2)}) collective-permute-start(bf16[3,8,128,128]{3,2,1,0:T(8,128)(2,1)} %get-tuple-element.50), channel_id=1, source_target_pairs={{0,1},{1,0},{2,3},{3,2},{4,5},{5,4},{6,7},{7,6},{8,9},{9,8},{10,11... | collective-permute-start | bytes 2359304 | tf_op jit(solution)/shard_map/ppermute | solution.py:492
  84.0 10.5 %copy-start = (bf16[8,384,256]{2,1,0:T(8,128)(2,1)}, bf16[8,384,256]{2,1,0:T(8,128)(2,1)S(1)}, u32[]{:S(2)}) copy-start(bf16[8,384,256]{2,1,0:T(8,128)(2,1)S(1)} %get-tuple-element.70.rows_ref) | copy-start | bytes 4718596
  84.0 8.5 %collective-permute-start.1 = (bf16[2,384,384]{2,1,0:T(8,128)(2,1)S(1)}, bf16[2,384,384]{2,1,0:T(8,128)(2,1)S(1)}, u32[]{:S(2)}, u32[]{:S(2)}) collective-permute-start(bf16[2,384,384]{2,1,0:T(8,128)(2,1)S(1)} %get-tuple-element.52), channel_id=1, source_target_pairs={{0,1},{1,0},{2,3},{3,2},{4,5},{5,4},{6,7},{7,6},{8,9},{9,8},{10,11... | collective-permute-start | bytes 1769480 | tf_op jit(solution)/shard_map/ppermute | solution.py:505
  94.5 29.1 %all-to-all-start.2 = ((bf16[8,384,128]{2,1,0:T(8,128)(2,1)}), bf16[8,384,128]{2,1,0:T(8,128)(2,1)S(1)}, u32[]{:S(2)}, u32[]{:S(2)}) async-start(bf16[8,384,128]{2,1,0:T(8,128)(2,1)} %get-tuple-element.53), calls=%async_computation.2 | async-start | bytes 1572864 | tf_op jit(solution)/shard_map/all_to_all | solution.py:435
  103.9 31.0 %collective-permute-start.2 = (bf16[3,8,128,128]{3,2,1,0:T(8,128)(2,1)}, bf16[3,8,128,128]{3,2,1,0:T(8,128)(2,1)S(1)}, u32[]{:S(2)}, u32[]{:S(2)}) collective-permute-start(bf16[3,8,128,128]{3,2,1,0:T(8,128)(2,1)} %get-tuple-element.74), channel_id=1, source_target_pairs={{0,1},{1,0},{2,3},{3,2},{4,5},{5,4},{6,7},{7,6},{8,9},{9,8},{10,11... | collective-permute-start | bytes 2359304 | tf_op jit(solution)/shard_map/ppermute | solution.py:582
  123.6 22.7 %copy-start.2 = (bf16[32,128]{1,0:T(8,128)(2,1)S(1)}, bf16[32,128]{1,0:T(8,128)(2,1)}, u32[]{:S(2)}) copy-start(bf16[32,128]{1,0:T(8,128)(2,1)} %key_ref.3) | copy-start | bytes 24580
  123.6 22.7 %copy-start.5 = (bf16[32,128]{1,0:T(8,128)(2,1)S(1)}, bf16[32,128]{1,0:T(8,128)(2,1)}, u32[]{:S(2)}) copy-start(bf16[32,128]{1,0:T(8,128)(2,1)} %param.14) | copy-start | bytes 24580
  125.5 18.7 %all-to-all-start.3 = ((bf16[32,16,128]{2,1,0:T(8,128)(2,1)}), bf16[32,16,128]{2,1,0:T(8,128)(2,1)S(1)}, u32[]{:S(2)}, u32[]{:S(2)}) async-start(bf16[32,16,128]{2,1,0:T(8,128)(2,1)} %shard_map.203), calls=%async_computation.3 | async-start | bytes 262144 | tf_op jit(solution)/shard_map/all_to_all | solution.py:435
  137.4 15.2 %copy-start.1 = (bf16[64,128]{1,0:T(8,128)(2,1)S(1)}, bf16[64,128]{1,0:T(8,128)(2,1)}, u32[]{:S(2)}) copy-start(bf16[64,128]{1,0:T(8,128)(2,1)} %val_ref.3) | copy-start | bytes 49156
  147.9 12.6 %all-to-all-start.4 = ((bf16[8,128,128]{2,1,0:T(8,128)(2,1)}), bf16[8,128,128]{2,1,0:T(8,128)(2,1)S(1)}, u32[]{:S(2)}, u32[]{:S(2)}) async-start(bf16[8,128,128]{2,1,0:T(8,128)(2,1)} %shard_map.204), calls=%async_computation.4 | async-start | bytes 524288 | tf_op jit(solution)/shard_map/all_to_all | solution.py:435
  171.9 17.8 %all-to-all-start.5 = ((bf16[32,48,128]{2,1,0:T(8,128)(2,1)}), bf16[32,48,128]{2,1,0:T(8,128)(2,1)S(1)}, u32[]{:S(2)}, u32[]{:S(2)}) async-start(bf16[32,48,128]{2,1,0:T(8,128)(2,1)} %get-tuple-element.64), calls=%async_computation.5 | async-start | bytes 786432 | tf_op jit(solution)/shard_map/all_to_all | solution.py:435
  177.2 12.5 %copy-start.3 = (bf16[32,128]{1,0:T(8,128)(2,1)S(1)}, bf16[32,128]{1,0:T(8,128)(2,1)}, u32[]{:S(2)}) copy-start(bf16[32,128]{1,0:T(8,128)(2,1)} %pre_ref.3) | copy-start | bytes 24580
  177.2 12.5 %copy-start.4 = (f32[32]{0:T(128)S(1)}, f32[32]{0:T(128)}, u32[]{:S(2)}) copy-start(f32[32]{0:T(128)} %param.19) | copy-start | bytes 388

commit v8 on v6

--- a/solution.py
+++ b/solution.py
@@ -56,6 +56,15 @@
 
 def row_of_peer(place):
     return iota((PEERS, SLOTS), 1) == iota((PEERS, SLOTS), 0) * PAD + place
+
+
+def start_all(pairs, sems):
+    copies = [
+        pltpu.make_async_copy(source, target, sems.at[k]) for k, (source, target) in enumerate(pairs)
+    ]
+    for copy in copies:
+        copy.start()
+    return copies
 
 
 def dispatch_kernel(
@@ -108,11 +117,10 @@
     send_ref[...] = block.astype(BF16)
 
 
-def arrival_kernel(got_ref, copies_ref, back_ref):
+def arrival_kernel(got_ref, copies_ref, back_ref, rows_ref, sems):
     got = got_ref[...].reshape(SLOTS, 2 * WIDTH)
-    rows = dot(ones_where(compact_rows((ROWS, SLOTS), 0)), got, 1, 0).astype(BF16)
-    for k in range(RING):
-        copies_ref[k] = rows
+    rows_ref[...] = dot(ones_where(compact_rows((ROWS, SLOTS), 0)), got, 1, 0).astype(BF16)
+    copies = start_all([(rows_ref, copies_ref.at[k]) for k in range(RING)], sems)
     both = dot(ones_where(row_of_peer(CAP)), got, 1, 0)
     state = both[:, :WIDTH] + both[:, WIDTH:]
     logs = dot(ones_where(row_of_peer(CAP + 1)), got, 1, 0)
@@ -134,6 +142,8 @@
     block = jnp.where(place == CAP + 1, low[:, None, :], block)
     block = jnp.where(place == CAP + 2, all_logs[:, None, :], block)
     back_ref[...] = block.astype(BF16)
+    for copy in copies:
+        copy.wait()
 
 
 def slice_kernel(core_ref, place_ref, gate_ref, up_ref, down_ref, own_ref, out_ref):
@@ -168,7 +178,8 @@
 
 
 def partial_kernel(
-    own_ref, got_ref, kept_ref, swapped_ref, out_ref, grads_ref, hidden_ref
+    own_ref, got_ref, kept_ref, swapped_ref, out_ref, grads_out, hidden_out,
+    grads_ref, hidden_ref, sems,
 ):
     grads = []
     for half in range(2):
@@ -181,13 +192,16 @@
         slope = gate_sig * (1.0 + gate_pre * (1.0 - gate_sig))
         grads.append((grad_hidden * up_pre * slope).astype(BF16))
         grads.append((grad_hidden * gate_act).astype(BF16))
-    grads = jnp.concatenate(grads, axis=1)
-    grads_ref[...] = grads
+    grads_ref[...] = jnp.concatenate(grads, axis=1)
+    copies = start_all([(grads_ref, grads_out), (hidden_ref, hidden_out)], sems)
+    grads = grads_ref[...]
     for k in range(RING):
         weights = jnp.concatenate(
             [kept_ref[0, k], kept_ref[1, k], swapped_ref[0, k], swapped_ref[1, k]], axis=1
         )
         out_ref[k] = dot(grads, weights, 1, 1).astype(BF16)
+    for copy in copies:
+        copy.wait()
 
 
 def weight_kernel(rows_ref, grads_ref, hidden_ref, own_ref, send_ref):
@@ -221,11 +235,11 @@
     send_ref[...] = rows + back_ref[...]
 
 
-def token_kernel(got_ref, pick_ref, cot_ref, copies_ref):
+def token_kernel(got_ref, pick_ref, cot_ref, copies_ref, rows_ref, sems):
     got = got_ref[...].reshape(SLOTS, WIDTH)
-    rows = (cot_ref[...].astype(F32) + dot(pick_ref[...], got, 0, 0)).astype(BF16)
-    for k in range(RING):
-        copies_ref[k] = rows
+    rows_ref[...] = (cot_ref[...].astype(F32) + dot(pick_ref[...], got, 0, 0)).astype(BF16)
+    for copy in start_all([(rows_ref, copies_ref.at[k]) for k in range(RING)], sems):
+        copy.wait()
 
 
 def state_kernel(place_ref, got_ref, state_ref, reach_ref):
@@ -251,10 +265,19 @@
 
 def source_kernel(
     place_ref, rows_ref, weight_ref, normed_ref, inv_ref, mix_ref, query_fwd_ref, query_bwd_ref,
-    send_ref, grad_ref,
+    send_ref, grad_ref, proj_ref, state_ref, sems,
 ):
     here = place_ref[0]
     rows = jnp.concatenate([rows_ref[c, k] for k in range(RING) for c in range(2)], axis=1)
+    lane = iota((KEY_DIM, WIDTH), 1)
+    for k in range(2 * RING):
+        part = dot(rows[:, k * WIDTH : (k + 1) * WIDTH], mix_ref[...], 0, 0)
+        for side in range(2):
+            at = side * VAL_DIM
+            both = jnp.where(lane < VAL_DIM, part[at : at + 32], part[at + 32 : at + 64])
+            proj_ref[2 * k + side] = both.astype(BF16)
+    first_part = pltpu.make_async_copy(proj_ref, send_ref.at[:, :KEY_DIM], sems.at[0])
+    first_part.start()
     grad = dot(rows, weight_ref[...], 1, 1)
     normed = normed_ref[...]
     mean = jnp.mean(grad * normed, axis=1, keepdims=True)
@@ -267,14 +290,12 @@
     for ref in (query_fwd_ref, query_bwd_ref):
         state = dot(ref[...], twice, 1, 0, EXACT)
         states.append(jnp.where(first, state[:half], state[half:]))
-    lane = iota((KEY_DIM, WIDTH), 1)
-    for k in range(2 * RING):
-        part = dot(rows[:, k * WIDTH : (k + 1) * WIDTH], mix_ref[...], 0, 0)
-        for side in range(2):
-            at, peer = side * VAL_DIM, 2 * k + side
-            both = jnp.where(lane < VAL_DIM, part[at : at + 32], part[at + 32 : at + 64])
-            send_ref[peer, :KEY_DIM] = both.astype(BF16)
-            send_ref[peer, KEY_DIM:] = jnp.where(peer < here, states[0], states[1]).astype(BF16)
+    for peer in range(PEERS):
+        state_ref[peer] = jnp.where(peer < here, states[0], states[1]).astype(BF16)
+    second_part = pltpu.make_async_copy(state_ref, send_ref.at[:, KEY_DIM:], sems.at[1])
+    second_part.start()
+    first_part.wait()
+    second_part.wait()
 
 
 def final_kernel(
@@ -322,6 +343,7 @@
 
 SCALAR = pl.BlockSpec(memory_space=pltpu.SMEM)
 WHOLE = pl.BlockSpec(memory_space=pltpu.VMEM)
+OUTSIDE = pl.BlockSpec(memory_space=pltpu.HBM)
 
 
 def on_chip(array):
@@ -332,7 +354,7 @@
     return pltpu.with_memory_space_constraint(array, pltpu.HBM)
 
 
-def call(kernel, outs, *args, scalars=0, stored=()):
+def call(kernel, outs, *args, scalars=0, stored=(), manual=(), scratch=()):
     shapes = [
         (pltpu.HBM if k in stored else pltpu.VMEM)(shape, dtype)
         for k, (shape, dtype) in enumerate(outs)
@@ -341,7 +363,8 @@
         kernel,
         out_shape=shapes,
         in_specs=[SCALAR] * scalars + [WHOLE] * (len(args) - scalars),
-        out_specs=[WHOLE] * len(shapes),
+        out_specs=[OUTSIDE if k in manual else WHOLE for k in range(len(shapes))],
+        scratch_shapes=list(scratch),
         compiler_params=pltpu.CompilerParams(vmem_limit_bytes=24 << 20),
     )(*args)
 
@@ -409,6 +432,8 @@
         [((RING, ROWS, 2 * WIDTH), BF16), ((PEERS, PAD, WIDTH), BF16)],
         on_chip(got),
         stored=(0, 1),
+        manual=(0,),
+        scratch=(pltpu.VMEM((ROWS, 2 * WIDTH), BF16), pltpu.SemaphoreType.DMA((RING,))),
     )
     rows = exchanged(copies, "y")
     kept, theirs = call(
@@ -443,6 +468,12 @@
         on_chip(kept),
         swapped,
         stored=(1, 2),
+        manual=(1, 2),
+        scratch=(
+            pltpu.VMEM((ROWS, 4 * WIDTH), BF16),
+            pltpu.VMEM((ROWS, 2 * WIDTH), BF16),
+            pltpu.SemaphoreType.DMA((2,)),
+        ),
     )
     parts = exchanged(partials, "y")
     (send,) = call(
@@ -450,7 +481,14 @@
     )
     returned = on_chip(exchanged(send, sp))
     (copies,) = call(
-        token_kernel, [((RING, TOK, WIDTH), BF16)], returned, off_chip(pick), off_chip(cotangent)
+        token_kernel,
+        [((RING, TOK, WIDTH), BF16)],
+        returned,
+        off_chip(pick),
+        off_chip(cotangent),
+        stored=(0,),
+        manual=(0,),
+        scratch=(pltpu.VMEM((TOK, WIDTH), BF16), pltpu.SemaphoreType.DMA((RING,))),
     )
     row = iota((TOK, TOK), 0)
     cum, queries, key_in, val_in, row, copies = lax.optimization_barrier(
@@ -497,6 +535,13 @@
         query_fwd,
         query_bwd,
         scalars=1,
+        stored=(0,),
+        manual=(0,),
+        scratch=(
+            pltpu.VMEM((PEERS, KEY_DIM, WIDTH), BF16),
+            pltpu.VMEM((PEERS, KEY_DIM // 2, WIDTH), BF16),
+            pltpu.SemaphoreType.DMA((2,)),
+        ),
     )
     got = exchanged(send, sp)
     own, send = call(

time: 174 us -> 175 us (level)
  no operation moved by 1% of the time
where the time goes in v8:
time: 175 us; the launch traced here: 174 us
  waiting for transfers between devices  78.2 us (45%)
  starting transfers between devices  31.7 us (18%)
  blocking collectives  30.2 us (17%)
  Pallas kernels  24.6 us (14%)
  matrix products  4.11 us (2%)
  other arithmetic  3.66 us (2%)
    all_to_all x5, waiting for transfers between devices, exchanged(): return lax.all_to_all(array, axis, split_axis=0, concat_axis=0, tiled=True)  74.5 us
    all_to_all x1, blocking collectives, exchanged(): return lax.all_to_all(array, axis, split_axis=0, concat_axis=0, tiled=True)  24.8 us
    pallas_call x12, Pallas kernels, call(): pl.pallas_call(kernel, out_shape=shapes, in_specs=[SCALAR] * scalars + [W...  24.6 us
    all_to_all x5, starting transfers between devices, exchanged(): return lax.all_to_all(array, axis, split_axis=0, concat_axis=0, tiled=True)  22.4 us
    all_gather x1, blocking collectives, body(): full_rows = lax.all_gather(full_rows, 'core', axis=0, tiled=False)  5.36 us
    ppermute x1, starting transfers between devices, body(): swapped = lax.ppermute(theirs, 'core', swap)  4.63 us
    ppermute x2, starting transfers between devices, body(): crossed = lax.ppermute(send, 'core', swap)  4.62 us
  transfers between devices with their start and end apart: 8, of which 7 were waited for; matrix products, arithmetic and copies ran while one was open for 2% of the time, Pallas kernels for 6%

profile of v8, /device:TPU:1, one launch (start us, length us, event | category | flops | bytes accessed | tf_op | source)
XLA Modules:
  0.0 174.1 jit_solution(3552183376675610284)
XLA Ops:
  0.6 1.8 %shard_map.197 = (bf16[32,16,256]{2,1,0:T(8,128)(2,1)S(1)}, bf16[512,128]{1,0:T(8,128)(2,1)}, f32[32,128]{1,0:T(8,128)S(1)}) custom-call(s32[2,128]{1,0:T(2,128)} %bitcast.72, f32[2,128]{1,0:T(2,128)} %bitcast.73, bf16[128,128]{1,0:T(8,128)(2,1)} %x_ref.1, bf16[128,128]{1,0:T(8,128)(2,1)} %cot_ref.3, bf16[32,128]{1,0:T(8,128)(2,1)} %key_ref.3, ...), custom_call_target="tpu_custom_call" | custom-call | tf_op jit(solution)/shard_map/pallas_call | solution.py:362
  2.4 24.8 %all_to_all.30.got_ref = bf16[32,16,256]{2,1,0:T(8,128)(2,1)S(1)} all-to-all(bf16[32,16,256]{2,1,0:T(8,128)(2,1)S(1)} %get-tuple-element.40), channel_id=1, replica_groups=mesh['z'=8,'x'=4,'y'=8,'core'=2] {'z','x'}, dimensions={0} | all-to-all | bytes 524288 | tf_op jit(solution)/shard_map/all_to_all | solution.py:410
  27.2 2.3 %shard_map.198 = (bf16[8,384,256]{2,1,0:T(8,128)(2,1)}, bf16[32,16,128]{2,1,0:T(8,128)(2,1)}) custom-call(bf16[32,16,256]{2,1,0:T(8,128)(2,1)S(1)} %all_to_all.30.got_ref), custom_call_target="tpu_custom_call" | custom-call | tf_op jit(solution)/shard_map/pallas_call | solution.py:362
  29.5 6.8 %all-to-all-start.1 = ((bf16[8,384,256]{2,1,0:T(8,128)(2,1)}), bf16[8,384,256]{2,1,0:T(8,128)(2,1)S(1)}, u32[]{:S(2)}, u32[]{:S(2)}) async-start(bf16[8,384,256]{2,1,0:T(8,128)(2,1)} %get-tuple-element.41), calls=%async_computation.1 | async-start | bytes 3145728 | tf_op jit(solution)/shard_map/all_to_all | solution.py:410
  36.3 2.4 %shard_map.199 = (bf16[3,8,128,128]{3,2,1,0:T(8,128)(2,1)S(1)}, bf16[3,8,128,128]{3,2,1,0:T(8,128)(2,1)}) custom-call(s32[1]{0:T(128)} %bitcast.6.core_ref, s32[1]{0:T(128)} %bitcast.2.place_ref, bf16[16,128,128]{2,1,0:T(8,128)(2,1)} %bitcast.65, bf16[16,128,128]{2,1,0:T(8,128)(2,1)} %bitcast.66, bf16[128,2048]{1,0:T(8,128)(2,1)} %bitcast.67), custom_call_target="tpu_custom_call" | custom-call | tf_op jit(solution)/shard_map/pallas_call | solution.py:362
  38.7 4.6 %collective-permute-start = (bf16[3,8,128,128]{3,2,1,0:T(8,128)(2,1)}, bf16[3,8,128,128]{3,2,1,0:T(8,128)(2,1)S(1)}, u32[]{:S(2)}, u32[]{:S(2)}) collective-permute-start(bf16[3,8,128,128]{3,2,1,0:T(8,128)(2,1)} %get-tuple-element.43), channel_id=1, source_target_pairs={{0,1},{1,0},{2,3},{3,2},{4,5},{5,4},{6,7},{7,6},{8,9},{9,8},{10,11... | collective-permute-start | bytes 2359304 | tf_op jit(solution)/shard_map/ppermute | solution.py:450
  43.4 2.1 %collective-permute-done.swapped_ref = bf16[3,8,128,128]{3,2,1,0:T(8,128)(2,1)S(1)} collective-permute-done((bf16[3,8,128,128]{3,2,1,0:T(8,128)(2,1)}, bf16[3,8,128,128]{3,2,1,0:T(8,128)(2,1)S(1)}, u32[]{:S(2)}, u32[]{:S(2)}) %collective-permute-start) | collective-permute-done | bytes 786464 | tf_op jit(solution)/shard_map/ppermute | solution.py:450
  45.5 31.3 %all-to-all-done.1.rows_ref = bf16[8,384,256]{2,1,0:T(8,128)(2,1)S(1)} async-done(((bf16[8,384,256]{2,1,0:T(8,128)(2,1)}), bf16[8,384,256]{2,1,0:T(8,128)(2,1)S(1)}, u32[]{:S(2)}, u32[]{:S(2)}) %all-to-all-start.1) | async-done | bytes 1572896 | tf_op jit(solution)/shard_map/all_to_all | solution.py:410
  76.7 0.0 copy-start
  76.7 0.8 shard_map.200
  77.5 0.4 copy-done
  77.9 2.4 %collective-permute-start.1 = (bf16[2,384,384]{2,1,0:T(8,128)(2,1)S(1)}, bf16[2,384,384]{2,1,0:T(8,128)(2,1)S(1)}, u32[]{:S(2)}, u32[]{:S(2)}) collective-permute-start(bf16[2,384,384]{2,1,0:T(8,128)(2,1)S(1)} %get-tuple-element.45), channel_id=1, source_target_pairs={{0,1},{1,0},{2,3},{3,2},{4,5},{5,4},{6,7},{7,6},{8,9},{9,8},{10,11... | collective-permute-start | bytes 1769480 | tf_op jit(solution)/shard_map/ppermute | solution.py:458
  80.3 1.6 collective-permute-done.1.got_ref
  81.9 2.5 %shard_map.201 = (bf16[8,384,128]{2,1,0:T(8,128)(2,1)}, bf16[384,512]{1,0:T(8,128)(2,1)}, bf16[384,256]{1,0:T(8,128)(2,1)}) custom-call(f32[2,384,384]{2,1,0:T(8,128)S(1)} %get-tuple-element.44.own_ref, bf16[2,384,384]{2,1,0:T(8,128)(2,1)S(1)} %collective-permute-done.1.got_ref, bf16[3,8,128,128]{3,2,1,0:T(8,128)(2,1)S(1)} %get-tuple-element.42.own_ref.kept_ref, ...), custom_call_target="tpu_custom_call" | custom-call | tf_op jit(solution)/shard_map/pallas_call | solution.py:362
  84.4 3.6 %all-to-all-start.2 = ((bf16[8,384,128]{2,1,0:T(8,128)(2,1)}), bf16[8,384,128]{2,1,0:T(8,128)(2,1)S(1)}, u32[]{:S(2)}, u32[]{:S(2)}) async-start(bf16[8,384,128]{2,1,0:T(8,128)(2,1)} %get-tuple-element.46), calls=%async_computation.2 | async-start | bytes 1572864 | tf_op jit(solution)/shard_map/all_to_all | solution.py:410
  88.0 3.8 %shard_map.207 = (bf16[3,8,128,128]{3,2,1,0:T(8,128)(2,1)}, bf16[3,8,128,128]{3,2,1,0:T(8,128)(2,1)}) custom-call(bf16[8,384,256]{2,1,0:T(8,128)(2,1)} %copy-done, bf16[384,512]{1,0:T(8,128)(2,1)} %get-tuple-element.63.grads_ref, bf16[384,256]{1,0:T(8,128)(2,1)} %get-tuple-element.64.hidden_ref), custom_call_target="tpu_custom_call" | custom-call | tf_op jit(solution)/shard_map/pallas_call | solution.py:362
  91.8 2.2 %collective-permute-start.2 = (bf16[3,8,128,128]{3,2,1,0:T(8,128)(2,1)}, bf16[3,8,128,128]{3,2,1,0:T(8,128)(2,1)S(1)}, u32[]{:S(2)}, u32[]{:S(2)}) collective-permute-start(bf16[3,8,128,128]{3,2,1,0:T(8,128)(2,1)} %get-tuple-element.66), channel_id=1, source_target_pairs={{0,1},{1,0},{2,3},{3,2},{4,5},{5,4},{6,7},{7,6},{8,9},{9,8},{10,11... | collective-permute-start | bytes 2359304 | tf_op jit(solution)/shard_map/ppermute | solution.py:555
  94.1 17.5 %all-to-all-done.2.parts_ref = bf16[8,384,128]{2,1,0:T(8,128)(2,1)S(1)} async-done(((bf16[8,384,128]{2,1,0:T(8,128)(2,1)}), bf16[8,384,128]{2,1,0:T(8,128)(2,1)S(1)}, u32[]{:S(2)}, u32[]{:S(2)}) %all-to-all-start.2) | async-done | bytes 786464 | tf_op jit(solution)/shard_map/all_to_all | solution.py:410
  111.5 0.0 copy-start.2
  111.5 0.0 copy-start.5
  111.5 1.9 %shard_map.202 = bf16[32,16,128]{2,1,0:T(8,128)(2,1)} custom-call(bf16[8,384,128]{2,1,0:T(8,128)(2,1)S(1)} %all-to-all-done.2.parts_ref, bf16[32,16,128]{2,1,0:T(8,128)(2,1)} %get-tuple-element.47.back_ref), custom_call_target="tpu_custom_call" | custom-call | tf_op jit(solution)/shard_map/pallas_call | solution.py:362
  113.5 4.7 %all-to-all-start.3 = ((bf16[32,16,128]{2,1,0:T(8,128)(2,1)}), bf16[32,16,128]{2,1,0:T(8,128)(2,1)S(1)}, u32[]{:S(2)}, u32[]{:S(2)}) async-start(bf16[32,16,128]{2,1,0:T(8,128)(2,1)} %shard_map.202), calls=%async_computation.3 | async-start | bytes 262144 | tf_op jit(solution)/shard_map/all_to_all | solution.py:410
  118.2 0.0 collective-permute-done.2.got_ref
  118.2 2.5 %shard_map.208 = (bf16[16,128,128]{2,1,0:T(8,128)(2,1)}, bf16[16,128,128]{2,1,0:T(8,128)(2,1)}, bf16[128,2048]{1,0:T(8,128)(2,1)}) custom-call(s32[1]{0:T(128)} %bitcast.6.core_ref, bf16[3,8,128,128]{3,2,1,0:T(8,128)(2,1)} %get-tuple-element.65.own_ref, bf16[3,8,128,128]{3,2,1,0:T(8,128)(2,1)S(1)} %collective-permute-done.2.got_ref), custom_call_target="tpu_custom_call" | custom-call | tf_op jit(solution)/shard_map/pallas_call | solution.py:362
  120.7 0.0 copy-start.1
  120.7 6.8 %all-to-all-done.3.got_ref = bf16[32,16,128]{2,1,0:T(8,128)(2,1)S(1)} async-done(((bf16[32,16,128]{2,1,0:T(8,128)(2,1)}), bf16[32,16,128]{2,1,0:T(8,128)(2,1)S(1)}, u32[]{:S(2)}, u32[]{:S(2)}) %all-to-all-start.3) | async-done | bytes 131104 | tf_op jit(solution)/shard_map/all_to_all | solution.py:410
  127.6 1.9 %shard_map.203 = bf16[8,128,128]{2,1,0:T(8,128)(2,1)} custom-call(bf16[32,16,128]{2,1,0:T(8,128)(2,1)S(1)} %all-to-all-done.3.got_ref, bf16[512,128]{1,0:T(8,128)(2,1)} %get-tuple-element.48.pick_ref, bf16[128,128]{1,0:T(8,128)(2,1)} %cot_ref.3), custom_call_target="tpu_custom_call" | custom-call | tf_op jit(solution)/shard_map/pallas_call | solution.py:362
  129.5 0.2 slice_reduce_fusion
  129.7 0.0 copy-done.2
  129.7 0.0 copy-done.5
  129.7 0.1 fusion.38
  129.8 0.9 shard_map.204
  130.7 0.2 fusion.35
  130.9 0.2 convolution_add_fusion.1
  131.1 0.1 copy.43
  131.2 3.4 %all-to-all-start.4 = ((bf16[8,128,128]{2,1,0:T(8,128)(2,1)}), bf16[8,128,128]{2,1,0:T(8,128)(2,1)S(1)}, u32[]{:S(2)}, u32[]{:S(2)}) async-start(bf16[8,128,128]{2,1,0:T(8,128)(2,1)} %shard_map.203), calls=%async_computation.4 | async-start | bytes 524288 | tf_op jit(solution)/shard_map/all_to_all | solution.py:410
  134.7 1.3 multiply_reduce_fusion
  135.9 0.0 copy-done.1
  136.0 0.2 multiply_reduce_fusion.1
  136.2 0.1 copy.44.inv_ref
  136.3 0.1 fusion.46
  136.4 0.1 pad_maximum_fusion.mix_ref
  136.5 7.3 %all-to-all-done.4 = bf16[8,128,128]{2,1,0:T(8,128)(2,1)S(1)} async-done(((bf16[8,128,128]{2,1,0:T(8,128)(2,1)}), bf16[8,128,128]{2,1,0:T(8,128)(2,1)S(1)}, u32[]{:S(2)}, u32[]{:S(2)}) %all-to-all-start.4) | async-done | bytes 262176 | tf_op jit(solution)/shard_map/all_to_all | solution.py:410
  143.8 5.4 %all-gather = bf16[16,128,128]{2,1,0:T(8,128)(2,1)S(1)} all-gather(bf16[8,128,128]{2,1,0:T(8,128)(2,1)S(1)} %all-to-all-done.4), channel_id=2, replica_groups=mesh['z'=8,'x'=4,'y'=8,'core'=2] {'core'}, dimensions={0}, use_global_device_ids=true | all-gather | bytes 786432 | tf_op jit(solution)/shard_map/all_gather | solution.py:498
  149.2 2.7 %shard_map.205 = (bf16[32,48,128]{2,1,0:T(8,128)(2,1)}, f32[128,64]{1,0:T(8,128)S(1)}) custom-call(s32[1]{0:T(128)} %bitcast.2.place_ref, bf16[2,8,128,128]{3,2,1,0:T(8,128)(2,1)S(1)} %bitcast.60, bf16[64,2048]{1,0:T(8,128)(2,1)} %bitcast.68, f32[128,64]{1,0:T(8,128)S(1)} %get-tuple-element.73.normed_ref, f32[128,1]{1,0:T(8,128)S(1)} %copy.44.inv_ref, ...), custom_call_target="tpu_custom_call" | custom-call | tf_op jit(solution)/shard_map/pallas_call | solution.py:362
  151.9 0.1 fusion.47
  152.0 0.1 fusion.33
  152.1 2.1 %fusion.7 = (f32[32,128]{1,0:T(8,128)S(1)}, f32[32,128]{1,0:T(8,128)S(1)}) fusion(f32[128,128]{1,0:T(8,128)S(1)} %fusion.47, f32[32,128]{1,0:T(8,128)S(1)} %get-tuple-element.78, f32[32,128]{1,0:T(8,128)S(1)} %convert.3, f32[32,128]{1,0:T(8,128)S(1)} %get-tuple-element.52.cum_ref, pred[128,128]{1,0:T(8,128)(4,1)S(1)} %iota_compare_fusion.1), kind=kLoop, calls=%fused_computation.10 | loop fusion | flops 6283264 | bytes 163840 | tf_op jit(solution)/shard_map/transpose(jvp())/reduce_sum | solution.py:373
  154.2 0.9 fusion.4
  155.2 3.9 %all-to-all-start.5 = ((bf16[32,48,128]{2,1,0:T(8,128)(2,1)}), bf16[32,48,128]{2,1,0:T(8,128)(2,1)S(1)}, u32[]{:S(2)}, u32[]{:S(2)}) async-start(bf16[32,48,128]{2,1,0:T(8,128)(2,1)} %get-tuple-element.57), calls=%async_computation.5 | async-start | bytes 786432 | tf_op jit(solution)/shard_map/all_to_all | solution.py:410
  159.1 0.9 fusion.39
  160.0 0.1 copy.45
  160.1 0.2 fusion.16.decay_mix_ref
  160.3 0.2 fusion.48.vals_mix_ref
  160.5 0.0 copy-start.3
  160.5 0.0 copy-start.4
  160.5 0.9 fusion.2
  161.4 11.6 %all-to-all-done.5.got_ref = bf16[32,48,128]{2,1,0:T(8,128)(2,1)S(1)} async-done(((bf16[32,48,128]{2,1,0:T(8,128)(2,1)}), bf16[32,48,128]{2,1,0:T(8,128)(2,1)S(1)}, u32[]{:S(2)}, u32[]{:S(2)}) %all-to-all-start.5) | async-done | bytes 393248 | tf_op jit(solution)/shard_map/all_to_all | solution.py:410
  173.0 0.0 copy-done.3
  173.0 0.0 copy-done.4
  173.0 1.1 shard_map.206
  (4 shorter events, 0.0 us)
Async XLA Ops:
  29.5 47.3 %all-to-all-start.1 = ((bf16[8,384,256]{2,1,0:T(8,128)(2,1)}), bf16[8,384,256]{2,1,0:T(8,128)(2,1)S(1)}, u32[]{:S(2)}, u32[]{:S(2)}) async-start(bf16[8,384,256]{2,1,0:T(8,128)(2,1)} %get-tuple-element.41), calls=%async_computation.1 | async-start | bytes 3145728 | tf_op jit(solution)/shard_map/all_to_all | solution.py:410
  38.7 6.7 %collective-permute-start = (bf16[3,8,128,128]{3,2,1,0:T(8,128)(2,1)}, bf16[3,8,128,128]{3,2,1,0:T(8,128)(2,1)S(1)}, u32[]{:S(2)}, u32[]{:S(2)}) collective-permute-start(bf16[3,8,128,128]{3,2,1,0:T(8,128)(2,1)} %get-tuple-element.43), channel_id=1, source_target_pairs={{0,1},{1,0},{2,3},{3,2},{4,5},{5,4},{6,7},{7,6},{8,9},{9,8},{10,11... | collective-permute-start | bytes 2359304 | tf_op jit(solution)/shard_map/ppermute | solution.py:450
  76.7 1.2 copy-start
  77.9 4.0 %collective-permute-start.1 = (bf16[2,384,384]{2,1,0:T(8,128)(2,1)S(1)}, bf16[2,384,384]{2,1,0:T(8,128)(2,1)S(1)}, u32[]{:S(2)}, u32[]{:S(2)}) collective-permute-start(bf16[2,384,384]{2,1,0:T(8,128)(2,1)S(1)} %get-tuple-element.45), channel_id=1, source_target_pairs={{0,1},{1,0},{2,3},{3,2},{4,5},{5,4},{6,7},{7,6},{8,9},{9,8},{10,11... | collective-permute-start | bytes 1769480 | tf_op jit(solution)/shard_map/ppermute | solution.py:458
  84.4 27.1 %all-to-all-start.2 = ((bf16[8,384,128]{2,1,0:T(8,128)(2,1)}), bf16[8,384,128]{2,1,0:T(8,128)(2,1)S(1)}, u32[]{:S(2)}, u32[]{:S(2)}) async-start(bf16[8,384,128]{2,1,0:T(8,128)(2,1)} %get-tuple-element.46), calls=%async_computation.2 | async-start | bytes 1572864 | tf_op jit(solution)/shard_map/all_to_all | solution.py:410
  91.8 26.4 %collective-permute-start.2 = (bf16[3,8,128,128]{3,2,1,0:T(8,128)(2,1)}, bf16[3,8,128,128]{3,2,1,0:T(8,128)(2,1)S(1)}, u32[]{:S(2)}, u32[]{:S(2)}) collective-permute-start(bf16[3,8,128,128]{3,2,1,0:T(8,128)(2,1)} %get-tuple-element.66), channel_id=1, source_target_pairs={{0,1},{1,0},{2,3},{3,2},{4,5},{5,4},{6,7},{7,6},{8,9},{9,8},{10,11... | collective-permute-start | bytes 2359304 | tf_op jit(solution)/shard_map/ppermute | solution.py:555
  111.5 18.1 %copy-start.2 = (bf16[32,128]{1,0:T(8,128)(2,1)S(1)}, bf16[32,128]{1,0:T(8,128)(2,1)}, u32[]{:S(2)}) copy-start(bf16[32,128]{1,0:T(8,128)(2,1)} %key_ref.3) | copy-start | bytes 24580
  111.5 18.2 %copy-start.5 = (bf16[32,128]{1,0:T(8,128)(2,1)S(1)}, bf16[32,128]{1,0:T(8,128)(2,1)}, u32[]{:S(2)}) copy-start(bf16[32,128]{1,0:T(8,128)(2,1)} %param.14) | copy-start | bytes 24580
  113.5 14.1 %all-to-all-start.3 = ((bf16[32,16,128]{2,1,0:T(8,128)(2,1)}), bf16[32,16,128]{2,1,0:T(8,128)(2,1)S(1)}, u32[]{:S(2)}, u32[]{:S(2)}) async-start(bf16[32,16,128]{2,1,0:T(8,128)(2,1)} %shard_map.202), calls=%async_computation.3 | async-start | bytes 262144 | tf_op jit(solution)/shard_map/all_to_all | solution.py:410
  120.7 15.2 %copy-start.1 = (bf16[64,128]{1,0:T(8,128)(2,1)S(1)}, bf16[64,128]{1,0:T(8,128)(2,1)}, u32[]{:S(2)}) copy-start(bf16[64,128]{1,0:T(8,128)(2,1)} %val_ref.3) | copy-start | bytes 49156
  131.2 12.6 %all-to-all-start.4 = ((bf16[8,128,128]{2,1,0:T(8,128)(2,1)}), bf16[8,128,128]{2,1,0:T(8,128)(2,1)S(1)}, u32[]{:S(2)}, u32[]{:S(2)}) async-start(bf16[8,128,128]{2,1,0:T(8,128)(2,1)} %shard_map.203), calls=%async_computation.4 | async-start | bytes 524288 | tf_op jit(solution)/shard_map/all_to_all | solution.py:410
  155.2 17.8 %all-to-all-start.5 = ((bf16[32,48,128]{2,1,0:T(8,128)(2,1)}), bf16[32,48,128]{2,1,0:T(8,128)(2,1)S(1)}, u32[]{:S(2)}, u32[]{:S(2)}) async-start(bf16[32,48,128]{2,1,0:T(8,128)(2,1)} %get-tuple-element.57), calls=%async_computation.5 | async-start | bytes 786432 | tf_op jit(solution)/shard_map/all_to_all | solution.py:410
  160.5 12.5 %copy-start.3 = (bf16[32,128]{1,0:T(8,128)(2,1)S(1)}, bf16[32,128]{1,0:T(8,128)(2,1)}, u32[]{:S(2)}) copy-start(bf16[32,128]{1,0:T(8,128)(2,1)} %pre_ref.3) | copy-start | bytes 24580
  160.5 12.5 %copy-start.4 = (f32[32]{0:T(128)S(1)}, f32[32]{0:T(128)}, u32[]{:S(2)}) copy-start(f32[32]{0:T(128)} %param.19) | copy-start | bytes 388

commit v9 on v8

--- a/solution.py
+++ b/solution.py
@@ -56,15 +56,6 @@
 
 def row_of_peer(place):
     return iota((PEERS, SLOTS), 1) == iota((PEERS, SLOTS), 0) * PAD + place
-
-
-def start_all(pairs, sems):
-    copies = [
-        pltpu.make_async_copy(source, target, sems.at[k]) for k, (source, target) in enumerate(pairs)
-    ]
-    for copy in copies:
-        copy.start()
-    return copies
 
 
 def dispatch_kernel(
@@ -117,10 +108,9 @@
     send_ref[...] = block.astype(BF16)
 
 
-def arrival_kernel(got_ref, copies_ref, back_ref, rows_ref, sems):
+def arrival_kernel(got_ref, rows_ref, back_ref):
     got = got_ref[...].reshape(SLOTS, 2 * WIDTH)
     rows_ref[...] = dot(ones_where(compact_rows((ROWS, SLOTS), 0)), got, 1, 0).astype(BF16)
-    copies = start_all([(rows_ref, copies_ref.at[k]) for k in range(RING)], sems)
     both = dot(ones_where(row_of_peer(CAP)), got, 1, 0)
     state = both[:, :WIDTH] + both[:, WIDTH:]
     logs = dot(ones_where(row_of_peer(CAP + 1)), got, 1, 0)
@@ -142,11 +132,12 @@
     block = jnp.where(place == CAP + 1, low[:, None, :], block)
     block = jnp.where(place == CAP + 2, all_logs[:, None, :], block)
     back_ref[...] = block.astype(BF16)
-    for copy in copies:
-        copy.wait()
-
-
-def slice_kernel(core_ref, place_ref, gate_ref, up_ref, down_ref, own_ref, out_ref):
+
+
+def slice_kernel(
+    core_ref, place_ref, ring_ref, gate_ref, up_ref, down_ref, proj_ref, own_ref, out_ref, near_ref
+):
+    near_ref[...] = proj_ref[...]
     core = core_ref[0]
     for side, ref in ((core, own_ref), (1 - core, out_ref)):
         for k in range(RING):
@@ -156,17 +147,23 @@
             ref[2, k] = down_ref[:, pl.ds(pl.multiple_of(at * WIDTH, WIDTH), WIDTH)]
 
 
-def forward_kernel(rows_ref, own_ref, swapped_ref, out_ref, send_ref):
+def sender(here, distance):
+    return lax.rem(here + RING - distance, RING)
+
+
+def forward_kernel(here_ref, *refs):
+    rows, (own_ref, swapped_ref, out_ref, send_ref) = refs[:RING], refs[RING:]
+    here = here_ref[0]
     pre = jnp.zeros((ROWS, 4 * WIDTH), F32)
     grad = jnp.zeros((ROWS, 2 * WIDTH), F32)
     for k in range(0, RING, 2):
         weights, downs = [], []
-        for j in (k, k + 1):
+        for j in (sender(here, k), sender(here, k + 1)):
             parts = [own_ref[0, j], own_ref[1, j], swapped_ref[0, j], swapped_ref[1, j]]
             weights.append(jnp.concatenate(parts, axis=1))
             downs.append(jnp.concatenate([own_ref[2, j], swapped_ref[2, j]], axis=0))
-        x = jnp.concatenate([rows_ref[k, :, :WIDTH], rows_ref[k + 1, :, :WIDTH]], axis=1)
-        y = jnp.concatenate([rows_ref[k, :, WIDTH:], rows_ref[k + 1, :, WIDTH:]], axis=1)
+        x = jnp.concatenate([rows[k][:, :WIDTH], rows[k + 1][:, :WIDTH]], axis=1)
+        y = jnp.concatenate([rows[k][:, WIDTH:], rows[k + 1][:, WIDTH:]], axis=1)
         pre = pre + dot(x, jnp.concatenate(weights, axis=0), 1, 0)
         grad = grad + dot(y, jnp.concatenate(downs, axis=1), 1, 1)
     mine = jnp.concatenate([pre[:, : 2 * WIDTH], grad[:, :WIDTH]], axis=1)
@@ -178,8 +175,7 @@
 
 
 def partial_kernel(
-    own_ref, got_ref, kept_ref, swapped_ref, out_ref, grads_out, hidden_out,
-    grads_ref, hidden_ref, sems,
+    own_ref, got_ref, kept_ref, swapped_ref, out_ref, grads_ref, hidden_ref
 ):
     grads = []
     for half in range(2):
@@ -192,28 +188,27 @@
         slope = gate_sig * (1.0 + gate_pre * (1.0 - gate_sig))
         grads.append((grad_hidden * up_pre * slope).astype(BF16))
         grads.append((grad_hidden * gate_act).astype(BF16))
-    grads_ref[...] = jnp.concatenate(grads, axis=1)
-    copies = start_all([(grads_ref, grads_out), (hidden_ref, hidden_out)], sems)
-    grads = grads_ref[...]
+    grads = jnp.concatenate(grads, axis=1)
+    grads_ref[...] = grads
     for k in range(RING):
         weights = jnp.concatenate(
             [kept_ref[0, k], kept_ref[1, k], swapped_ref[0, k], swapped_ref[1, k]], axis=1
         )
         out_ref[k] = dot(grads, weights, 1, 1).astype(BF16)
-    for copy in copies:
-        copy.wait()
-
-
-def weight_kernel(rows_ref, grads_ref, hidden_ref, own_ref, send_ref):
+
+
+def weight_kernel(here_ref, *refs):
+    rows, (grads_ref, hidden_ref, own_ref, send_ref) = refs[:RING], refs[RING:]
     grads, hidden = grads_ref[...], hidden_ref[...]
     for k in range(RING):
-        both = dot(rows_ref[k, :, :WIDTH], grads, 0, 0).astype(BF16)
-        down = dot(hidden, rows_ref[k, :, WIDTH:], 0, 0).astype(BF16)
+        j = sender(here_ref[0], k)
+        both = dot(rows[k][:, :WIDTH], grads, 0, 0).astype(BF16)
+        down = dot(hidden, rows[k][:, WIDTH:], 0, 0).astype(BF16)
         for half, ref in enumerate((own_ref, send_ref)):
             at = 2 * half * WIDTH
-            ref[0, k] = both[:, at : at + WIDTH]
-            ref[1, k] = both[:, at + WIDTH : at + 2 * WIDTH]
-            ref[2, k] = down[half * WIDTH : (half + 1) * WIDTH]
+            ref[0, j] = both[:, at : at + WIDTH]
+            ref[1, j] = both[:, at + WIDTH : at + 2 * WIDTH]
+            ref[2, j] = down[half * WIDTH : (half + 1) * WIDTH]
 
 
 def joined_kernel(core_ref, own_ref, got_ref, gate_ref, up_ref, down_ref):
@@ -235,11 +230,11 @@
     send_ref[...] = rows + back_ref[...]
 
 
-def token_kernel(got_ref, pick_ref, cot_ref, copies_ref, rows_ref, sems):
+def token_kernel(got_ref, pick_ref, cot_ref, copies_ref):
     got = got_ref[...].reshape(SLOTS, WIDTH)
-    rows_ref[...] = (cot_ref[...].astype(F32) + dot(pick_ref[...], got, 0, 0)).astype(BF16)
-    for copy in start_all([(rows_ref, copies_ref.at[k]) for k in range(RING)], sems):
-        copy.wait()
+    rows = (cot_ref[...].astype(F32) + dot(pick_ref[...], got, 0, 0)).astype(BF16)
+    for k in range(RING):
+        copies_ref[k] = rows
 
 
 def state_kernel(place_ref, got_ref, state_ref, reach_ref):
@@ -403,6 +398,7 @@
     core = lax.axis_index("core")
     core_at = core.reshape(1).astype(jnp.int32)
     place_at = lax.axis_index(sp).reshape(1).astype(jnp.int32)
+    ring_at = lax.axis_index("y").reshape(1).astype(jnp.int32)
     speed = channel_decay_speed.reshape(1, KEY_DIM)
     swap = [(0, 1), (1, 0)]
 
@@ -427,33 +423,40 @@
         stored=(1,),
     )
     got = exchanged(send, sp)
-    copies, back = call(
-        arrival_kernel,
-        [((RING, ROWS, 2 * WIDTH), BF16), ((PEERS, PAD, WIDTH), BF16)],
-        on_chip(got),
-        stored=(0, 1),
-        manual=(0,),
-        scratch=(pltpu.VMEM((ROWS, 2 * WIDTH), BF16), pltpu.SemaphoreType.DMA((RING,))),
-    )
-    rows = exchanged(copies, "y")
-    kept, theirs = call(
+    kept, theirs, proj = call(
         slice_kernel,
-        [((3, RING, WIDTH, WIDTH), BF16)] * 2,
+        [((3, RING, WIDTH, WIDTH), BF16)] * 2 + [((VAL_DIM, MODEL), BF16)],
         core_at,
         place_at,
+        ring_at,
         off_chip(gate_blocks),
         off_chip(up_blocks),
         off_chip(down),
-        scalars=2,
+        off_chip(output_weight_matrix.T),
+        scalars=3,
         stored=(1,),
     )
     swapped = lax.ppermute(theirs, "core", swap)
+    rows, back = call(
+        arrival_kernel,
+        [((ROWS, 2 * WIDTH), BF16), ((PEERS, PAD, WIDTH), BF16)],
+        on_chip(got),
+        stored=(1,),
+    )
+    shards = {0: rows}
+    for distance in (4, 3, 5, 2, 6, 1, 7):
+        shards[distance] = lax.ppermute(
+            rows, "y", [(k, (k + distance) % RING) for k in range(RING)]
+        )
+    shards = [on_chip(shards[distance]) for distance in range(RING)]
     own, send = call(
         forward_kernel,
         [((2, ROWS, 3 * WIDTH), F32), ((2, ROWS, 3 * WIDTH), BF16)],
-        rows,
+        ring_at,
+        *shards,
         on_chip(kept),
         swapped,
+        scalars=1,
     )
     crossed = lax.ppermute(send, "core", swap)
     partials, grads, hidden = call(
@@ -467,28 +470,19 @@
         on_chip(crossed),
         on_chip(kept),
         swapped,
-        stored=(1, 2),
-        manual=(1, 2),
-        scratch=(
-            pltpu.VMEM((ROWS, 4 * WIDTH), BF16),
-            pltpu.VMEM((ROWS, 2 * WIDTH), BF16),
-            pltpu.SemaphoreType.DMA((2,)),
-        ),
     )
     parts = exchanged(partials, "y")
     (send,) = call(
-        return_kernel, [((PEERS, PAD, WIDTH), BF16)], on_chip(parts), off_chip(back)
+        return_kernel, [((PEERS, PAD, WIDTH), BF16)], on_chip(parts), on_chip(back)
     )
     returned = on_chip(exchanged(send, sp))
     (copies,) = call(
         token_kernel,
         [((RING, TOK, WIDTH), BF16)],
         returned,
-        off_chip(pick),
-        off_chip(cotangent),
+        on_chip(pick),
+        cotangent,
         stored=(0,),
-        manual=(0,),
-        scratch=(pltpu.VMEM((TOK, WIDTH), BF16), pltpu.SemaphoreType.DMA((RING,))),
     )
     row = iota((TOK, TOK), 0)
     cum, queries, key_in, val_in, row, copies = lax.optimization_barrier(
@@ -528,7 +522,7 @@
         [((PEERS, 3 * KEY_DIM // 2, WIDTH), BF16), ((TOK, VAL_DIM), F32)],
         place_at,
         on_chip(full_rows),
-        off_chip(output_weight_matrix.T),
+        on_chip(proj),
         normed_t,
         inv_rms.reshape(TOK, 1),
         mix_twice,
@@ -547,10 +541,11 @@
     own, send = call(
         weight_kernel,
         [((3, RING, WIDTH, WIDTH), BF16)] * 2,
-        off_chip(rows),
-        off_chip(grads),
-        off_chip(hidden),
-        stored=range(2),
+        ring_at,
+        *shards,
+        on_chip(grads),
+        on_chip(hidden),
+        scalars=1,
     )
     crossed = lax.ppermute(send, "core", swap)
     grad_gate, grad_up, grad_down = call(
@@ -561,8 +556,8 @@
             ((WIDTH, MODEL), BF16),
         ],
         core_at,
-        off_chip(own),
-        crossed,
+        on_chip(own),
+        on_chip(crossed),
         scalars=1,
         stored=range(3),
     )
@@ -635,4 +630,6 @@
         P(sp, tp, None),
     )
 
-    return jax.shard_map(body, mesh=fine, in_specs=in_specs, out_specs=out_specs, check_vma=False)
+    return jax.shard_map(
+        body, mesh=fine, in_specs=in_specs, out_specs=out_specs, check_vma=False
+    )

time: 175 us -> 179 us (1.023)
  starting transfers between devices: 31.7 us -> 67.1 us
  blocking collectives: 30.2 us -> 5.36 us
  Pallas kernels: 24.6 us -> 18.1 us
  waiting for transfers between devices: 78.2 us -> 73.8 us
  local copies, waits for them, and re-layouts: 0.88 us -> 4.75 us
    ppermute x0 -> x7, starting transfers between devices: none -> 28.5 us  [body(): lax.ppermute(rows, 'y', [(k, (k + distance) % RING) for k in range(RING)])]
    all_to_all x1 -> x0, blocking collectives: 24.8 us -> none  [exchanged(): return lax.all_to_all(array, axis, split_axis=0, concat_axis=0, tiled=True)]
    all_to_all x5, waiting for transfers between devices: 74.5 us -> 49.9 us  [exchanged(): return lax.all_to_all(array, axis, split_axis=0, concat_axis=0, tiled=True)]
    ppermute x0 -> x7, waiting for transfers between devices: none -> 22.3 us  [body(): lax.ppermute(rows, 'y', [(k, (k + distance) % RING) for k in range(RING)])]
    all_to_all x5, starting transfers between devices: 22.4 us -> 29.4 us  [exchanged(): return lax.all_to_all(array, axis, split_axis=0, concat_axis=0, tiled=True)]
    pallas_call x12, Pallas kernels: 24.6 us -> 18.1 us  [call(): pl.pallas_call(kernel, out_shape=shapes, in_specs=[SCALAR] * scalars + [W...]
    unnamed x12 -> x24, local copies, waits for them, and re-layouts: 0.4 us -> 4.27 us
    ppermute x1, waiting for transfers between devices: 2.1 us -> 0.01 us  [body(): swapped = lax.ppermute(theirs, 'core', swap)]
  transfers between devices with their start and end apart: 8 -> 15, of which waited for: 7 -> 10; matrix products, arithmetic and copies ran while one was open for 2% -> 2% of each run, Pallas kernels for 6% -> 5%
where the time goes in v9:
time: 179 us; the launch traced here: 178 us
  waiting for transfers between devices  73.8 us (41%)
  starting transfers between devices  67.1 us (37%)
  Pallas kernels  18.1 us (10%)
  blocking collectives  5.36 us (3%)
  local copies, waits for them, and re-layouts  4.75 us (3%)
  matrix products  4.12 us (2%)
  other arithmetic  3.66 us (2%)
    all_to_all x5, waiting for transfers between devices, exchanged(): return lax.all_to_all(array, axis, split_axis=0, concat_axis=0, tiled=True)  49.9 us
    all_to_all x5, starting transfers between devices, exchanged(): return lax.all_to_all(array, axis, split_axis=0, concat_axis=0, tiled=True)  29.4 us
    ppermute x7, starting transfers between devices, body(): lax.ppermute(rows, 'y', [(k, (k + distance) % RING) for k in range(RING)])  28.5 us
    ppermute x7, waiting for transfers between devices, body(): lax.ppermute(rows, 'y', [(k, (k + distance) % RING) for k in range(RING)])  22.3 us
    pallas_call x12, Pallas kernels, call(): pl.pallas_call(kernel, out_shape=shapes, in_specs=[SCALAR] * scalars + [W...  18.1 us
    ppermute x2, starting transfers between devices, body(): crossed = lax.ppermute(send, 'core', swap)  6.4 us
    all_gather x1, blocking collectives, body(): full_rows = lax.all_gather(full_rows, 'core', axis=0, tiled=False)  5.36 us
    unnamed x24, local copies, waits for them, and re-layouts  4.27 us
  transfers between devices with their start and end apart: 15, of which 10 were waited for; matrix products, arithmetic and copies ran while one was open for 2% of the time, Pallas kernels for 5%

profile of v9, /device:TPU:1, one launch (start us, length us, event | category | flops | bytes accessed | tf_op | source)
XLA Modules:
  0.0 177.9 jit_solution(9692399783137288021)
XLA Ops:
  0.6 2.3 %shard_map.197 = (bf16[32,16,256]{2,1,0:T(8,128)(2,1)}, bf16[512,128]{1,0:T(8,128)(2,1)}, f32[32,128]{1,0:T(8,128)S(1)}) custom-call(s32[2,128]{1,0:T(2,128)} %bitcast.73, f32[2,128]{1,0:T(2,128)} %bitcast.74, bf16[128,128]{1,0:T(8,128)(2,1)} %x_ref.1, bf16[128,128]{1,0:T(8,128)(2,1)} %cot_ref.3, bf16[32,128]{1,0:T(8,128)(2,1)} %key_ref.3, ...), custom_call_target="tpu_custom_call" | custom-call | tf_op jit(solution)/shard_map/pallas_call | solution.py:357
  3.0 13.7 %all-to-all-start = ((bf16[32,16,256]{2,1,0:T(8,128)(2,1)}), bf16[32,16,256]{2,1,0:T(8,128)(2,1)S(1)}, u32[]{:S(2)}, u32[]{:S(2)}) async-start(bf16[32,16,256]{2,1,0:T(8,128)(2,1)} %get-tuple-element.41), calls=%async_computation | async-start | bytes 524288 | tf_op jit(solution)/shard_map/all_to_all | solution.py:406
  16.7 2.4 %shard_map.199 = (bf16[3,8,128,128]{3,2,1,0:T(8,128)(2,1)S(1)}, bf16[3,8,128,128]{3,2,1,0:T(8,128)(2,1)}, bf16[64,2048]{1,0:T(8,128)(2,1)S(1)}) custom-call(s32[1]{0:T(128)} %bitcast.7.core_ref, s32[1]{0:T(128)} %bitcast.2.place_ref, s32[1]{0:T(128)} %bitcast.6.ring_ref.here_ref, bf16[16,128,128]{2,1,0:T(8,128)(2,1)} %bitcast.66, ...), custom_call_target="tpu_custom_call" | custom-call | tf_op jit(solution)/shard_map/pallas_call | solution.py:357
  19.1 2.9 %collective-permute-start.7 = (bf16[3,8,128,128]{3,2,1,0:T(8,128)(2,1)}, bf16[3,8,128,128]{3,2,1,0:T(8,128)(2,1)S(1)}, u32[]{:S(2)}, u32[]{:S(2)}) collective-permute-start(bf16[3,8,128,128]{3,2,1,0:T(8,128)(2,1)} %get-tuple-element.44), channel_id=1, source_target_pairs={{0,1},{1,0},{2,3},{3,2},{4,5},{5,4},{6,7},{7,6},{8,9},{9,8},{10,11... | collective-permute-start | bytes 2359304 | tf_op jit(solution)/shard_map/ppermute | solution.py:439
  22.0 6.0 %all-to-all-done.got_ref = bf16[32,16,256]{2,1,0:T(8,128)(2,1)S(1)} async-done(((bf16[32,16,256]{2,1,0:T(8,128)(2,1)}), bf16[32,16,256]{2,1,0:T(8,128)(2,1)S(1)}, u32[]{:S(2)}, u32[]{:S(2)}) %all-to-all-start) | async-done | bytes 262176 | tf_op jit(solution)/shard_map/all_to_all | solution.py:406
  28.0 1.5 shard_map.198
  29.5 3.2 %collective-permute-start = (bf16[384,256]{1,0:T(8,128)(2,1)S(1)}, bf16[384,256]{1,0:T(8,128)(2,1)S(1)}, u32[]{:S(2)}, u32[]{:S(2)}) collective-permute-start(bf16[384,256]{1,0:T(8,128)(2,1)S(1)} %get-tuple-element.42.refs_0_), channel_id=1, source_target_pairs={{0,2},{2,4},{4,6},{6,8},{8,10},{10,12},{12,14},{14,0},{1,3},{3,5},... | collective-permute-start | bytes 589832 | tf_op jit(solution)/shard_map/ppermute | solution.py:448
  32.7 4.2 %collective-permute-start.1 = (bf16[384,256]{1,0:T(8,128)(2,1)S(1)}, bf16[384,256]{1,0:T(8,128)(2,1)S(1)}, u32[]{:S(2)}, u32[]{:S(2)}) collective-permute-start(bf16[384,256]{1,0:T(8,128)(2,1)S(1)} %get-tuple-element.42.refs_0_), channel_id=1, source_target_pairs={{0,4},{2,6},{4,8},{6,10},{8,12},{10,14},{12,0},{14,2},{1,5},{3,7},... | collective-permute-start | bytes 589832 | tf_op jit(solution)/shard_map/ppermute | solution.py:448
  36.9 4.6 %collective-permute-start.2 = (bf16[384,256]{1,0:T(8,128)(2,1)S(1)}, bf16[384,256]{1,0:T(8,128)(2,1)S(1)}, u32[]{:S(2)}, u32[]{:S(2)}) collective-permute-start(bf16[384,256]{1,0:T(8,128)(2,1)S(1)} %get-tuple-element.42.refs_0_), channel_id=1, source_target_pairs={{0,6},{2,8},{4,10},{6,12},{8,14},{10,0},{12,2},{14,4},{1,7},{3,9},... | collective-permute-start | bytes 589832 | tf_op jit(solution)/shard_map/ppermute | solution.py:448
  41.6 3.5 %collective-permute-start.3 = (bf16[384,256]{1,0:T(8,128)(2,1)S(1)}, bf16[384,256]{1,0:T(8,128)(2,1)S(1)}, u32[]{:S(2)}, u32[]{:S(2)}) collective-permute-start(bf16[384,256]{1,0:T(8,128)(2,1)S(1)} %get-tuple-element.42.refs_0_), channel_id=1, source_target_pairs={{0,8},{2,10},{4,12},{6,14},{8,0},{10,2},{12,4},{14,6},{1,9},{3,11}... | collective-permute-start | bytes 589832 | tf_op jit(solution)/shard_map/ppermute | solution.py:448
  45.1 4.9 %collective-permute-start.4 = (bf16[384,256]{1,0:T(8,128)(2,1)S(1)}, bf16[384,256]{1,0:T(8,128)(2,1)S(1)}, u32[]{:S(2)}, u32[]{:S(2)}) collective-permute-start(bf16[384,256]{1,0:T(8,128)(2,1)S(1)} %get-tuple-element.42.refs_0_), channel_id=1, source_target_pairs={{0,10},{2,12},{4,14},{6,0},{8,2},{10,4},{12,6},{14,8},{1,11},{3,13... | collective-permute-start | bytes 589832 | tf_op jit(solution)/shard_map/ppermute | solution.py:448
  50.0 5.0 %collective-permute-start.5 = (bf16[384,256]{1,0:T(8,128)(2,1)S(1)}, bf16[384,256]{1,0:T(8,128)(2,1)S(1)}, u32[]{:S(2)}, u32[]{:S(2)}) collective-permute-start(bf16[384,256]{1,0:T(8,128)(2,1)S(1)} %get-tuple-element.42.refs_0_), channel_id=1, source_target_pairs={{0,12},{2,14},{4,0},{6,2},{8,4},{10,6},{12,8},{14,10},{1,13},{3,15... | collective-permute-start | bytes 589832 | tf_op jit(solution)/shard_map/ppermute | solution.py:448
  55.0 0.0 collective-permute-done.2.refs_3_
  55.0 3.0 %collective-permute-start.6 = (bf16[384,256]{1,0:T(8,128)(2,1)S(1)}, bf16[384,256]{1,0:T(8,128)(2,1)S(1)}, u32[]{:S(2)}, u32[]{:S(2)}) collective-permute-start(bf16[384,256]{1,0:T(8,128)(2,1)S(1)} %get-tuple-element.42.refs_0_), channel_id=1, source_target_pairs={{0,14},{2,0},{4,2},{6,4},{8,6},{10,8},{12,10},{14,12},{1,15},{3,1}... | collective-permute-start | bytes 589832 | tf_op jit(solution)/shard_map/ppermute | solution.py:448
  58.0 6.4 %collective-permute-done.3.refs_4_ = bf16[384,256]{1,0:T(8,128)(2,1)S(1)} collective-permute-done((bf16[384,256]{1,0:T(8,128)(2,1)S(1)}, bf16[384,256]{1,0:T(8,128)(2,1)S(1)}, u32[]{:S(2)}, u32[]{:S(2)}) %collective-permute-start.3) | collective-permute-done | bytes 196640 | tf_op jit(solution)/shard_map/ppermute | solution.py:448
  64.4 5.4 %collective-permute-done.4.refs_5_ = bf16[384,256]{1,0:T(8,128)(2,1)S(1)} collective-permute-done((bf16[384,256]{1,0:T(8,128)(2,1)S(1)}, bf16[384,256]{1,0:T(8,128)(2,1)S(1)}, u32[]{:S(2)}, u32[]{:S(2)}) %collective-permute-start.4) | collective-permute-done | bytes 196640 | tf_op jit(solution)/shard_map/ppermute | solution.py:448
  69.8 8.0 %collective-permute-done.5.refs_6_ = bf16[384,256]{1,0:T(8,128)(2,1)S(1)} collective-permute-done((bf16[384,256]{1,0:T(8,128)(2,1)S(1)}, bf16[384,256]{1,0:T(8,128)(2,1)S(1)}, u32[]{:S(2)}, u32[]{:S(2)}) %collective-permute-start.5) | collective-permute-done | bytes 196640 | tf_op jit(solution)/shard_map/ppermute | solution.py:448
  77.8 2.5 %collective-permute-done.6.refs_7_ = bf16[384,256]{1,0:T(8,128)(2,1)S(1)} collective-permute-done((bf16[384,256]{1,0:T(8,128)(2,1)S(1)}, bf16[384,256]{1,0:T(8,128)(2,1)S(1)}, u32[]{:S(2)}, u32[]{:S(2)}) %collective-permute-start.6) | collective-permute-done | bytes 196640 | tf_op jit(solution)/shard_map/ppermute | solution.py:448
  80.3 0.8 shard_map.200
  81.1 3.8 %collective-permute-start.8 = (bf16[2,384,384]{2,1,0:T(8,128)(2,1)S(1)}, bf16[2,384,384]{2,1,0:T(8,128)(2,1)S(1)}, u32[]{:S(2)}, u32[]{:S(2)}) collective-permute-start(bf16[2,384,384]{2,1,0:T(8,128)(2,1)S(1)} %get-tuple-element.46), channel_id=1, source_target_pairs={{0,1},{1,0},{2,3},{3,2},{4,5},{5,4},{6,7},{7,6},{8,9},{9,8},{10,11... | collective-permute-start | bytes 1769480 | tf_op jit(solution)/shard_map/ppermute | solution.py:461
  85.0 1.6 collective-permute-done.8.got_ref
  86.6 2.0 %shard_map.201 = (bf16[8,384,128]{2,1,0:T(8,128)(2,1)}, bf16[384,512]{1,0:T(8,128)(2,1)S(1)}, bf16[384,256]{1,0:T(8,128)(2,1)S(1)}) custom-call(f32[2,384,384]{2,1,0:T(8,128)S(1)} %get-tuple-element.45.own_ref, bf16[2,384,384]{2,1,0:T(8,128)(2,1)S(1)} %collective-permute-done.8.got_ref, bf16[3,8,128,128]{3,2,1,0:T(8,128)(2,1)S(1)} %get-tuple-element.43.refs_8_.kept_ref, ...), custom_call_target="tpu_custom_call" | custom-call | tf_op jit(solution)/shard_map/pallas_call | solution.py:357
  88.6 0.7 copy-done
  89.4 0.7 copy-done.3
  90.0 3.7 %all-to-all-start.1 = ((bf16[8,384,128]{2,1,0:T(8,128)(2,1)}), bf16[8,384,128]{2,1,0:T(8,128)(2,1)S(1)}, u32[]{:S(2)}, u32[]{:S(2)}) async-start(bf16[8,384,128]{2,1,0:T(8,128)(2,1)} %get-tuple-element.47), calls=%async_computation.1 | async-start | bytes 1572864 | tf_op jit(solution)/shard_map/all_to_all | solution.py:406
  93.7 1.0 copy-done.1
  94.7 0.9 copy-done.4
  95.6 2.1 %shard_map.207 = (bf16[3,8,128,128]{3,2,1,0:T(8,128)(2,1)S(1)}, bf16[3,8,128,128]{3,2,1,0:T(8,128)(2,1)}) custom-call(s32[1]{0:T(128)} %bitcast.6.ring_ref.here_ref, bf16[384,256]{1,0:T(8,128)(2,1)S(1)} %get-tuple-element.42.refs_0_, bf16[384,256]{1,0:T(8,128)(2,1)S(1)} %collective-permute-done.refs_1_, bf16[384,256]{1,0:T(8,128)(2,1)S(1)} %collective-permute-done.1.refs_2_, ...), custom_call_target="tpu_custom_call" | custom-call | tf_op jit(solution)/shard_map/pallas_call | solution.py:357
  97.7 2.6 %collective-permute-start.9 = (bf16[3,8,128,128]{3,2,1,0:T(8,128)(2,1)}, bf16[3,8,128,128]{3,2,1,0:T(8,128)(2,1)S(1)}, u32[]{:S(2)}, u32[]{:S(2)}) collective-permute-start(bf16[3,8,128,128]{3,2,1,0:T(8,128)(2,1)} %get-tuple-element.68), channel_id=1, source_target_pairs={{0,1},{1,0},{2,3},{3,2},{4,5},{5,4},{6,7},{7,6},{8,9},{9,8},{10,11... | collective-permute-start | bytes 2359304 | tf_op jit(solution)/shard_map/ppermute | solution.py:550
  100.3 17.0 %all-to-all-done.1.parts_ref = bf16[8,384,128]{2,1,0:T(8,128)(2,1)S(1)} async-done(((bf16[8,384,128]{2,1,0:T(8,128)(2,1)}), bf16[8,384,128]{2,1,0:T(8,128)(2,1)S(1)}, u32[]{:S(2)}, u32[]{:S(2)}) %all-to-all-start.1) | async-done | bytes 786464 | tf_op jit(solution)/shard_map/all_to_all | solution.py:406
  117.3 0.9 copy-done.7
  118.2 1.0 shard_map.202
  119.2 4.7 %all-to-all-start.2 = ((bf16[32,16,128]{2,1,0:T(8,128)(2,1)}), bf16[32,16,128]{2,1,0:T(8,128)(2,1)S(1)}, u32[]{:S(2)}, u32[]{:S(2)}) async-start(bf16[32,16,128]{2,1,0:T(8,128)(2,1)} %shard_map.202), calls=%async_computation.2 | async-start | bytes 262144 | tf_op jit(solution)/shard_map/all_to_all | solution.py:406
  123.9 0.0 copy-start.11
  123.9 1.3 shard_map.208
  125.3 8.0 %all-to-all-done.2.got_ref = bf16[32,16,128]{2,1,0:T(8,128)(2,1)S(1)} async-done(((bf16[32,16,128]{2,1,0:T(8,128)(2,1)}), bf16[32,16,128]{2,1,0:T(8,128)(2,1)S(1)}, u32[]{:S(2)}, u32[]{:S(2)}) %all-to-all-start.2) | async-done | bytes 131104 | tf_op jit(solution)/shard_map/all_to_all | solution.py:406
  133.3 0.9 shard_map.203
  134.2 0.2 slice_reduce_fusion
  134.5 0.1 fusion.38
  134.5 0.9 shard_map.204
  135.4 0.2 fusion.35
  135.6 0.2 convolution_add_fusion.1
  135.9 0.1 copy.43
  136.0 3.4 %all-to-all-start.3 = ((bf16[8,128,128]{2,1,0:T(8,128)(2,1)}), bf16[8,128,128]{2,1,0:T(8,128)(2,1)S(1)}, u32[]{:S(2)}, u32[]{:S(2)}) async-start(bf16[8,128,128]{2,1,0:T(8,128)(2,1)} %shard_map.203), calls=%async_computation.3 | async-start | bytes 524288 | tf_op jit(solution)/shard_map/all_to_all | solution.py:406
  139.4 1.3 multiply_reduce_fusion
  140.7 0.2 multiply_reduce_fusion.1
  140.9 0.1 copy.44.inv_ref
  141.1 0.1 fusion.46
  141.2 0.1 pad_maximum_fusion.mix_ref
  141.2 7.3 %all-to-all-done.3 = bf16[8,128,128]{2,1,0:T(8,128)(2,1)S(1)} async-done(((bf16[8,128,128]{2,1,0:T(8,128)(2,1)}), bf16[8,128,128]{2,1,0:T(8,128)(2,1)S(1)}, u32[]{:S(2)}, u32[]{:S(2)}) %all-to-all-start.3) | async-done | bytes 262176 | tf_op jit(solution)/shard_map/all_to_all | solution.py:406
  148.6 5.4 %all-gather = bf16[16,128,128]{2,1,0:T(8,128)(2,1)S(1)} all-gather(bf16[8,128,128]{2,1,0:T(8,128)(2,1)S(1)} %all-to-all-done.3), channel_id=2, replica_groups=mesh['z'=8,'x'=4,'y'=8,'core'=2] {'core'}, dimensions={0}, use_global_device_ids=true | all-gather | bytes 786432 | tf_op jit(solution)/shard_map/all_gather | solution.py:492
  153.9 1.7 shard_map.205
  155.7 0.1 fusion.47
  155.8 0.1 fusion.33
  155.9 2.1 %fusion.7 = (f32[32,128]{1,0:T(8,128)S(1)}, f32[32,128]{1,0:T(8,128)S(1)}) fusion(f32[128,128]{1,0:T(8,128)S(1)} %fusion.47, f32[32,128]{1,0:T(8,128)S(1)} %get-tuple-element.80, f32[32,128]{1,0:T(8,128)S(1)} %convert.3, f32[32,128]{1,0:T(8,128)S(1)} %get-tuple-element.54.cum_ref, pred[128,128]{1,0:T(8,128)(4,1)S(1)} %iota_compare_fusion.1), kind=kLoop, calls=%fused_computation.10 | loop fusion | flops 6283264 | bytes 163840 | tf_op jit(solution)/shard_map/transpose(jvp())/reduce_sum | solution.py:368
  158.0 0.9 fusion.4
  159.0 3.9 %all-to-all-start.4 = ((bf16[32,48,128]{2,1,0:T(8,128)(2,1)}), bf16[32,48,128]{2,1,0:T(8,128)(2,1)S(1)}, u32[]{:S(2)}, u32[]{:S(2)}) async-start(bf16[32,48,128]{2,1,0:T(8,128)(2,1)} %get-tuple-element.59), calls=%async_computation.4 | async-start | bytes 786432 | tf_op jit(solution)/shard_map/all_to_all | solution.py:406
  162.9 0.9 fusion.39
  163.8 0.1 copy.45
  163.9 0.2 fusion.16.decay_mix_ref
  164.1 0.2 fusion.48.vals_mix_ref
  164.3 0.9 fusion.2
  165.2 11.5 %all-to-all-done.4.got_ref = bf16[32,48,128]{2,1,0:T(8,128)(2,1)S(1)} async-done(((bf16[32,48,128]{2,1,0:T(8,128)(2,1)}), bf16[32,48,128]{2,1,0:T(8,128)(2,1)S(1)}, u32[]{:S(2)}, u32[]{:S(2)}) %all-to-all-start.4) | async-done | bytes 393248 | tf_op jit(solution)/shard_map/all_to_all | solution.py:406
  176.8 1.1 shard_map.206
  (26 shorter events, 0.1 us)
Async XLA Ops:
  3.0 25.0 %all-to-all-start = ((bf16[32,16,256]{2,1,0:T(8,128)(2,1)}), bf16[32,16,256]{2,1,0:T(8,128)(2,1)S(1)}, u32[]{:S(2)}, u32[]{:S(2)}) async-start(bf16[32,16,256]{2,1,0:T(8,128)(2,1)} %get-tuple-element.41), calls=%async_computation | async-start | bytes 524288 | tf_op jit(solution)/shard_map/all_to_all | solution.py:406
  19.1 61.2 %collective-permute-start.7 = (bf16[3,8,128,128]{3,2,1,0:T(8,128)(2,1)}, bf16[3,8,128,128]{3,2,1,0:T(8,128)(2,1)S(1)}, u32[]{:S(2)}, u32[]{:S(2)}) collective-permute-start(bf16[3,8,128,128]{3,2,1,0:T(8,128)(2,1)} %get-tuple-element.44), channel_id=1, source_target_pairs={{0,1},{1,0},{2,3},{3,2},{4,5},{5,4},{6,7},{7,6},{8,9},{9,8},{10,11... | collective-permute-start | bytes 2359304 | tf_op jit(solution)/shard_map/ppermute | solution.py:439
  29.5 15.6 %collective-permute-start = (bf16[384,256]{1,0:T(8,128)(2,1)S(1)}, bf16[384,256]{1,0:T(8,128)(2,1)S(1)}, u32[]{:S(2)}, u32[]{:S(2)}) collective-permute-start(bf16[384,256]{1,0:T(8,128)(2,1)S(1)} %get-tuple-element.42.refs_0_), channel_id=1, source_target_pairs={{0,2},{2,4},{4,6},{6,8},{8,10},{10,12},{12,14},{14,0},{1,3},{3,5},... | collective-permute-start | bytes 589832 | tf_op jit(solution)/shard_map/ppermute | solution.py:448
  32.7 17.3 %collective-permute-start.1 = (bf16[384,256]{1,0:T(8,128)(2,1)S(1)}, bf16[384,256]{1,0:T(8,128)(2,1)S(1)}, u32[]{:S(2)}, u32[]{:S(2)}) collective-permute-start(bf16[384,256]{1,0:T(8,128)(2,1)S(1)} %get-tuple-element.42.refs_0_), channel_id=1, source_target_pairs={{0,4},{2,6},{4,8},{6,10},{8,12},{10,14},{12,0},{14,2},{1,5},{3,7},... | collective-permute-start | bytes 589832 | tf_op jit(solution)/shard_map/ppermute | solution.py:448
  36.9 18.1 %collective-permute-start.2 = (bf16[384,256]{1,0:T(8,128)(2,1)S(1)}, bf16[384,256]{1,0:T(8,128)(2,1)S(1)}, u32[]{:S(2)}, u32[]{:S(2)}) collective-permute-start(bf16[384,256]{1,0:T(8,128)(2,1)S(1)} %get-tuple-element.42.refs_0_), channel_id=1, source_target_pairs={{0,6},{2,8},{4,10},{6,12},{8,14},{10,0},{12,2},{14,4},{1,7},{3,9},... | collective-permute-start | bytes 589832 | tf_op jit(solution)/shard_map/ppermute | solution.py:448
  41.6 22.8 %collective-permute-start.3 = (bf16[384,256]{1,0:T(8,128)(2,1)S(1)}, bf16[384,256]{1,0:T(8,128)(2,1)S(1)}, u32[]{:S(2)}, u32[]{:S(2)}) collective-permute-start(bf16[384,256]{1,0:T(8,128)(2,1)S(1)} %get-tuple-element.42.refs_0_), channel_id=1, source_target_pairs={{0,8},{2,10},{4,12},{6,14},{8,0},{10,2},{12,4},{14,6},{1,9},{3,11}... | collective-permute-start | bytes 589832 | tf_op jit(solution)/shard_map/ppermute | solution.py:448
  45.1 24.7 %collective-permute-start.4 = (bf16[384,256]{1,0:T(8,128)(2,1)S(1)}, bf16[384,256]{1,0:T(8,128)(2,1)S(1)}, u32[]{:S(2)}, u32[]{:S(2)}) collective-permute-start(bf16[384,256]{1,0:T(8,128)(2,1)S(1)} %get-tuple-element.42.refs_0_), channel_id=1, source_target_pairs={{0,10},{2,12},{4,14},{6,0},{8,2},{10,4},{12,6},{14,8},{1,11},{3,13... | collective-permute-start | bytes 589832 | tf_op jit(solution)/shard_map/ppermute | solution.py:448
  50.0 27.8 %collective-permute-start.5 = (bf16[384,256]{1,0:T(8,128)(2,1)S(1)}, bf16[384,256]{1,0:T(8,128)(2,1)S(1)}, u32[]{:S(2)}, u32[]{:S(2)}) collective-permute-start(bf16[384,256]{1,0:T(8,128)(2,1)S(1)} %get-tuple-element.42.refs_0_), channel_id=1, source_target_pairs={{0,12},{2,14},{4,0},{6,2},{8,4},{10,6},{12,8},{14,10},{1,13},{3,15... | collective-permute-start | bytes 589832 | tf_op jit(solution)/shard_map/ppermute | solution.py:448
  55.0 25.3 %collective-permute-start.6 = (bf16[384,256]{1,0:T(8,128)(2,1)S(1)}, bf16[384,256]{1,0:T(8,128)(2,1)S(1)}, u32[]{:S(2)}, u32[]{:S(2)}) collective-permute-start(bf16[384,256]{1,0:T(8,128)(2,1)S(1)} %get-tuple-element.42.refs_0_), channel_id=1, source_target_pairs={{0,14},{2,0},{4,2},{6,4},{8,6},{10,8},{12,10},{14,12},{1,15},{3,1}... | collective-permute-start | bytes 589832 | tf_op jit(solution)/shard_map/ppermute | solution.py:448
  81.1 5.5 %collective-permute-start.8 = (bf16[2,384,384]{2,1,0:T(8,128)(2,1)S(1)}, bf16[2,384,384]{2,1,0:T(8,128)(2,1)S(1)}, u32[]{:S(2)}, u32[]{:S(2)}) collective-permute-start(bf16[2,384,384]{2,1,0:T(8,128)(2,1)S(1)} %get-tuple-element.46), channel_id=1, source_target_pairs={{0,1},{1,0},{2,3},{3,2},{4,5},{5,4},{6,7},{7,6},{8,9},{9,8},{10,11... | collective-permute-start | bytes 1769480 | tf_op jit(solution)/shard_map/ppermute | solution.py:461
  88.6 0.7 copy-start
  89.4 0.7 copy-start.3
  90.0 27.2 %all-to-all-start.1 = ((bf16[8,384,128]{2,1,0:T(8,128)(2,1)}), bf16[8,384,128]{2,1,0:T(8,128)(2,1)S(1)}, u32[]{:S(2)}, u32[]{:S(2)}) async-start(bf16[8,384,128]{2,1,0:T(8,128)(2,1)} %get-tuple-element.47), calls=%async_computation.1 | async-start | bytes 1572864 | tf_op jit(solution)/shard_map/all_to_all | solution.py:406
  93.7 1.0 copy-start.1
  94.7 0.9 copy-start.4
  97.7 26.2 %collective-permute-start.9 = (bf16[3,8,128,128]{3,2,1,0:T(8,128)(2,1)}, bf16[3,8,128,128]{3,2,1,0:T(8,128)(2,1)S(1)}, u32[]{:S(2)}, u32[]{:S(2)}) collective-permute-start(bf16[3,8,128,128]{3,2,1,0:T(8,128)(2,1)} %get-tuple-element.68), channel_id=1, source_target_pairs={{0,1},{1,0},{2,3},{3,2},{4,5},{5,4},{6,7},{7,6},{8,9},{9,8},{10,11... | collective-permute-start | bytes 2359304 | tf_op jit(solution)/shard_map/ppermute | solution.py:550
  117.3 0.9 copy-start.7
  119.2 14.1 %copy-start.5 = (bf16[512,128]{1,0:T(8,128)(2,1)S(1)}, bf16[512,128]{1,0:T(8,128)(2,1)}, u32[]{:S(2)}) copy-start(bf16[512,128]{1,0:T(8,128)(2,1)} %get-tuple-element.49.pick_ref) | copy-start | bytes 393220
  119.2 14.1 %copy-start.6 = (bf16[128,128]{1,0:T(8,128)(2,1)S(1)}, bf16[128,128]{1,0:T(8,128)(2,1)}, u32[]{:S(2)}) copy-start(bf16[128,128]{1,0:T(8,128)(2,1)} %cot_ref.3) | copy-start | bytes 98308
  119.2 15.2 %copy-start.8 = (bf16[32,128]{1,0:T(8,128)(2,1)S(1)}, bf16[32,128]{1,0:T(8,128)(2,1)}, u32[]{:S(2)}) copy-start(bf16[32,128]{1,0:T(8,128)(2,1)} %key_ref.3) | copy-start | bytes 24580
  119.2 14.1 %all-to-all-start.2 = ((bf16[32,16,128]{2,1,0:T(8,128)(2,1)}), bf16[32,16,128]{2,1,0:T(8,128)(2,1)S(1)}, u32[]{:S(2)}, u32[]{:S(2)}) async-start(bf16[32,16,128]{2,1,0:T(8,128)(2,1)} %shard_map.202), calls=%async_computation.2 | async-start | bytes 262144 | tf_op jit(solution)/shard_map/all_to_all | solution.py:406
  123.9 10.5 %copy-start.11 = (bf16[32,128]{1,0:T(8,128)(2,1)S(1)}, bf16[32,128]{1,0:T(8,128)(2,1)}, u32[]{:S(2)}) copy-start(bf16[32,128]{1,0:T(8,128)(2,1)} %param.14) | copy-start | bytes 24580
  134.2 6.5 %copy-start.2 = (bf16[64,128]{1,0:T(8,128)(2,1)S(1)}, bf16[64,128]{1,0:T(8,128)(2,1)}, u32[]{:S(2)}) copy-start(bf16[64,128]{1,0:T(8,128)(2,1)} %val_ref.3) | copy-start | bytes 49156
  136.0 12.6 %all-to-all-start.3 = ((bf16[8,128,128]{2,1,0:T(8,128)(2,1)}), bf16[8,128,128]{2,1,0:T(8,128)(2,1)S(1)}, u32[]{:S(2)}, u32[]{:S(2)}) async-start(bf16[8,128,128]{2,1,0:T(8,128)(2,1)} %shard_map.203), calls=%async_computation.3 | async-start | bytes 524288 | tf_op jit(solution)/shard_map/all_to_all | solution.py:406
  159.0 17.8 %all-to-all-start.4 = ((bf16[32,48,128]{2,1,0:T(8,128)(2,1)}), bf16[32,48,128]{2,1,0:T(8,128)(2,1)S(1)}, u32[]{:S(2)}, u32[]{:S(2)}) async-start(bf16[32,48,128]{2,1,0:T(8,128)(2,1)} %get-tuple-element.59), calls=%async_computation.4 | async-start | bytes 786432 | tf_op jit(solution)/shard_map/all_to_all | solution.py:406
  164.3 12.5 %copy-start.9 = (bf16[32,128]{1,0:T(8,128)(2,1)S(1)}, bf16[32,128]{1,0:T(8,128)(2,1)}, u32[]{:S(2)}) copy-start(bf16[32,128]{1,0:T(8,128)(2,1)} %pre_ref.3) | copy-start | bytes 24580
  164.3 12.5 %copy-start.10 = (f32[32]{0:T(128)S(1)}, f32[32]{0:T(128)}, u32[]{:S(2)}) copy-start(f32[32]{0:T(128)} %param.19) | copy-start | bytes 388

commit v10 on v9

--- a/solution.py
+++ b/solution.py
@@ -108,9 +108,11 @@
     send_ref[...] = block.astype(BF16)
 
 
-def arrival_kernel(got_ref, rows_ref, back_ref):
+def arrival_kernel(got_ref, copies_ref, back_ref):
     got = got_ref[...].reshape(SLOTS, 2 * WIDTH)
-    rows_ref[...] = dot(ones_where(compact_rows((ROWS, SLOTS), 0)), got, 1, 0).astype(BF16)
+    rows = dot(ones_where(compact_rows((ROWS, SLOTS), 0)), got, 1, 0).astype(BF16)
+    for k in range(RING):
+        copies_ref[k] = rows
     both = dot(ones_where(row_of_peer(CAP)), got, 1, 0)
     state = both[:, :WIDTH] + both[:, WIDTH:]
     logs = dot(ones_where(row_of_peer(CAP + 1)), got, 1, 0)
@@ -135,7 +137,7 @@
 
 
 def slice_kernel(
-    core_ref, place_ref, ring_ref, gate_ref, up_ref, down_ref, proj_ref, own_ref, out_ref, near_ref
+    core_ref, place_ref, gate_ref, up_ref, down_ref, proj_ref, own_ref, out_ref, near_ref
 ):
     near_ref[...] = proj_ref[...]
     core = core_ref[0]
@@ -147,23 +149,17 @@
             ref[2, k] = down_ref[:, pl.ds(pl.multiple_of(at * WIDTH, WIDTH), WIDTH)]
 
 
-def sender(here, distance):
-    return lax.rem(here + RING - distance, RING)
-
-
-def forward_kernel(here_ref, *refs):
-    rows, (own_ref, swapped_ref, out_ref, send_ref) = refs[:RING], refs[RING:]
-    here = here_ref[0]
+def forward_kernel(rows_ref, own_ref, swapped_ref, out_ref, send_ref):
     pre = jnp.zeros((ROWS, 4 * WIDTH), F32)
     grad = jnp.zeros((ROWS, 2 * WIDTH), F32)
     for k in range(0, RING, 2):
         weights, downs = [], []
-        for j in (sender(here, k), sender(here, k + 1)):
+        for j in (k, k + 1):
             parts = [own_ref[0, j], own_ref[1, j], swapped_ref[0, j], swapped_ref[1, j]]
             weights.append(jnp.concatenate(parts, axis=1))
             downs.append(jnp.concatenate([own_ref[2, j], swapped_ref[2, j]], axis=0))
-        x = jnp.concatenate([rows[k][:, :WIDTH], rows[k + 1][:, :WIDTH]], axis=1)
-        y = jnp.concatenate([rows[k][:, WIDTH:], rows[k + 1][:, WIDTH:]], axis=1)
+        x = jnp.concatenate([rows_ref[k, :, :WIDTH], rows_ref[k + 1, :, :WIDTH]], axis=1)
+        y = jnp.concatenate([rows_ref[k, :, WIDTH:], rows_ref[k + 1, :, WIDTH:]], axis=1)
         pre = pre + dot(x, jnp.concatenate(weights, axis=0), 1, 0)
         grad = grad + dot(y, jnp.concatenate(downs, axis=1), 1, 1)
     mine = jnp.concatenate([pre[:, : 2 * WIDTH], grad[:, :WIDTH]], axis=1)
@@ -197,18 +193,16 @@
         out_ref[k] = dot(grads, weights, 1, 1).astype(BF16)
 
 
-def weight_kernel(here_ref, *refs):
-    rows, (grads_ref, hidden_ref, own_ref, send_ref) = refs[:RING], refs[RING:]
+def weight_kernel(rows_ref, grads_ref, hidden_ref, own_ref, send_ref):
     grads, hidden = grads_ref[...], hidden_ref[...]
     for k in range(RING):
-        j = sender(here_ref[0], k)
-        both = dot(rows[k][:, :WIDTH], grads, 0, 0).astype(BF16)
-        down = dot(hidden, rows[k][:, WIDTH:], 0, 0).astype(BF16)
+        both = dot(rows_ref[k, :, :WIDTH], grads, 0, 0).astype(BF16)
+        down = dot(hidden, rows_ref[k, :, WIDTH:], 0, 0).astype(BF16)
         for half, ref in enumerate((own_ref, send_ref)):
             at = 2 * half * WIDTH
-            ref[0, j] = both[:, at : at + WIDTH]
-            ref[1, j] = both[:, at + WIDTH : at + 2 * WIDTH]
-            ref[2, j] = down[half * WIDTH : (half + 1) * WIDTH]
+            ref[0, k] = both[:, at : at + WIDTH]
+            ref[1, k] = both[:, at + WIDTH : at + 2 * WIDTH]
+            ref[2, k] = down[half * WIDTH : (half + 1) * WIDTH]
 
 
 def joined_kernel(core_ref, own_ref, got_ref, gate_ref, up_ref, down_ref):
@@ -398,7 +392,6 @@
     core = lax.axis_index("core")
     core_at = core.reshape(1).astype(jnp.int32)
     place_at = lax.axis_index(sp).reshape(1).astype(jnp.int32)
-    ring_at = lax.axis_index("y").reshape(1).astype(jnp.int32)
     speed = channel_decay_speed.reshape(1, KEY_DIM)
     swap = [(0, 1), (1, 0)]
 
@@ -428,35 +421,27 @@
         [((3, RING, WIDTH, WIDTH), BF16)] * 2 + [((VAL_DIM, MODEL), BF16)],
         core_at,
         place_at,
-        ring_at,
         off_chip(gate_blocks),
         off_chip(up_blocks),
         off_chip(down),
         off_chip(output_weight_matrix.T),
-        scalars=3,
+        scalars=2,
         stored=(1,),
     )
     swapped = lax.ppermute(theirs, "core", swap)
-    rows, back = call(
+    copies, back = call(
         arrival_kernel,
-        [((ROWS, 2 * WIDTH), BF16), ((PEERS, PAD, WIDTH), BF16)],
+        [((RING, ROWS, 2 * WIDTH), BF16), ((PEERS, PAD, WIDTH), BF16)],
         on_chip(got),
         stored=(1,),
     )
-    shards = {0: rows}
-    for distance in (4, 3, 5, 2, 6, 1, 7):
-        shards[distance] = lax.ppermute(
-            rows, "y", [(k, (k + distance) % RING) for k in range(RING)]
-        )
-    shards = [on_chip(shards[distance]) for distance in range(RING)]
+    rows = exchanged(copies, "y")
     own, send = call(
         forward_kernel,
         [((2, ROWS, 3 * WIDTH), F32), ((2, ROWS, 3 * WIDTH), BF16)],
-        ring_at,
-        *shards,
+        rows,
         on_chip(kept),
         swapped,
-        scalars=1,
     )
     crossed = lax.ppermute(send, "core", swap)
     partials, grads, hidden = call(
@@ -541,11 +526,9 @@
     own, send = call(
         weight_kernel,
         [((3, RING, WIDTH, WIDTH), BF16)] * 2,
-        ring_at,
-        *shards,
+        on_chip(rows),
         on_chip(grads),
         on_chip(hidden),
-        scalars=1,
     )
     crossed = lax.ppermute(send, "core", swap)
     grad_gate, grad_up, grad_down = call(
@@ -630,6 +613,4 @@
         P(sp, tp, None),
     )
 
-    return jax.shard_map(
-        body, mesh=fine, in_specs=in_specs, out_specs=out_specs, check_vma=False
-    )
+    return jax.shard_map(body, mesh=fine, in_specs=in_specs, out_specs=out_specs, check_vma=False)

time: 179 us -> 172 us (0.961)
  starting transfers between devices: 67.1 us -> 31.8 us
  blocking collectives: 5.36 us -> 30.2 us
  waiting for transfers between devices: 73.8 us -> 79.3 us
    ppermute x7 -> x0, starting transfers between devices: 28.5 us -> none  [body(): lax.ppermute(rows, 'y', [(k, (k + distance) % RING) for k in range(RING)])]
    all_to_all x5, waiting for transfers between devices: 49.9 us -> 75.6 us  [exchanged(): return lax.all_to_all(array, axis, split_axis=0, concat_axis=0, tiled=True)]
    all_to_all x0 -> x1, blocking collectives: none -> 24.8 us  [exchanged(): return lax.all_to_all(array, axis, split_axis=0, concat_axis=0, tiled=True)]
    ppermute x7 -> x0, waiting for transfers between devices: 22.3 us -> none  [body(): lax.ppermute(rows, 'y', [(k, (k + distance) % RING) for k in range(RING)])]
    all_to_all x5, starting transfers between devices: 29.4 us -> 22.4 us  [exchanged(): return lax.all_to_all(array, axis, split_axis=0, concat_axis=0, tiled=True)]
    ppermute x1, waiting for transfers between devices: 0.01 us -> 2.1 us  [body(): swapped = lax.ppermute(theirs, 'core', swap)]
    unnamed x24 -> x26, local copies, waits for them, and re-layouts: 4.27 us -> 4.15 us
  transfers between devices with their start and end apart: 15 -> 8, of which waited for: 10 -> 7; matrix products, arithmetic and copies ran while one was open for 2% -> 2% of each run, Pallas kernels for 5% -> 4%
where the time goes in v10:
time: 172 us; the launch traced here: 171 us
  waiting for transfers between devices  79.3 us (46%)
  starting transfers between devices  31.8 us (18%)
  blocking collectives  30.2 us (18%)
  Pallas kernels  16.6 us (10%)
  local copies, waits for them, and re-layouts  4.63 us (3%)
  matrix products  4.12 us (2%)
  other arithmetic  3.66 us (2%)
    all_to_all x5, waiting for transfers between devices, exchanged(): return lax.all_to_all(array, axis, split_axis=0, concat_axis=0, tiled=True)  75.6 us
    all_to_all x1, blocking collectives, exchanged(): return lax.all_to_all(array, axis, split_axis=0, concat_axis=0, tiled=True)  24.8 us
    all_to_all x5, starting transfers between devices, exchanged(): return lax.all_to_all(array, axis, split_axis=0, concat_axis=0, tiled=True)  22.4 us
    pallas_call x12, Pallas kernels, call(): pl.pallas_call(kernel, out_shape=shapes, in_specs=[SCALAR] * scalars + [W...  16.6 us
    all_gather x1, blocking collectives, body(): full_rows = lax.all_gather(full_rows, 'core', axis=0, tiled=False)  5.36 us
    ppermute x2, starting transfers between devices, body(): crossed = lax.ppermute(send, 'core', swap)  4.81 us
    ppermute x1, starting transfers between devices, body(): swapped = lax.ppermute(theirs, 'core', swap)  4.62 us
    unnamed x26, local copies, waits for them, and re-layouts  4.15 us
  transfers between devices with their start and end apart: 8, of which 7 were waited for; matrix products, arithmetic and copies ran while one was open for 2% of the time, Pallas kernels for 4%

profile of v10, /device:TPU:1, one launch (start us, length us, event | category | flops | bytes accessed | tf_op | source)
XLA Modules:
  0.0 171.2 jit_solution(9211966750847357659)
XLA Ops:
  0.6 1.8 %shard_map.197 = (bf16[32,16,256]{2,1,0:T(8,128)(2,1)S(1)}, bf16[512,128]{1,0:T(8,128)(2,1)}, f32[32,128]{1,0:T(8,128)S(1)}) custom-call(s32[2,128]{1,0:T(2,128)} %bitcast.72, f32[2,128]{1,0:T(2,128)} %bitcast.73, bf16[128,128]{1,0:T(8,128)(2,1)} %x_ref.1, bf16[128,128]{1,0:T(8,128)(2,1)} %cot_ref.3, bf16[32,128]{1,0:T(8,128)(2,1)} %key_ref.3, ...), custom_call_target="tpu_custom_call" | custom-call | tf_op jit(solution)/shard_map/pallas_call | solution.py:351
  2.4 24.8 %all_to_all.30.got_ref = bf16[32,16,256]{2,1,0:T(8,128)(2,1)S(1)} all-to-all(bf16[32,16,256]{2,1,0:T(8,128)(2,1)S(1)} %get-tuple-element.41), channel_id=1, replica_groups=mesh['z'=8,'x'=4,'y'=8,'core'=2] {'z','x'}, dimensions={0} | all-to-all | bytes 524288 | tf_op jit(solution)/shard_map/all_to_all | solution.py:399
  27.2 1.5 shard_map.198
  28.8 6.8 %all-to-all-start.1 = ((bf16[8,384,256]{2,1,0:T(8,128)(2,1)}), bf16[8,384,256]{2,1,0:T(8,128)(2,1)S(1)}, u32[]{:S(2)}, u32[]{:S(2)}) async-start(bf16[8,384,256]{2,1,0:T(8,128)(2,1)} %get-tuple-element.42), calls=%async_computation.1 | async-start | bytes 3145728 | tf_op jit(solution)/shard_map/all_to_all | solution.py:399
  35.6 2.4 %shard_map.199 = (bf16[3,8,128,128]{3,2,1,0:T(8,128)(2,1)S(1)}, bf16[3,8,128,128]{3,2,1,0:T(8,128)(2,1)}, bf16[64,2048]{1,0:T(8,128)(2,1)S(1)}) custom-call(s32[1]{0:T(128)} %bitcast.6.core_ref, s32[1]{0:T(128)} %bitcast.2.place_ref, bf16[16,128,128]{2,1,0:T(8,128)(2,1)} %bitcast.65, bf16[16,128,128]{2,1,0:T(8,128)(2,1)} %bitcast.66, ...), custom_call_target="tpu_custom_call" | custom-call | tf_op jit(solution)/shard_map/pallas_call | solution.py:351
  38.0 0.7 copy-done.1
  38.7 4.6 %collective-permute-start = (bf16[3,8,128,128]{3,2,1,0:T(8,128)(2,1)}, bf16[3,8,128,128]{3,2,1,0:T(8,128)(2,1)S(1)}, u32[]{:S(2)}, u32[]{:S(2)}) collective-permute-start(bf16[3,8,128,128]{3,2,1,0:T(8,128)(2,1)} %get-tuple-element.44), channel_id=1, source_target_pairs={{0,1},{1,0},{2,3},{3,2},{4,5},{5,4},{6,7},{7,6},{8,9},{9,8},{10,11... | collective-permute-start | bytes 2359304 | tf_op jit(solution)/shard_map/ppermute | solution.py:431
  43.3 2.1 %collective-permute-done.swapped_ref = bf16[3,8,128,128]{3,2,1,0:T(8,128)(2,1)S(1)} collective-permute-done((bf16[3,8,128,128]{3,2,1,0:T(8,128)(2,1)}, bf16[3,8,128,128]{3,2,1,0:T(8,128)(2,1)S(1)}, u32[]{:S(2)}, u32[]{:S(2)}) %collective-permute-start) | collective-permute-done | bytes 786464 | tf_op jit(solution)/shard_map/ppermute | solution.py:431
  45.4 30.6 %all-to-all-done.1.rows_ref = bf16[8,384,256]{2,1,0:T(8,128)(2,1)S(1)} async-done(((bf16[8,384,256]{2,1,0:T(8,128)(2,1)}), bf16[8,384,256]{2,1,0:T(8,128)(2,1)S(1)}, u32[]{:S(2)}, u32[]{:S(2)}) %all-to-all-start.1) | async-done | bytes 1572896 | tf_op jit(solution)/shard_map/all_to_all | solution.py:399
  76.0 0.8 shard_map.200
  76.8 2.4 %collective-permute-start.1 = (bf16[2,384,384]{2,1,0:T(8,128)(2,1)S(1)}, bf16[2,384,384]{2,1,0:T(8,128)(2,1)S(1)}, u32[]{:S(2)}, u32[]{:S(2)}) collective-permute-start(bf16[2,384,384]{2,1,0:T(8,128)(2,1)S(1)} %get-tuple-element.46), channel_id=1, source_target_pairs={{0,1},{1,0},{2,3},{3,2},{4,5},{5,4},{6,7},{7,6},{8,9},{9,8},{10,11... | collective-permute-start | bytes 1769480 | tf_op jit(solution)/shard_map/ppermute | solution.py:446
  79.2 1.6 collective-permute-done.1.got_ref
  80.8 1.1 shard_map.201
  81.9 0.0 copy-start
  81.9 0.9 copy-done
  82.8 0.7 copy-done.4
  83.5 3.5 %all-to-all-start.2 = ((bf16[8,384,128]{2,1,0:T(8,128)(2,1)}), bf16[8,384,128]{2,1,0:T(8,128)(2,1)S(1)}, u32[]{:S(2)}, u32[]{:S(2)}) async-start(bf16[8,384,128]{2,1,0:T(8,128)(2,1)} %copy-done), calls=%async_computation.2 | async-start | bytes 1572864 | tf_op jit(solution)/shard_map/all_to_all | solution.py:399
  87.1 0.0 copy-start.5
  87.1 0.9 copy-done.5
  88.0 2.0 %shard_map.207 = (bf16[3,8,128,128]{3,2,1,0:T(8,128)(2,1)S(1)}, bf16[3,8,128,128]{3,2,1,0:T(8,128)(2,1)}) custom-call(bf16[8,384,256]{2,1,0:T(8,128)(2,1)S(1)} %all-to-all-done.1.rows_ref, bf16[384,512]{1,0:T(8,128)(2,1)S(1)} %get-tuple-element.65.grads_ref, bf16[384,256]{1,0:T(8,128)(2,1)S(1)} %copy-done.5), custom_call_target="tpu_custom_call" | custom-call | tf_op jit(solution)/shard_map/pallas_call | solution.py:351
  90.0 2.4 %collective-permute-start.2 = (bf16[3,8,128,128]{3,2,1,0:T(8,128)(2,1)}, bf16[3,8,128,128]{3,2,1,0:T(8,128)(2,1)S(1)}, u32[]{:S(2)}, u32[]{:S(2)}) collective-permute-start(bf16[3,8,128,128]{3,2,1,0:T(8,128)(2,1)} %get-tuple-element.68), channel_id=1, source_target_pairs={{0,1},{1,0},{2,3},{3,2},{4,5},{5,4},{6,7},{7,6},{8,9},{9,8},{10,11... | collective-permute-start | bytes 2359304 | tf_op jit(solution)/shard_map/ppermute | solution.py:533
  92.4 18.2 %all-to-all-done.2.parts_ref = bf16[8,384,128]{2,1,0:T(8,128)(2,1)S(1)} async-done(((bf16[8,384,128]{2,1,0:T(8,128)(2,1)}), bf16[8,384,128]{2,1,0:T(8,128)(2,1)S(1)}, u32[]{:S(2)}, u32[]{:S(2)}) %all-to-all-start.2) | async-done | bytes 786464 | tf_op jit(solution)/shard_map/all_to_all | solution.py:399
  110.6 0.9 copy-done.8
  111.5 1.0 shard_map.202
  112.5 4.7 %all-to-all-start.3 = ((bf16[32,16,128]{2,1,0:T(8,128)(2,1)}), bf16[32,16,128]{2,1,0:T(8,128)(2,1)S(1)}, u32[]{:S(2)}, u32[]{:S(2)}) async-start(bf16[32,16,128]{2,1,0:T(8,128)(2,1)} %shard_map.202), calls=%async_computation.3 | async-start | bytes 262144 | tf_op jit(solution)/shard_map/all_to_all | solution.py:399
  117.2 0.0 collective-permute-done.2.got_ref
  117.2 1.3 shard_map.208
  118.6 8.0 %all-to-all-done.3.got_ref = bf16[32,16,128]{2,1,0:T(8,128)(2,1)S(1)} async-done(((bf16[32,16,128]{2,1,0:T(8,128)(2,1)}), bf16[32,16,128]{2,1,0:T(8,128)(2,1)S(1)}, u32[]{:S(2)}, u32[]{:S(2)}) %all-to-all-start.3) | async-done | bytes 131104 | tf_op jit(solution)/shard_map/all_to_all | solution.py:399
  126.6 0.0 copy-done.6
  126.6 0.0 copy-done.7
  126.6 0.9 shard_map.203
  127.5 0.2 slice_reduce_fusion
  127.7 0.0 copy-done.9
  127.8 0.0 copy-done.12
  127.8 0.1 fusion.38
  127.9 0.9 shard_map.204
  128.8 0.2 fusion.35
  128.9 0.2 convolution_add_fusion.1
  129.2 0.1 copy.43
  129.3 3.4 %all-to-all-start.4 = ((bf16[8,128,128]{2,1,0:T(8,128)(2,1)}), bf16[8,128,128]{2,1,0:T(8,128)(2,1)S(1)}, u32[]{:S(2)}, u32[]{:S(2)}) async-start(bf16[8,128,128]{2,1,0:T(8,128)(2,1)} %shard_map.203), calls=%async_computation.4 | async-start | bytes 524288 | tf_op jit(solution)/shard_map/all_to_all | solution.py:399
  132.7 1.3 multiply_reduce_fusion
  134.0 0.0 copy-done.3
  134.0 0.2 multiply_reduce_fusion.1
  134.3 0.1 copy.44.inv_ref
  134.4 0.1 fusion.46
  134.5 0.1 pad_maximum_fusion.mix_ref
  134.6 7.3 %all-to-all-done.4 = bf16[8,128,128]{2,1,0:T(8,128)(2,1)S(1)} async-done(((bf16[8,128,128]{2,1,0:T(8,128)(2,1)}), bf16[8,128,128]{2,1,0:T(8,128)(2,1)S(1)}, u32[]{:S(2)}, u32[]{:S(2)}) %all-to-all-start.4) | async-done | bytes 262176 | tf_op jit(solution)/shard_map/all_to_all | solution.py:399
  141.9 5.4 %all-gather = bf16[16,128,128]{2,1,0:T(8,128)(2,1)S(1)} all-gather(bf16[8,128,128]{2,1,0:T(8,128)(2,1)S(1)} %all-to-all-done.4), channel_id=2, replica_groups=mesh['z'=8,'x'=4,'y'=8,'core'=2] {'core'}, dimensions={0}, use_global_device_ids=true | all-gather | bytes 786432 | tf_op jit(solution)/shard_map/all_gather | solution.py:477
  147.3 0.0 copy-done.2
  147.3 1.7 %shard_map.205 = (bf16[32,48,128]{2,1,0:T(8,128)(2,1)}, f32[128,64]{1,0:T(8,128)S(1)}) custom-call(s32[1]{0:T(128)} %bitcast.2.place_ref, bf16[2,8,128,128]{3,2,1,0:T(8,128)(2,1)S(1)} %bitcast.60, bf16[64,2048]{1,0:T(8,128)(2,1)S(1)} %copy-done.2, f32[128,64]{1,0:T(8,128)S(1)} %get-tuple-element.75.normed_ref, f32[128,1]{1,0:T(8,128)S(1)} %copy.44.inv_ref, ...), custom_call_target="tpu_custom_call" | custom-call | tf_op jit(solution)/shard_map/pallas_call | solution.py:351
  149.0 0.1 fusion.47
  149.1 0.1 fusion.33
  149.2 2.1 %fusion.7 = (f32[32,128]{1,0:T(8,128)S(1)}, f32[32,128]{1,0:T(8,128)S(1)}) fusion(f32[128,128]{1,0:T(8,128)S(1)} %fusion.47, f32[32,128]{1,0:T(8,128)S(1)} %get-tuple-element.80, f32[32,128]{1,0:T(8,128)S(1)} %convert.3, f32[32,128]{1,0:T(8,128)S(1)} %get-tuple-element.54.cum_ref, pred[128,128]{1,0:T(8,128)(4,1)S(1)} %iota_compare_fusion.1), kind=kLoop, calls=%fused_computation.10 | loop fusion | flops 6283264 | bytes 163840 | tf_op jit(solution)/shard_map/transpose(jvp())/reduce_sum | solution.py:362
  151.4 0.9 fusion.4
  152.3 3.9 %all-to-all-start.5 = ((bf16[32,48,128]{2,1,0:T(8,128)(2,1)}), bf16[32,48,128]{2,1,0:T(8,128)(2,1)S(1)}, u32[]{:S(2)}, u32[]{:S(2)}) async-start(bf16[32,48,128]{2,1,0:T(8,128)(2,1)} %get-tuple-element.59), calls=%async_computation.5 | async-start | bytes 786432 | tf_op jit(solution)/shard_map/all_to_all | solution.py:399
  156.2 0.9 fusion.39
  157.1 0.1 copy.45
  157.2 0.2 fusion.16.decay_mix_ref
  157.4 0.2 fusion.48.vals_mix_ref
  157.6 0.9 fusion.2
  158.6 11.6 %all-to-all-done.5.got_ref = bf16[32,48,128]{2,1,0:T(8,128)(2,1)S(1)} async-done(((bf16[32,48,128]{2,1,0:T(8,128)(2,1)}), bf16[32,48,128]{2,1,0:T(8,128)(2,1)S(1)}, u32[]{:S(2)}, u32[]{:S(2)}) %all-to-all-start.5) | async-done | bytes 393248 | tf_op jit(solution)/shard_map/all_to_all | solution.py:399
  170.1 0.0 copy-done.10
  170.1 0.0 copy-done.11
  170.1 1.1 shard_map.206
  (15 shorter events, 0.1 us)
Async XLA Ops:
  28.8 47.3 %all-to-all-start.1 = ((bf16[8,384,256]{2,1,0:T(8,128)(2,1)}), bf16[8,384,256]{2,1,0:T(8,128)(2,1)S(1)}, u32[]{:S(2)}, u32[]{:S(2)}) async-start(bf16[8,384,256]{2,1,0:T(8,128)(2,1)} %get-tuple-element.42), calls=%async_computation.1 | async-start | bytes 3145728 | tf_op jit(solution)/shard_map/all_to_all | solution.py:399
  38.0 0.7 copy-start.1
  38.7 6.7 %collective-permute-start = (bf16[3,8,128,128]{3,2,1,0:T(8,128)(2,1)}, bf16[3,8,128,128]{3,2,1,0:T(8,128)(2,1)S(1)}, u32[]{:S(2)}, u32[]{:S(2)}) collective-permute-start(bf16[3,8,128,128]{3,2,1,0:T(8,128)(2,1)} %get-tuple-element.44), channel_id=1, source_target_pairs={{0,1},{1,0},{2,3},{3,2},{4,5},{5,4},{6,7},{7,6},{8,9},{9,8},{10,11... | collective-permute-start | bytes 2359304 | tf_op jit(solution)/shard_map/ppermute | solution.py:431
  76.8 4.0 %collective-permute-start.1 = (bf16[2,384,384]{2,1,0:T(8,128)(2,1)S(1)}, bf16[2,384,384]{2,1,0:T(8,128)(2,1)S(1)}, u32[]{:S(2)}, u32[]{:S(2)}) collective-permute-start(bf16[2,384,384]{2,1,0:T(8,128)(2,1)S(1)} %get-tuple-element.46), channel_id=1, source_target_pairs={{0,1},{1,0},{2,3},{3,2},{4,5},{5,4},{6,7},{7,6},{8,9},{9,8},{10,11... | collective-permute-start | bytes 1769480 | tf_op jit(solution)/shard_map/ppermute | solution.py:446
  81.9 0.9 copy-start
  82.8 0.7 copy-start.4
  83.5 27.1 %all-to-all-start.2 = ((bf16[8,384,128]{2,1,0:T(8,128)(2,1)}), bf16[8,384,128]{2,1,0:T(8,128)(2,1)S(1)}, u32[]{:S(2)}, u32[]{:S(2)}) async-start(bf16[8,384,128]{2,1,0:T(8,128)(2,1)} %copy-done), calls=%async_computation.2 | async-start | bytes 1572864 | tf_op jit(solution)/shard_map/all_to_all | solution.py:399
  87.1 0.9 copy-start.5
  90.0 36.6 %copy-start.6 = (bf16[512,128]{1,0:T(8,128)(2,1)S(1)}, bf16[512,128]{1,0:T(8,128)(2,1)}, u32[]{:S(2)}) copy-start(bf16[512,128]{1,0:T(8,128)(2,1)} %get-tuple-element.49.pick_ref) | copy-start | bytes 393220
  90.0 36.6 %copy-start.7 = (bf16[128,128]{1,0:T(8,128)(2,1)S(1)}, bf16[128,128]{1,0:T(8,128)(2,1)}, u32[]{:S(2)}) copy-start(bf16[128,128]{1,0:T(8,128)(2,1)} %cot_ref.3) | copy-start | bytes 98308
  90.0 27.2 %collective-permute-start.2 = (bf16[3,8,128,128]{3,2,1,0:T(8,128)(2,1)}, bf16[3,8,128,128]{3,2,1,0:T(8,128)(2,1)S(1)}, u32[]{:S(2)}, u32[]{:S(2)}) collective-permute-start(bf16[3,8,128,128]{3,2,1,0:T(8,128)(2,1)} %get-tuple-element.68), channel_id=1, source_target_pairs={{0,1},{1,0},{2,3},{3,2},{4,5},{5,4},{6,7},{7,6},{8,9},{9,8},{10,11... | collective-permute-start | bytes 2359304 | tf_op jit(solution)/shard_map/ppermute | solution.py:533
  110.6 0.9 copy-start.8
  111.5 16.2 %copy-start.9 = (bf16[32,128]{1,0:T(8,128)(2,1)S(1)}, bf16[32,128]{1,0:T(8,128)(2,1)}, u32[]{:S(2)}) copy-start(bf16[32,128]{1,0:T(8,128)(2,1)} %key_ref.3) | copy-start | bytes 24580
  111.5 16.3 %copy-start.12 = (bf16[32,128]{1,0:T(8,128)(2,1)S(1)}, bf16[32,128]{1,0:T(8,128)(2,1)}, u32[]{:S(2)}) copy-start(bf16[32,128]{1,0:T(8,128)(2,1)} %param.14) | copy-start | bytes 24580
  112.5 14.1 %all-to-all-start.3 = ((bf16[32,16,128]{2,1,0:T(8,128)(2,1)}), bf16[32,16,128]{2,1,0:T(8,128)(2,1)S(1)}, u32[]{:S(2)}, u32[]{:S(2)}) async-start(bf16[32,16,128]{2,1,0:T(8,128)(2,1)} %shard_map.202), calls=%async_computation.3 | async-start | bytes 262144 | tf_op jit(solution)/shard_map/all_to_all | solution.py:399
  118.6 15.4 %copy-start.3 = (bf16[64,128]{1,0:T(8,128)(2,1)S(1)}, bf16[64,128]{1,0:T(8,128)(2,1)}, u32[]{:S(2)}) copy-start(bf16[64,128]{1,0:T(8,128)(2,1)} %val_ref.3) | copy-start | bytes 49156
  127.9 19.4 %copy-start.2 = (bf16[64,2048]{1,0:T(8,128)(2,1)S(1)}, bf16[64,2048]{1,0:T(8,128)(2,1)}, u32[]{:S(2)}) copy-start(bf16[64,2048]{1,0:T(8,128)(2,1)} %copy-done.1) | copy-start | bytes 786436
  129.3 12.6 %all-to-all-start.4 = ((bf16[8,128,128]{2,1,0:T(8,128)(2,1)}), bf16[8,128,128]{2,1,0:T(8,128)(2,1)S(1)}, u32[]{:S(2)}, u32[]{:S(2)}) async-start(bf16[8,128,128]{2,1,0:T(8,128)(2,1)} %shard_map.203), calls=%async_computation.4 | async-start | bytes 524288 | tf_op jit(solution)/shard_map/all_to_all | solution.py:399
  152.3 17.8 %all-to-all-start.5 = ((bf16[32,48,128]{2,1,0:T(8,128)(2,1)}), bf16[32,48,128]{2,1,0:T(8,128)(2,1)S(1)}, u32[]{:S(2)}, u32[]{:S(2)}) async-start(bf16[32,48,128]{2,1,0:T(8,128)(2,1)} %get-tuple-element.59), calls=%async_computation.5 | async-start | bytes 786432 | tf_op jit(solution)/shard_map/all_to_all | solution.py:399
  157.6 12.5 %copy-start.10 = (bf16[32,128]{1,0:T(8,128)(2,1)S(1)}, bf16[32,128]{1,0:T(8,128)(2,1)}, u32[]{:S(2)}) copy-start(bf16[32,128]{1,0:T(8,128)(2,1)} %pre_ref.3) | copy-start | bytes 24580
  157.6 12.5 %copy-start.11 = (f32[32]{0:T(128)S(1)}, f32[32]{0:T(128)}, u32[]{:S(2)}) copy-start(f32[32]{0:T(128)} %param.19) | copy-start | bytes 388
